TPU v7x, 256 devices: a whole 4x4x8 slice. The times are simulated.
256 devices in a mesh: sp: 64 (over z, x, core), tp: 4 (over y).
Axes of the slice: x: 4, y: 4, z: 8, core: 2. Of those that a mesh axis runs over, the one named last changes fastest.
Arguments:
- tokens: bfloat16 [16384, 1024], P(('sp', 'tp')), may hold values from -6 to 6
- norm_gain: float32 [1024], replicated, may hold values from 0.1 to 1.9
- w_query: bfloat16 [1024, 1024], P('sp', 'tp'), may hold values from -0.1875 to 0.1875
- w_key: bfloat16 [1024, 1024], P('sp', 'tp'), may hold values from -0.1875 to 0.1875
- w_value: bfloat16 [1024, 1024], P('sp', 'tp'), may hold values from -0.1875 to 0.1875
- w_forget: bfloat16 [1024, 16], P('sp', 'tp'), may hold values from -0.375 to 0.375
- forget_offset: float32 [16], P('tp'), may hold values from 1 to 3.5
- w_out_t: bfloat16 [1024, 1024], P('sp', 'tp'), may hold values from -0.1875 to 0.1875
- out_gain: float32 [1024], replicated, may hold values from 0.1 to 1.9
Outputs:
- mixed: bfloat16 [16384, 1024], P(('sp', 'tp'))
All inputs are finite; a program needn't handle non-finite values.
Results may differ from a plain program's by a relative error of at most 0.015.
Values may be sent and summed in bfloat16 or wider, within the bound.
No kernel may reach another device: no remote copies, remote signals or barrier semaphores. Data moves between devices by JAX's collectives and lax.ppermute only.
A program may use at most 192 MiB of HBM per device.

v0:
```python
import functools
import math

import jax
import jax.numpy as jnp
from jax import lax
from jax.experimental import pallas as pl
from jax.experimental.pallas import tpu as pltpu
from jax.sharding import Mesh
from jax.sharding import PartitionSpec as P


AXES = ("z", "x", "c", "y")
NZ, NX, NC, NY = 8, 4, 2, 4
SIZES = {"z": NZ, "x": NX, "c": NC, "y": NY}
D = 1024
HD = 64
TOTAL = 16384
OWN = 64
BLK = 256
KEYS = 1024
QS = 2048
PAY = 144
EPS = 1e-06
LOW = -1e30
F32 = jnp.float32
BF16 = jnp.bfloat16


VMEM = pl.BlockSpec(memory_space=pltpu.VMEM)
SMEM = pl.BlockSpec(memory_space=pltpu.SMEM)


def call(body, outs, ins, scratch=(), flops=1e8, aliases=None):
    return pl.pallas_call(
        body,
        out_shape=outs,
        in_specs=ins,
        out_specs=jax.tree.map(lambda _: VMEM, outs),
        scratch_shapes=list(scratch),
        input_output_aliases=aliases or {},
        cost_estimate=pl.CostEstimate(
            flops=int(flops), bytes_accessed=1 << 20, transcendentals=0
        ),
        compiler_params=pltpu.CompilerParams(vmem_limit_bytes=24 << 20),
    )


def shift(x, axis, k):
    n = SIZES[axis]
    return lax.ppermute(x, axis, [(i, (i + k) % n) for i in range(n)])


def direct(x, axis):
    return [x] + [shift(x, axis, k) for k in range(1, SIZES[axis])]


def three_parts(x):
    hi = x.astype(BF16)
    rest = x - hi.astype(F32)
    mid = rest.astype(BF16)
    low = (rest - mid.astype(F32)).astype(BF16)
    return hi, mid, low


def project_body(idx, offs, *refs):
    toks = refs[:8]
    gain, w_own, w_sib = refs[8:11]
    q_out, kv_out, cum_out = refs[11:14]
    w, rows = refs[14:]
    x, c, y = idx[1], idx[2], idx[3]
    for z in range(NZ):
        for xx in range(NX):
            base = z * 128 + xx * 32
            own_at = pl.multiple_of(base + c * 16, 16)
            sib_at = pl.multiple_of(base + (1 - c) * 16, 16)
            w[pl.ds(own_at, 16), :] = w_own[z, xx * 16 : xx * 16 + 16, :]
            w[pl.ds(sib_at, 16), :] = w_sib[z, xx * 16 : xx * 16 + 16, :]
    for half in range(2):
        for outer in range(4):
            tok = toks[half * 4 + outer][...].astype(F32)
            scale = lax.rsqrt(jnp.mean(tok * tok, axis=-1, keepdims=True) + EPS)
            normed = (tok * scale * gain[...]).astype(BF16)
            out = jnp.dot(normed, w[...], preferred_element_type=F32)
            for inner in range(4):
                kx, ky = (outer, inner) if half == 0 else (inner, outer)
                xx = lax.rem(x - kx + NX, NX)
                yy = lax.rem(y - ky + NY, NY)
                at = pl.multiple_of(xx * BLK + yy * OWN + half * 32, 32)
                rows[pl.ds(at, 32), :] = out[inner * 32 : inner * 32 + 32, :]
    before = lax.broadcasted_iota(jnp.int32, (BLK, BLK), 0)
    after = lax.broadcasted_iota(jnp.int32, (BLK, BLK), 1)
    ones = jnp.where(before <= after, 1.0, 0.0).astype(BF16)
    for b in range(4):
        t = rows[b * BLK : (b + 1) * BLK, :].T
        lanes = slice(b * BLK, (b + 1) * BLK)
        q_out[:, lanes] = t[:64].astype(BF16)
        kv_out[:, lanes] = t[64:192].astype(BF16)
        logit = t[192:200] + offs[x] + math.log(TOTAL)
        gate = jnp.minimum(logit, 0.0) - jnp.log1p(jnp.exp(-jnp.abs(logit)))
        hi, mid, low = three_parts(gate)
        cum = jnp.dot(hi, ones, preferred_element_type=F32)
        cum = cum + jnp.dot(mid, ones, preferred_element_type=F32)
        cum = cum + jnp.dot(low, ones, preferred_element_type=F32)
        cum_out[:, lanes] = cum


def prepare_body(idx, q_own, q_sib, kv, cum_own, cum_sib, q_out, pay_out):
    c = idx[2]
    q_out[80:128, :] = jnp.zeros((48, QS), BF16)
    row = lax.broadcasted_iota(jnp.int32, (16, QS), 0)
    q_out[64:80, :] = jnp.where(row < 3, 1.0, 0.0).astype(BF16)
    for b in range(4):
        lanes = slice(b * BLK, (b + 1) * BLK)
        own_at = pl.multiple_of((2 * b + c) * BLK, BLK)
        sib_at = pl.multiple_of((2 * b + 1 - c) * BLK, BLK)
        q_out[0:64, pl.ds(own_at, BLK)] = q_own[:, lanes] * jnp.asarray(0.125, BF16)
        q_out[0:64, pl.ds(sib_at, BLK)] = q_sib[:, lanes] * jnp.asarray(0.125, BF16)
    own = [cum_own[:, b * BLK + BLK - 1 : b * BLK + BLK] for b in range(4)]
    sib = [cum_sib[:, b * BLK + BLK - 1 : b * BLK + BLK] for b in range(4)]
    ahead = jnp.zeros_like(own[0])
    bases = []
    for b in range(4):
        bases.append(ahead + jnp.where(c == 1, sib[b], 0.0))
        ahead = ahead + (own[b] + sib[b])
    total = ahead
    pay_out[0:64, :] = kv[0:64, :]
    pay_out[80:144, :] = kv[64:128, :]
    row = lax.broadcasted_iota(jnp.int32, (16, BLK), 0)
    for b in range(4):
        lanes = slice(b * BLK, (b + 1) * BLK)
        bias = (total - bases[b]) - cum_own[:, lanes]
        parts = [p[0:1].astype(F32) for p in three_parts(bias)]
        totals = [p[0:1].astype(F32) for p in three_parts(jnp.broadcast_to(total, bias.shape))]
        block = jnp.zeros((16, BLK), F32)
        for i, part in enumerate(parts + totals):
            block = jnp.where(row == i, part, block)
        pay_out[64:80, lanes] = block.astype(BF16)


def chunk_total(pay):
    rows = pay[64:80, 0:BLK].astype(F32)
    return rows[3:4] + rows[4:5] + rows[5:6]


def place_chunk(pay, i, kx, vx):
    fill = jnp.zeros((48, 128), F32)
    for r in range(8):
        lanes = slice(r * 128, (r + 1) * 128)
        tile = jnp.concatenate([pay[0:80, lanes].astype(F32), fill], axis=0)
        kx[i, lanes, :] = tile.T.astype(BF16)
    vx[i, 0:64, :] = pay[80:144, :]
    vx[i, 64:80, :] = jnp.ones((16, KEYS), BF16)


def absorb(count, q, acc, m, kx, vx, move, c=None):
    if c is not None:
        key = lax.broadcasted_iota(jnp.int32, (KEYS, BLK), 0)
        key_pos = key + (key // BLK + c) * BLK
        query = lax.broadcasted_iota(jnp.int32, (KEYS, BLK), 1)

    def two_tiles(t, carry):
        i = t // 4
        lanes, s = [], []
        for u in range(2):
            b = (t % 4) * 2 + u
            at = pl.ds(pl.multiple_of(b * BLK, BLK), BLK)
            part = jnp.dot(kx[i], q[:, at], preferred_element_type=F32)
            if c is not None:
                part = jnp.where(key_pos <= query + b * BLK, part, LOW)
            lanes.append(at)
            s.append(part)
        by = move[i, 0:1]
        for u in range(2):
            old = m[i, 0:1, lanes[u]]
            new = jnp.maximum(old, jnp.max(s[u], axis=0, keepdims=True) + by)
            p = jnp.exp(s[u] - (new - by)).astype(BF16)
            part = jnp.dot(vx[i], p, preferred_element_type=F32)
            acc[i, :, lanes[u]] = acc[i, :, lanes[u]] * jnp.exp(old - new) + part
            m[i, :, lanes[u]] = jnp.broadcast_to(new, (8, BLK))
        return carry

    lax.fori_loop(0, count * 4, two_tiles, 0)


def first_body(idx, q, pay, acc, m, sums, kx, vx, move):
    acc[...] = jnp.zeros_like(acc)
    m[...] = jnp.full(m.shape, LOW, F32)
    move[...] = jnp.zeros_like(move)
    place_chunk(pay, 0, kx, vx)
    absorb(1, q, acc, m, kx, vx, move, idx[2])
    sums[...] = jnp.broadcast_to(chunk_total(pay), sums.shape)


def step_body(k, idx, q, *refs):
    z = idx[0]
    n_pay = 2 if k < 4 else 1
    pays, refs = refs[:n_pay], refs[n_pay:]
    acc0, m0, sums0, refs = refs[0], refs[1], refs[2], refs[3:]
    if k < 4:
        acc, m, sums, kx, vx, move = refs
    else:
        out, kx, vx, move, sums = refs
        acc, m = acc0, m0
    sums[...] = sums0[...]
    count = (z >= k).astype(jnp.int32)

    @pl.when(z >= k)
    def _():
        place_chunk(pays[0], 0, kx, vx)
        move[0] = sums0[...]
        sums[...] = sums0[...] + jnp.broadcast_to(chunk_total(pays[0]), sums.shape)

    if k < 4:
        count = count + (z + k >= 8).astype(jnp.int32)

        @pl.when(z + k >= 8)
        def _():
            place_chunk(pays[1], 1, kx, vx)
            move[1] = jnp.zeros(sums.shape, F32)
            m[1] = m[1] + chunk_total(pays[1])[:, 0:1]

    absorb(count, q, acc, m, kx, vx, move)
    if k == 4:
        c = idx[2]
        row = lax.broadcasted_iota(jnp.int32, (8, BLK), 0)
        for b in range(4):
            for other in range(2):
                at = 2 * b + (c if other == 0 else 1 - c)
                lanes = pl.ds(pl.multiple_of(at * BLK, BLK), BLK)
                m_a = m[0, 0:1, lanes]
                m_b = m[1, 0:1, lanes] + sums[0:1]
                top = jnp.maximum(m_a, m_b)
                both = acc[0, :, lanes] * jnp.exp(m_a - top) + acc[1, :, lanes] * jnp.exp(m_b - top)
                to = slice(b * BLK, (b + 1) * BLK)
                out[other, 0:64, to] = both[0:64]
                out[other, 64:72, to] = jnp.where(row < 4, both[64:65], top)


def merge_body(own, sib, out):
    a, b = own[...], sib[...]
    m_a, m_b = a[68:69], b[68:69]
    top = jnp.maximum(m_a, m_b)
    f_a, f_b = jnp.exp(m_a - top), jnp.exp(m_b - top)
    total = a[64:65] * f_a + b[64:65] * f_b
    att = (a[0:64] * f_a + b[0:64] * f_b) / total
    att = jnp.concatenate([att, jnp.zeros_like(att)], axis=0)
    for r in range(8):
        out[r * 128 : (r + 1) * 128, :] = att[:, r * 128 : (r + 1) * 128].T[:, 0:64].astype(BF16)


def final_body(idx, att, gain, w_all, out, w):
    c = idx[2]
    for xs in range(NX):
        for ys in range(NY):
            for other in range(2):
                cc = c if other == 0 else 1 - c
                for z in range(NZ):
                    at = pl.multiple_of(z * 128 + xs * 32 + cc * 16, 16)
                    w[pl.ds(at, 16), ys * 256 : ys * 256 + 256] = w_all[xs * NY + ys, other, z]
    pieces = [att[xs * NY + ys] for ys in range(NY) for xs in range(NX)]
    joined = jnp.concatenate(pieces, axis=1)
    proj = lax.dot_general(joined, w[...], (((1,), (1,)), ((), ())), preferred_element_type=F32)
    scale = lax.rsqrt(jnp.mean(proj * proj, axis=-1, keepdims=True) + EPS)
    out[...] = (proj * scale * gain[...]).astype(BF16)


def shards(tokens, norm_gain, w_query, w_key, w_value, w_forget, forget_offset, w_out_t, out_gain):
    sds = jax.ShapeDtypeStruct
    idx = jnp.stack([lax.axis_index(a) for a in AXES]).astype(jnp.int32)

    tok_a = direct(tokens[:32], "y")
    tok_b = direct(tokens[32:], "x")
    toks = direct(jnp.concatenate(tok_a, axis=0), "x")
    toks = toks + direct(jnp.concatenate(tok_b, axis=0), "y")

    heads = [w.reshape(16, NX, HD) for w in (w_query, w_key, w_value)]
    heads.append(jnp.broadcast_to(w_forget[:, :, None], (16, NX, HD)))
    per_head = jnp.concatenate(heads, axis=2).transpose(1, 0, 2)
    w_x = lax.all_to_all(per_head, "x", 0, 0, tiled=True).reshape(64, 256)
    chunk = jnp.concatenate([w_x, w_out_t], axis=0)
    w_own = lax.all_to_all(jnp.broadcast_to(chunk[None], (NZ, 80, 256)), "z", 0, 0, tiled=True)
    w_sib = shift(w_own, "c", 1)

    q_own, kv, cum_own = call(
        project_body,
        (sds((64, KEYS), BF16), sds((128, KEYS), BF16), sds((8, KEYS), F32)),
        [SMEM, SMEM] + [VMEM] * 11,
        [pltpu.VMEM((D, 256), BF16), pltpu.VMEM((KEYS, 256), F32)],
        2e9,
    )(idx, forget_offset, *toks, norm_gain[None], w_own, w_sib)

    q_sib = shift(q_own, "c", 1)
    cum_sib = shift(cum_own, "c", 1)
    q, pay = call(
        prepare_body, (sds((128, QS), BF16), sds((PAY, KEYS), BF16)), [SMEM] + [VMEM] * 5
    )(idx, q_own, q_sib, kv, cum_own, cum_sib)

    acc_t, m_t, sums_t = sds((2, 80, QS), F32), sds((2, 8, QS), F32), sds((8, BLK), F32)
    work = [
        pltpu.VMEM((2, KEYS, 128), BF16),
        pltpu.VMEM((2, 80, KEYS), BF16),
        pltpu.VMEM((2, 8, BLK), F32),
    ]
    right = shift(pay, "z", 1)
    left = shift(pay, "z", -1)
    acc, m, sums = call(
        first_body, (acc_t, m_t, sums_t), [SMEM, VMEM, VMEM], work, 3e9
    )(idx, q, pay)

    w_o = jnp.stack([w_own[:, 64:], w_sib[:, 64:]])
    w_o, _ = lax.optimization_barrier((w_o, sums))
    w_o = jnp.broadcast_to(w_o[None], (16, 2, 8, 16, 256))
    w_o = lax.all_to_all(w_o, ("x", "y"), 0, 0, tiled=True)

    for k in range(1, 5):
        pays = (right, left) if k < 4 else (right,)
        if k < 4:
            right = shift(pays[0], "z", 1)
        if k < 3:
            left = shift(pays[1], "z", -1)
        ins = (idx, q) + pays + (acc, m, sums)
        if k < 4:
            outs, scratch, aliases = (acc_t, m_t, sums_t), work, {4: 0, 5: 1}
        else:
            outs, aliases = sds((2, 72, KEYS), F32), None
            scratch = work + [pltpu.VMEM(sums_t.shape, F32)]
        res = call(
            functools.partial(step_body, k),
            outs,
            [SMEM] + [VMEM] * (len(ins) - 1),
            scratch,
            6e9,
            aliases,
        )(*ins)
        if k < 4:
            acc, m, sums = res
    sib = shift(res[1], "c", 1)
    att = call(merge_body, sds((KEYS, HD), BF16), [VMEM, VMEM])(res[0], sib)
    att = lax.all_to_all(att.reshape(16, 64, HD), ("x", "y"), 0, 0, tiled=True)
    return call(
        final_body, sds((OWN, D), BF16), [SMEM] + [VMEM] * 3, [pltpu.VMEM((D, D), BF16)]
    )(idx, att, out_gain[None], w_o)


def solution(mesh):
    finer = Mesh(mesh.devices.reshape(NZ, NX, NC, NY), AXES)
    sp = ("z", "x", "c")

    return jax.shard_map(
        shards,
        mesh=finer,
        in_specs=(
            P(AXES, None),
            P(),
            P(sp, "y"),
            P(sp, "y"),
            P(sp, "y"),
            P(sp, "y"),
            P("y"),
            P(sp, "y"),
            P(),
        ),
        out_specs=P(AXES, None),
        check_vma=False,
    )
```

profile of v0, /device:TPU:192, one launch (start us, length us, event | category | flops | bytes accessed | tf_op | source)
XLA Modules:
  0.0 163.3 jit_solution(7686229269792428256)
XLA Ops:
  0.0 0.8 copy.18
  0.8 0.8 reshape.18
  1.6 0.8 reshape.19
  2.4 0.8 reshape.20
  3.4 9.5 %all_to_all.20 = bf16[4,16,256]{2,1,0:T(8,128)(2,1)S(1)} all-to-all(bf16[4,16,256]{2,1,0:T(8,128)(2,1)S(1)} %copy.19), channel_id=1, replica_groups=mesh['z'=8,'x'=4,'c'=2,'y'=4] {'x'}, dimensions={0} | all-to-all | bytes 65536 | tf_op jit(solution)/shard_map/all_to_all | solution.py:280
  12.9 0.7 pad_maximum_fusion.3
  13.6 0.7 broadcast_in_dim.12
  14.4 6.3 %all-to-all-start.1 = ((bf16[8,80,256]{2,1,0:T(8,128)(2,1)}), bf16[8,80,256]{2,1,0:T(8,128)(2,1)S(1)}, u32[]{:S(2)}, u32[]{:S(2)}) async-start(bf16[8,80,256]{2,1,0:T(8,128)(2,1)} %broadcast_in_dim.12), calls=%async_computation.1 | async-start | bytes 655360 | tf_op jit(solution)/shard_map/all_to_all | solution.py:282
  21.3 2.1 %collective-permute-start.7 = (bf16[32,1024]{1,0:T(8,128)(2,1)S(1)}, bf16[32,1024]{1,0:T(8,128)(2,1)S(1)}, u32[]{:S(2)}, u32[]{:S(2)}) collective-permute-start(bf16[32,1024]{1,0:T(8,128)(2,1)S(1)} %get-tuple-element.43), channel_id=1, source_target_pairs={{0,16},{8,24},{16,0},{24,8},{1,17},{9,25},{17,1},{25,9},{2,18},{10... | collective-permute-start | bytes 196616 | tf_op jit(solution)/shard_map/ppermute | solution.py:51
  23.4 1.1 collective-permute-start.8
  24.5 1.8 %collective-permute-done.6 = bf16[32,1024]{1,0:T(8,128)(2,1)S(1)} collective-permute-done((bf16[32,1024]{1,0:T(8,128)(2,1)S(1)}, bf16[32,1024]{1,0:T(8,128)(2,1)S(1)}, u32[]{:S(2)}, u32[]{:S(2)}) %collective-permute-start.6) | collective-permute-done | bytes 65568 | tf_op jit(solution)/shard_map/ppermute | solution.py:51
  26.2 0.9 collective-permute-done.7
  27.1 0.7 collective-permute-done.8
  27.8 3.3 %collective-permute-start.10 = (bf16[128,1024]{1,0:T(8,128)(2,1)S(1)}, bf16[128,1024]{1,0:T(8,128)(2,1)S(1)}, u32[]{:S(2)}, u32[]{:S(2)}) collective-permute-start(bf16[128,1024]{1,0:T(8,128)(2,1)S(1)} %pad_maximum_fusion.1.refs_4_), channel_id=1, source_target_pairs={{0,2},{1,3},{2,0},{3,1},{4,6},{5,7},{6,4},{7,5},{8,10},{9,11},{10,... | collective-permute-start | bytes 786440 | tf_op jit(solution)/shard_map/ppermute | solution.py:51
  31.1 1.1 collective-permute-start.11
  32.2 1.0 collective-permute-start
  33.1 0.7 collective-permute-start.1
  33.9 2.6 %collective-permute-start.2 = (bf16[32,1024]{1,0:T(8,128)(2,1)S(1)}, bf16[32,1024]{1,0:T(8,128)(2,1)S(1)}, u32[]{:S(2)}, u32[]{:S(2)}) collective-permute-start(bf16[32,1024]{1,0:T(8,128)(2,1)S(1)} %get-tuple-element.44), channel_id=1, source_target_pairs={{0,3},{1,0},{2,1},{3,2},{4,7},{5,4},{6,5},{7,6},{8,11},{9,8},{10,9... | collective-permute-start | bytes 196616 | tf_op jit(solution)/shard_map/ppermute | solution.py:51
  36.5 1.9 %collective-permute-done = bf16[32,1024]{1,0:T(8,128)(2,1)S(1)} collective-permute-done((bf16[32,1024]{1,0:T(8,128)(2,1)S(1)}, bf16[32,1024]{1,0:T(8,128)(2,1)S(1)}, u32[]{:S(2)}, u32[]{:S(2)}) %collective-permute-start) | collective-permute-done | bytes 65568 | tf_op jit(solution)/shard_map/ppermute | solution.py:51
  38.4 1.6 collective-permute-start.9
  40.0 3.2 %collective-permute-done.2 = bf16[32,1024]{1,0:T(8,128)(2,1)S(1)} collective-permute-done((bf16[32,1024]{1,0:T(8,128)(2,1)S(1)}, bf16[32,1024]{1,0:T(8,128)(2,1)S(1)}, u32[]{:S(2)}, u32[]{:S(2)}) %collective-permute-start.2) | collective-permute-done | bytes 65568 | tf_op jit(solution)/shard_map/ppermute | solution.py:51
  43.2 1.1 collective-permute-start.3
  44.3 3.1 %collective-permute-start.4 = (bf16[128,1024]{1,0:T(8,128)(2,1)S(1)}, bf16[128,1024]{1,0:T(8,128)(2,1)S(1)}, u32[]{:S(2)}, u32[]{:S(2)}) collective-permute-start(bf16[128,1024]{1,0:T(8,128)(2,1)S(1)} %pad_maximum_fusion.refs_0_), channel_id=1, source_target_pairs={{0,16},{8,24},{16,0},{24,8},{1,17},{9,25},{17,1},{25,9},{2,18},{10... | collective-permute-start | bytes 786440 | tf_op jit(solution)/shard_map/ppermute | solution.py:51
  47.5 6.2 %collective-permute-done.3.refs_1_ = bf16[128,1024]{1,0:T(8,128)(2,1)S(1)} collective-permute-done((bf16[128,1024]{1,0:T(8,128)(2,1)S(1)}, bf16[128,1024]{1,0:T(8,128)(2,1)S(1)}, u32[]{:S(2)}, u32[]{:S(2)}) %collective-permute-start.3) | collective-permute-done | bytes 262176 | tf_op jit(solution)/shard_map/ppermute | solution.py:51
  53.7 2.9 %collective-permute-done.4.refs_2_ = bf16[128,1024]{1,0:T(8,128)(2,1)S(1)} collective-permute-done((bf16[128,1024]{1,0:T(8,128)(2,1)S(1)}, bf16[128,1024]{1,0:T(8,128)(2,1)S(1)}, u32[]{:S(2)}, u32[]{:S(2)}) %collective-permute-start.4) | collective-permute-done | bytes 262176 | tf_op jit(solution)/shard_map/ppermute | solution.py:51
  56.6 2.2 %shard_map.91 = (bf16[64,1024]{1,0:T(8,128)(2,1)S(1)}, bf16[128,1024]{1,0:T(8,128)(2,1)S(1)}, f32[8,1024]{1,0:T(8,128)S(1)}) custom-call(s32[4]{0:T(128)S(1)} %pad_add_fusion.idx, f32[4]{0:T(128)S(1)} %copy-done.2, bf16[128,1024]{1,0:T(8,128)(2,1)S(1)} %pad_maximum_fusion.refs_0_, bf16[128,1024]{1,0:T(8,128)(2,1)S(1)} %collective-permute-done.3.refs_1_, ...), custom_call_target="tpu_custom_call" | custom-call | flops 2000000000 | bytes 1048576 | tf_op jit(solution)/shard_map/pallas_call | solution.py:285
  59.2 0.9 collective-permute-done.14.cum_sib
  60.1 0.6 shard_map.92
  60.8 0.8 collective-permute-start.15
  61.6 1.5 collective-permute-start.19
  63.1 4.7 %shard_map.93 = (f32[2,80,2048]{2,1,0:T(8,128)S(1)}, f32[2,8,2048]{2,1,0:T(8,128)S(1)}, f32[8,256]{1,0:T(8,128)S(1)}) custom-call(s32[4]{0:T(128)S(1)} %pad_add_fusion.idx, bf16[128,2048]{1,0:T(8,128)(2,1)S(1)} %get-tuple-element.26.q, bf16[144,1024]{1,0:T(8,128)(2,1)S(1)} %get-tuple-element.27.pay), custom_call_target="tpu_custom_call" | custom-call | flops 3000000000 | bytes 1048576 | tf_op jit(solution)/shard_map/pallas_call | solution.py:307
  67.8 2.5 %collective-permute-done.15.refs_0_ = bf16[144,1024]{1,0:T(8,128)(2,1)S(1)} collective-permute-done((bf16[144,1024]{1,0:T(8,128)(2,1)S(1)}, bf16[144,1024]{1,0:T(8,128)(2,1)S(1)}, u32[]{:S(2)}, u32[]{:S(2)}) %collective-permute-start.15) | collective-permute-done | bytes 294944 | tf_op jit(solution)/shard_map/ppermute | solution.py:51
  70.8 1.5 collective-permute-start.20
  72.3 4.9 %shard_map.94 = (f32[2,80,2048]{2,1,0:T(8,128)S(1)}, f32[2,8,2048]{2,1,0:T(8,128)S(1)}, f32[8,256]{1,0:T(8,128)S(1)}) custom-call(s32[4]{0:T(128)S(1)} %pad_add_fusion.idx, bf16[128,2048]{1,0:T(8,128)(2,1)S(1)} %get-tuple-element.26.q, bf16[144,1024]{1,0:T(8,128)(2,1)S(1)} %collective-permute-done.15.refs_0_, ...), custom_call_target="tpu_custom_call", output_to_operand_aliasing={{0}: (4, {}), {1}: (5, {})} | custom-call | flops 6000000000 | bytes 1048576 | tf_op jit(solution)/shard_map/pallas_call | solution.py:328
  77.2 1.5 collective-permute-done.16.refs_0_
  78.7 3.5 %collective-permute-start.17 = (bf16[144,1024]{1,0:T(8,128)(2,1)S(1)}, bf16[144,1024]{1,0:T(8,128)(2,1)S(1)}, u32[]{:S(2)}, u32[]{:S(2)}) collective-permute-start(bf16[144,1024]{1,0:T(8,128)(2,1)S(1)} %collective-permute-done.16.refs_0_), channel_id=1, source_target_pairs={{0,32},{32,64},{64,96},{96,128},{128,160},{160,192},{192,224},{224... | collective-permute-start | bytes 884744 | tf_op jit(solution)/shard_map/ppermute | solution.py:51
  82.2 9.2 %shard_map.95 = (f32[2,80,2048]{2,1,0:T(8,128)S(1)}, f32[2,8,2048]{2,1,0:T(8,128)S(1)}, f32[8,256]{1,0:T(8,128)S(1)}) custom-call(s32[4]{0:T(128)S(1)} %pad_add_fusion.idx, bf16[128,2048]{1,0:T(8,128)(2,1)S(1)} %get-tuple-element.26.q, bf16[144,1024]{1,0:T(8,128)(2,1)S(1)} %collective-permute-done.16.refs_0_, ...), custom_call_target="tpu_custom_call", output_to_operand_aliasing={{0}: (4, {}), {1}: (5, {})} | custom-call | flops 6000000000 | bytes 1048576 | tf_op jit(solution)/shard_map/pallas_call | solution.py:328
  91.5 2.1 %collective-permute-start.18 = (bf16[144,1024]{1,0:T(8,128)(2,1)S(1)}, bf16[144,1024]{1,0:T(8,128)(2,1)S(1)}, u32[]{:S(2)}, u32[]{:S(2)}) collective-permute-start(bf16[144,1024]{1,0:T(8,128)(2,1)S(1)} %collective-permute-done.17.refs_0_), channel_id=1, source_target_pairs={{0,32},{32,64},{64,96},{96,128},{128,160},{160,192},{192,224},{224... | collective-permute-start | bytes 884744 | tf_op jit(solution)/shard_map/ppermute | solution.py:51
  93.6 9.2 %shard_map.96 = (f32[2,80,2048]{2,1,0:T(8,128)S(1)}, f32[2,8,2048]{2,1,0:T(8,128)S(1)}, f32[8,256]{1,0:T(8,128)S(1)}) custom-call(s32[4]{0:T(128)S(1)} %pad_add_fusion.idx, bf16[128,2048]{1,0:T(8,128)(2,1)S(1)} %get-tuple-element.26.q, bf16[144,1024]{1,0:T(8,128)(2,1)S(1)} %collective-permute-done.17.refs_0_, ...), custom_call_target="tpu_custom_call", output_to_operand_aliasing={{0}: (4, {}), {1}: (5, {})} | custom-call | flops 6000000000 | bytes 1048576 | tf_op jit(solution)/shard_map/pallas_call | solution.py:328
  102.8 5.0 %shard_map.97 = f32[2,72,1024]{2,1,0:T(8,128)S(1)} custom-call(s32[4]{0:T(128)S(1)} %pad_add_fusion.idx, bf16[128,2048]{1,0:T(8,128)(2,1)S(1)} %get-tuple-element.26.q, bf16[144,1024]{1,0:T(8,128)(2,1)S(1)} %collective-permute-done.18.refs_0_, f32[2,80,2048]{2,1,0:T(8,128)S(1)} %get-tuple-element.37.refs_1_, f32[2,8,2048]{2,1,0:T(8,128)S(1)} %get-tuple-element.38.refs_2_, ...), custom_call_target="tpu_custom_call" | custom-call | flops 6000000000 | bytes 1048576 | tf_op jit(solution)/shard_map/pallas_call | solution.py:328
  108.0 1.6 collective-permute-done.22.sib
  109.7 0.9 reshape.23
  110.6 8.3 %all-to-all-start.2 = ((bf16[16,2,2048]{2,1,0:T(2,128)(2,1)}), bf16[16,2,2048]{2,1,0:T(2,128)(2,1)S(1)}, u32[]{:S(2)}, u32[]{:S(2)}) async-start(bf16[16,2,2048]{2,1,0:T(2,128)(2,1)} %reshape.23), calls=%async_computation.2 | async-start | bytes 262144 | tf_op jit(solution)/shard_map/all_to_all | solution.py:340
  118.9 7.8 %all-to-all-done.2 = bf16[16,2,2048]{2,1,0:T(2,128)(2,1)S(1)} async-done(((bf16[16,2,2048]{2,1,0:T(2,128)(2,1)}), bf16[16,2,2048]{2,1,0:T(2,128)(2,1)S(1)}, u32[]{:S(2)}, u32[]{:S(2)}) %all-to-all-start.2) | async-done | bytes 131104 | tf_op jit(solution)/shard_map/all_to_all | solution.py:340
  126.7 1.6 broadcast_in_dim.28
  128.3 3.8 %all-to-all-start.3 = ((bf16[16,2,8,16,256]{4,3,2,1,0:T(8,128)(2,1)}), bf16[16,2,8,16,256]{4,3,2,1,0:T(8,128)(2,1)S(1)}, u32[]{:S(2)}, u32[]{:S(2)}) async-start(bf16[16,2,8,16,256]{4,3,2,1,0:T(8,128)(2,1)} %broadcast_in_dim.28), calls=%async_computation.3 | async-start | bytes 4194304 | tf_op jit(solution)/shard_map/all_to_all | solution.py:314
  132.4 28.6 %all-to-all-done.3.w_all = bf16[16,2,8,16,256]{4,3,2,1,0:T(8,128)(2,1)S(1)} async-done(((bf16[16,2,8,16,256]{4,3,2,1,0:T(8,128)(2,1)}), bf16[16,2,8,16,256]{4,3,2,1,0:T(8,128)(2,1)S(1)}, u32[]{:S(2)}, u32[]{:S(2)}) %all-to-all-start.3) | async-done | bytes 2097184 | tf_op jit(solution)/shard_map/all_to_all | solution.py:314
  161.0 2.3 %shard_map.99 = bf16[64,1024]{1,0:T(8,128)(2,1)} custom-call(s32[4]{0:T(128)S(1)} %pad_add_fusion.idx, bf16[16,64,64]{2,1,0:T(8,128)(2,1)S(1)} %reshape.24.att, f32[1,1024]{1,0:T(1,128)S(1)} %bitcast.19, bf16[16,2,8,16,256]{4,3,2,1,0:T(8,128)(2,1)S(1)} %all-to-all-done.3.w_all), custom_call_target="tpu_custom_call" | custom-call | flops 100000000 | bytes 1048576 | tf_op jit(solution)/shard_map/pallas_call | solution.py:341
  (42 shorter events, 2.6 us)
Async XLA Ops:
  0.0 20.7 %copy-start.3 = (bf16[64,1024]{1,0:T(8,128)(2,1)S(1)}, bf16[64,1024]{1,0:T(8,128)(2,1)}, u32[]{:S(2)}) copy-start(bf16[64,1024]{1,0:T(8,128)(2,1)} %param.9) | copy-start | bytes 393220
  3.3 53.2 %copy-start.1 = (f32[1024]{0:T(1024)S(1)}, f32[1024]{0:T(1024)}, u32[]{:S(2)}) copy-start(f32[1024]{0:T(1024)} %param.10) | copy-start | bytes 12292
  3.4 53.2 %copy-start.2 = (f32[4]{0:T(128)S(1)}, f32[4]{0:T(128)}, u32[]{:S(2)}) copy-start(f32[4]{0:T(128)} %offs.1) | copy-start | bytes 52
  14.4 25.6 %all-to-all-start.1 = ((bf16[8,80,256]{2,1,0:T(8,128)(2,1)}), bf16[8,80,256]{2,1,0:T(8,128)(2,1)S(1)}, u32[]{:S(2)}, u32[]{:S(2)}) async-start(bf16[8,80,256]{2,1,0:T(8,128)(2,1)} %broadcast_in_dim.12), calls=%async_computation.1 | async-start | bytes 655360 | tf_op jit(solution)/shard_map/all_to_all | solution.py:282
  20.7 5.6 %collective-permute-start.6 = (bf16[32,1024]{1,0:T(8,128)(2,1)S(1)}, bf16[32,1024]{1,0:T(8,128)(2,1)S(1)}, u32[]{:S(2)}, u32[]{:S(2)}) collective-permute-start(bf16[32,1024]{1,0:T(8,128)(2,1)S(1)} %get-tuple-element.43), channel_id=1, source_target_pairs={{0,8},{8,16},{16,24},{24,0},{1,9},{9,17},{17,25},{25,1},{2,10},{10... | collective-permute-start | bytes 196616 | tf_op jit(solution)/shard_map/ppermute | solution.py:51
  21.3 5.8 %collective-permute-start.7 = (bf16[32,1024]{1,0:T(8,128)(2,1)S(1)}, bf16[32,1024]{1,0:T(8,128)(2,1)S(1)}, u32[]{:S(2)}, u32[]{:S(2)}) collective-permute-start(bf16[32,1024]{1,0:T(8,128)(2,1)S(1)} %get-tuple-element.43), channel_id=1, source_target_pairs={{0,16},{8,24},{16,0},{24,8},{1,17},{9,25},{17,1},{25,9},{2,18},{10... | collective-permute-start | bytes 196616 | tf_op jit(solution)/shard_map/ppermute | solution.py:51
  23.4 4.4 %collective-permute-start.8 = (bf16[32,1024]{1,0:T(8,128)(2,1)S(1)}, bf16[32,1024]{1,0:T(8,128)(2,1)S(1)}, u32[]{:S(2)}, u32[]{:S(2)}) collective-permute-start(bf16[32,1024]{1,0:T(8,128)(2,1)S(1)} %get-tuple-element.43), channel_id=1, source_target_pairs={{0,24},{8,0},{16,8},{24,16},{1,25},{9,1},{17,9},{25,17},{2,26},{10... | collective-permute-start | bytes 196616 | tf_op jit(solution)/shard_map/ppermute | solution.py:51
  27.8 16.5 %collective-permute-start.10 = (bf16[128,1024]{1,0:T(8,128)(2,1)S(1)}, bf16[128,1024]{1,0:T(8,128)(2,1)S(1)}, u32[]{:S(2)}, u32[]{:S(2)}) collective-permute-start(bf16[128,1024]{1,0:T(8,128)(2,1)S(1)} %pad_maximum_fusion.1.refs_4_), channel_id=1, source_target_pairs={{0,2},{1,3},{2,0},{3,1},{4,6},{5,7},{6,4},{7,5},{8,10},{9,11},{10,... | collective-permute-start | bytes 786440 | tf_op jit(solution)/shard_map/ppermute | solution.py:51
  31.1 16.3 %collective-permute-start.11 = (bf16[128,1024]{1,0:T(8,128)(2,1)S(1)}, bf16[128,1024]{1,0:T(8,128)(2,1)S(1)}, u32[]{:S(2)}, u32[]{:S(2)}) collective-permute-start(bf16[128,1024]{1,0:T(8,128)(2,1)S(1)} %pad_maximum_fusion.1.refs_4_), channel_id=1, source_target_pairs={{0,3},{1,0},{2,1},{3,2},{4,7},{5,4},{6,5},{7,6},{8,11},{9,8},{10,9... | collective-permute-start | bytes 786440 | tf_op jit(solution)/shard_map/ppermute | solution.py:51
  32.2 6.2 %collective-permute-start = (bf16[32,1024]{1,0:T(8,128)(2,1)S(1)}, bf16[32,1024]{1,0:T(8,128)(2,1)S(1)}, u32[]{:S(2)}, u32[]{:S(2)}) collective-permute-start(bf16[32,1024]{1,0:T(8,128)(2,1)S(1)} %get-tuple-element.44), channel_id=1, source_target_pairs={{0,1},{1,2},{2,3},{3,0},{4,5},{5,6},{6,7},{7,4},{8,9},{9,10},{10,1... | collective-permute-start | bytes 196616 | tf_op jit(solution)/shard_map/ppermute | solution.py:51
  33.1 6.8 %collective-permute-start.1 = (bf16[32,1024]{1,0:T(8,128)(2,1)S(1)}, bf16[32,1024]{1,0:T(8,128)(2,1)S(1)}, u32[]{:S(2)}, u32[]{:S(2)}) collective-permute-start(bf16[32,1024]{1,0:T(8,128)(2,1)S(1)} %get-tuple-element.44), channel_id=1, source_target_pairs={{0,2},{1,3},{2,0},{3,1},{4,6},{5,7},{6,4},{7,5},{8,10},{9,11},{10,... | collective-permute-start | bytes 196616 | tf_op jit(solution)/shard_map/ppermute | solution.py:51
  33.9 9.3 %collective-permute-start.2 = (bf16[32,1024]{1,0:T(8,128)(2,1)S(1)}, bf16[32,1024]{1,0:T(8,128)(2,1)S(1)}, u32[]{:S(2)}, u32[]{:S(2)}) collective-permute-start(bf16[32,1024]{1,0:T(8,128)(2,1)S(1)} %get-tuple-element.44), channel_id=1, source_target_pairs={{0,3},{1,0},{2,1},{3,2},{4,7},{5,4},{6,5},{7,6},{8,11},{9,8},{10,9... | collective-permute-start | bytes 196616 | tf_op jit(solution)/shard_map/ppermute | solution.py:51
  38.4 9.1 %collective-permute-start.9 = (bf16[128,1024]{1,0:T(8,128)(2,1)S(1)}, bf16[128,1024]{1,0:T(8,128)(2,1)S(1)}, u32[]{:S(2)}, u32[]{:S(2)}) collective-permute-start(bf16[128,1024]{1,0:T(8,128)(2,1)S(1)} %pad_maximum_fusion.1.refs_4_), channel_id=1, source_target_pairs={{0,1},{1,2},{2,3},{3,0},{4,5},{5,6},{6,7},{7,4},{8,9},{9,10},{10,1... | collective-permute-start | bytes 786440 | tf_op jit(solution)/shard_map/ppermute | solution.py:51
  40.0 16.6 %collective-permute-start.12 = (bf16[8,80,256]{2,1,0:T(8,128)(2,1)S(1)}, bf16[8,80,256]{2,1,0:T(8,128)(2,1)S(1)}, u32[]{:S(2)}, u32[]{:S(2)}) collective-permute-start(bf16[8,80,256]{2,1,0:T(8,128)(2,1)S(1)} %all-to-all-done.1.refs_9_), channel_id=1, source_target_pairs={{0,4},{4,0},{1,5},{5,1},{2,6},{6,2},{3,7},{7,3},{8,12},{12,8},{9,1... | collective-permute-start | bytes 983048 | tf_op jit(solution)/shard_map/ppermute | solution.py:51
  43.2 10.5 %collective-permute-start.3 = (bf16[128,1024]{1,0:T(8,128)(2,1)S(1)}, bf16[128,1024]{1,0:T(8,128)(2,1)S(1)}, u32[]{:S(2)}, u32[]{:S(2)}) collective-permute-start(bf16[128,1024]{1,0:T(8,128)(2,1)S(1)} %pad_maximum_fusion.refs_0_), channel_id=1, source_target_pairs={{0,8},{8,16},{16,24},{24,0},{1,9},{9,17},{17,25},{25,1},{2,10},{10... | collective-permute-start | bytes 786440 | tf_op jit(solution)/shard_map/ppermute | solution.py:51
  44.3 12.2 %collective-permute-start.4 = (bf16[128,1024]{1,0:T(8,128)(2,1)S(1)}, bf16[128,1024]{1,0:T(8,128)(2,1)S(1)}, u32[]{:S(2)}, u32[]{:S(2)}) collective-permute-start(bf16[128,1024]{1,0:T(8,128)(2,1)S(1)} %pad_maximum_fusion.refs_0_), channel_id=1, source_target_pairs={{0,16},{8,24},{16,0},{24,8},{1,17},{9,25},{17,1},{25,9},{2,18},{10... | collective-permute-start | bytes 786440 | tf_op jit(solution)/shard_map/ppermute | solution.py:51
  47.4 9.1 %collective-permute-start.5 = (bf16[128,1024]{1,0:T(8,128)(2,1)S(1)}, bf16[128,1024]{1,0:T(8,128)(2,1)S(1)}, u32[]{:S(2)}, u32[]{:S(2)}) collective-permute-start(bf16[128,1024]{1,0:T(8,128)(2,1)S(1)} %pad_maximum_fusion.refs_0_), channel_id=1, source_target_pairs={{0,24},{8,0},{16,8},{24,16},{1,25},{9,1},{17,9},{25,17},{2,26},{10... | collective-permute-start | bytes 786440 | tf_op jit(solution)/shard_map/ppermute | solution.py:51
  58.7 1.4 collective-permute-start.13
  58.7 1.4 collective-permute-start.14
  60.8 9.5 %collective-permute-start.15 = (bf16[144,1024]{1,0:T(8,128)(2,1)S(1)}, bf16[144,1024]{1,0:T(8,128)(2,1)S(1)}, u32[]{:S(2)}, u32[]{:S(2)}) collective-permute-start(bf16[144,1024]{1,0:T(8,128)(2,1)S(1)} %get-tuple-element.27.pay), channel_id=1, source_target_pairs={{0,32},{32,64},{64,96},{96,128},{128,160},{160,192},{192,224},{224... | collective-permute-start | bytes 884744 | tf_op jit(solution)/shard_map/ppermute | solution.py:51
  61.6 9.2 %collective-permute-start.19 = (bf16[144,1024]{1,0:T(8,128)(2,1)S(1)}, bf16[144,1024]{1,0:T(8,128)(2,1)S(1)}, u32[]{:S(2)}, u32[]{:S(2)}) collective-permute-start(bf16[144,1024]{1,0:T(8,128)(2,1)S(1)} %get-tuple-element.27.pay), channel_id=1, source_target_pairs={{0,224},{32,0},{64,32},{96,64},{128,96},{160,128},{192,160},{224,1... | collective-permute-start | bytes 884744 | tf_op jit(solution)/shard_map/ppermute | solution.py:51
  70.3 8.4 %collective-permute-start.16 = (bf16[144,1024]{1,0:T(8,128)(2,1)S(1)}, bf16[144,1024]{1,0:T(8,128)(2,1)S(1)}, u32[]{:S(2)}, u32[]{:S(2)}) collective-permute-start(bf16[144,1024]{1,0:T(8,128)(2,1)S(1)} %collective-permute-done.15.refs_0_), channel_id=1, source_target_pairs={{0,32},{32,64},{64,96},{96,128},{128,160},{160,192},{192,224},{224... | collective-permute-start | bytes 884744 | tf_op jit(solution)/shard_map/ppermute | solution.py:51
  70.8 11.4 %collective-permute-start.20 = (bf16[144,1024]{1,0:T(8,128)(2,1)S(1)}, bf16[144,1024]{1,0:T(8,128)(2,1)S(1)}, u32[]{:S(2)}, u32[]{:S(2)}) collective-permute-start(bf16[144,1024]{1,0:T(8,128)(2,1)S(1)} %collective-permute-done.19.refs_1_), channel_id=1, source_target_pairs={{0,224},{32,0},{64,32},{96,64},{128,96},{160,128},{192,160},{224,1... | collective-permute-start | bytes 884744 | tf_op jit(solution)/shard_map/ppermute | solution.py:51
  78.7 12.8 %collective-permute-start.17 = (bf16[144,1024]{1,0:T(8,128)(2,1)S(1)}, bf16[144,1024]{1,0:T(8,128)(2,1)S(1)}, u32[]{:S(2)}, u32[]{:S(2)}) collective-permute-start(bf16[144,1024]{1,0:T(8,128)(2,1)S(1)} %collective-permute-done.16.refs_0_), channel_id=1, source_target_pairs={{0,32},{32,64},{64,96},{96,128},{128,160},{160,192},{192,224},{224... | collective-permute-start | bytes 884744 | tf_op jit(solution)/shard_map/ppermute | solution.py:51
  82.2 11.4 %collective-permute-start.21 = (bf16[144,1024]{1,0:T(8,128)(2,1)S(1)}, bf16[144,1024]{1,0:T(8,128)(2,1)S(1)}, u32[]{:S(2)}, u32[]{:S(2)}) collective-permute-start(bf16[144,1024]{1,0:T(8,128)(2,1)S(1)} %collective-permute-done.20.refs_1_), channel_id=1, source_target_pairs={{0,224},{32,0},{64,32},{96,64},{128,96},{160,128},{192,160},{224,1... | collective-permute-start | bytes 884744 | tf_op jit(solution)/shard_map/ppermute | solution.py:51
  91.5 11.4 %collective-permute-start.18 = (bf16[144,1024]{1,0:T(8,128)(2,1)S(1)}, bf16[144,1024]{1,0:T(8,128)(2,1)S(1)}, u32[]{:S(2)}, u32[]{:S(2)}) collective-permute-start(bf16[144,1024]{1,0:T(8,128)(2,1)S(1)} %collective-permute-done.17.refs_0_), channel_id=1, source_target_pairs={{0,32},{32,64},{64,96},{96,128},{128,160},{160,192},{192,224},{224... | collective-permute-start | bytes 884744 | tf_op jit(solution)/shard_map/ppermute | solution.py:51
  107.9 1.7 %collective-permute-start.22 = (f32[72,1024]{1,0:T(8,128)S(1)}, f32[72,1024]{1,0:T(8,128)S(1)}, u32[]{:S(2)}, u32[]{:S(2)}) collective-permute-start(f32[72,1024]{1,0:T(8,128)S(1)} %get-tuple-element.41), channel_id=1, source_target_pairs={{0,4},{4,0},{1,5},{5,1},{2,6},{6,2},{3,7},{7,3},{8,12},{12,8},{9,1... | collective-permute-start | bytes 884744 | tf_op jit(solution)/shard_map/ppermute | solution.py:51
  110.6 16.1 %all-to-all-start.2 = ((bf16[16,2,2048]{2,1,0:T(2,128)(2,1)}), bf16[16,2,2048]{2,1,0:T(2,128)(2,1)S(1)}, u32[]{:S(2)}, u32[]{:S(2)}) async-start(bf16[16,2,2048]{2,1,0:T(2,128)(2,1)} %reshape.23), calls=%async_computation.2 | async-start | bytes 262144 | tf_op jit(solution)/shard_map/all_to_all | solution.py:340
  128.3 32.7 %copy-start = (f32[1024]{0:T(1024)S(1)}, f32[1024]{0:T(1024)}, u32[]{:S(2)}) copy-start(f32[1024]{0:T(1024)} %param.17) | copy-start | bytes 12292
  128.3 32.7 %all-to-all-start.3 = ((bf16[16,2,8,16,256]{4,3,2,1,0:T(8,128)(2,1)}), bf16[16,2,8,16,256]{4,3,2,1,0:T(8,128)(2,1)S(1)}, u32[]{:S(2)}, u32[]{:S(2)}) async-start(bf16[16,2,8,16,256]{4,3,2,1,0:T(8,128)(2,1)} %broadcast_in_dim.28), calls=%async_computation.3 | async-start | bytes 4194304 | tf_op jit(solution)/shard_map/all_to_all | solution.py:314
where the time goes:
time: 164 us; the launch traced here: 163 us
  waiting for transfers between devices  60.3 us (37%)
  starting transfers between devices  47.2 us (29%)
  Pallas kernels  38.3 us (23%)
  blocking collectives  9.54 us (6%)
  local copies, waits for them, and re-layouts  6.77 us (4%)
    ppermute x23, starting transfers between devices, shift(): return lax.ppermute(x, axis, [(i, (i + k) % n) for i in range(n)])  28.8 us
    all_to_all x1, waiting for transfers between devices, shards(): w_o = lax.all_to_all(w_o, ('x', 'y'), 0, 0, tiled=True)  28.6 us
    pallas_call x4, Pallas kernels, shards(): call(functools.partial(step_body, k), outs, [SMEM] + [VMEM] * (len(ins) -...  28.4 us
    ppermute x23, waiting for transfers between devices, shift(): return lax.ppermute(x, axis, [(i, (i + k) % n) for i in range(n)])  23.9 us
    all_to_all x1, blocking collectives, shards(): w_x = lax.all_to_all(per_head, 'x', 0, 0, tiled=True).reshape(64, 256)  9.54 us
    all_to_all x1, starting transfers between devices, shards(): att = lax.all_to_all(att.reshape(16, 64, HD), ('x', 'y'), 0, 0, tiled=True)  8.25 us
    all_to_all x1, waiting for transfers between devices, shards(): att = lax.all_to_all(att.reshape(16, 64, HD), ('x', 'y'), 0, 0, tiled=True)  7.8 us
    all_to_all x1, starting transfers between devices, shards(): lax.all_to_all(jnp.broadcast_to(chunk[None], (NZ, 80, 256)), 'z', 0, 0, t...  6.3 us
  transfers between devices with their start and end apart: 26, of which 13 were waited for; matrix products, arithmetic and copies ran while one was open for 0% of the time, Pallas kernels for 17%

commit v1 on v0

--- a/solution.py
+++ b/solution.py
@@ -55,6 +55,14 @@
     return [x] + [shift(x, axis, k) for k in range(1, SIZES[axis])]
 
 
+def step_right(x, k):
+    return lax.ppermute(x, "z", [(i, i + 1) for i in range(k - 1, NZ - 1)])
+
+
+def step_left(x, k):
+    return lax.ppermute(x, "z", [((i - k + 1) % NZ, (i - k) % NZ) for i in range(3)])
+
+
 def three_parts(x):
     hi = x.astype(BF16)
     rest = x - hi.astype(F32)
@@ -63,15 +71,33 @@
     return hi, mid, low
 
 
+def pack_body(idx, tok, wq, wk, wv, wf, lo, hi, p0, p1, p2, p3, heads):
+    x = idx[1]
+    lo[...] = tok[0:32, :]
+    hi[...] = tok[32:64, :]
+    for h in range(NX):
+        lanes = slice(h * HD, (h + 1) * HD)
+        gate = jnp.broadcast_to(wf[:, h : h + 1].astype(F32), (16, HD)).astype(BF16)
+        heads[h] = jnp.concatenate([wq[:, lanes], wk[:, lanes], wv[:, lanes], gate], axis=1)
+    for k, out in enumerate((p0, p1, p2, p3)):
+        out[...] = heads[lax.rem(x + k, NX)]
+
+
+def spread_body(p0, p1, p2, p3, wo, out):
+    for z in range(NZ):
+        for k, piece in enumerate((p0, p1, p2, p3, wo)):
+            out[z, k * 16 : k * 16 + 16, :] = piece[...]
+
+
 def project_body(idx, offs, *refs):
     toks = refs[:8]
     gain, w_own, w_sib = refs[8:11]
-    q_out, kv_out, cum_out = refs[11:14]
+    qc_out, kv_out, cum_out = refs[11:14]
     w, rows = refs[14:]
     x, c, y = idx[1], idx[2], idx[3]
     for z in range(NZ):
         for xx in range(NX):
-            base = z * 128 + xx * 32
+            base = z * 128 + lax.rem(x - xx + NX, NX) * 32
             own_at = pl.multiple_of(base + c * 16, 16)
             sib_at = pl.multiple_of(base + (1 - c) * 16, 16)
             w[pl.ds(own_at, 16), :] = w_own[z, xx * 16 : xx * 16 + 16, :]
@@ -94,7 +120,7 @@
     for b in range(4):
         t = rows[b * BLK : (b + 1) * BLK, :].T
         lanes = slice(b * BLK, (b + 1) * BLK)
-        q_out[:, lanes] = t[:64].astype(BF16)
+        qc_out[0:64, lanes] = t[:64].astype(BF16)
         kv_out[:, lanes] = t[64:192].astype(BF16)
         logit = t[192:200] + offs[x] + math.log(TOTAL)
         gate = jnp.minimum(logit, 0.0) - jnp.log1p(jnp.exp(-jnp.abs(logit)))
@@ -103,9 +129,14 @@
         cum = cum + jnp.dot(mid, ones, preferred_element_type=F32)
         cum = cum + jnp.dot(low, ones, preferred_element_type=F32)
         cum_out[:, lanes] = cum
-
-
-def prepare_body(idx, q_own, q_sib, kv, cum_own, cum_sib, q_out, pay_out):
+        row = lax.broadcasted_iota(jnp.int32, (16, BLK), 0)
+        block = jnp.zeros((16, BLK), F32)
+        for i, part in enumerate(three_parts(cum[0:1])):
+            block = jnp.where(row == i, part.astype(F32), block)
+        qc_out[64:80, lanes] = block.astype(BF16)
+
+
+def prepare_body(idx, q_own, q_sib, kv, cum_own, q_out, pay_out):
     c = idx[2]
     q_out[80:128, :] = jnp.zeros((48, QS), BF16)
     row = lax.broadcasted_iota(jnp.int32, (16, QS), 0)
@@ -114,10 +145,14 @@
         lanes = slice(b * BLK, (b + 1) * BLK)
         own_at = pl.multiple_of((2 * b + c) * BLK, BLK)
         sib_at = pl.multiple_of((2 * b + 1 - c) * BLK, BLK)
-        q_out[0:64, pl.ds(own_at, BLK)] = q_own[:, lanes] * jnp.asarray(0.125, BF16)
-        q_out[0:64, pl.ds(sib_at, BLK)] = q_sib[:, lanes] * jnp.asarray(0.125, BF16)
-    own = [cum_own[:, b * BLK + BLK - 1 : b * BLK + BLK] for b in range(4)]
-    sib = [cum_sib[:, b * BLK + BLK - 1 : b * BLK + BLK] for b in range(4)]
+        q_out[0:64, pl.ds(own_at, BLK)] = q_own[0:64, lanes] * jnp.asarray(0.125, BF16)
+        q_out[0:64, pl.ds(sib_at, BLK)] = q_sib[0:64, lanes] * jnp.asarray(0.125, BF16)
+    own, sib = [], []
+    for b in range(4):
+        end = slice(b * BLK + BLK - 1, b * BLK + BLK)
+        own.append(cum_own[:, end])
+        parts = q_sib[64:80, b * BLK + 128 : b * BLK + BLK].astype(F32)[:, 127:128]
+        sib.append(jnp.broadcast_to(parts[0:1] + parts[1:2] + parts[2:3], (8, 1)))
     ahead = jnp.zeros_like(own[0])
     bases = []
     for b in range(4):
@@ -153,42 +188,65 @@
     vx[i, 64:80, :] = jnp.ones((16, KEYS), BF16)
 
 
-def absorb(count, q, acc, m, kx, vx, move, c=None):
+def absorb(count, q, acc, m, kx, vx, move, work, c=None):
+    tiles = QS // BLK
+    bufs, tops, probs, fades = work[0:2], work[2:4], work[4:6], work[6:8]
     if c is not None:
         key = lax.broadcasted_iota(jnp.int32, (KEYS, BLK), 0)
         key_pos = key + (key // BLK + c) * BLK
         query = lax.broadcasted_iota(jnp.int32, (KEYS, BLK), 1)
 
-    def two_tiles(t, carry):
-        i = t // 4
-        lanes, s = [], []
-        for u in range(2):
-            b = (t % 4) * 2 + u
-            at = pl.ds(pl.multiple_of(b * BLK, BLK), BLK)
-            part = jnp.dot(kx[i], q[:, at], preferred_element_type=F32)
-            if c is not None:
-                part = jnp.where(key_pos <= query + b * BLK, part, LOW)
-            lanes.append(at)
-            s.append(part)
+    def lanes_of(t):
+        return pl.ds(pl.multiple_of((t % tiles) * BLK, BLK), BLK)
+
+    def score(t, slot):
+        s = jnp.dot(kx[t // tiles], q[:, lanes_of(t)], preferred_element_type=F32)
+        if c is not None:
+            s = jnp.where(key_pos <= query + (t % tiles) * BLK, s, LOW)
+        bufs[slot][...] = s
+        tops[slot][...] = jnp.broadcast_to(jnp.max(s, axis=0, keepdims=True), (8, BLK))
+
+    def weigh(t, slot):
+        i, lanes = t // tiles, lanes_of(t)
         by = move[i, 0:1]
-        for u in range(2):
-            old = m[i, 0:1, lanes[u]]
-            new = jnp.maximum(old, jnp.max(s[u], axis=0, keepdims=True) + by)
-            p = jnp.exp(s[u] - (new - by)).astype(BF16)
-            part = jnp.dot(vx[i], p, preferred_element_type=F32)
-            acc[i, :, lanes[u]] = acc[i, :, lanes[u]] * jnp.exp(old - new) + part
-            m[i, :, lanes[u]] = jnp.broadcast_to(new, (8, BLK))
-        return carry
-
-    lax.fori_loop(0, count * 4, two_tiles, 0)
-
-
-def first_body(idx, q, pay, acc, m, sums, kx, vx, move):
+        old = m[i, 0:1, lanes]
+        new = jnp.maximum(old, tops[slot][0:1] + by)
+        probs[slot][...] = jnp.exp(bufs[slot][...] - (new - by)).astype(BF16)
+        fades[slot][...] = jnp.broadcast_to(jnp.exp(old - new), (8, BLK))
+        m[i, :, lanes] = jnp.broadcast_to(new, (8, BLK))
+
+    def add(t, slot):
+        i, lanes = t // tiles, lanes_of(t)
+        part = jnp.dot(vx[i], probs[slot][...], preferred_element_type=F32)
+        acc[i, :, lanes] = acc[i, :, lanes] * fades[slot][0:1] + part
+
+    @pl.when(count > 0)
+    def _():
+        probs[1][...] = jnp.zeros((KEYS, BLK), BF16)
+        fades[1][...] = jnp.ones((8, BLK), F32)
+        score(0, 0)
+        last = count * tiles - 1
+
+        def two_tiles(j, carry):
+            t = 2 * j
+            add(jnp.maximum(t - 1, 0), 1)
+            weigh(t, 0)
+            score(t + 1, 1)
+            add(t, 0)
+            weigh(t + 1, 1)
+            score(jnp.minimum(t + 2, last), 0)
+            return carry
+
+        lax.fori_loop(0, count * (tiles // 2), two_tiles, 0)
+        add(last, 1)
+
+
+def first_body(idx, q, pay, acc, m, sums, kx, vx, move, *bufs):
     acc[...] = jnp.zeros_like(acc)
     m[...] = jnp.full(m.shape, LOW, F32)
     move[...] = jnp.zeros_like(move)
     place_chunk(pay, 0, kx, vx)
-    absorb(1, q, acc, m, kx, vx, move, idx[2])
+    absorb(1, q, acc, m, kx, vx, move, bufs, idx[2])
     sums[...] = jnp.broadcast_to(chunk_total(pay), sums.shape)
 
 
@@ -198,9 +256,9 @@
     pays, refs = refs[:n_pay], refs[n_pay:]
     acc0, m0, sums0, refs = refs[0], refs[1], refs[2], refs[3:]
     if k < 4:
-        acc, m, sums, kx, vx, move = refs
+        acc, m, sums, kx, vx, move, *bufs = refs
     else:
-        out, kx, vx, move, sums = refs
+        out_own, out_sib, kx, vx, move, *bufs, sums = refs
         acc, m = acc0, m0
     sums[...] = sums0[...]
     count = (z >= k).astype(jnp.int32)
@@ -220,7 +278,7 @@
             move[1] = jnp.zeros(sums.shape, F32)
             m[1] = m[1] + chunk_total(pays[1])[:, 0:1]
 
-    absorb(count, q, acc, m, kx, vx, move)
+    absorb(count, q, acc, m, kx, vx, move, bufs)
     if k == 4:
         c = idx[2]
         row = lax.broadcasted_iota(jnp.int32, (8, BLK), 0)
@@ -233,8 +291,9 @@
                 top = jnp.maximum(m_a, m_b)
                 both = acc[0, :, lanes] * jnp.exp(m_a - top) + acc[1, :, lanes] * jnp.exp(m_b - top)
                 to = slice(b * BLK, (b + 1) * BLK)
-                out[other, 0:64, to] = both[0:64]
-                out[other, 64:72, to] = jnp.where(row < 4, both[64:65], top)
+                out = out_own if other == 0 else out_sib
+                out[0:64, to] = both[0:64]
+                out[64:72, to] = jnp.where(row < 4, both[64:65], top)
 
 
 def merge_body(own, sib, out):
@@ -249,15 +308,20 @@
         out[r * 128 : (r + 1) * 128, :] = att[:, r * 128 : (r + 1) * 128].T[:, 0:64].astype(BF16)
 
 
-def final_body(idx, att, gain, w_all, out, w):
-    c = idx[2]
-    for xs in range(NX):
-        for ys in range(NY):
+def assemble_body(idx, w0, w1, w2, w3, w):
+    x, c, y = idx[1], idx[2], idx[3]
+    for ky, ref in enumerate((w0, w1, w2, w3)):
+        cols = pl.ds(pl.multiple_of(lax.rem(y - ky + NY, NY) * 256, 256), 256)
+        for kx in range(NX):
+            xx = lax.rem(x - kx + NX, NX)
             for other in range(2):
                 cc = c if other == 0 else 1 - c
                 for z in range(NZ):
-                    at = pl.multiple_of(z * 128 + xs * 32 + cc * 16, 16)
-                    w[pl.ds(at, 16), ys * 256 : ys * 256 + 256] = w_all[xs * NY + ys, other, z]
+                    at = pl.multiple_of(z * 128 + xx * 32 + cc * 16, 16)
+                    w[pl.ds(at, 16), cols] = ref[kx, other, z]
+
+
+def final_body(att, gain, w, out):
     pieces = [att[xs * NY + ys] for ys in range(NY) for xs in range(NX)]
     joined = jnp.concatenate(pieces, axis=1)
     proj = lax.dot_general(joined, w[...], (((1,), (1,)), ((), ())), preferred_element_type=F32)
@@ -269,61 +333,71 @@
     sds = jax.ShapeDtypeStruct
     idx = jnp.stack([lax.axis_index(a) for a in AXES]).astype(jnp.int32)
 
-    tok_a = direct(tokens[:32], "y")
-    tok_b = direct(tokens[32:], "x")
+    half, piece = sds((32, D), BF16), sds((16, 256), BF16)
+    tok_lo, tok_hi, *pieces = call(
+        pack_body,
+        (half, half, piece, piece, piece, piece),
+        [SMEM] + [VMEM] * 5,
+        [pltpu.VMEM((NX, 16, 256), BF16)],
+    )(idx, tokens, w_query, w_key, w_value, w_forget)
+
+    pieces = [pieces[0]] + [shift(pieces[k], "x", k) for k in range(1, NX)]
+    tok_a = direct(tok_lo, "y")
+    tok_b = direct(tok_hi, "x")
     toks = direct(jnp.concatenate(tok_a, axis=0), "x")
     toks = toks + direct(jnp.concatenate(tok_b, axis=0), "y")
-
-    heads = [w.reshape(16, NX, HD) for w in (w_query, w_key, w_value)]
-    heads.append(jnp.broadcast_to(w_forget[:, :, None], (16, NX, HD)))
-    per_head = jnp.concatenate(heads, axis=2).transpose(1, 0, 2)
-    w_x = lax.all_to_all(per_head, "x", 0, 0, tiled=True).reshape(64, 256)
-    chunk = jnp.concatenate([w_x, w_out_t], axis=0)
-    w_own = lax.all_to_all(jnp.broadcast_to(chunk[None], (NZ, 80, 256)), "z", 0, 0, tiled=True)
+    chunk = call(spread_body, sds((NZ, 80, 256), BF16), [VMEM] * 5)(*pieces, w_out_t)
+    w_own = lax.all_to_all(chunk, "z", 0, 0, tiled=True)
     w_sib = shift(w_own, "c", 1)
 
     q_own, kv, cum_own = call(
         project_body,
-        (sds((64, KEYS), BF16), sds((128, KEYS), BF16), sds((8, KEYS), F32)),
+        (sds((80, KEYS), BF16), sds((128, KEYS), BF16), sds((8, KEYS), F32)),
         [SMEM, SMEM] + [VMEM] * 11,
         [pltpu.VMEM((D, 256), BF16), pltpu.VMEM((KEYS, 256), F32)],
         2e9,
     )(idx, forget_offset, *toks, norm_gain[None], w_own, w_sib)
 
     q_sib = shift(q_own, "c", 1)
-    cum_sib = shift(cum_own, "c", 1)
     q, pay = call(
-        prepare_body, (sds((128, QS), BF16), sds((PAY, KEYS), BF16)), [SMEM] + [VMEM] * 5
-    )(idx, q_own, q_sib, kv, cum_own, cum_sib)
+        prepare_body, (sds((128, QS), BF16), sds((PAY, KEYS), BF16)), [SMEM] + [VMEM] * 4
+    )(idx, q_own, q_sib, kv, cum_own)
 
     acc_t, m_t, sums_t = sds((2, 80, QS), F32), sds((2, 8, QS), F32), sds((8, BLK), F32)
     work = [
         pltpu.VMEM((2, KEYS, 128), BF16),
         pltpu.VMEM((2, 80, KEYS), BF16),
         pltpu.VMEM((2, 8, BLK), F32),
+        pltpu.VMEM((KEYS, BLK), F32),
+        pltpu.VMEM((KEYS, BLK), F32),
+        pltpu.VMEM((8, BLK), F32),
+        pltpu.VMEM((8, BLK), F32),
+        pltpu.VMEM((KEYS, BLK), BF16),
+        pltpu.VMEM((KEYS, BLK), BF16),
+        pltpu.VMEM((8, BLK), F32),
+        pltpu.VMEM((8, BLK), F32),
     ]
-    right = shift(pay, "z", 1)
-    left = shift(pay, "z", -1)
+    right = step_right(pay, 1)
+    left = step_left(pay, 1)
     acc, m, sums = call(
         first_body, (acc_t, m_t, sums_t), [SMEM, VMEM, VMEM], work, 3e9
     )(idx, q, pay)
 
     w_o = jnp.stack([w_own[:, 64:], w_sib[:, 64:]])
     w_o, _ = lax.optimization_barrier((w_o, sums))
-    w_o = jnp.broadcast_to(w_o[None], (16, 2, 8, 16, 256))
-    w_o = lax.all_to_all(w_o, ("x", "y"), 0, 0, tiled=True)
+    w_o = direct(w_o, "x")
 
     for k in range(1, 5):
         pays = (right, left) if k < 4 else (right,)
         if k < 4:
-            right = shift(pays[0], "z", 1)
+            right = step_right(pays[0], k + 1)
         if k < 3:
-            left = shift(pays[1], "z", -1)
+            left = step_left(pays[1], k + 1)
         ins = (idx, q) + pays + (acc, m, sums)
         if k < 4:
             outs, scratch, aliases = (acc_t, m_t, sums_t), work, {4: 0, 5: 1}
         else:
-            outs, aliases = sds((2, 72, KEYS), F32), None
+            outs, aliases = (sds((72, KEYS), F32), sds((72, KEYS), F32)), None
             scratch = work + [pltpu.VMEM(sums_t.shape, F32)]
         res = call(
             functools.partial(step_body, k),
@@ -335,12 +409,14 @@
         )(*ins)
         if k < 4:
             acc, m, sums = res
+        if k == 1:
+            w_o, _ = lax.optimization_barrier((jnp.stack(w_o), sums))
+            w_o = direct(w_o, "y")
     sib = shift(res[1], "c", 1)
+    w_full = call(assemble_body, sds((D, D), BF16), [SMEM] + [VMEM] * 4)(idx, *w_o)
     att = call(merge_body, sds((KEYS, HD), BF16), [VMEM, VMEM])(res[0], sib)
     att = lax.all_to_all(att.reshape(16, 64, HD), ("x", "y"), 0, 0, tiled=True)
-    return call(
-        final_body, sds((OWN, D), BF16), [SMEM] + [VMEM] * 3, [pltpu.VMEM((D, D), BF16)]
-    )(idx, att, out_gain[None], w_o)
+    return call(final_body, sds((OWN, D), BF16), [VMEM] * 3)(att, out_gain[None], w_full)
 
 
 def solution(mesh):

time: 164 us -> 134 us (0.82)
  the two profiles are of different devices: /device:TPU:192 before, /device:TPU:160 now
where the time goes in v1:
time: 134 us; the launch traced here: 133 us
  starting transfers between devices  61.6 us (46%)
  waiting for transfers between devices  31.6 us (24%)
  Pallas kernels  30 us (22%)
  local copies, waits for them, and re-layouts  9.33 us (7%)
    ppermute x24, starting transfers between devices, shift(): return lax.ppermute(x, axis, [(i, (i + k) % n) for i in range(n)])  30.3 us
    ppermute x24, waiting for transfers between devices, shift(): return lax.ppermute(x, axis, [(i, (i + k) % n) for i in range(n)])  27.4 us
    pallas_call x4, Pallas kernels, shards(): call(functools.partial(step_body, k), outs, [SMEM] + [VMEM] * (len(ins) -...  18.8 us
    ppermute x4, starting transfers between devices, step_right(): return lax.ppermute(x, 'z', [(i, i + 1) for i in range(k - 1, NZ - 1)])  17.2 us
    unnamed x33, local copies, waits for them, and re-layouts  9.3 us
    all_to_all x1, starting transfers between devices, shards(): w_own = lax.all_to_all(chunk, 'z', 0, 0, tiled=True)  6.75 us
    all_to_all x1, starting transfers between devices, shards(): att = lax.all_to_all(att.reshape(16, 64, HD), ('x', 'y'), 0, 0, tiled=True)  4.72 us
    pallas_call x1, Pallas kernels, shards(): call(first_body, (acc_t, m_t, sums_t), [SMEM, VMEM, VMEM], work, 30000000...  4.39 us
  transfers between devices with their start and end apart: 33, of which 14 were waited for; matrix products, arithmetic and copies ran while one was open for 1% of the time, Pallas kernels for 19%

profile of v1, /device:TPU:160, one launch (start us, length us, event | category | flops | bytes accessed | tf_op | source)
XLA Modules:
  0.0 133.1 jit_solution(11764351504572157523)
XLA Ops:
  0.0 0.8 copy.16.wf
  0.9 0.9 copy-done.5
  4.5 3.1 %collective-permute-start.2 = (bf16[32,1024]{1,0:T(8,128)(2,1)S(1)}, bf16[32,1024]{1,0:T(8,128)(2,1)S(1)}, u32[]{:S(2)}, u32[]{:S(2)}) collective-permute-start(bf16[32,1024]{1,0:T(8,128)(2,1)S(1)} %get-tuple-element.32), channel_id=1, source_target_pairs={{0,3},{1,0},{2,1},{3,2},{4,7},{5,4},{6,5},{7,6},{8,11},{9,8},{10,9... | collective-permute-start | bytes 196616 | tf_op jit(solution)/shard_map/ppermute | solution.py:51
  8.2 1.5 %collective-permute-start.12 = (bf16[16,256]{1,0:T(8,128)(2,1)S(1)}, bf16[16,256]{1,0:T(8,128)(2,1)S(1)}, u32[]{:S(2)}, u32[]{:S(2)}) collective-permute-start(bf16[16,256]{1,0:T(8,128)(2,1)S(1)} %get-tuple-element.35), channel_id=1, source_target_pairs={{0,8},{8,16},{16,24},{24,0},{1,9},{9,17},{17,25},{25,1},{2,10},{10... | collective-permute-start | bytes 24584 | tf_op jit(solution)/shard_map/ppermute | solution.py:51
  9.7 2.7 %collective-permute-start.13 = (bf16[16,256]{1,0:T(8,128)(2,1)S(1)}, bf16[16,256]{1,0:T(8,128)(2,1)S(1)}, u32[]{:S(2)}, u32[]{:S(2)}) collective-permute-start(bf16[16,256]{1,0:T(8,128)(2,1)S(1)} %get-tuple-element.36), channel_id=1, source_target_pairs={{0,16},{8,24},{16,0},{24,8},{1,17},{9,25},{17,1},{25,9},{2,18},{10... | collective-permute-start | bytes 24584 | tf_op jit(solution)/shard_map/ppermute | solution.py:51
  12.4 1.4 %collective-permute-start.14 = (bf16[16,256]{1,0:T(8,128)(2,1)S(1)}, bf16[16,256]{1,0:T(8,128)(2,1)S(1)}, u32[]{:S(2)}, u32[]{:S(2)}) collective-permute-start(bf16[16,256]{1,0:T(8,128)(2,1)S(1)} %get-tuple-element.37), channel_id=1, source_target_pairs={{0,24},{8,0},{16,8},{24,16},{1,25},{9,1},{17,9},{25,17},{2,26},{10... | collective-permute-start | bytes 24584 | tf_op jit(solution)/shard_map/ppermute | solution.py:51
  13.9 1.0 collective-permute-start
  14.9 1.7 %collective-permute-start.8 = (bf16[32,1024]{1,0:T(8,128)(2,1)S(1)}, bf16[32,1024]{1,0:T(8,128)(2,1)S(1)}, u32[]{:S(2)}, u32[]{:S(2)}) collective-permute-start(bf16[32,1024]{1,0:T(8,128)(2,1)S(1)} %get-tuple-element.33), channel_id=1, source_target_pairs={{0,24},{8,0},{16,8},{24,16},{1,25},{9,1},{17,9},{25,17},{2,26},{10... | collective-permute-start | bytes 196616 | tf_op jit(solution)/shard_map/ppermute | solution.py:51
  18.4 6.8 %all-to-all-start = ((bf16[8,80,256]{2,1,0:T(8,128)(2,1)}), bf16[8,80,256]{2,1,0:T(8,128)(2,1)S(1)}, u32[]{:S(2)}, u32[]{:S(2)}) async-start(bf16[8,80,256]{2,1,0:T(8,128)(2,1)} %shard_map.92), calls=%async_computation | async-start | bytes 655360 | tf_op jit(solution)/shard_map/all_to_all | solution.py:350
  25.2 3.4 %collective-permute-start.7 = (bf16[32,1024]{1,0:T(8,128)(2,1)S(1)}, bf16[32,1024]{1,0:T(8,128)(2,1)S(1)}, u32[]{:S(2)}, u32[]{:S(2)}) collective-permute-start(bf16[32,1024]{1,0:T(8,128)(2,1)S(1)} %get-tuple-element.33), channel_id=1, source_target_pairs={{0,16},{8,24},{16,0},{24,8},{1,17},{9,25},{17,1},{25,9},{2,18},{10... | collective-permute-start | bytes 196616 | tf_op jit(solution)/shard_map/ppermute | solution.py:51
  28.6 2.4 %collective-permute-done.7 = bf16[32,1024]{1,0:T(8,128)(2,1)S(1)} collective-permute-done((bf16[32,1024]{1,0:T(8,128)(2,1)S(1)}, bf16[32,1024]{1,0:T(8,128)(2,1)S(1)}, u32[]{:S(2)}, u32[]{:S(2)}) %collective-permute-start.7) | collective-permute-done | bytes 65568 | tf_op jit(solution)/shard_map/ppermute | solution.py:51
  31.1 2.3 %collective-permute-start.11 = (bf16[128,1024]{1,0:T(8,128)(2,1)S(1)}, bf16[128,1024]{1,0:T(8,128)(2,1)S(1)}, u32[]{:S(2)}, u32[]{:S(2)}) collective-permute-start(bf16[128,1024]{1,0:T(8,128)(2,1)S(1)} %constant_dynamic-update-slice_fusion.4.refs_4_), channel_id=1, source_target_pairs={{0,3},{1,0},{2,1},{3,2},{4,7},{5,4},{6,5},{7,6},{8,11},{9,8},{10,9... | collective-permute-start | bytes 786440 | tf_op jit(solution)/shard_map/ppermute | solution.py:51
  33.4 1.7 %collective-permute-start.10 = (bf16[128,1024]{1,0:T(8,128)(2,1)S(1)}, bf16[128,1024]{1,0:T(8,128)(2,1)S(1)}, u32[]{:S(2)}, u32[]{:S(2)}) collective-permute-start(bf16[128,1024]{1,0:T(8,128)(2,1)S(1)} %constant_dynamic-update-slice_fusion.4.refs_4_), channel_id=1, source_target_pairs={{0,2},{1,3},{2,0},{3,1},{4,6},{5,7},{6,4},{7,5},{8,10},{9,11},{10,... | collective-permute-start | bytes 786440 | tf_op jit(solution)/shard_map/ppermute | solution.py:51
  35.6 3.0 %collective-permute-start.5 = (bf16[128,1024]{1,0:T(8,128)(2,1)S(1)}, bf16[128,1024]{1,0:T(8,128)(2,1)S(1)}, u32[]{:S(2)}, u32[]{:S(2)}) collective-permute-start(bf16[128,1024]{1,0:T(8,128)(2,1)S(1)} %constant_dynamic-update-slice_fusion.refs_0_), channel_id=1, source_target_pairs={{0,24},{8,0},{16,8},{24,16},{1,25},{9,1},{17,9},{25,17},{2,26},{10... | collective-permute-start | bytes 786440 | tf_op jit(solution)/shard_map/ppermute | solution.py:51
  38.6 2.1 %collective-permute-done.11.refs_7_ = bf16[128,1024]{1,0:T(8,128)(2,1)S(1)} collective-permute-done((bf16[128,1024]{1,0:T(8,128)(2,1)S(1)}, bf16[128,1024]{1,0:T(8,128)(2,1)S(1)}, u32[]{:S(2)}, u32[]{:S(2)}) %collective-permute-start.11) | collective-permute-done | bytes 262176 | tf_op jit(solution)/shard_map/ppermute | solution.py:51
  42.3 2.1 %collective-permute-done.9.refs_5_ = bf16[128,1024]{1,0:T(8,128)(2,1)S(1)} collective-permute-done((bf16[128,1024]{1,0:T(8,128)(2,1)S(1)}, bf16[128,1024]{1,0:T(8,128)(2,1)S(1)}, u32[]{:S(2)}, u32[]{:S(2)}) %collective-permute-start.9) | collective-permute-done | bytes 262176 | tf_op jit(solution)/shard_map/ppermute | solution.py:51
  44.4 6.1 %collective-permute-done.5.refs_3_ = bf16[128,1024]{1,0:T(8,128)(2,1)S(1)} collective-permute-done((bf16[128,1024]{1,0:T(8,128)(2,1)S(1)}, bf16[128,1024]{1,0:T(8,128)(2,1)S(1)}, u32[]{:S(2)}, u32[]{:S(2)}) %collective-permute-start.5) | collective-permute-done | bytes 262176 | tf_op jit(solution)/shard_map/ppermute | solution.py:51
  50.4 0.9 collective-permute-done.4.refs_2_
  51.4 2.8 %collective-permute-done.3.refs_1_ = bf16[128,1024]{1,0:T(8,128)(2,1)S(1)} collective-permute-done((bf16[128,1024]{1,0:T(8,128)(2,1)S(1)}, bf16[128,1024]{1,0:T(8,128)(2,1)S(1)}, u32[]{:S(2)}, u32[]{:S(2)}) %collective-permute-start.3) | collective-permute-done | bytes 262176 | tf_op jit(solution)/shard_map/ppermute | solution.py:51
  54.1 2.1 %shard_map.93 = (bf16[80,1024]{1,0:T(8,128)(2,1)S(1)}, bf16[128,1024]{1,0:T(8,128)(2,1)S(1)}, f32[8,1024]{1,0:T(8,128)S(1)}) custom-call(s32[4]{0:T(128)S(1)} %pad_add_fusion.idx, f32[4]{0:T(128)S(1)} %copy-done.11, bf16[128,1024]{1,0:T(8,128)(2,1)S(1)} %constant_dynamic-update-slice_fusion.refs_0_, bf16[128,1024]{1,0:T(8,128)(2,1)S(1)} %collective-permute-done.3.refs_1_, ...), custom_call_target="tpu_custom_call" | custom-call | flops 2000000000 | bytes 1048576 | tf_op jit(solution)/shard_map/pallas_call | solution.py:353
  56.4 1.3 %collective-permute-done.16.q_sib = bf16[80,1024]{1,0:T(8,128)(2,1)S(1)} collective-permute-done((bf16[80,1024]{1,0:T(8,128)(2,1)S(1)}, bf16[80,1024]{1,0:T(8,128)(2,1)S(1)}, u32[]{:S(2)}, u32[]{:S(2)}) %collective-permute-start.16) | collective-permute-done | bytes 163872 | tf_op jit(solution)/shard_map/ppermute | solution.py:51
  59.1 2.5 %collective-permute-start.17 = (bf16[144,1024]{1,0:T(8,128)(2,1)S(1)}, bf16[144,1024]{1,0:T(8,128)(2,1)S(1)}, u32[]{:S(2)}, u32[]{:S(2)}) collective-permute-start(bf16[144,1024]{1,0:T(8,128)(2,1)S(1)} %get-tuple-element.42.pay), channel_id=1, source_target_pairs={{0,32},{32,64},{64,96},{96,128},{128,160},{160,192},{192,224},{1,3... | collective-permute-start | bytes 884744 | tf_op jit(solution)/shard_map/ppermute | solution.py:59
  61.6 4.4 %shard_map.95 = (f32[2,80,2048]{2,1,0:T(8,128)S(1)}, f32[2,8,2048]{2,1,0:T(8,128)S(1)}, f32[8,256]{1,0:T(8,128)S(1)}) custom-call(s32[4]{0:T(128)S(1)} %pad_add_fusion.idx, bf16[128,2048]{1,0:T(8,128)(2,1)S(1)} %get-tuple-element.41.q, bf16[144,1024]{1,0:T(8,128)(2,1)S(1)} %get-tuple-element.42.pay), custom_call_target="tpu_custom_call" | custom-call | flops 3000000000 | bytes 1048576 | tf_op jit(solution)/shard_map/pallas_call | solution.py:382
  66.7 0.8 collective-permute-start.26
  67.5 0.8 collective-permute-start.25
  68.3 4.1 %collective-permute-done.27 = bf16[2,8,16,256]{3,2,1,0:T(8,128)(2,1)S(1)} collective-permute-done((bf16[2,8,16,256]{3,2,1,0:T(8,128)(2,1)S(1)}, bf16[2,8,16,256]{3,2,1,0:T(8,128)(2,1)S(1)}, u32[]{:S(2)}, u32[]{:S(2)}) %collective-permute-start.27) | collective-permute-done | bytes 131104 | tf_op jit(solution)/shard_map/ppermute | solution.py:51
  72.4 1.8 %collective-permute-done.26 = bf16[2,8,16,256]{3,2,1,0:T(8,128)(2,1)S(1)} collective-permute-done((bf16[2,8,16,256]{3,2,1,0:T(8,128)(2,1)S(1)}, bf16[2,8,16,256]{3,2,1,0:T(8,128)(2,1)S(1)}, u32[]{:S(2)}, u32[]{:S(2)}) %collective-permute-start.26) | collective-permute-done | bytes 131104 | tf_op jit(solution)/shard_map/ppermute | solution.py:51
  74.2 1.7 %collective-permute-done.25 = bf16[2,8,16,256]{3,2,1,0:T(8,128)(2,1)S(1)} collective-permute-done((bf16[2,8,16,256]{3,2,1,0:T(8,128)(2,1)S(1)}, bf16[2,8,16,256]{3,2,1,0:T(8,128)(2,1)S(1)}, u32[]{:S(2)}, u32[]{:S(2)}) %collective-permute-start.25) | collective-permute-done | bytes 131104 | tf_op jit(solution)/shard_map/ppermute | solution.py:51
  76.7 3.7 %collective-permute-start.18 = (bf16[144,1024]{1,0:T(8,128)(2,1)S(1)}, bf16[144,1024]{1,0:T(8,128)(2,1)S(1)}, u32[]{:S(2)}, u32[]{:S(2)}) collective-permute-start(bf16[144,1024]{1,0:T(8,128)(2,1)S(1)} %collective-permute-done.17.refs_0_), channel_id=1, source_target_pairs={{32,64},{64,96},{96,128},{128,160},{160,192},{192,224},{33,65},{65... | collective-permute-start | bytes 884744 | tf_op jit(solution)/shard_map/ppermute | solution.py:59
  80.4 3.9 %shard_map.96 = (f32[2,80,2048]{2,1,0:T(8,128)S(1)}, f32[2,8,2048]{2,1,0:T(8,128)S(1)}, f32[8,256]{1,0:T(8,128)S(1)}) custom-call(s32[4]{0:T(128)S(1)} %pad_add_fusion.idx, bf16[128,2048]{1,0:T(8,128)(2,1)S(1)} %get-tuple-element.41.q, bf16[144,1024]{1,0:T(8,128)(2,1)S(1)} %collective-permute-done.17.refs_0_, ...), custom_call_target="tpu_custom_call", output_to_operand_aliasing={{0}: (4, {}), {1}: (5, {})} | custom-call | flops 6000000000 | bytes 1048576 | tf_op jit(solution)/shard_map/pallas_call | solution.py:402
  84.3 2.1 %collective-permute-start.30 = (bf16[4,2,8,16,256]{4,3,2,1,0:T(8,128)(2,1)S(1)}, bf16[4,2,8,16,256]{4,3,2,1,0:T(8,128)(2,1)S(1)}, u32[]{:S(2)}, u32[]{:S(2)}) collective-permute-start(bf16[4,2,8,16,256]{4,3,2,1,0:T(8,128)(2,1)S(1)} %pad_maximum_fusion.w0), channel_id=1, source_target_pairs={{0,3},{1,0},{2,1},{3,2},{4,7},{5,4},{6,5},{7,6},{8,11},{9,8},{10,9... | collective-permute-start | bytes 1572872 | tf_op jit(solution)/shard_map/ppermute | solution.py:51
  87.7 1.3 collective-permute-start.23
  89.0 5.2 %collective-permute-start.19 = (bf16[144,1024]{1,0:T(8,128)(2,1)S(1)}, bf16[144,1024]{1,0:T(8,128)(2,1)S(1)}, u32[]{:S(2)}, u32[]{:S(2)}) collective-permute-start(bf16[144,1024]{1,0:T(8,128)(2,1)S(1)} %collective-permute-done.18.refs_0_), channel_id=1, source_target_pairs={{64,96},{96,128},{128,160},{160,192},{192,224},{65,97},{97,129},{1... | collective-permute-start | bytes 884744 | tf_op jit(solution)/shard_map/ppermute | solution.py:59
  94.2 3.9 %shard_map.97 = (f32[2,80,2048]{2,1,0:T(8,128)S(1)}, f32[2,8,2048]{2,1,0:T(8,128)S(1)}, f32[8,256]{1,0:T(8,128)S(1)}) custom-call(s32[4]{0:T(128)S(1)} %pad_add_fusion.idx, bf16[128,2048]{1,0:T(8,128)(2,1)S(1)} %get-tuple-element.41.q, bf16[144,1024]{1,0:T(8,128)(2,1)S(1)} %collective-permute-done.18.refs_0_, ...), custom_call_target="tpu_custom_call", output_to_operand_aliasing={{0}: (4, {}), {1}: (5, {})} | custom-call | flops 6000000000 | bytes 1048576 | tf_op jit(solution)/shard_map/pallas_call | solution.py:402
  98.1 1.1 collective-permute-done.19.refs_0_
  99.2 5.9 %collective-permute-start.20 = (bf16[144,1024]{1,0:T(8,128)(2,1)S(1)}, bf16[144,1024]{1,0:T(8,128)(2,1)S(1)}, u32[]{:S(2)}, u32[]{:S(2)}) collective-permute-start(bf16[144,1024]{1,0:T(8,128)(2,1)S(1)} %collective-permute-done.19.refs_0_), channel_id=1, source_target_pairs={{96,128},{128,160},{160,192},{192,224},{97,129},{129,161},{161,193... | collective-permute-start | bytes 884744 | tf_op jit(solution)/shard_map/ppermute | solution.py:59
  105.1 6.7 %shard_map.98 = (f32[2,80,2048]{2,1,0:T(8,128)S(1)}, f32[2,8,2048]{2,1,0:T(8,128)S(1)}, f32[8,256]{1,0:T(8,128)S(1)}) custom-call(s32[4]{0:T(128)S(1)} %pad_add_fusion.idx, bf16[128,2048]{1,0:T(8,128)(2,1)S(1)} %get-tuple-element.41.q, bf16[144,1024]{1,0:T(8,128)(2,1)S(1)} %collective-permute-done.19.refs_0_, ...), custom_call_target="tpu_custom_call", output_to_operand_aliasing={{0}: (4, {}), {1}: (5, {})} | custom-call | flops 6000000000 | bytes 1048576 | tf_op jit(solution)/shard_map/pallas_call | solution.py:402
  111.8 4.2 %shard_map.99 = (f32[72,1024]{1,0:T(8,128)S(1)}, f32[72,1024]{1,0:T(8,128)S(1)}) custom-call(s32[4]{0:T(128)S(1)} %pad_add_fusion.idx, bf16[128,2048]{1,0:T(8,128)(2,1)S(1)} %get-tuple-element.41.q, bf16[144,1024]{1,0:T(8,128)(2,1)S(1)} %collective-permute-done.20.refs_0_, f32[2,80,2048]{2,1,0:T(8,128)S(1)} %get-tuple-element.52.refs_1_, ...), custom_call_target="tpu_custom_call" | custom-call | flops 6000000000 | bytes 1048576 | tf_op jit(solution)/shard_map/pallas_call | solution.py:402
  116.1 1.6 %collective-permute-done.24.sib = f32[72,1024]{1,0:T(8,128)S(1)} collective-permute-done((f32[72,1024]{1,0:T(8,128)S(1)}, f32[72,1024]{1,0:T(8,128)S(1)}, u32[]{:S(2)}, u32[]{:S(2)}) %collective-permute-start.24) | collective-permute-done | bytes 294944 | tf_op jit(solution)/shard_map/ppermute | solution.py:51
  117.9 0.9 reshape.4
  118.8 4.7 %all-to-all-start.1 = ((bf16[16,2,2048]{2,1,0:T(2,128)(2,1)}), bf16[16,2,2048]{2,1,0:T(2,128)(2,1)S(1)}, u32[]{:S(2)}, u32[]{:S(2)}) async-start(bf16[16,2,2048]{2,1,0:T(2,128)(2,1)} %reshape.4), calls=%async_computation.1 | async-start | bytes 262144 | tf_op jit(solution)/shard_map/all_to_all | solution.py:418
  123.6 0.8 copy-done
  124.3 0.8 copy-done.2
  125.1 1.0 copy-done.1
  126.2 1.0 copy-done.3
  127.2 1.0 shard_map.101.w
  128.3 3.1 %all-to-all-done.1 = bf16[16,2,2048]{2,1,0:T(2,128)(2,1)S(1)} async-done(((bf16[16,2,2048]{2,1,0:T(2,128)(2,1)}), bf16[16,2,2048]{2,1,0:T(2,128)(2,1)S(1)}, u32[]{:S(2)}, u32[]{:S(2)}) %all-to-all-start.1) | async-done | bytes 131104 | tf_op jit(solution)/shard_map/all_to_all | solution.py:418
  131.6 1.5 %shard_map.102 = bf16[64,1024]{1,0:T(8,128)(2,1)} custom-call(bf16[16,64,64]{2,1,0:T(8,128)(2,1)S(1)} %reshape.5.att, f32[1,1024]{1,0:T(1,128)S(1)} %bitcast.16, bf16[1024,1024]{1,0:T(8,128)(2,1)S(1)} %shard_map.101.w), custom_call_target="tpu_custom_call" | custom-call | flops 100000000 | bytes 1048576 | tf_op jit(solution)/shard_map/pallas_call | solution.py:419
  (70 shorter events, 11.9 us)
Async XLA Ops:
  0.0 54.1 %copy-start.10 = (f32[1024]{0:T(1024)S(1)}, f32[1024]{0:T(1024)}, u32[]{:S(2)}) copy-start(f32[1024]{0:T(1024)} %param.10) | copy-start | bytes 12292
  0.0 54.1 %copy-start.11 = (f32[4]{0:T(128)S(1)}, f32[4]{0:T(128)}, u32[]{:S(2)}) copy-start(f32[4]{0:T(128)} %offs.1) | copy-start | bytes 52
  0.9 0.9 copy-start.5
  1.8 0.7 copy-start.6
  2.5 0.7 copy-start.7
  3.2 0.7 copy-start.8
  4.5 31.0 %collective-permute-start.2 = (bf16[32,1024]{1,0:T(8,128)(2,1)S(1)}, bf16[32,1024]{1,0:T(8,128)(2,1)S(1)}, u32[]{:S(2)}, u32[]{:S(2)}) collective-permute-start(bf16[32,1024]{1,0:T(8,128)(2,1)S(1)} %get-tuple-element.32), channel_id=1, source_target_pairs={{0,3},{1,0},{2,1},{3,2},{4,7},{5,4},{6,5},{7,6},{8,11},{9,8},{10,9... | collective-permute-start | bytes 196616 | tf_op jit(solution)/shard_map/ppermute | solution.py:51
  7.6 27.8 %collective-permute-start.1 = (bf16[32,1024]{1,0:T(8,128)(2,1)S(1)}, bf16[32,1024]{1,0:T(8,128)(2,1)S(1)}, u32[]{:S(2)}, u32[]{:S(2)}) collective-permute-start(bf16[32,1024]{1,0:T(8,128)(2,1)S(1)} %get-tuple-element.32), channel_id=1, source_target_pairs={{0,2},{1,3},{2,0},{3,1},{4,6},{5,7},{6,4},{7,5},{8,10},{9,11},{10,... | collective-permute-start | bytes 196616 | tf_op jit(solution)/shard_map/ppermute | solution.py:51
  8.2 5.7 %collective-permute-start.12 = (bf16[16,256]{1,0:T(8,128)(2,1)S(1)}, bf16[16,256]{1,0:T(8,128)(2,1)S(1)}, u32[]{:S(2)}, u32[]{:S(2)}) collective-permute-start(bf16[16,256]{1,0:T(8,128)(2,1)S(1)} %get-tuple-element.35), channel_id=1, source_target_pairs={{0,8},{8,16},{16,24},{24,0},{1,9},{9,17},{17,25},{25,1},{2,10},{10... | collective-permute-start | bytes 24584 | tf_op jit(solution)/shard_map/ppermute | solution.py:51
  9.7 5.2 %collective-permute-start.13 = (bf16[16,256]{1,0:T(8,128)(2,1)S(1)}, bf16[16,256]{1,0:T(8,128)(2,1)S(1)}, u32[]{:S(2)}, u32[]{:S(2)}) collective-permute-start(bf16[16,256]{1,0:T(8,128)(2,1)S(1)} %get-tuple-element.36), channel_id=1, source_target_pairs={{0,16},{8,24},{16,0},{24,8},{1,17},{9,25},{17,1},{25,9},{2,18},{10... | collective-permute-start | bytes 24584 | tf_op jit(solution)/shard_map/ppermute | solution.py:51
  12.4 4.2 %collective-permute-start.14 = (bf16[16,256]{1,0:T(8,128)(2,1)S(1)}, bf16[16,256]{1,0:T(8,128)(2,1)S(1)}, u32[]{:S(2)}, u32[]{:S(2)}) collective-permute-start(bf16[16,256]{1,0:T(8,128)(2,1)S(1)} %get-tuple-element.37), channel_id=1, source_target_pairs={{0,24},{8,0},{16,8},{24,16},{1,25},{9,1},{17,9},{25,17},{2,26},{10... | collective-permute-start | bytes 24584 | tf_op jit(solution)/shard_map/ppermute | solution.py:51
  13.9 21.2 %collective-permute-start = (bf16[32,1024]{1,0:T(8,128)(2,1)S(1)}, bf16[32,1024]{1,0:T(8,128)(2,1)S(1)}, u32[]{:S(2)}, u32[]{:S(2)}) collective-permute-start(bf16[32,1024]{1,0:T(8,128)(2,1)S(1)} %get-tuple-element.32), channel_id=1, source_target_pairs={{0,1},{1,2},{2,3},{3,0},{4,5},{5,6},{6,7},{7,4},{8,9},{9,10},{10,1... | collective-permute-start | bytes 196616 | tf_op jit(solution)/shard_map/ppermute | solution.py:51
  14.9 16.1 %collective-permute-start.8 = (bf16[32,1024]{1,0:T(8,128)(2,1)S(1)}, bf16[32,1024]{1,0:T(8,128)(2,1)S(1)}, u32[]{:S(2)}, u32[]{:S(2)}) collective-permute-start(bf16[32,1024]{1,0:T(8,128)(2,1)S(1)} %get-tuple-element.33), channel_id=1, source_target_pairs={{0,24},{8,0},{16,8},{24,16},{1,25},{9,1},{17,9},{25,17},{2,26},{10... | collective-permute-start | bytes 196616 | tf_op jit(solution)/shard_map/ppermute | solution.py:51
  16.6 8.6 %collective-permute-start.6 = (bf16[32,1024]{1,0:T(8,128)(2,1)S(1)}, bf16[32,1024]{1,0:T(8,128)(2,1)S(1)}, u32[]{:S(2)}, u32[]{:S(2)}) collective-permute-start(bf16[32,1024]{1,0:T(8,128)(2,1)S(1)} %get-tuple-element.33), channel_id=1, source_target_pairs={{0,8},{8,16},{16,24},{24,0},{1,9},{9,17},{17,25},{25,1},{2,10},{10... | collective-permute-start | bytes 196616 | tf_op jit(solution)/shard_map/ppermute | solution.py:51
  17.0 0.7 copy-start.9
  18.4 17.0 %all-to-all-start = ((bf16[8,80,256]{2,1,0:T(8,128)(2,1)}), bf16[8,80,256]{2,1,0:T(8,128)(2,1)S(1)}, u32[]{:S(2)}, u32[]{:S(2)}) async-start(bf16[8,80,256]{2,1,0:T(8,128)(2,1)} %shard_map.92), calls=%async_computation | async-start | bytes 655360 | tf_op jit(solution)/shard_map/all_to_all | solution.py:350
  25.2 5.9 %collective-permute-start.7 = (bf16[32,1024]{1,0:T(8,128)(2,1)S(1)}, bf16[32,1024]{1,0:T(8,128)(2,1)S(1)}, u32[]{:S(2)}, u32[]{:S(2)}) collective-permute-start(bf16[32,1024]{1,0:T(8,128)(2,1)S(1)} %get-tuple-element.33), channel_id=1, source_target_pairs={{0,16},{8,24},{16,0},{24,8},{1,17},{9,25},{17,1},{25,9},{2,18},{10... | collective-permute-start | bytes 196616 | tf_op jit(solution)/shard_map/ppermute | solution.py:51
  31.1 9.6 %collective-permute-start.11 = (bf16[128,1024]{1,0:T(8,128)(2,1)S(1)}, bf16[128,1024]{1,0:T(8,128)(2,1)S(1)}, u32[]{:S(2)}, u32[]{:S(2)}) collective-permute-start(bf16[128,1024]{1,0:T(8,128)(2,1)S(1)} %constant_dynamic-update-slice_fusion.4.refs_4_), channel_id=1, source_target_pairs={{0,3},{1,0},{2,1},{3,2},{4,7},{5,4},{6,5},{7,6},{8,11},{9,8},{10,9... | collective-permute-start | bytes 786440 | tf_op jit(solution)/shard_map/ppermute | solution.py:51
  33.4 8.2 %collective-permute-start.10 = (bf16[128,1024]{1,0:T(8,128)(2,1)S(1)}, bf16[128,1024]{1,0:T(8,128)(2,1)S(1)}, u32[]{:S(2)}, u32[]{:S(2)}) collective-permute-start(bf16[128,1024]{1,0:T(8,128)(2,1)S(1)} %constant_dynamic-update-slice_fusion.4.refs_4_), channel_id=1, source_target_pairs={{0,2},{1,3},{2,0},{3,1},{4,6},{5,7},{6,4},{7,5},{8,10},{9,11},{10,... | collective-permute-start | bytes 786440 | tf_op jit(solution)/shard_map/ppermute | solution.py:51
  35.1 9.3 %collective-permute-start.9 = (bf16[128,1024]{1,0:T(8,128)(2,1)S(1)}, bf16[128,1024]{1,0:T(8,128)(2,1)S(1)}, u32[]{:S(2)}, u32[]{:S(2)}) collective-permute-start(bf16[128,1024]{1,0:T(8,128)(2,1)S(1)} %constant_dynamic-update-slice_fusion.4.refs_4_), channel_id=1, source_target_pairs={{0,1},{1,2},{2,3},{3,0},{4,5},{5,6},{6,7},{7,4},{8,9},{9,10},{10,1... | collective-permute-start | bytes 786440 | tf_op jit(solution)/shard_map/ppermute | solution.py:51
  35.4 18.7 %collective-permute-start.15 = (bf16[8,80,256]{2,1,0:T(8,128)(2,1)S(1)}, bf16[8,80,256]{2,1,0:T(8,128)(2,1)S(1)}, u32[]{:S(2)}, u32[]{:S(2)}) collective-permute-start(bf16[8,80,256]{2,1,0:T(8,128)(2,1)S(1)} %all-to-all-done.refs_9_), channel_id=1, source_target_pairs={{0,4},{4,0},{1,5},{5,1},{2,6},{6,2},{3,7},{7,3},{8,12},{12,8},{9,1... | collective-permute-start | bytes 983048 | tf_op jit(solution)/shard_map/ppermute | solution.py:51
  35.6 14.9 %collective-permute-start.5 = (bf16[128,1024]{1,0:T(8,128)(2,1)S(1)}, bf16[128,1024]{1,0:T(8,128)(2,1)S(1)}, u32[]{:S(2)}, u32[]{:S(2)}) collective-permute-start(bf16[128,1024]{1,0:T(8,128)(2,1)S(1)} %constant_dynamic-update-slice_fusion.refs_0_), channel_id=1, source_target_pairs={{0,24},{8,0},{16,8},{24,16},{1,25},{9,1},{17,9},{25,17},{2,26},{10... | collective-permute-start | bytes 786440 | tf_op jit(solution)/shard_map/ppermute | solution.py:51
  40.7 10.7 %collective-permute-start.4 = (bf16[128,1024]{1,0:T(8,128)(2,1)S(1)}, bf16[128,1024]{1,0:T(8,128)(2,1)S(1)}, u32[]{:S(2)}, u32[]{:S(2)}) collective-permute-start(bf16[128,1024]{1,0:T(8,128)(2,1)S(1)} %constant_dynamic-update-slice_fusion.refs_0_), channel_id=1, source_target_pairs={{0,16},{8,24},{16,0},{24,8},{1,17},{9,25},{17,1},{25,9},{2,18},{10... | collective-permute-start | bytes 786440 | tf_op jit(solution)/shard_map/ppermute | solution.py:51
  41.7 12.5 %collective-permute-start.3 = (bf16[128,1024]{1,0:T(8,128)(2,1)S(1)}, bf16[128,1024]{1,0:T(8,128)(2,1)S(1)}, u32[]{:S(2)}, u32[]{:S(2)}) collective-permute-start(bf16[128,1024]{1,0:T(8,128)(2,1)S(1)} %constant_dynamic-update-slice_fusion.refs_0_), channel_id=1, source_target_pairs={{0,8},{8,16},{16,24},{24,0},{1,9},{9,17},{17,25},{25,1},{2,10},{10... | collective-permute-start | bytes 786440 | tf_op jit(solution)/shard_map/ppermute | solution.py:51
  56.3 1.5 %collective-permute-start.16 = (bf16[80,1024]{1,0:T(8,128)(2,1)S(1)}, bf16[80,1024]{1,0:T(8,128)(2,1)S(1)}, u32[]{:S(2)}, u32[]{:S(2)}) collective-permute-start(bf16[80,1024]{1,0:T(8,128)(2,1)S(1)} %get-tuple-element.38.q_own), channel_id=1, source_target_pairs={{0,4},{4,0},{1,5},{5,1},{2,6},{6,2},{3,7},{7,3},{8,12},{12,8},{9,1... | collective-permute-start | bytes 491528 | tf_op jit(solution)/shard_map/ppermute | solution.py:51
  58.4 17.6 %collective-permute-start.21 = (bf16[144,1024]{1,0:T(8,128)(2,1)S(1)}, bf16[144,1024]{1,0:T(8,128)(2,1)S(1)}, u32[]{:S(2)}, u32[]{:S(2)}) collective-permute-start(bf16[144,1024]{1,0:T(8,128)(2,1)S(1)} %get-tuple-element.42.pay), channel_id=1, source_target_pairs={{0,224},{32,0},{64,32},{1,225},{33,1},{65,33},{2,226},{34,2},{66,3... | collective-permute-start | bytes 884744 | tf_op jit(solution)/shard_map/ppermute | solution.py:63
  59.1 17.6 %collective-permute-start.17 = (bf16[144,1024]{1,0:T(8,128)(2,1)S(1)}, bf16[144,1024]{1,0:T(8,128)(2,1)S(1)}, u32[]{:S(2)}, u32[]{:S(2)}) collective-permute-start(bf16[144,1024]{1,0:T(8,128)(2,1)S(1)} %get-tuple-element.42.pay), channel_id=1, source_target_pairs={{0,32},{32,64},{64,96},{96,128},{128,160},{160,192},{192,224},{1,3... | collective-permute-start | bytes 884744 | tf_op jit(solution)/shard_map/ppermute | solution.py:59
  66.0 6.4 %collective-permute-start.27 = (bf16[2,8,16,256]{3,2,1,0:T(8,128)(2,1)S(1)}, bf16[2,8,16,256]{3,2,1,0:T(8,128)(2,1)S(1)}, u32[]{:S(2)}, u32[]{:S(2)}) collective-permute-start(bf16[2,8,16,256]{3,2,1,0:T(8,128)(2,1)S(1)} %pad_maximum_fusion.1), channel_id=1, source_target_pairs={{0,24},{8,0},{16,8},{24,16},{1,25},{9,1},{17,9},{25,17},{2,26},{10... | collective-permute-start | bytes 393224 | tf_op jit(solution)/shard_map/ppermute | solution.py:51
  66.7 7.6 %collective-permute-start.26 = (bf16[2,8,16,256]{3,2,1,0:T(8,128)(2,1)S(1)}, bf16[2,8,16,256]{3,2,1,0:T(8,128)(2,1)S(1)}, u32[]{:S(2)}, u32[]{:S(2)}) collective-permute-start(bf16[2,8,16,256]{3,2,1,0:T(8,128)(2,1)S(1)} %pad_maximum_fusion.1), channel_id=1, source_target_pairs={{0,16},{8,24},{16,0},{24,8},{1,17},{9,25},{17,1},{25,9},{2,18},{10... | collective-permute-start | bytes 393224 | tf_op jit(solution)/shard_map/ppermute | solution.py:51
  67.5 8.5 %collective-permute-start.25 = (bf16[2,8,16,256]{3,2,1,0:T(8,128)(2,1)S(1)}, bf16[2,8,16,256]{3,2,1,0:T(8,128)(2,1)S(1)}, u32[]{:S(2)}, u32[]{:S(2)}) collective-permute-start(bf16[2,8,16,256]{3,2,1,0:T(8,128)(2,1)S(1)} %pad_maximum_fusion.1), channel_id=1, source_target_pairs={{0,8},{8,16},{16,24},{24,0},{1,9},{9,17},{17,25},{25,1},{2,10},{10... | collective-permute-start | bytes 393224 | tf_op jit(solution)/shard_map/ppermute | solution.py:51
  76.0 11.6 %collective-permute-start.22 = (bf16[144,1024]{1,0:T(8,128)(2,1)S(1)}, bf16[144,1024]{1,0:T(8,128)(2,1)S(1)}, u32[]{:S(2)}, u32[]{:S(2)}) collective-permute-start(bf16[144,1024]{1,0:T(8,128)(2,1)S(1)} %collective-permute-done.21.refs_1_), channel_id=1, source_target_pairs={{224,192},{0,224},{32,0},{225,193},{1,225},{33,1},{226,194},{2,226... | collective-permute-start | bytes 884744 | tf_op jit(solution)/shard_map/ppermute | solution.py:63
  76.7 12.2 %collective-permute-start.18 = (bf16[144,1024]{1,0:T(8,128)(2,1)S(1)}, bf16[144,1024]{1,0:T(8,128)(2,1)S(1)}, u32[]{:S(2)}, u32[]{:S(2)}) collective-permute-start(bf16[144,1024]{1,0:T(8,128)(2,1)S(1)} %collective-permute-done.17.refs_0_), channel_id=1, source_target_pairs={{32,64},{64,96},{96,128},{128,160},{160,192},{192,224},{33,65},{65... | collective-permute-start | bytes 884744 | tf_op jit(solution)/shard_map/ppermute | solution.py:59
  84.3 39.2 %collective-permute-start.30 = (bf16[4,2,8,16,256]{4,3,2,1,0:T(8,128)(2,1)S(1)}, bf16[4,2,8,16,256]{4,3,2,1,0:T(8,128)(2,1)S(1)}, u32[]{:S(2)}, u32[]{:S(2)}) collective-permute-start(bf16[4,2,8,16,256]{4,3,2,1,0:T(8,128)(2,1)S(1)} %pad_maximum_fusion.w0), channel_id=1, source_target_pairs={{0,3},{1,0},{2,1},{3,2},{4,7},{5,4},{6,5},{7,6},{8,11},{9,8},{10,9... | collective-permute-start | bytes 1572872 | tf_op jit(solution)/shard_map/ppermute | solution.py:51
  86.4 37.1 %collective-permute-start.29 = (bf16[4,2,8,16,256]{4,3,2,1,0:T(8,128)(2,1)S(1)}, bf16[4,2,8,16,256]{4,3,2,1,0:T(8,128)(2,1)S(1)}, u32[]{:S(2)}, u32[]{:S(2)}) collective-permute-start(bf16[4,2,8,16,256]{4,3,2,1,0:T(8,128)(2,1)S(1)} %pad_maximum_fusion.w0), channel_id=1, source_target_pairs={{0,2},{1,3},{2,0},{3,1},{4,6},{5,7},{6,4},{7,5},{8,10},{9,11},{10,... | collective-permute-start | bytes 1572872 | tf_op jit(solution)/shard_map/ppermute | solution.py:51
  86.9 37.4 %collective-permute-start.28 = (bf16[4,2,8,16,256]{4,3,2,1,0:T(8,128)(2,1)S(1)}, bf16[4,2,8,16,256]{4,3,2,1,0:T(8,128)(2,1)S(1)}, u32[]{:S(2)}, u32[]{:S(2)}) collective-permute-start(bf16[4,2,8,16,256]{4,3,2,1,0:T(8,128)(2,1)S(1)} %pad_maximum_fusion.w0), channel_id=1, source_target_pairs={{0,1},{1,2},{2,3},{3,0},{4,5},{5,6},{6,7},{7,4},{8,9},{9,10},{10,1... | collective-permute-start | bytes 1572872 | tf_op jit(solution)/shard_map/ppermute | solution.py:51
  87.7 17.4 %collective-permute-start.23 = (bf16[144,1024]{1,0:T(8,128)(2,1)S(1)}, bf16[144,1024]{1,0:T(8,128)(2,1)S(1)}, u32[]{:S(2)}, u32[]{:S(2)}) collective-permute-start(bf16[144,1024]{1,0:T(8,128)(2,1)S(1)} %collective-permute-done.22.refs_1_), channel_id=1, source_target_pairs={{192,160},{224,192},{0,224},{193,161},{225,193},{1,225},{194,162},... | collective-permute-start | bytes 884744 | tf_op jit(solution)/shard_map/ppermute | solution.py:63
  89.0 10.2 %collective-permute-start.19 = (bf16[144,1024]{1,0:T(8,128)(2,1)S(1)}, bf16[144,1024]{1,0:T(8,128)(2,1)S(1)}, u32[]{:S(2)}, u32[]{:S(2)}) collective-permute-start(bf16[144,1024]{1,0:T(8,128)(2,1)S(1)} %collective-permute-done.18.refs_0_), channel_id=1, source_target_pairs={{64,96},{96,128},{128,160},{160,192},{192,224},{65,97},{97,129},{1... | collective-permute-start | bytes 884744 | tf_op jit(solution)/shard_map/ppermute | solution.py:59
  99.2 12.6 %collective-permute-start.20 = (bf16[144,1024]{1,0:T(8,128)(2,1)S(1)}, bf16[144,1024]{1,0:T(8,128)(2,1)S(1)}, u32[]{:S(2)}, u32[]{:S(2)}) collective-permute-start(bf16[144,1024]{1,0:T(8,128)(2,1)S(1)} %collective-permute-done.19.refs_0_), channel_id=1, source_target_pairs={{96,128},{128,160},{160,192},{192,224},{97,129},{129,161},{161,193... | collective-permute-start | bytes 884744 | tf_op jit(solution)/shard_map/ppermute | solution.py:59
  116.0 1.7 %collective-permute-start.24 = (f32[72,1024]{1,0:T(8,128)S(1)}, f32[72,1024]{1,0:T(8,128)S(1)}, u32[]{:S(2)}, u32[]{:S(2)}) collective-permute-start(f32[72,1024]{1,0:T(8,128)S(1)} %get-tuple-element.56), channel_id=1, source_target_pairs={{0,4},{4,0},{1,5},{5,1},{2,6},{6,2},{3,7},{7,3},{8,12},{12,8},{9,1... | collective-permute-start | bytes 884744 | tf_op jit(solution)/shard_map/ppermute | solution.py:51
  118.8 12.8 %copy-start.4 = (f32[1024]{0:T(1024)S(1)}, f32[1024]{0:T(1024)}, u32[]{:S(2)}) copy-start(f32[1024]{0:T(1024)} %param.17) | copy-start | bytes 12292
  118.8 12.6 %all-to-all-start.1 = ((bf16[16,2,2048]{2,1,0:T(2,128)(2,1)}), bf16[16,2,2048]{2,1,0:T(2,128)(2,1)S(1)}, u32[]{:S(2)}, u32[]{:S(2)}) async-start(bf16[16,2,2048]{2,1,0:T(2,128)(2,1)} %reshape.4), calls=%async_computation.1 | async-start | bytes 262144 | tf_op jit(solution)/shard_map/all_to_all | solution.py:418
  123.5 0.8 copy-start
  124.3 0.8 copy-start.2
  125.1 1.0 copy-start.1
  126.2 1.0 copy-start.3

commit v2 on v1

--- a/solution.py
+++ b/solution.py
@@ -71,22 +71,47 @@
     return hi, mid, low
 
 
-def pack_body(idx, tok, wq, wk, wv, wf, lo, hi, p0, p1, p2, p3, heads):
+def pack_body(idx, tok, wq, wk, wv, wf, wo, lo, hi, p0, o0, s1, s2, s3, qv, kv, vv, fv, heads, sems):
     x = idx[1]
-    lo[...] = tok[0:32, :]
-    hi[...] = tok[32:64, :]
+    sends = (s1, s2, s3)
+    pairs = [(wq, qv), (wk, kv), (wv, vv), (wf, fv), (wo, o0)]
+    pairs += [(tok.at[32:64], s.at[0:32]) for s in sends]
+    pairs += [(tok.at[0:32], lo), (tok.at[32:64], hi)]
+    copies = [pltpu.make_async_copy(a, b, sems.at[i]) for i, (a, b) in enumerate(pairs)]
+    for copy in copies:
+        copy.start()
+    for s in sends:
+        s[32:48, 512:1024] = jnp.zeros((16, 512), BF16)
+    for copy in copies[:5]:
+        copy.wait()
+    head = lax.broadcasted_iota(jnp.int32, (NX, HD), 0)
+    gates = fv[...].astype(F32)
     for h in range(NX):
         lanes = slice(h * HD, (h + 1) * HD)
-        gate = jnp.broadcast_to(wf[:, h : h + 1].astype(F32), (16, HD)).astype(BF16)
-        heads[h] = jnp.concatenate([wq[:, lanes], wk[:, lanes], wv[:, lanes], gate], axis=1)
-    for k, out in enumerate((p0, p1, p2, p3)):
-        out[...] = heads[lax.rem(x + k, NX)]
-
-
-def spread_body(p0, p1, p2, p3, wo, out):
+        pick = jnp.where(head == h, 1.0, 0.0)
+        gate = lax.dot_general(
+            gates, pick, (((0,), (0,)), ((), ())), precision=lax.Precision.HIGHEST,
+            preferred_element_type=F32,
+        )
+        heads[h] = jnp.concatenate([qv[:, lanes], kv[:, lanes], vv[:, lanes], gate.astype(BF16)], axis=1)
+    p0[...] = heads[x]
+    for k, s in enumerate(sends):
+        s[32:48, 0:256] = heads[lax.rem(x + k + 1, NX)]
+        s[32:48, 256:512] = o0[...]
+    for copy in copies[5:]:
+        copy.wait()
+
+
+def spread_body(hi, p0, o0, r1, r2, r3, out, toks):
+    toks[0:32, :] = hi[...]
+    for k, r in enumerate((r1, r2, r3)):
+        toks[32 * k + 32 : 32 * k + 64, :] = r[0:32, :]
     for z in range(NZ):
-        for k, piece in enumerate((p0, p1, p2, p3, wo)):
-            out[z, k * 16 : k * 16 + 16, :] = piece[...]
+        out[z, 0:16, :] = p0[...]
+        out[z, 64:80, :] = o0[...]
+        for k, r in enumerate((r1, r2, r3)):
+            out[z, 16 * k + 16 : 16 * k + 32, :] = r[32:48, 0:256]
+            out[z, 16 * k + 80 : 16 * k + 96, :] = r[32:48, 256:512]
 
 
 def project_body(idx, offs, *refs):
@@ -318,7 +343,7 @@
                 cc = c if other == 0 else 1 - c
                 for z in range(NZ):
                     at = pl.multiple_of(z * 128 + xx * 32 + cc * 16, 16)
-                    w[pl.ds(at, 16), cols] = ref[kx, other, z]
+                    w[pl.ds(at, 16), cols] = ref[other, z, kx * 16 : kx * 16 + 16, :]
 
 
 def final_body(att, gain, w, out):
@@ -333,21 +358,23 @@
     sds = jax.ShapeDtypeStruct
     idx = jnp.stack([lax.axis_index(a) for a in AXES]).astype(jnp.int32)
 
-    half, piece = sds((32, D), BF16), sds((16, 256), BF16)
-    tok_lo, tok_hi, *pieces = call(
+    half, piece, send = sds((32, D), BF16), sds((16, 256), BF16), sds((48, D), BF16)
+    own_w = pltpu.VMEM((16, 256), BF16)
+    lo, hi, p0, o0, *sends = call(
         pack_body,
-        (half, half, piece, piece, piece, piece),
-        [SMEM] + [VMEM] * 5,
-        [pltpu.VMEM((NX, 16, 256), BF16)],
-    )(idx, tokens, w_query, w_key, w_value, w_forget)
-
-    pieces = [pieces[0]] + [shift(pieces[k], "x", k) for k in range(1, NX)]
-    tok_a = direct(tok_lo, "y")
-    tok_b = direct(tok_hi, "x")
-    toks = direct(jnp.concatenate(tok_a, axis=0), "x")
-    toks = toks + direct(jnp.concatenate(tok_b, axis=0), "y")
-    chunk = call(spread_body, sds((NZ, 80, 256), BF16), [VMEM] * 5)(*pieces, w_out_t)
+        (half, half, piece, piece, send, send, send),
+        [SMEM] + [pl.BlockSpec(memory_space=pl.ANY)] * 6,
+        [own_w, own_w, own_w, pltpu.VMEM((NX, 16), BF16), pltpu.VMEM((NX, 16, 256), BF16)]
+        + [pltpu.SemaphoreType.DMA((10,))],
+    )(idx, tokens, w_query, w_key, w_value, w_forget.T, w_out_t)
+
+    got = [shift(sends[k - 1], "x", k) for k in range(1, NX)]
+    tok_a = direct(lo, "y")
+    chunk, tok_b = call(
+        spread_body, (sds((NZ, 128, 256), BF16), sds((128, D), BF16)), [VMEM] * 6
+    )(hi, p0, o0, *got)
     w_own = lax.all_to_all(chunk, "z", 0, 0, tiled=True)
+    toks = direct(jnp.concatenate(tok_a, axis=0), "x") + direct(tok_b, "y")
     w_sib = shift(w_own, "c", 1)
 
     q_own, kv, cum_own = call(
@@ -385,7 +412,7 @@
 
     w_o = jnp.stack([w_own[:, 64:], w_sib[:, 64:]])
     w_o, _ = lax.optimization_barrier((w_o, sums))
-    w_o = direct(w_o, "x")
+    w_o = direct(w_o, "y")
 
     for k in range(1, 5):
         pays = (right, left) if k < 4 else (right,)
@@ -409,9 +436,6 @@
         )(*ins)
         if k < 4:
             acc, m, sums = res
-        if k == 1:
-            w_o, _ = lax.optimization_barrier((jnp.stack(w_o), sums))
-            w_o = direct(w_o, "y")
     sib = shift(res[1], "c", 1)
     w_full = call(assemble_body, sds((D, D), BF16), [SMEM] + [VMEM] * 4)(idx, *w_o)
     att = call(merge_body, sds((KEYS, HD), BF16), [VMEM, VMEM])(res[0], sib)

time: 134 us -> 129 us (0.963)
  starting transfers between devices: 61.6 us -> 54.3 us
  waiting for transfers between devices: 31.6 us -> 33.1 us
    ppermute x24 -> x18, starting transfers between devices: 30.3 us -> 20.3 us  [shift(): return lax.ppermute(x, axis, [(i, (i + k) % n) for i in range(n)])]
    ppermute x4, waiting for transfers between devices: 1.11 us -> 4.77 us  [step_right(): return lax.ppermute(x, 'z', [(i, i + 1) for i in range(k - 1, NZ - 1)])]
    all_to_all x1, starting transfers between devices: 4.72 us -> 7.64 us  [shards(): att = lax.all_to_all(att.reshape(16, 64, HD), ('x', 'y'), 0, 0, tiled=True)]
    ppermute x24 -> x18, waiting for transfers between devices: 27.4 us -> 25.2 us  [shift(): return lax.ppermute(x, axis, [(i, (i + k) % n) for i in range(n)])]
    unnamed x33 -> x31, local copies, waits for them, and re-layouts: 9.3 us -> 9.21 us
  transfers between devices with their start and end apart: 33 -> 27, of which waited for: 14 -> 15; matrix products, arithmetic and copies ran while one was open for 1% -> 1% of each run, Pallas kernels for 19% -> 19%
where the time goes in v2:
time: 129 us; the launch traced here: 128 us
  starting transfers between devices  54.3 us (42%)
  waiting for transfers between devices  33.1 us (26%)
  Pallas kernels  30.7 us (24%)
  local copies, waits for them, and re-layouts  9.25 us (7%)
    ppermute x18, waiting for transfers between devices, shift(): return lax.ppermute(x, axis, [(i, (i + k) % n) for i in range(n)])  25.2 us
    ppermute x18, starting transfers between devices, shift(): return lax.ppermute(x, axis, [(i, (i + k) % n) for i in range(n)])  20.3 us
    pallas_call x4, Pallas kernels, shards(): call(functools.partial(step_body, k), outs, [SMEM] + [VMEM] * (len(ins) -...  18.5 us
    ppermute x4, starting transfers between devices, step_right(): return lax.ppermute(x, 'z', [(i, i + 1) for i in range(k - 1, NZ - 1)])  17 us
    unnamed x31, local copies, waits for them, and re-layouts  9.21 us
    all_to_all x1, starting transfers between devices, shards(): att = lax.all_to_all(att.reshape(16, 64, HD), ('x', 'y'), 0, 0, tiled=True)  7.64 us
    all_to_all x1, starting transfers between devices, shards(): w_own = lax.all_to_all(chunk, 'z', 0, 0, tiled=True)  6.75 us
    ppermute x4, waiting for transfers between devices, step_right(): return lax.ppermute(x, 'z', [(i, i + 1) for i in range(k - 1, NZ - 1)])  4.77 us
  transfers between devices with their start and end apart: 27, of which 15 were waited for; matrix products, arithmetic and copies ran while one was open for 1% of the time, Pallas kernels for 19%

profile of v2, /device:TPU:160, one launch (start us, length us, event | category | flops | bytes accessed | tf_op | source)
XLA Modules:
  0.0 127.8 jit_solution(16209463224178388550)
XLA Ops:
  0.1 0.9 copy-done.5
  1.0 0.7 copy-done.6
  4.5 1.4 %shard_map.91 = (bf16[32,1024]{1,0:T(8,128)(2,1)S(1)}, bf16[32,1024]{1,0:T(8,128)(2,1)S(1)}, bf16[16,256]{1,0:T(8,128)(2,1)S(1)}, bf16[16,256]{1,0:T(8,128)(2,1)...) custom-call(s32[4]{0:T(128)S(1)} %pad_add_fusion.idx, ...), custom_call_target="tpu_custom_call" | custom-call | flops 100000000 | bytes 1048576 | tf_op jit(solution)/shard_map/pallas_call | solution.py:363
  5.9 1.6 %collective-permute-start.6 = (bf16[48,1024]{1,0:T(8,128)(2,1)S(1)}, bf16[48,1024]{1,0:T(8,128)(2,1)S(1)}, u32[]{:S(2)}, u32[]{:S(2)}) collective-permute-start(bf16[48,1024]{1,0:T(8,128)(2,1)S(1)} %get-tuple-element.38), channel_id=1, source_target_pairs={{0,8},{8,16},{16,24},{24,0},{1,9},{9,17},{17,25},{25,1},{2,10},{10... | collective-permute-start | bytes 294920 | tf_op jit(solution)/shard_map/ppermute | solution.py:51
  7.5 2.7 %collective-permute-start.7 = (bf16[48,1024]{1,0:T(8,128)(2,1)S(1)}, bf16[48,1024]{1,0:T(8,128)(2,1)S(1)}, u32[]{:S(2)}, u32[]{:S(2)}) collective-permute-start(bf16[48,1024]{1,0:T(8,128)(2,1)S(1)} %get-tuple-element.39), channel_id=1, source_target_pairs={{0,16},{8,24},{16,0},{24,8},{1,17},{9,25},{17,1},{25,9},{2,18},{10... | collective-permute-start | bytes 294920 | tf_op jit(solution)/shard_map/ppermute | solution.py:51
  10.2 1.4 %collective-permute-start.8 = (bf16[48,1024]{1,0:T(8,128)(2,1)S(1)}, bf16[48,1024]{1,0:T(8,128)(2,1)S(1)}, u32[]{:S(2)}, u32[]{:S(2)}) collective-permute-start(bf16[48,1024]{1,0:T(8,128)(2,1)S(1)} %get-tuple-element.40), channel_id=1, source_target_pairs={{0,24},{8,0},{16,8},{24,16},{1,25},{9,1},{17,9},{25,17},{2,26},{10... | collective-permute-start | bytes 294920 | tf_op jit(solution)/shard_map/ppermute | solution.py:51
  12.0 2.8 %collective-permute-done.7.r2 = bf16[48,1024]{1,0:T(8,128)(2,1)S(1)} collective-permute-done((bf16[48,1024]{1,0:T(8,128)(2,1)S(1)}, bf16[48,1024]{1,0:T(8,128)(2,1)S(1)}, u32[]{:S(2)}, u32[]{:S(2)}) %collective-permute-start.7) | collective-permute-done | bytes 98336 | tf_op jit(solution)/shard_map/ppermute | solution.py:51
  14.8 0.9 shard_map.92
  15.7 6.8 %all-to-all-start = ((bf16[8,128,256]{2,1,0:T(8,128)(2,1)}), bf16[8,128,256]{2,1,0:T(8,128)(2,1)S(1)}, u32[]{:S(2)}, u32[]{:S(2)}) async-start(bf16[8,128,256]{2,1,0:T(8,128)(2,1)} %get-tuple-element.42), calls=%async_computation | async-start | bytes 1048576 | tf_op jit(solution)/shard_map/all_to_all | solution.py:376
  22.4 3.0 %collective-permute-start.2 = (bf16[32,1024]{1,0:T(8,128)(2,1)S(1)}, bf16[32,1024]{1,0:T(8,128)(2,1)S(1)}, u32[]{:S(2)}, u32[]{:S(2)}) collective-permute-start(bf16[32,1024]{1,0:T(8,128)(2,1)S(1)} %get-tuple-element.34), channel_id=1, source_target_pairs={{0,3},{1,0},{2,1},{3,2},{4,7},{5,4},{6,5},{7,6},{8,11},{9,8},{10,9... | collective-permute-start | bytes 196616 | tf_op jit(solution)/shard_map/ppermute | solution.py:51
  26.1 1.0 collective-permute-start
  27.1 4.9 %collective-permute-done = bf16[32,1024]{1,0:T(8,128)(2,1)S(1)} collective-permute-done((bf16[32,1024]{1,0:T(8,128)(2,1)S(1)}, bf16[32,1024]{1,0:T(8,128)(2,1)S(1)}, u32[]{:S(2)}, u32[]{:S(2)}) %collective-permute-start) | collective-permute-done | bytes 65568 | tf_op jit(solution)/shard_map/ppermute | solution.py:51
  32.0 2.7 %collective-permute-start.5 = (bf16[128,1024]{1,0:T(8,128)(2,1)S(1)}, bf16[128,1024]{1,0:T(8,128)(2,1)S(1)}, u32[]{:S(2)}, u32[]{:S(2)}) collective-permute-start(bf16[128,1024]{1,0:T(8,128)(2,1)S(1)} %constant_dynamic-update-slice_fusion.refs_0_), channel_id=1, source_target_pairs={{0,24},{8,0},{16,8},{24,16},{1,25},{9,1},{17,9},{25,17},{2,26},{10... | collective-permute-start | bytes 786440 | tf_op jit(solution)/shard_map/ppermute | solution.py:51
  34.7 0.8 collective-permute-start.4
  36.2 2.4 %collective-permute-start.11 = (bf16[128,1024]{1,0:T(8,128)(2,1)S(1)}, bf16[128,1024]{1,0:T(8,128)(2,1)S(1)}, u32[]{:S(2)}, u32[]{:S(2)}) collective-permute-start(bf16[128,1024]{1,0:T(8,128)(2,1)S(1)} %get-tuple-element.41.refs_4_), channel_id=1, source_target_pairs={{0,3},{1,0},{2,1},{3,2},{4,7},{5,4},{6,5},{7,6},{8,11},{9,8},{10,9... | collective-permute-start | bytes 786440 | tf_op jit(solution)/shard_map/ppermute | solution.py:51
  38.6 4.6 %collective-permute-done.5.refs_3_ = bf16[128,1024]{1,0:T(8,128)(2,1)S(1)} collective-permute-done((bf16[128,1024]{1,0:T(8,128)(2,1)S(1)}, bf16[128,1024]{1,0:T(8,128)(2,1)S(1)}, u32[]{:S(2)}, u32[]{:S(2)}) %collective-permute-start.5) | collective-permute-done | bytes 262176 | tf_op jit(solution)/shard_map/ppermute | solution.py:51
  43.1 1.0 collective-permute-start.10
  44.2 1.1 collective-permute-done.4.refs_2_
  45.3 2.9 %collective-permute-done.3.refs_1_ = bf16[128,1024]{1,0:T(8,128)(2,1)S(1)} collective-permute-done((bf16[128,1024]{1,0:T(8,128)(2,1)S(1)}, bf16[128,1024]{1,0:T(8,128)(2,1)S(1)}, u32[]{:S(2)}, u32[]{:S(2)}) %collective-permute-start.3) | collective-permute-done | bytes 262176 | tf_op jit(solution)/shard_map/ppermute | solution.py:51
  48.2 2.0 %collective-permute-done.11.refs_7_ = bf16[128,1024]{1,0:T(8,128)(2,1)S(1)} collective-permute-done((bf16[128,1024]{1,0:T(8,128)(2,1)S(1)}, bf16[128,1024]{1,0:T(8,128)(2,1)S(1)}, u32[]{:S(2)}, u32[]{:S(2)}) %collective-permute-start.11) | collective-permute-done | bytes 262176 | tf_op jit(solution)/shard_map/ppermute | solution.py:51
  50.2 1.0 collective-permute-done.10.refs_6_
  51.2 2.7 %collective-permute-done.9.refs_5_ = bf16[128,1024]{1,0:T(8,128)(2,1)S(1)} collective-permute-done((bf16[128,1024]{1,0:T(8,128)(2,1)S(1)}, bf16[128,1024]{1,0:T(8,128)(2,1)S(1)}, u32[]{:S(2)}, u32[]{:S(2)}) %collective-permute-start.9) | collective-permute-done | bytes 262176 | tf_op jit(solution)/shard_map/ppermute | solution.py:51
  53.9 2.2 %shard_map.93 = (bf16[80,1024]{1,0:T(8,128)(2,1)S(1)}, bf16[128,1024]{1,0:T(8,128)(2,1)S(1)}, f32[8,1024]{1,0:T(8,128)S(1)}) custom-call(s32[4]{0:T(128)S(1)} %pad_add_fusion.idx, f32[4]{0:T(128)S(1)} %copy-done.12, bf16[128,1024]{1,0:T(8,128)(2,1)S(1)} %constant_dynamic-update-slice_fusion.refs_0_, bf16[128,1024]{1,0:T(8,128)(2,1)S(1)} %collective-permute-done.3.refs_1_, ...), custom_call_target="tpu_custom_call" | custom-call | flops 2000000000 | bytes 1048576 | tf_op jit(solution)/shard_map/pallas_call | solution.py:380
  56.2 1.4 %collective-permute-done.13.q_sib = bf16[80,1024]{1,0:T(8,128)(2,1)S(1)} collective-permute-done((bf16[80,1024]{1,0:T(8,128)(2,1)S(1)}, bf16[80,1024]{1,0:T(8,128)(2,1)S(1)}, u32[]{:S(2)}, u32[]{:S(2)}) %collective-permute-start.13) | collective-permute-done | bytes 163872 | tf_op jit(solution)/shard_map/ppermute | solution.py:51
  58.9 3.3 %collective-permute-start.14 = (bf16[144,1024]{1,0:T(8,128)(2,1)S(1)}, bf16[144,1024]{1,0:T(8,128)(2,1)S(1)}, u32[]{:S(2)}, u32[]{:S(2)}) collective-permute-start(bf16[144,1024]{1,0:T(8,128)(2,1)S(1)} %get-tuple-element.47.pay), channel_id=1, source_target_pairs={{0,32},{32,64},{64,96},{96,128},{128,160},{160,192},{192,224},{1,3... | collective-permute-start | bytes 884744 | tf_op jit(solution)/shard_map/ppermute | solution.py:59
  62.3 4.4 %shard_map.95 = (f32[2,80,2048]{2,1,0:T(8,128)S(1)}, f32[2,8,2048]{2,1,0:T(8,128)S(1)}, f32[8,256]{1,0:T(8,128)S(1)}) custom-call(s32[4]{0:T(128)S(1)} %pad_add_fusion.idx, bf16[128,2048]{1,0:T(8,128)(2,1)S(1)} %get-tuple-element.46.q, bf16[144,1024]{1,0:T(8,128)(2,1)S(1)} %get-tuple-element.47.pay), custom_call_target="tpu_custom_call" | custom-call | flops 3000000000 | bytes 1048576 | tf_op jit(solution)/shard_map/pallas_call | solution.py:409
  66.7 0.7 collective-permute-start.24
  68.0 0.8 collective-permute-start.22
  69.8 3.1 %collective-permute-start.15 = (bf16[144,1024]{1,0:T(8,128)(2,1)S(1)}, bf16[144,1024]{1,0:T(8,128)(2,1)S(1)}, u32[]{:S(2)}, u32[]{:S(2)}) collective-permute-start(bf16[144,1024]{1,0:T(8,128)(2,1)S(1)} %collective-permute-done.14.refs_0_), channel_id=1, source_target_pairs={{32,64},{64,96},{96,128},{128,160},{160,192},{192,224},{33,65},{65... | collective-permute-start | bytes 884744 | tf_op jit(solution)/shard_map/ppermute | solution.py:59
  73.0 3.9 %shard_map.96 = (f32[2,80,2048]{2,1,0:T(8,128)S(1)}, f32[2,8,2048]{2,1,0:T(8,128)S(1)}, f32[8,256]{1,0:T(8,128)S(1)}) custom-call(s32[4]{0:T(128)S(1)} %pad_add_fusion.idx, bf16[128,2048]{1,0:T(8,128)(2,1)S(1)} %get-tuple-element.46.q, bf16[144,1024]{1,0:T(8,128)(2,1)S(1)} %collective-permute-done.14.refs_0_, ...), custom_call_target="tpu_custom_call", output_to_operand_aliasing={{0}: (4, {}), {1}: (5, {})} | custom-call | flops 6000000000 | bytes 1048576 | tf_op jit(solution)/shard_map/pallas_call | solution.py:429
  76.9 1.3 %collective-permute-start.20 = (bf16[144,1024]{1,0:T(8,128)(2,1)S(1)}, bf16[144,1024]{1,0:T(8,128)(2,1)S(1)}, u32[]{:S(2)}, u32[]{:S(2)}) collective-permute-start(bf16[144,1024]{1,0:T(8,128)(2,1)S(1)} %collective-permute-done.19.refs_1_), channel_id=1, source_target_pairs={{192,160},{224,192},{0,224},{193,161},{225,193},{1,225},{194,162},... | collective-permute-start | bytes 884744 | tf_op jit(solution)/shard_map/ppermute | solution.py:63
  78.2 2.6 %collective-permute-done.15.refs_0_ = bf16[144,1024]{1,0:T(8,128)(2,1)S(1)} collective-permute-done((bf16[144,1024]{1,0:T(8,128)(2,1)S(1)}, bf16[144,1024]{1,0:T(8,128)(2,1)S(1)}, u32[]{:S(2)}, u32[]{:S(2)}) %collective-permute-start.15) | collective-permute-done | bytes 294944 | tf_op jit(solution)/shard_map/ppermute | solution.py:59
  80.8 4.7 %collective-permute-start.16 = (bf16[144,1024]{1,0:T(8,128)(2,1)S(1)}, bf16[144,1024]{1,0:T(8,128)(2,1)S(1)}, u32[]{:S(2)}, u32[]{:S(2)}) collective-permute-start(bf16[144,1024]{1,0:T(8,128)(2,1)S(1)} %collective-permute-done.15.refs_0_), channel_id=1, source_target_pairs={{64,96},{96,128},{128,160},{160,192},{192,224},{65,97},{97,129},{1... | collective-permute-start | bytes 884744 | tf_op jit(solution)/shard_map/ppermute | solution.py:59
  85.4 3.9 %shard_map.97 = (f32[2,80,2048]{2,1,0:T(8,128)S(1)}, f32[2,8,2048]{2,1,0:T(8,128)S(1)}, f32[8,256]{1,0:T(8,128)S(1)}) custom-call(s32[4]{0:T(128)S(1)} %pad_add_fusion.idx, bf16[128,2048]{1,0:T(8,128)(2,1)S(1)} %get-tuple-element.46.q, bf16[144,1024]{1,0:T(8,128)(2,1)S(1)} %collective-permute-done.15.refs_0_, ...), custom_call_target="tpu_custom_call", output_to_operand_aliasing={{0}: (4, {}), {1}: (5, {})} | custom-call | flops 6000000000 | bytes 1048576 | tf_op jit(solution)/shard_map/pallas_call | solution.py:429
  89.3 1.9 %collective-permute-done.16.refs_0_ = bf16[144,1024]{1,0:T(8,128)(2,1)S(1)} collective-permute-done((bf16[144,1024]{1,0:T(8,128)(2,1)S(1)}, bf16[144,1024]{1,0:T(8,128)(2,1)S(1)}, u32[]{:S(2)}, u32[]{:S(2)}) %collective-permute-start.16) | collective-permute-done | bytes 294944 | tf_op jit(solution)/shard_map/ppermute | solution.py:59
  91.2 5.8 %collective-permute-start.17 = (bf16[144,1024]{1,0:T(8,128)(2,1)S(1)}, bf16[144,1024]{1,0:T(8,128)(2,1)S(1)}, u32[]{:S(2)}, u32[]{:S(2)}) collective-permute-start(bf16[144,1024]{1,0:T(8,128)(2,1)S(1)} %collective-permute-done.16.refs_0_), channel_id=1, source_target_pairs={{96,128},{128,160},{160,192},{192,224},{97,129},{129,161},{161,193... | collective-permute-start | bytes 884744 | tf_op jit(solution)/shard_map/ppermute | solution.py:59
  97.1 6.7 %shard_map.98 = (f32[2,80,2048]{2,1,0:T(8,128)S(1)}, f32[2,8,2048]{2,1,0:T(8,128)S(1)}, f32[8,256]{1,0:T(8,128)S(1)}) custom-call(s32[4]{0:T(128)S(1)} %pad_add_fusion.idx, bf16[128,2048]{1,0:T(8,128)(2,1)S(1)} %get-tuple-element.46.q, bf16[144,1024]{1,0:T(8,128)(2,1)S(1)} %collective-permute-done.16.refs_0_, ...), custom_call_target="tpu_custom_call", output_to_operand_aliasing={{0}: (4, {}), {1}: (5, {})} | custom-call | flops 6000000000 | bytes 1048576 | tf_op jit(solution)/shard_map/pallas_call | solution.py:429
  103.8 4.0 %shard_map.99 = (f32[72,1024]{1,0:T(8,128)S(1)}, f32[72,1024]{1,0:T(8,128)S(1)}) custom-call(s32[4]{0:T(128)S(1)} %pad_add_fusion.idx, bf16[128,2048]{1,0:T(8,128)(2,1)S(1)} %get-tuple-element.46.q, bf16[144,1024]{1,0:T(8,128)(2,1)S(1)} %collective-permute-done.17.refs_0_, f32[2,80,2048]{2,1,0:T(8,128)S(1)} %get-tuple-element.57.refs_1_, ...), custom_call_target="tpu_custom_call" | custom-call | flops 6000000000 | bytes 1048576 | tf_op jit(solution)/shard_map/pallas_call | solution.py:429
  107.9 1.6 %collective-permute-done.21.sib = f32[72,1024]{1,0:T(8,128)S(1)} collective-permute-done((f32[72,1024]{1,0:T(8,128)S(1)}, f32[72,1024]{1,0:T(8,128)S(1)}, u32[]{:S(2)}, u32[]{:S(2)}) %collective-permute-start.21) | collective-permute-done | bytes 294944 | tf_op jit(solution)/shard_map/ppermute | solution.py:51
  109.7 0.9 reshape.4
  110.6 7.6 %all-to-all-start.1 = ((bf16[16,2,2048]{2,1,0:T(2,128)(2,1)}), bf16[16,2,2048]{2,1,0:T(2,128)(2,1)S(1)}, u32[]{:S(2)}, u32[]{:S(2)}) async-start(bf16[16,2,2048]{2,1,0:T(2,128)(2,1)} %reshape.4), calls=%async_computation.1 | async-start | bytes 262144 | tf_op jit(solution)/shard_map/all_to_all | solution.py:442
  118.3 0.8 copy-done
  119.1 0.8 copy-done.2
  119.9 1.0 copy-done.1
  120.9 1.0 copy-done.3
  122.0 1.0 shard_map.101.w
  123.0 3.1 %all-to-all-done.1 = bf16[16,2,2048]{2,1,0:T(2,128)(2,1)S(1)} async-done(((bf16[16,2,2048]{2,1,0:T(2,128)(2,1)}), bf16[16,2,2048]{2,1,0:T(2,128)(2,1)S(1)}, u32[]{:S(2)}, u32[]{:S(2)}) %all-to-all-start.1) | async-done | bytes 131104 | tf_op jit(solution)/shard_map/all_to_all | solution.py:442
  126.3 1.5 %shard_map.102 = bf16[64,1024]{1,0:T(8,128)(2,1)} custom-call(bf16[16,64,64]{2,1,0:T(8,128)(2,1)S(1)} %reshape.5.att, f32[1,1024]{1,0:T(1,128)S(1)} %bitcast.13, bf16[1024,1024]{1,0:T(8,128)(2,1)S(1)} %shard_map.101.w), custom_call_target="tpu_custom_call" | custom-call | flops 100000000 | bytes 1048576 | tf_op jit(solution)/shard_map/pallas_call | solution.py:443
  (54 shorter events, 8.2 us)
Async XLA Ops:
  0.1 0.9 copy-start.5
  1.0 0.7 copy-start.6
  1.7 0.7 copy-start.7
  2.4 0.7 copy-start.8
  3.1 0.7 copy-start.9
  3.8 0.7 copy-start.11
  5.9 48.0 %copy-start.10 = (f32[1024]{0:T(1024)S(1)}, f32[1024]{0:T(1024)}, u32[]{:S(2)}) copy-start(f32[1024]{0:T(1024)} %param.10) | copy-start | bytes 12292
  5.9 48.0 %copy-start.12 = (f32[4]{0:T(128)S(1)}, f32[4]{0:T(128)}, u32[]{:S(2)}) copy-start(f32[4]{0:T(128)} %offs.1) | copy-start | bytes 52
  5.9 6.1 %collective-permute-start.6 = (bf16[48,1024]{1,0:T(8,128)(2,1)S(1)}, bf16[48,1024]{1,0:T(8,128)(2,1)S(1)}, u32[]{:S(2)}, u32[]{:S(2)}) collective-permute-start(bf16[48,1024]{1,0:T(8,128)(2,1)S(1)} %get-tuple-element.38), channel_id=1, source_target_pairs={{0,8},{8,16},{16,24},{24,0},{1,9},{9,17},{17,25},{25,1},{2,10},{10... | collective-permute-start | bytes 294920 | tf_op jit(solution)/shard_map/ppermute | solution.py:51
  7.5 7.3 %collective-permute-start.7 = (bf16[48,1024]{1,0:T(8,128)(2,1)S(1)}, bf16[48,1024]{1,0:T(8,128)(2,1)S(1)}, u32[]{:S(2)}, u32[]{:S(2)}) collective-permute-start(bf16[48,1024]{1,0:T(8,128)(2,1)S(1)} %get-tuple-element.39), channel_id=1, source_target_pairs={{0,16},{8,24},{16,0},{24,8},{1,17},{9,25},{17,1},{25,9},{2,18},{10... | collective-permute-start | bytes 294920 | tf_op jit(solution)/shard_map/ppermute | solution.py:51
  10.2 4.6 %collective-permute-start.8 = (bf16[48,1024]{1,0:T(8,128)(2,1)S(1)}, bf16[48,1024]{1,0:T(8,128)(2,1)S(1)}, u32[]{:S(2)}, u32[]{:S(2)}) collective-permute-start(bf16[48,1024]{1,0:T(8,128)(2,1)S(1)} %get-tuple-element.40), channel_id=1, source_target_pairs={{0,24},{8,0},{16,8},{24,16},{1,25},{9,1},{17,9},{25,17},{2,26},{10... | collective-permute-start | bytes 294920 | tf_op jit(solution)/shard_map/ppermute | solution.py:51
  15.7 19.8 %all-to-all-start = ((bf16[8,128,256]{2,1,0:T(8,128)(2,1)}), bf16[8,128,256]{2,1,0:T(8,128)(2,1)S(1)}, u32[]{:S(2)}, u32[]{:S(2)}) async-start(bf16[8,128,256]{2,1,0:T(8,128)(2,1)} %get-tuple-element.42), calls=%async_computation | async-start | bytes 1048576 | tf_op jit(solution)/shard_map/all_to_all | solution.py:376
  22.4 9.5 %collective-permute-start.2 = (bf16[32,1024]{1,0:T(8,128)(2,1)S(1)}, bf16[32,1024]{1,0:T(8,128)(2,1)S(1)}, u32[]{:S(2)}, u32[]{:S(2)}) collective-permute-start(bf16[32,1024]{1,0:T(8,128)(2,1)S(1)} %get-tuple-element.34), channel_id=1, source_target_pairs={{0,3},{1,0},{2,1},{3,2},{4,7},{5,4},{6,5},{7,6},{8,11},{9,8},{10,9... | collective-permute-start | bytes 196616 | tf_op jit(solution)/shard_map/ppermute | solution.py:51
  25.5 6.5 %collective-permute-start.1 = (bf16[32,1024]{1,0:T(8,128)(2,1)S(1)}, bf16[32,1024]{1,0:T(8,128)(2,1)S(1)}, u32[]{:S(2)}, u32[]{:S(2)}) collective-permute-start(bf16[32,1024]{1,0:T(8,128)(2,1)S(1)} %get-tuple-element.34), channel_id=1, source_target_pairs={{0,2},{1,3},{2,0},{3,1},{4,6},{5,7},{6,4},{7,5},{8,10},{9,11},{10,... | collective-permute-start | bytes 196616 | tf_op jit(solution)/shard_map/ppermute | solution.py:51
  26.1 5.8 %collective-permute-start = (bf16[32,1024]{1,0:T(8,128)(2,1)S(1)}, bf16[32,1024]{1,0:T(8,128)(2,1)S(1)}, u32[]{:S(2)}, u32[]{:S(2)}) collective-permute-start(bf16[32,1024]{1,0:T(8,128)(2,1)S(1)} %get-tuple-element.34), channel_id=1, source_target_pairs={{0,1},{1,2},{2,3},{3,0},{4,5},{5,6},{6,7},{7,4},{8,9},{9,10},{10,1... | collective-permute-start | bytes 196616 | tf_op jit(solution)/shard_map/ppermute | solution.py:51
  32.0 11.2 %collective-permute-start.5 = (bf16[128,1024]{1,0:T(8,128)(2,1)S(1)}, bf16[128,1024]{1,0:T(8,128)(2,1)S(1)}, u32[]{:S(2)}, u32[]{:S(2)}) collective-permute-start(bf16[128,1024]{1,0:T(8,128)(2,1)S(1)} %constant_dynamic-update-slice_fusion.refs_0_), channel_id=1, source_target_pairs={{0,24},{8,0},{16,8},{24,16},{1,25},{9,1},{17,9},{25,17},{2,26},{10... | collective-permute-start | bytes 786440 | tf_op jit(solution)/shard_map/ppermute | solution.py:51
  34.7 10.6 %collective-permute-start.4 = (bf16[128,1024]{1,0:T(8,128)(2,1)S(1)}, bf16[128,1024]{1,0:T(8,128)(2,1)S(1)}, u32[]{:S(2)}, u32[]{:S(2)}) collective-permute-start(bf16[128,1024]{1,0:T(8,128)(2,1)S(1)} %constant_dynamic-update-slice_fusion.refs_0_), channel_id=1, source_target_pairs={{0,16},{8,24},{16,0},{24,8},{1,17},{9,25},{17,1},{25,9},{2,18},{10... | collective-permute-start | bytes 786440 | tf_op jit(solution)/shard_map/ppermute | solution.py:51
  35.5 18.4 %collective-permute-start.12 = (bf16[8,128,256]{2,1,0:T(8,128)(2,1)S(1)}, bf16[8,128,256]{2,1,0:T(8,128)(2,1)S(1)}, u32[]{:S(2)}, u32[]{:S(2)}) collective-permute-start(bf16[8,128,256]{2,1,0:T(8,128)(2,1)S(1)} %all-to-all-done.refs_9_), channel_id=1, source_target_pairs={{0,4},{4,0},{1,5},{5,1},{2,6},{6,2},{3,7},{7,3},{8,12},{12,8},{9,1... | collective-permute-start | bytes 1572872 | tf_op jit(solution)/shard_map/ppermute | solution.py:51
  35.5 12.7 %collective-permute-start.3 = (bf16[128,1024]{1,0:T(8,128)(2,1)S(1)}, bf16[128,1024]{1,0:T(8,128)(2,1)S(1)}, u32[]{:S(2)}, u32[]{:S(2)}) collective-permute-start(bf16[128,1024]{1,0:T(8,128)(2,1)S(1)} %constant_dynamic-update-slice_fusion.refs_0_), channel_id=1, source_target_pairs={{0,8},{8,16},{16,24},{24,0},{1,9},{9,17},{17,25},{25,1},{2,10},{10... | collective-permute-start | bytes 786440 | tf_op jit(solution)/shard_map/ppermute | solution.py:51
  36.2 14.0 %collective-permute-start.11 = (bf16[128,1024]{1,0:T(8,128)(2,1)S(1)}, bf16[128,1024]{1,0:T(8,128)(2,1)S(1)}, u32[]{:S(2)}, u32[]{:S(2)}) collective-permute-start(bf16[128,1024]{1,0:T(8,128)(2,1)S(1)} %get-tuple-element.41.refs_4_), channel_id=1, source_target_pairs={{0,3},{1,0},{2,1},{3,2},{4,7},{5,4},{6,5},{7,6},{8,11},{9,8},{10,9... | collective-permute-start | bytes 786440 | tf_op jit(solution)/shard_map/ppermute | solution.py:51
  43.1 8.1 %collective-permute-start.10 = (bf16[128,1024]{1,0:T(8,128)(2,1)S(1)}, bf16[128,1024]{1,0:T(8,128)(2,1)S(1)}, u32[]{:S(2)}, u32[]{:S(2)}) collective-permute-start(bf16[128,1024]{1,0:T(8,128)(2,1)S(1)} %get-tuple-element.41.refs_4_), channel_id=1, source_target_pairs={{0,2},{1,3},{2,0},{3,1},{4,6},{5,7},{6,4},{7,5},{8,10},{9,11},{10,... | collective-permute-start | bytes 786440 | tf_op jit(solution)/shard_map/ppermute | solution.py:51
  45.3 8.6 %collective-permute-start.9 = (bf16[128,1024]{1,0:T(8,128)(2,1)S(1)}, bf16[128,1024]{1,0:T(8,128)(2,1)S(1)}, u32[]{:S(2)}, u32[]{:S(2)}) collective-permute-start(bf16[128,1024]{1,0:T(8,128)(2,1)S(1)} %get-tuple-element.41.refs_4_), channel_id=1, source_target_pairs={{0,1},{1,2},{2,3},{3,0},{4,5},{5,6},{6,7},{7,4},{8,9},{9,10},{10,1... | collective-permute-start | bytes 786440 | tf_op jit(solution)/shard_map/ppermute | solution.py:51
  56.1 1.5 %collective-permute-start.13 = (bf16[80,1024]{1,0:T(8,128)(2,1)S(1)}, bf16[80,1024]{1,0:T(8,128)(2,1)S(1)}, u32[]{:S(2)}, u32[]{:S(2)}) collective-permute-start(bf16[80,1024]{1,0:T(8,128)(2,1)S(1)} %get-tuple-element.43.q_own), channel_id=1, source_target_pairs={{0,4},{4,0},{1,5},{5,1},{2,6},{6,2},{3,7},{7,3},{8,12},{12,8},{9,1... | collective-permute-start | bytes 491528 | tf_op jit(solution)/shard_map/ppermute | solution.py:51
  58.2 10.6 %collective-permute-start.18 = (bf16[144,1024]{1,0:T(8,128)(2,1)S(1)}, bf16[144,1024]{1,0:T(8,128)(2,1)S(1)}, u32[]{:S(2)}, u32[]{:S(2)}) collective-permute-start(bf16[144,1024]{1,0:T(8,128)(2,1)S(1)} %get-tuple-element.47.pay), channel_id=1, source_target_pairs={{0,224},{32,0},{64,32},{1,225},{33,1},{65,33},{2,226},{34,2},{66,3... | collective-permute-start | bytes 884744 | tf_op jit(solution)/shard_map/ppermute | solution.py:63
  58.9 10.9 %collective-permute-start.14 = (bf16[144,1024]{1,0:T(8,128)(2,1)S(1)}, bf16[144,1024]{1,0:T(8,128)(2,1)S(1)}, u32[]{:S(2)}, u32[]{:S(2)}) collective-permute-start(bf16[144,1024]{1,0:T(8,128)(2,1)S(1)} %get-tuple-element.47.pay), channel_id=1, source_target_pairs={{0,32},{32,64},{64,96},{96,128},{128,160},{160,192},{192,224},{1,3... | collective-permute-start | bytes 884744 | tf_op jit(solution)/shard_map/ppermute | solution.py:59
  66.7 51.6 %collective-permute-start.24 = (bf16[2,8,64,256]{3,2,1,0:T(8,128)(2,1)S(1)}, bf16[2,8,64,256]{3,2,1,0:T(8,128)(2,1)S(1)}, u32[]{:S(2)}, u32[]{:S(2)}) collective-permute-start(bf16[2,8,64,256]{3,2,1,0:T(8,128)(2,1)S(1)} %pad_maximum_fusion.w0), channel_id=1, source_target_pairs={{0,3},{1,0},{2,1},{3,2},{4,7},{5,4},{6,5},{7,6},{8,11},{9,8},{10,9... | collective-permute-start | bytes 1572872 | tf_op jit(solution)/shard_map/ppermute | solution.py:51
  67.4 50.8 %collective-permute-start.23 = (bf16[2,8,64,256]{3,2,1,0:T(8,128)(2,1)S(1)}, bf16[2,8,64,256]{3,2,1,0:T(8,128)(2,1)S(1)}, u32[]{:S(2)}, u32[]{:S(2)}) collective-permute-start(bf16[2,8,64,256]{3,2,1,0:T(8,128)(2,1)S(1)} %pad_maximum_fusion.w0), channel_id=1, source_target_pairs={{0,2},{1,3},{2,0},{3,1},{4,6},{5,7},{6,4},{7,5},{8,10},{9,11},{10,... | collective-permute-start | bytes 1572872 | tf_op jit(solution)/shard_map/ppermute | solution.py:51
  68.0 51.1 %collective-permute-start.22 = (bf16[2,8,64,256]{3,2,1,0:T(8,128)(2,1)S(1)}, bf16[2,8,64,256]{3,2,1,0:T(8,128)(2,1)S(1)}, u32[]{:S(2)}, u32[]{:S(2)}) collective-permute-start(bf16[2,8,64,256]{3,2,1,0:T(8,128)(2,1)S(1)} %pad_maximum_fusion.w0), channel_id=1, source_target_pairs={{0,1},{1,2},{2,3},{3,0},{4,5},{5,6},{6,7},{7,4},{8,9},{9,10},{10,1... | collective-permute-start | bytes 1572872 | tf_op jit(solution)/shard_map/ppermute | solution.py:51
  68.8 8.1 %collective-permute-start.19 = (bf16[144,1024]{1,0:T(8,128)(2,1)S(1)}, bf16[144,1024]{1,0:T(8,128)(2,1)S(1)}, u32[]{:S(2)}, u32[]{:S(2)}) collective-permute-start(bf16[144,1024]{1,0:T(8,128)(2,1)S(1)} %collective-permute-done.18.refs_1_), channel_id=1, source_target_pairs={{224,192},{0,224},{32,0},{225,193},{1,225},{33,1},{226,194},{2,226... | collective-permute-start | bytes 884744 | tf_op jit(solution)/shard_map/ppermute | solution.py:63
  69.8 10.9 %collective-permute-start.15 = (bf16[144,1024]{1,0:T(8,128)(2,1)S(1)}, bf16[144,1024]{1,0:T(8,128)(2,1)S(1)}, u32[]{:S(2)}, u32[]{:S(2)}) collective-permute-start(bf16[144,1024]{1,0:T(8,128)(2,1)S(1)} %collective-permute-done.14.refs_0_), channel_id=1, source_target_pairs={{32,64},{64,96},{96,128},{128,160},{160,192},{192,224},{33,65},{65... | collective-permute-start | bytes 884744 | tf_op jit(solution)/shard_map/ppermute | solution.py:59
  76.9 20.1 %collective-permute-start.20 = (bf16[144,1024]{1,0:T(8,128)(2,1)S(1)}, bf16[144,1024]{1,0:T(8,128)(2,1)S(1)}, u32[]{:S(2)}, u32[]{:S(2)}) collective-permute-start(bf16[144,1024]{1,0:T(8,128)(2,1)S(1)} %collective-permute-done.19.refs_1_), channel_id=1, source_target_pairs={{192,160},{224,192},{0,224},{193,161},{225,193},{1,225},{194,162},... | collective-permute-start | bytes 884744 | tf_op jit(solution)/shard_map/ppermute | solution.py:63
  80.8 10.4 %collective-permute-start.16 = (bf16[144,1024]{1,0:T(8,128)(2,1)S(1)}, bf16[144,1024]{1,0:T(8,128)(2,1)S(1)}, u32[]{:S(2)}, u32[]{:S(2)}) collective-permute-start(bf16[144,1024]{1,0:T(8,128)(2,1)S(1)} %collective-permute-done.15.refs_0_), channel_id=1, source_target_pairs={{64,96},{96,128},{128,160},{160,192},{192,224},{65,97},{97,129},{1... | collective-permute-start | bytes 884744 | tf_op jit(solution)/shard_map/ppermute | solution.py:59
  91.2 12.6 %collective-permute-start.17 = (bf16[144,1024]{1,0:T(8,128)(2,1)S(1)}, bf16[144,1024]{1,0:T(8,128)(2,1)S(1)}, u32[]{:S(2)}, u32[]{:S(2)}) collective-permute-start(bf16[144,1024]{1,0:T(8,128)(2,1)S(1)} %collective-permute-done.16.refs_0_), channel_id=1, source_target_pairs={{96,128},{128,160},{160,192},{192,224},{97,129},{129,161},{161,193... | collective-permute-start | bytes 884744 | tf_op jit(solution)/shard_map/ppermute | solution.py:59
  107.8 1.7 %collective-permute-start.21 = (f32[72,1024]{1,0:T(8,128)S(1)}, f32[72,1024]{1,0:T(8,128)S(1)}, u32[]{:S(2)}, u32[]{:S(2)}) collective-permute-start(f32[72,1024]{1,0:T(8,128)S(1)} %get-tuple-element.61), channel_id=1, source_target_pairs={{0,4},{4,0},{1,5},{5,1},{2,6},{6,2},{3,7},{7,3},{8,12},{12,8},{9,1... | collective-permute-start | bytes 884744 | tf_op jit(solution)/shard_map/ppermute | solution.py:51
  110.6 15.7 %copy-start.4 = (f32[1024]{0:T(1024)S(1)}, f32[1024]{0:T(1024)}, u32[]{:S(2)}) copy-start(f32[1024]{0:T(1024)} %param.17) | copy-start | bytes 12292
  110.6 15.5 %all-to-all-start.1 = ((bf16[16,2,2048]{2,1,0:T(2,128)(2,1)}), bf16[16,2,2048]{2,1,0:T(2,128)(2,1)S(1)}, u32[]{:S(2)}, u32[]{:S(2)}) async-start(bf16[16,2,2048]{2,1,0:T(2,128)(2,1)} %reshape.4), calls=%async_computation.1 | async-start | bytes 262144 | tf_op jit(solution)/shard_map/all_to_all | solution.py:442
  118.2 0.8 copy-start
  119.1 0.8 copy-start.2
  119.9 1.0 copy-start.1
  120.9 1.0 copy-start.3

commit v3 on v2

--- a/solution.py
+++ b/solution.py
@@ -71,35 +71,28 @@
     return hi, mid, low
 
 
-def pack_body(idx, tok, wq, wk, wv, wf, wo, lo, hi, p0, o0, s1, s2, s3, qv, kv, vv, fv, heads, sems):
+def pack_body(idx, tok, w, lo, hi, p0, o0, s1, s2, s3, heads):
     x = idx[1]
-    sends = (s1, s2, s3)
-    pairs = [(wq, qv), (wk, kv), (wv, vv), (wf, fv), (wo, o0)]
-    pairs += [(tok.at[32:64], s.at[0:32]) for s in sends]
-    pairs += [(tok.at[0:32], lo), (tok.at[32:64], hi)]
-    copies = [pltpu.make_async_copy(a, b, sems.at[i]) for i, (a, b) in enumerate(pairs)]
-    for copy in copies:
-        copy.start()
-    for s in sends:
-        s[32:48, 512:1024] = jnp.zeros((16, 512), BF16)
-    for copy in copies[:5]:
-        copy.wait()
-    head = lax.broadcasted_iota(jnp.int32, (NX, HD), 0)
-    gates = fv[...].astype(F32)
+    lo[...] = tok[0:32, :]
+    hi[...] = tok[32:64, :]
+    o0[...] = w[48:64, :]
+    head = lax.broadcasted_iota(jnp.int32, (16, HD), 0)
+    gates = w[64:80, 0:128].astype(F32)
     for h in range(NX):
         lanes = slice(h * HD, (h + 1) * HD)
         pick = jnp.where(head == h, 1.0, 0.0)
         gate = lax.dot_general(
             gates, pick, (((0,), (0,)), ((), ())), precision=lax.Precision.HIGHEST,
             preferred_element_type=F32,
-        )
-        heads[h] = jnp.concatenate([qv[:, lanes], kv[:, lanes], vv[:, lanes], gate.astype(BF16)], axis=1)
+        )[0:16]
+        mine = [w[0:16, lanes], w[16:32, lanes], w[32:48, lanes], gate.astype(BF16)]
+        heads[h] = jnp.concatenate(mine, axis=1)
     p0[...] = heads[x]
-    for k, s in enumerate(sends):
+    for k, s in enumerate((s1, s2, s3)):
+        s[0:32, :] = tok[32:64, :]
         s[32:48, 0:256] = heads[lax.rem(x + k + 1, NX)]
-        s[32:48, 256:512] = o0[...]
-    for copy in copies[5:]:
-        copy.wait()
+        s[32:48, 256:512] = w[48:64, :]
+        s[32:48, 512:1024] = jnp.zeros((16, 512), BF16)
 
 
 def spread_body(hi, p0, o0, r1, r2, r3, out, toks):
@@ -213,37 +206,44 @@
     vx[i, 64:80, :] = jnp.ones((16, KEYS), BF16)
 
 
-def absorb(count, q, acc, m, kx, vx, move, work, c=None):
+def stages(q, acc, m, kx, vx, move, work):
     tiles = QS // BLK
     bufs, tops, probs, fades = work[0:2], work[2:4], work[4:6], work[6:8]
-    if c is not None:
-        key = lax.broadcasted_iota(jnp.int32, (KEYS, BLK), 0)
-        key_pos = key + (key // BLK + c) * BLK
-        query = lax.broadcasted_iota(jnp.int32, (KEYS, BLK), 1)
 
     def lanes_of(t):
+        if isinstance(t, int):
+            return slice((t % tiles) * BLK, (t % tiles + 1) * BLK)
         return pl.ds(pl.multiple_of((t % tiles) * BLK, BLK), BLK)
 
-    def score(t, slot):
-        s = jnp.dot(kx[t // tiles], q[:, lanes_of(t)], preferred_element_type=F32)
-        if c is not None:
-            s = jnp.where(key_pos <= query + (t % tiles) * BLK, s, LOW)
-        bufs[slot][...] = s
+    def score(t, slot, n=KEYS, allowed=None):
+        s = jnp.dot(kx[t // tiles, 0:n], q[:, lanes_of(t)], preferred_element_type=F32)
+        if allowed is not None:
+            last = jnp.where(allowed, s[n - BLK : n], LOW)
+            s = last if n == BLK else jnp.concatenate([s[0 : n - BLK], last], axis=0)
+        bufs[slot][0:n] = s
         tops[slot][...] = jnp.broadcast_to(jnp.max(s, axis=0, keepdims=True), (8, BLK))
 
-    def weigh(t, slot):
+    def weigh(t, slot, n=KEYS):
         i, lanes = t // tiles, lanes_of(t)
         by = move[i, 0:1]
         old = m[i, 0:1, lanes]
         new = jnp.maximum(old, tops[slot][0:1] + by)
-        probs[slot][...] = jnp.exp(bufs[slot][...] - (new - by)).astype(BF16)
+        probs[slot][0:n] = jnp.exp(bufs[slot][0:n] - (new - by)).astype(BF16)
         fades[slot][...] = jnp.broadcast_to(jnp.exp(old - new), (8, BLK))
         m[i, :, lanes] = jnp.broadcast_to(new, (8, BLK))
 
-    def add(t, slot):
+    def add(t, slot, n=KEYS):
         i, lanes = t // tiles, lanes_of(t)
-        part = jnp.dot(vx[i], probs[slot][...], preferred_element_type=F32)
+        part = jnp.dot(vx[i, :, 0:n], probs[slot][0:n], preferred_element_type=F32)
         acc[i, :, lanes] = acc[i, :, lanes] * fades[slot][0:1] + part
+
+    return score, weigh, add
+
+
+def absorb(count, q, acc, m, kx, vx, move, work):
+    tiles = QS // BLK
+    score, weigh, add = stages(q, acc, m, kx, vx, move, work)
+    probs, fades = work[4:6], work[6:8]
 
     @pl.when(count > 0)
     def _():
@@ -271,7 +271,19 @@
     m[...] = jnp.full(m.shape, LOW, F32)
     move[...] = jnp.zeros_like(move)
     place_chunk(pay, 0, kx, vx)
-    absorb(1, q, acc, m, kx, vx, move, bufs, idx[2])
+    score, weigh, add = stages(q, acc, m, kx, vx, move, bufs)
+    key = lax.broadcasted_iota(jnp.int32, (BLK, BLK), 0)
+    query = lax.broadcasted_iota(jnp.int32, (BLK, BLK), 1)
+    tiles = QS // BLK
+    meets = [(b // 2 + 1) * BLK for b in range(tiles)]
+    masks = [key + (idx[2] - odd) * BLK <= query for odd in range(2)]
+    for b in range(tiles + 2):
+        if b < tiles:
+            score(b, b % 2, meets[b], masks[b % 2])
+        if 0 <= b - 1 < tiles:
+            weigh(b - 1, (b - 1) % 2, meets[b - 1])
+        if 0 <= b - 2:
+            add(b - 2, (b - 2) % 2, meets[b - 2])
     sums[...] = jnp.broadcast_to(chunk_total(pay), sums.shape)
 
 
@@ -321,7 +333,9 @@
                 out[64:72, to] = jnp.where(row < 4, both[64:65], top)
 
 
-def merge_body(own, sib, out):
+def merge_body(idx, own, sib, *outs):
+    x = idx[1]
+    outs, parts = outs[:NX], outs[NX]
     a, b = own[...], sib[...]
     m_a, m_b = a[68:69], b[68:69]
     top = jnp.maximum(m_a, m_b)
@@ -330,7 +344,20 @@
     att = (a[0:64] * f_a + b[0:64] * f_b) / total
     att = jnp.concatenate([att, jnp.zeros_like(att)], axis=0)
     for r in range(8):
-        out[r * 128 : (r + 1) * 128, :] = att[:, r * 128 : (r + 1) * 128].T[:, 0:64].astype(BF16)
+        tile = att[:, r * 128 : (r + 1) * 128].T[:, 0:64].astype(BF16)
+        parts[r // 2, (r % 2) * 128 : (r % 2) * 128 + 128, :] = tile
+    for k, out in enumerate(outs):
+        out[...] = parts[lax.rem(x + k, NX)]
+
+
+def regroup_body(idx, h0, h1, h2, h3, *outs):
+    x, y = idx[1], idx[3]
+    outs, heads = outs[:NY], outs[NY]
+    for k, h in enumerate((h0, h1, h2, h3)):
+        heads[lax.rem(x - k + NX, NX)] = h[...]
+    for k, out in enumerate(outs):
+        rows = pl.ds(pl.multiple_of(lax.rem(y + k, NY) * OWN, OWN), OWN)
+        out[...] = jnp.concatenate([heads[i, rows, :] for i in range(NX)], axis=1)
 
 
 def assemble_body(idx, w0, w1, w2, w3, w):
@@ -346,10 +373,14 @@
                     w[pl.ds(at, 16), cols] = ref[other, z, kx * 16 : kx * 16 + 16, :]
 
 
-def final_body(att, gain, w, out):
-    pieces = [att[xs * NY + ys] for ys in range(NY) for xs in range(NX)]
-    joined = jnp.concatenate(pieces, axis=1)
-    proj = lax.dot_general(joined, w[...], (((1,), (1,)), ((), ())), preferred_element_type=F32)
+def final_body(idx, a0, a1, a2, a3, gain, w, out, joined):
+    y = idx[3]
+    for k, a in enumerate((a0, a1, a2, a3)):
+        cols = pl.ds(pl.multiple_of(lax.rem(y - k + NY, NY) * 256, 256), 256)
+        joined[:, cols] = a[...]
+    proj = lax.dot_general(
+        joined[...], w[...], (((1,), (1,)), ((), ())), preferred_element_type=F32
+    )
     scale = lax.rsqrt(jnp.mean(proj * proj, axis=-1, keepdims=True) + EPS)
     out[...] = (proj * scale * gain[...]).astype(BF16)
 
@@ -359,14 +390,14 @@
     idx = jnp.stack([lax.axis_index(a) for a in AXES]).astype(jnp.int32)
 
     half, piece, send = sds((32, D), BF16), sds((16, 256), BF16), sds((48, D), BF16)
-    own_w = pltpu.VMEM((16, 256), BF16)
+    gate_rows = jnp.pad(w_forget.T, ((0, 16 - NX), (0, 256 - 16)))
+    weights = jnp.concatenate([w_query, w_key, w_value, w_out_t, gate_rows], axis=0)
     lo, hi, p0, o0, *sends = call(
         pack_body,
         (half, half, piece, piece, send, send, send),
-        [SMEM] + [pl.BlockSpec(memory_space=pl.ANY)] * 6,
-        [own_w, own_w, own_w, pltpu.VMEM((NX, 16), BF16), pltpu.VMEM((NX, 16, 256), BF16)]
-        + [pltpu.SemaphoreType.DMA((10,))],
-    )(idx, tokens, w_query, w_key, w_value, w_forget.T, w_out_t)
+        [SMEM, VMEM, VMEM],
+        [pltpu.VMEM((NX, 16, 256), BF16)],
+    )(idx, tokens, weights)
 
     got = [shift(sends[k - 1], "x", k) for k in range(1, NX)]
     tok_a = direct(lo, "y")
@@ -386,8 +417,11 @@
     )(idx, forget_offset, *toks, norm_gain[None], w_own, w_sib)
 
     q_sib = shift(q_own, "c", 1)
+    w_o = direct(jnp.stack([w_own[:, 64:], w_sib[:, 64:]]), "y")
     q, pay = call(
-        prepare_body, (sds((128, QS), BF16), sds((PAY, KEYS), BF16)), [SMEM] + [VMEM] * 4
+        prepare_body,
+        (sds((128, QS), BF16), sds((PAY, KEYS), BF16)),
+        [SMEM] + [VMEM] * 4,
     )(idx, q_own, q_sib, kv, cum_own)
 
     acc_t, m_t, sums_t = sds((2, 80, QS), F32), sds((2, 8, QS), F32), sds((8, BLK), F32)
@@ -409,10 +443,6 @@
     acc, m, sums = call(
         first_body, (acc_t, m_t, sums_t), [SMEM, VMEM, VMEM], work, 3e9
     )(idx, q, pay)
-
-    w_o = jnp.stack([w_own[:, 64:], w_sib[:, 64:]])
-    w_o, _ = lax.optimization_barrier((w_o, sums))
-    w_o = direct(w_o, "y")
 
     for k in range(1, 5):
         pays = (right, left) if k < 4 else (right,)
@@ -438,9 +468,24 @@
             acc, m, sums = res
     sib = shift(res[1], "c", 1)
     w_full = call(assemble_body, sds((D, D), BF16), [SMEM] + [VMEM] * 4)(idx, *w_o)
-    att = call(merge_body, sds((KEYS, HD), BF16), [VMEM, VMEM])(res[0], sib)
-    att = lax.all_to_all(att.reshape(16, 64, HD), ("x", "y"), 0, 0, tiled=True)
-    return call(final_body, sds((OWN, D), BF16), [VMEM] * 3)(att, out_gain[None], w_full)
+    rows = sds((BLK, HD), BF16)
+    parts = call(
+        merge_body, (rows,) * NX, [SMEM, VMEM, VMEM], [pltpu.VMEM((NX, BLK, HD), BF16)]
+    )(idx, res[0], sib)
+    parts = [parts[0]] + [shift(parts[k], "x", k) for k in range(1, NX)]
+    parts = call(
+        regroup_body,
+        (sds((OWN, 256), BF16),) * NY,
+        [SMEM] + [VMEM] * NX,
+        [pltpu.VMEM((NX, BLK, HD), BF16)],
+    )(idx, *parts)
+    parts = [parts[0]] + [shift(parts[k], "y", k) for k in range(1, NY)]
+    return call(
+        final_body,
+        sds((OWN, D), BF16),
+        [SMEM] + [VMEM] * (NY + 2),
+        [pltpu.VMEM((OWN, D), BF16)],
+    )(idx, *parts, out_gain[None], w_full)
 
 
 def solution(mesh):

time: 129 us -> 132 us (1.023)
  the two profiles are of different devices: /device:TPU:160 before, /device:TPU:192 now
where the time goes in v3:
time: 132 us; the launch traced here: 131 us
  starting transfers between devices  61.3 us (46%)
  Pallas kernels  33.2 us (25%)
  waiting for transfers between devices  31.9 us (24%)
  local copies, waits for them, and re-layouts  4.45 us (3%)
    ppermute x24, starting transfers between devices, shift(): return lax.ppermute(x, axis, [(i, (i + k) % n) for i in range(n)])  37.8 us
    ppermute x24, waiting for transfers between devices, shift(): return lax.ppermute(x, axis, [(i, (i + k) % n) for i in range(n)])  29.1 us
    pallas_call x4, Pallas kernels, shards(): call(functools.partial(step_body, k), outs, [SMEM] + [VMEM] * (len(ins) -...  21.3 us
    ppermute x4, starting transfers between devices, step_right(): return lax.ppermute(x, 'z', [(i, i + 1) for i in range(k - 1, NZ - 1)])  13.2 us
    all_to_all x1, starting transfers between devices, shards(): w_own = lax.all_to_all(chunk, 'z', 0, 0, tiled=True)  6.3 us
    ppermute x3, starting transfers between devices, step_left(): lax.ppermute(x, 'z', [((i - k + 1) % NZ, (i - k) % NZ) for i in range(3)])  3.89 us
    unnamed x15, local copies, waits for them, and re-layouts  3.73 us
    ppermute x4, waiting for transfers between devices, step_right(): return lax.ppermute(x, 'z', [(i, i + 1) for i in range(k - 1, NZ - 1)])  2.79 us
  transfers between devices with their start and end apart: 32, of which 16 were waited for; matrix products, arithmetic and copies ran while one was open for 0% of the time, Pallas kernels for 20%

profile of v3, /device:TPU:192, one launch (start us, length us, event | category | flops | bytes accessed | tf_op | source)
XLA Modules:
  0.0 131.2 jit_solution(12043401257088705649)
XLA Ops:
  3.6 0.9 copy-done.1
  4.5 1.0 shard_map.91
  5.5 1.6 %collective-permute-start.6 = (bf16[48,1024]{1,0:T(8,128)(2,1)S(1)}, bf16[48,1024]{1,0:T(8,128)(2,1)S(1)}, u32[]{:S(2)}, u32[]{:S(2)}) collective-permute-start(bf16[48,1024]{1,0:T(8,128)(2,1)S(1)} %get-tuple-element.45), channel_id=1, source_target_pairs={{0,8},{8,16},{16,24},{24,0},{1,9},{9,17},{17,25},{25,1},{2,10},{10... | collective-permute-start | bytes 294920 | tf_op jit(solution)/shard_map/ppermute | solution.py:51
  7.1 2.7 %collective-permute-start.7 = (bf16[48,1024]{1,0:T(8,128)(2,1)S(1)}, bf16[48,1024]{1,0:T(8,128)(2,1)S(1)}, u32[]{:S(2)}, u32[]{:S(2)}) collective-permute-start(bf16[48,1024]{1,0:T(8,128)(2,1)S(1)} %get-tuple-element.46), channel_id=1, source_target_pairs={{0,16},{8,24},{16,0},{24,8},{1,17},{9,25},{17,1},{25,9},{2,18},{10... | collective-permute-start | bytes 294920 | tf_op jit(solution)/shard_map/ppermute | solution.py:51
  9.8 1.4 %collective-permute-start.8 = (bf16[48,1024]{1,0:T(8,128)(2,1)S(1)}, bf16[48,1024]{1,0:T(8,128)(2,1)S(1)}, u32[]{:S(2)}, u32[]{:S(2)}) collective-permute-start(bf16[48,1024]{1,0:T(8,128)(2,1)S(1)} %get-tuple-element.47), channel_id=1, source_target_pairs={{0,24},{8,0},{16,8},{24,16},{1,25},{9,1},{17,9},{25,17},{2,26},{10... | collective-permute-start | bytes 294920 | tf_op jit(solution)/shard_map/ppermute | solution.py:51
  11.6 2.8 %collective-permute-done.7.r2 = bf16[48,1024]{1,0:T(8,128)(2,1)S(1)} collective-permute-done((bf16[48,1024]{1,0:T(8,128)(2,1)S(1)}, bf16[48,1024]{1,0:T(8,128)(2,1)S(1)}, u32[]{:S(2)}, u32[]{:S(2)}) %collective-permute-start.7) | collective-permute-done | bytes 98336 | tf_op jit(solution)/shard_map/ppermute | solution.py:51
  14.4 0.9 shard_map.92
  15.3 6.3 %all-to-all-start = ((bf16[8,128,256]{2,1,0:T(8,128)(2,1)}), bf16[8,128,256]{2,1,0:T(8,128)(2,1)S(1)}, u32[]{:S(2)}, u32[]{:S(2)}) async-start(bf16[8,128,256]{2,1,0:T(8,128)(2,1)} %get-tuple-element.49), calls=%async_computation | async-start | bytes 1048576 | tf_op jit(solution)/shard_map/all_to_all | solution.py:407
  21.6 1.6 %collective-permute-start = (bf16[32,1024]{1,0:T(8,128)(2,1)S(1)}, bf16[32,1024]{1,0:T(8,128)(2,1)S(1)}, u32[]{:S(2)}, u32[]{:S(2)}) collective-permute-start(bf16[32,1024]{1,0:T(8,128)(2,1)S(1)} %get-tuple-element.41), channel_id=1, source_target_pairs={{0,1},{1,2},{2,3},{3,0},{4,5},{5,6},{6,7},{7,4},{8,9},{9,10},{10,1... | collective-permute-start | bytes 196616 | tf_op jit(solution)/shard_map/ppermute | solution.py:51
  23.1 2.9 %collective-permute-start.1 = (bf16[32,1024]{1,0:T(8,128)(2,1)S(1)}, bf16[32,1024]{1,0:T(8,128)(2,1)S(1)}, u32[]{:S(2)}, u32[]{:S(2)}) collective-permute-start(bf16[32,1024]{1,0:T(8,128)(2,1)S(1)} %get-tuple-element.41), channel_id=1, source_target_pairs={{0,2},{1,3},{2,0},{3,1},{4,6},{5,7},{6,4},{7,5},{8,10},{9,11},{10,... | collective-permute-start | bytes 196616 | tf_op jit(solution)/shard_map/ppermute | solution.py:51
  26.0 1.3 %collective-permute-start.2 = (bf16[32,1024]{1,0:T(8,128)(2,1)S(1)}, bf16[32,1024]{1,0:T(8,128)(2,1)S(1)}, u32[]{:S(2)}, u32[]{:S(2)}) collective-permute-start(bf16[32,1024]{1,0:T(8,128)(2,1)S(1)} %get-tuple-element.41), channel_id=1, source_target_pairs={{0,3},{1,0},{2,1},{3,2},{4,7},{5,4},{6,5},{7,6},{8,11},{9,8},{10,9... | collective-permute-start | bytes 196616 | tf_op jit(solution)/shard_map/ppermute | solution.py:51
  27.4 1.6 %collective-permute-done.1 = bf16[32,1024]{1,0:T(8,128)(2,1)S(1)} collective-permute-done((bf16[32,1024]{1,0:T(8,128)(2,1)S(1)}, bf16[32,1024]{1,0:T(8,128)(2,1)S(1)}, u32[]{:S(2)}, u32[]{:S(2)}) %collective-permute-start.1) | collective-permute-done | bytes 65568 | tf_op jit(solution)/shard_map/ppermute | solution.py:51
  29.0 1.3 %collective-permute-done.2 = bf16[32,1024]{1,0:T(8,128)(2,1)S(1)} collective-permute-done((bf16[32,1024]{1,0:T(8,128)(2,1)S(1)}, bf16[32,1024]{1,0:T(8,128)(2,1)S(1)}, u32[]{:S(2)}, u32[]{:S(2)}) %collective-permute-start.2) | collective-permute-done | bytes 65568 | tf_op jit(solution)/shard_map/ppermute | solution.py:51
  30.3 1.3 %collective-permute-start.3 = (bf16[128,1024]{1,0:T(8,128)(2,1)S(1)}, bf16[128,1024]{1,0:T(8,128)(2,1)S(1)}, u32[]{:S(2)}, u32[]{:S(2)}) collective-permute-start(bf16[128,1024]{1,0:T(8,128)(2,1)S(1)} %constant_dynamic-update-slice_fusion.5.refs_0_), channel_id=1, source_target_pairs={{0,8},{8,16},{16,24},{24,0},{1,9},{9,17},{17,25},{25,1},{2,10},{10... | collective-permute-start | bytes 786440 | tf_op jit(solution)/shard_map/ppermute | solution.py:51
  31.6 2.8 %collective-permute-start.4 = (bf16[128,1024]{1,0:T(8,128)(2,1)S(1)}, bf16[128,1024]{1,0:T(8,128)(2,1)S(1)}, u32[]{:S(2)}, u32[]{:S(2)}) collective-permute-start(bf16[128,1024]{1,0:T(8,128)(2,1)S(1)} %constant_dynamic-update-slice_fusion.5.refs_0_), channel_id=1, source_target_pairs={{0,16},{8,24},{16,0},{24,8},{1,17},{9,25},{17,1},{25,9},{2,18},{10... | collective-permute-start | bytes 786440 | tf_op jit(solution)/shard_map/ppermute | solution.py:51
  34.4 2.4 %collective-permute-start.5 = (bf16[128,1024]{1,0:T(8,128)(2,1)S(1)}, bf16[128,1024]{1,0:T(8,128)(2,1)S(1)}, u32[]{:S(2)}, u32[]{:S(2)}) collective-permute-start(bf16[128,1024]{1,0:T(8,128)(2,1)S(1)} %constant_dynamic-update-slice_fusion.5.refs_0_), channel_id=1, source_target_pairs={{0,24},{8,0},{16,8},{24,16},{1,25},{9,1},{17,9},{25,17},{2,26},{10... | collective-permute-start | bytes 786440 | tf_op jit(solution)/shard_map/ppermute | solution.py:51
  36.8 3.2 %collective-permute-start.10 = (bf16[128,1024]{1,0:T(8,128)(2,1)S(1)}, bf16[128,1024]{1,0:T(8,128)(2,1)S(1)}, u32[]{:S(2)}, u32[]{:S(2)}) collective-permute-start(bf16[128,1024]{1,0:T(8,128)(2,1)S(1)} %get-tuple-element.48.refs_4_), channel_id=1, source_target_pairs={{0,2},{1,3},{2,0},{3,1},{4,6},{5,7},{6,4},{7,5},{8,10},{9,11},{10,... | collective-permute-start | bytes 786440 | tf_op jit(solution)/shard_map/ppermute | solution.py:51
  40.2 2.6 %collective-permute-start.11 = (bf16[128,1024]{1,0:T(8,128)(2,1)S(1)}, bf16[128,1024]{1,0:T(8,128)(2,1)S(1)}, u32[]{:S(2)}, u32[]{:S(2)}) collective-permute-start(bf16[128,1024]{1,0:T(8,128)(2,1)S(1)} %get-tuple-element.48.refs_4_), channel_id=1, source_target_pairs={{0,3},{1,0},{2,1},{3,2},{4,7},{5,4},{6,5},{7,6},{8,11},{9,8},{10,9... | collective-permute-start | bytes 786440 | tf_op jit(solution)/shard_map/ppermute | solution.py:51
  43.6 0.8 collective-permute-done.5.refs_3_
  44.4 3.1 %collective-permute-done.10.refs_6_ = bf16[128,1024]{1,0:T(8,128)(2,1)S(1)} collective-permute-done((bf16[128,1024]{1,0:T(8,128)(2,1)S(1)}, bf16[128,1024]{1,0:T(8,128)(2,1)S(1)}, u32[]{:S(2)}, u32[]{:S(2)}) %collective-permute-start.10) | collective-permute-done | bytes 262176 | tf_op jit(solution)/shard_map/ppermute | solution.py:51
  47.5 5.3 %collective-permute-done.11.refs_7_ = bf16[128,1024]{1,0:T(8,128)(2,1)S(1)} collective-permute-done((bf16[128,1024]{1,0:T(8,128)(2,1)S(1)}, bf16[128,1024]{1,0:T(8,128)(2,1)S(1)}, u32[]{:S(2)}, u32[]{:S(2)}) %collective-permute-start.11) | collective-permute-done | bytes 262176 | tf_op jit(solution)/shard_map/ppermute | solution.py:51
  52.7 2.2 %shard_map.93 = (bf16[80,1024]{1,0:T(8,128)(2,1)S(1)}, bf16[128,1024]{1,0:T(8,128)(2,1)S(1)}, f32[8,1024]{1,0:T(8,128)S(1)}) custom-call(s32[4]{0:T(128)S(1)} %pad_add_fusion.idx, f32[4]{0:T(128)S(1)} %copy-done.3, bf16[128,1024]{1,0:T(8,128)(2,1)S(1)} %constant_dynamic-update-slice_fusion.5.refs_0_, bf16[128,1024]{1,0:T(8,128)(2,1)S(1)} %collective-permute-done.3.refs_1_, ...), custom_call_target="tpu_custom_call" | custom-call | flops 2000000000 | bytes 1048576 | tf_op jit(solution)/shard_map/pallas_call | solution.py:411
  55.0 1.4 %collective-permute-done.13.q_sib = bf16[80,1024]{1,0:T(8,128)(2,1)S(1)} collective-permute-done((bf16[80,1024]{1,0:T(8,128)(2,1)S(1)}, bf16[80,1024]{1,0:T(8,128)(2,1)S(1)}, u32[]{:S(2)}, u32[]{:S(2)}) %collective-permute-start.13) | collective-permute-done | bytes 163872 | tf_op jit(solution)/shard_map/ppermute | solution.py:51
  57.0 1.9 %collective-permute-start.14 = (bf16[144,1024]{1,0:T(8,128)(2,1)S(1)}, bf16[144,1024]{1,0:T(8,128)(2,1)S(1)}, u32[]{:S(2)}, u32[]{:S(2)}) collective-permute-start(bf16[144,1024]{1,0:T(8,128)(2,1)S(1)} %get-tuple-element.54.pay), channel_id=1, source_target_pairs={{0,32},{32,64},{64,96},{96,128},{128,160},{160,192},{192,224},{1,3... | collective-permute-start | bytes 884744 | tf_op jit(solution)/shard_map/ppermute | solution.py:59
  59.7 1.6 %collective-permute-start.28 = (bf16[2,8,64,256]{3,2,1,0:T(8,128)(2,1)S(1)}, bf16[2,8,64,256]{3,2,1,0:T(8,128)(2,1)S(1)}, u32[]{:S(2)}, u32[]{:S(2)}) collective-permute-start(bf16[2,8,64,256]{3,2,1,0:T(8,128)(2,1)S(1)} %pad_maximum_fusion.w0), channel_id=1, source_target_pairs={{0,1},{1,2},{2,3},{3,0},{4,5},{5,6},{6,7},{7,4},{8,9},{9,10},{10,1... | collective-permute-start | bytes 1572872 | tf_op jit(solution)/shard_map/ppermute | solution.py:51
  61.3 2.7 %collective-permute-start.29 = (bf16[2,8,64,256]{3,2,1,0:T(8,128)(2,1)S(1)}, bf16[2,8,64,256]{3,2,1,0:T(8,128)(2,1)S(1)}, u32[]{:S(2)}, u32[]{:S(2)}) collective-permute-start(bf16[2,8,64,256]{3,2,1,0:T(8,128)(2,1)S(1)} %pad_maximum_fusion.w0), channel_id=1, source_target_pairs={{0,2},{1,3},{2,0},{3,1},{4,6},{5,7},{6,4},{7,5},{8,10},{9,11},{10,... | collective-permute-start | bytes 1572872 | tf_op jit(solution)/shard_map/ppermute | solution.py:51
  64.1 1.3 %collective-permute-start.30 = (bf16[2,8,64,256]{3,2,1,0:T(8,128)(2,1)S(1)}, bf16[2,8,64,256]{3,2,1,0:T(8,128)(2,1)S(1)}, u32[]{:S(2)}, u32[]{:S(2)}) collective-permute-start(bf16[2,8,64,256]{3,2,1,0:T(8,128)(2,1)S(1)} %pad_maximum_fusion.w0), channel_id=1, source_target_pairs={{0,3},{1,0},{2,1},{3,2},{4,7},{5,4},{6,5},{7,6},{8,11},{9,8},{10,9... | collective-permute-start | bytes 1572872 | tf_op jit(solution)/shard_map/ppermute | solution.py:51
  65.4 2.6 %shard_map.95 = (f32[2,80,2048]{2,1,0:T(8,128)S(1)}, f32[2,8,2048]{2,1,0:T(8,128)S(1)}, f32[8,256]{1,0:T(8,128)S(1)}) custom-call(s32[4]{0:T(128)S(1)} %pad_add_fusion.idx, bf16[128,2048]{1,0:T(8,128)(2,1)S(1)} %get-tuple-element.53.q, bf16[144,1024]{1,0:T(8,128)(2,1)S(1)} %get-tuple-element.54.pay), custom_call_target="tpu_custom_call" | custom-call | flops 3000000000 | bytes 1048576 | tf_op jit(solution)/shard_map/pallas_call | solution.py:443
  68.1 2.1 %collective-permute-start.15 = (bf16[144,1024]{1,0:T(8,128)(2,1)S(1)}, bf16[144,1024]{1,0:T(8,128)(2,1)S(1)}, u32[]{:S(2)}, u32[]{:S(2)}) collective-permute-start(bf16[144,1024]{1,0:T(8,128)(2,1)S(1)} %collective-permute-done.14.refs_0_), channel_id=1, source_target_pairs={{32,64},{64,96},{96,128},{128,160},{160,192},{192,224},{33,65},{65... | collective-permute-start | bytes 884744 | tf_op jit(solution)/shard_map/ppermute | solution.py:59
  70.2 1.3 collective-permute-start.19
  71.5 3.9 %shard_map.96 = (f32[2,80,2048]{2,1,0:T(8,128)S(1)}, f32[2,8,2048]{2,1,0:T(8,128)S(1)}, f32[8,256]{1,0:T(8,128)S(1)}) custom-call(s32[4]{0:T(128)S(1)} %pad_add_fusion.idx, bf16[128,2048]{1,0:T(8,128)(2,1)S(1)} %get-tuple-element.53.q, bf16[144,1024]{1,0:T(8,128)(2,1)S(1)} %collective-permute-done.14.refs_0_, ...), custom_call_target="tpu_custom_call", output_to_operand_aliasing={{0}: (4, {}), {1}: (5, {})} | custom-call | flops 6000000000 | bytes 1048576 | tf_op jit(solution)/shard_map/pallas_call | solution.py:459
  75.4 2.8 %collective-permute-done.15.refs_0_ = bf16[144,1024]{1,0:T(8,128)(2,1)S(1)} collective-permute-done((bf16[144,1024]{1,0:T(8,128)(2,1)S(1)}, bf16[144,1024]{1,0:T(8,128)(2,1)S(1)}, u32[]{:S(2)}, u32[]{:S(2)}) %collective-permute-start.15) | collective-permute-done | bytes 294944 | tf_op jit(solution)/shard_map/ppermute | solution.py:59
  78.2 5.3 %collective-permute-start.16 = (bf16[144,1024]{1,0:T(8,128)(2,1)S(1)}, bf16[144,1024]{1,0:T(8,128)(2,1)S(1)}, u32[]{:S(2)}, u32[]{:S(2)}) collective-permute-start(bf16[144,1024]{1,0:T(8,128)(2,1)S(1)} %collective-permute-done.15.refs_0_), channel_id=1, source_target_pairs={{64,96},{96,128},{128,160},{160,192},{192,224},{65,97},{97,129},{1... | collective-permute-start | bytes 884744 | tf_op jit(solution)/shard_map/ppermute | solution.py:59
  83.5 1.9 %collective-permute-start.20 = (bf16[144,1024]{1,0:T(8,128)(2,1)S(1)}, bf16[144,1024]{1,0:T(8,128)(2,1)S(1)}, u32[]{:S(2)}, u32[]{:S(2)}) collective-permute-start(bf16[144,1024]{1,0:T(8,128)(2,1)S(1)} %collective-permute-done.19.refs_1_), channel_id=1, source_target_pairs={{192,160},{224,192},{0,224},{193,161},{225,193},{1,225},{194,162},... | collective-permute-start | bytes 884744 | tf_op jit(solution)/shard_map/ppermute | solution.py:63
  85.4 6.7 %shard_map.97 = (f32[2,80,2048]{2,1,0:T(8,128)S(1)}, f32[2,8,2048]{2,1,0:T(8,128)S(1)}, f32[8,256]{1,0:T(8,128)S(1)}) custom-call(s32[4]{0:T(128)S(1)} %pad_add_fusion.idx, bf16[128,2048]{1,0:T(8,128)(2,1)S(1)} %get-tuple-element.53.q, bf16[144,1024]{1,0:T(8,128)(2,1)S(1)} %collective-permute-done.15.refs_0_, ...), custom_call_target="tpu_custom_call", output_to_operand_aliasing={{0}: (4, {}), {1}: (5, {})} | custom-call | flops 6000000000 | bytes 1048576 | tf_op jit(solution)/shard_map/pallas_call | solution.py:459
  92.1 3.9 %collective-permute-start.17 = (bf16[144,1024]{1,0:T(8,128)(2,1)S(1)}, bf16[144,1024]{1,0:T(8,128)(2,1)S(1)}, u32[]{:S(2)}, u32[]{:S(2)}) collective-permute-start(bf16[144,1024]{1,0:T(8,128)(2,1)S(1)} %collective-permute-done.16.refs_0_), channel_id=1, source_target_pairs={{96,128},{128,160},{160,192},{192,224},{97,129},{129,161},{161,193... | collective-permute-start | bytes 884744 | tf_op jit(solution)/shard_map/ppermute | solution.py:59
  96.1 6.7 %shard_map.98 = (f32[2,80,2048]{2,1,0:T(8,128)S(1)}, f32[2,8,2048]{2,1,0:T(8,128)S(1)}, f32[8,256]{1,0:T(8,128)S(1)}) custom-call(s32[4]{0:T(128)S(1)} %pad_add_fusion.idx, bf16[128,2048]{1,0:T(8,128)(2,1)S(1)} %get-tuple-element.53.q, bf16[144,1024]{1,0:T(8,128)(2,1)S(1)} %collective-permute-done.16.refs_0_, ...), custom_call_target="tpu_custom_call", output_to_operand_aliasing={{0}: (4, {}), {1}: (5, {})} | custom-call | flops 6000000000 | bytes 1048576 | tf_op jit(solution)/shard_map/pallas_call | solution.py:459
  102.8 4.0 %shard_map.99 = (f32[72,1024]{1,0:T(8,128)S(1)}, f32[72,1024]{1,0:T(8,128)S(1)}) custom-call(s32[4]{0:T(128)S(1)} %pad_add_fusion.idx, bf16[128,2048]{1,0:T(8,128)(2,1)S(1)} %get-tuple-element.53.q, bf16[144,1024]{1,0:T(8,128)(2,1)S(1)} %collective-permute-done.17.refs_0_, f32[2,80,2048]{2,1,0:T(8,128)S(1)} %get-tuple-element.64.refs_1_, ...), custom_call_target="tpu_custom_call" | custom-call | flops 6000000000 | bytes 1048576 | tf_op jit(solution)/shard_map/pallas_call | solution.py:459
  106.9 1.6 %collective-permute-done.21.sib = f32[72,1024]{1,0:T(8,128)S(1)} collective-permute-done((f32[72,1024]{1,0:T(8,128)S(1)}, f32[72,1024]{1,0:T(8,128)S(1)}, u32[]{:S(2)}, u32[]{:S(2)}) %collective-permute-start.21) | collective-permute-done | bytes 294944 | tf_op jit(solution)/shard_map/ppermute | solution.py:51
  109.3 2.0 %collective-permute-start.23 = (bf16[256,64]{1,0:T(8,128)(2,1)S(1)}, bf16[256,64]{1,0:T(8,128)(2,1)S(1)}, u32[]{:S(2)}, u32[]{:S(2)}) collective-permute-start(bf16[256,64]{1,0:T(8,128)(2,1)S(1)} %get-tuple-element.71), channel_id=1, source_target_pairs={{0,16},{8,24},{16,0},{24,8},{1,17},{9,25},{17,1},{25,9},{2,18},{10... | collective-permute-start | bytes 98312 | tf_op jit(solution)/shard_map/ppermute | solution.py:51
  111.4 4.7 %collective-permute-done.22.h1 = bf16[256,64]{1,0:T(8,128)(2,1)S(1)} collective-permute-done((bf16[256,64]{1,0:T(8,128)(2,1)S(1)}, bf16[256,64]{1,0:T(8,128)(2,1)S(1)}, u32[]{:S(2)}, u32[]{:S(2)}) %collective-permute-start.22) | collective-permute-done | bytes 32800 | tf_op jit(solution)/shard_map/ppermute | solution.py:51
  116.1 4.3 %collective-permute-done.24.h3 = bf16[256,64]{1,0:T(8,128)(2,1)S(1)} collective-permute-done((bf16[256,64]{1,0:T(8,128)(2,1)S(1)}, bf16[256,64]{1,0:T(8,128)(2,1)S(1)}, u32[]{:S(2)}, u32[]{:S(2)}) %collective-permute-start.24) | collective-permute-done | bytes 32800 | tf_op jit(solution)/shard_map/ppermute | solution.py:51
  121.0 1.4 %collective-permute-start.25 = (bf16[64,256]{1,0:T(8,128)(2,1)S(1)}, bf16[64,256]{1,0:T(8,128)(2,1)S(1)}, u32[]{:S(2)}, u32[]{:S(2)}) collective-permute-start(bf16[64,256]{1,0:T(8,128)(2,1)S(1)} %get-tuple-element.74), channel_id=1, source_target_pairs={{0,1},{1,2},{2,3},{3,0},{4,5},{5,6},{6,7},{7,4},{8,9},{9,10},{10,1... | collective-permute-start | bytes 98312 | tf_op jit(solution)/shard_map/ppermute | solution.py:51
  122.5 2.8 %collective-permute-start.26 = (bf16[64,256]{1,0:T(8,128)(2,1)S(1)}, bf16[64,256]{1,0:T(8,128)(2,1)S(1)}, u32[]{:S(2)}, u32[]{:S(2)}) collective-permute-start(bf16[64,256]{1,0:T(8,128)(2,1)S(1)} %get-tuple-element.75), channel_id=1, source_target_pairs={{0,2},{1,3},{2,0},{3,1},{4,6},{5,7},{6,4},{7,5},{8,10},{9,11},{10,... | collective-permute-start | bytes 98312 | tf_op jit(solution)/shard_map/ppermute | solution.py:51
  125.2 1.3 %collective-permute-start.27 = (bf16[64,256]{1,0:T(8,128)(2,1)S(1)}, bf16[64,256]{1,0:T(8,128)(2,1)S(1)}, u32[]{:S(2)}, u32[]{:S(2)}) collective-permute-start(bf16[64,256]{1,0:T(8,128)(2,1)S(1)} %get-tuple-element.76), channel_id=1, source_target_pairs={{0,3},{1,0},{2,1},{3,2},{4,7},{5,4},{6,5},{7,6},{8,11},{9,8},{10,9... | collective-permute-start | bytes 98312 | tf_op jit(solution)/shard_map/ppermute | solution.py:51
  126.6 1.0 shard_map.102.w
  127.9 1.3 collective-permute-done.27.a3
  129.1 2.1 %shard_map.103 = bf16[64,1024]{1,0:T(8,128)(2,1)} custom-call(s32[4]{0:T(128)S(1)} %pad_add_fusion.idx, bf16[64,256]{1,0:T(8,128)(2,1)S(1)} %get-tuple-element.73.a0, bf16[64,256]{1,0:T(8,128)(2,1)S(1)} %collective-permute-done.25.a1, bf16[64,256]{1,0:T(8,128)(2,1)S(1)} %collective-permute-done.26.a2, bf16[64,256]{1,0:T(8,128)(2,1)S(1)} %collective-permute-done.27.a3, ...), custom_call_target="tpu_custom_call" | custom-call | flops 100000000 | bytes 1048576 | tf_op jit(solution)/shard_map/pallas_call | solution.py:483
  (50 shorter events, 8.5 us)
Async XLA Ops:
  3.6 0.9 copy-start.1
  5.5 47.3 %copy-start.2 = (f32[1024]{0:T(1024)S(1)}, f32[1024]{0:T(1024)}, u32[]{:S(2)}) copy-start(f32[1024]{0:T(1024)} %param.10) | copy-start | bytes 12292
  5.5 47.3 %copy-start.3 = (f32[4]{0:T(128)S(1)}, f32[4]{0:T(128)}, u32[]{:S(2)}) copy-start(f32[4]{0:T(128)} %offs.1) | copy-start | bytes 52
  5.5 6.1 %collective-permute-start.6 = (bf16[48,1024]{1,0:T(8,128)(2,1)S(1)}, bf16[48,1024]{1,0:T(8,128)(2,1)S(1)}, u32[]{:S(2)}, u32[]{:S(2)}) collective-permute-start(bf16[48,1024]{1,0:T(8,128)(2,1)S(1)} %get-tuple-element.45), channel_id=1, source_target_pairs={{0,8},{8,16},{16,24},{24,0},{1,9},{9,17},{17,25},{25,1},{2,10},{10... | collective-permute-start | bytes 294920 | tf_op jit(solution)/shard_map/ppermute | solution.py:51
  7.1 7.3 %collective-permute-start.7 = (bf16[48,1024]{1,0:T(8,128)(2,1)S(1)}, bf16[48,1024]{1,0:T(8,128)(2,1)S(1)}, u32[]{:S(2)}, u32[]{:S(2)}) collective-permute-start(bf16[48,1024]{1,0:T(8,128)(2,1)S(1)} %get-tuple-element.46), channel_id=1, source_target_pairs={{0,16},{8,24},{16,0},{24,8},{1,17},{9,25},{17,1},{25,9},{2,18},{10... | collective-permute-start | bytes 294920 | tf_op jit(solution)/shard_map/ppermute | solution.py:51
  9.8 4.6 %collective-permute-start.8 = (bf16[48,1024]{1,0:T(8,128)(2,1)S(1)}, bf16[48,1024]{1,0:T(8,128)(2,1)S(1)}, u32[]{:S(2)}, u32[]{:S(2)}) collective-permute-start(bf16[48,1024]{1,0:T(8,128)(2,1)S(1)} %get-tuple-element.47), channel_id=1, source_target_pairs={{0,24},{8,0},{16,8},{24,16},{1,25},{9,1},{17,9},{25,17},{2,26},{10... | collective-permute-start | bytes 294920 | tf_op jit(solution)/shard_map/ppermute | solution.py:51
  15.3 19.2 %all-to-all-start = ((bf16[8,128,256]{2,1,0:T(8,128)(2,1)}), bf16[8,128,256]{2,1,0:T(8,128)(2,1)S(1)}, u32[]{:S(2)}, u32[]{:S(2)}) async-start(bf16[8,128,256]{2,1,0:T(8,128)(2,1)} %get-tuple-element.49), calls=%async_computation | async-start | bytes 1048576 | tf_op jit(solution)/shard_map/all_to_all | solution.py:407
  21.6 5.8 %collective-permute-start = (bf16[32,1024]{1,0:T(8,128)(2,1)S(1)}, bf16[32,1024]{1,0:T(8,128)(2,1)S(1)}, u32[]{:S(2)}, u32[]{:S(2)}) collective-permute-start(bf16[32,1024]{1,0:T(8,128)(2,1)S(1)} %get-tuple-element.41), channel_id=1, source_target_pairs={{0,1},{1,2},{2,3},{3,0},{4,5},{5,6},{6,7},{7,4},{8,9},{9,10},{10,1... | collective-permute-start | bytes 196616 | tf_op jit(solution)/shard_map/ppermute | solution.py:51
  23.1 5.8 %collective-permute-start.1 = (bf16[32,1024]{1,0:T(8,128)(2,1)S(1)}, bf16[32,1024]{1,0:T(8,128)(2,1)S(1)}, u32[]{:S(2)}, u32[]{:S(2)}) collective-permute-start(bf16[32,1024]{1,0:T(8,128)(2,1)S(1)} %get-tuple-element.41), channel_id=1, source_target_pairs={{0,2},{1,3},{2,0},{3,1},{4,6},{5,7},{6,4},{7,5},{8,10},{9,11},{10,... | collective-permute-start | bytes 196616 | tf_op jit(solution)/shard_map/ppermute | solution.py:51
  26.0 4.3 %collective-permute-start.2 = (bf16[32,1024]{1,0:T(8,128)(2,1)S(1)}, bf16[32,1024]{1,0:T(8,128)(2,1)S(1)}, u32[]{:S(2)}, u32[]{:S(2)}) collective-permute-start(bf16[32,1024]{1,0:T(8,128)(2,1)S(1)} %get-tuple-element.41), channel_id=1, source_target_pairs={{0,3},{1,0},{2,1},{3,2},{4,7},{5,4},{6,5},{7,6},{8,11},{9,8},{10,9... | collective-permute-start | bytes 196616 | tf_op jit(solution)/shard_map/ppermute | solution.py:51
  30.3 9.9 %collective-permute-start.3 = (bf16[128,1024]{1,0:T(8,128)(2,1)S(1)}, bf16[128,1024]{1,0:T(8,128)(2,1)S(1)}, u32[]{:S(2)}, u32[]{:S(2)}) collective-permute-start(bf16[128,1024]{1,0:T(8,128)(2,1)S(1)} %constant_dynamic-update-slice_fusion.5.refs_0_), channel_id=1, source_target_pairs={{0,8},{8,16},{16,24},{24,0},{1,9},{9,17},{17,25},{25,1},{2,10},{10... | collective-permute-start | bytes 786440 | tf_op jit(solution)/shard_map/ppermute | solution.py:51
  31.6 11.3 %collective-permute-start.4 = (bf16[128,1024]{1,0:T(8,128)(2,1)S(1)}, bf16[128,1024]{1,0:T(8,128)(2,1)S(1)}, u32[]{:S(2)}, u32[]{:S(2)}) collective-permute-start(bf16[128,1024]{1,0:T(8,128)(2,1)S(1)} %constant_dynamic-update-slice_fusion.5.refs_0_), channel_id=1, source_target_pairs={{0,16},{8,24},{16,0},{24,8},{1,17},{9,25},{17,1},{25,9},{2,18},{10... | collective-permute-start | bytes 786440 | tf_op jit(solution)/shard_map/ppermute | solution.py:51
  34.4 18.3 %collective-permute-start.12 = (bf16[8,128,256]{2,1,0:T(8,128)(2,1)S(1)}, bf16[8,128,256]{2,1,0:T(8,128)(2,1)S(1)}, u32[]{:S(2)}, u32[]{:S(2)}) collective-permute-start(bf16[8,128,256]{2,1,0:T(8,128)(2,1)S(1)} %all-to-all-done.refs_9_), channel_id=1, source_target_pairs={{0,4},{4,0},{1,5},{5,1},{2,6},{6,2},{3,7},{7,3},{8,12},{12,8},{9,1... | collective-permute-start | bytes 1572872 | tf_op jit(solution)/shard_map/ppermute | solution.py:51
  34.4 9.9 %collective-permute-start.5 = (bf16[128,1024]{1,0:T(8,128)(2,1)S(1)}, bf16[128,1024]{1,0:T(8,128)(2,1)S(1)}, u32[]{:S(2)}, u32[]{:S(2)}) collective-permute-start(bf16[128,1024]{1,0:T(8,128)(2,1)S(1)} %constant_dynamic-update-slice_fusion.5.refs_0_), channel_id=1, source_target_pairs={{0,24},{8,0},{16,8},{24,16},{1,25},{9,1},{17,9},{25,17},{2,26},{10... | collective-permute-start | bytes 786440 | tf_op jit(solution)/shard_map/ppermute | solution.py:51
  36.8 10.7 %collective-permute-start.10 = (bf16[128,1024]{1,0:T(8,128)(2,1)S(1)}, bf16[128,1024]{1,0:T(8,128)(2,1)S(1)}, u32[]{:S(2)}, u32[]{:S(2)}) collective-permute-start(bf16[128,1024]{1,0:T(8,128)(2,1)S(1)} %get-tuple-element.48.refs_4_), channel_id=1, source_target_pairs={{0,2},{1,3},{2,0},{3,1},{4,6},{5,7},{6,4},{7,5},{8,10},{9,11},{10,... | collective-permute-start | bytes 786440 | tf_op jit(solution)/shard_map/ppermute | solution.py:51
  40.2 12.5 %collective-permute-start.11 = (bf16[128,1024]{1,0:T(8,128)(2,1)S(1)}, bf16[128,1024]{1,0:T(8,128)(2,1)S(1)}, u32[]{:S(2)}, u32[]{:S(2)}) collective-permute-start(bf16[128,1024]{1,0:T(8,128)(2,1)S(1)} %get-tuple-element.48.refs_4_), channel_id=1, source_target_pairs={{0,3},{1,0},{2,1},{3,2},{4,7},{5,4},{6,5},{7,6},{8,11},{9,8},{10,9... | collective-permute-start | bytes 786440 | tf_op jit(solution)/shard_map/ppermute | solution.py:51
  43.0 9.7 %collective-permute-start.9 = (bf16[128,1024]{1,0:T(8,128)(2,1)S(1)}, bf16[128,1024]{1,0:T(8,128)(2,1)S(1)}, u32[]{:S(2)}, u32[]{:S(2)}) collective-permute-start(bf16[128,1024]{1,0:T(8,128)(2,1)S(1)} %get-tuple-element.48.refs_4_), channel_id=1, source_target_pairs={{0,1},{1,2},{2,3},{3,0},{4,5},{5,6},{6,7},{7,4},{8,9},{9,10},{10,1... | collective-permute-start | bytes 786440 | tf_op jit(solution)/shard_map/ppermute | solution.py:51
  54.9 1.5 %collective-permute-start.13 = (bf16[80,1024]{1,0:T(8,128)(2,1)S(1)}, bf16[80,1024]{1,0:T(8,128)(2,1)S(1)}, u32[]{:S(2)}, u32[]{:S(2)}) collective-permute-start(bf16[80,1024]{1,0:T(8,128)(2,1)S(1)} %get-tuple-element.50.q_own), channel_id=1, source_target_pairs={{0,4},{4,0},{1,5},{5,1},{2,6},{6,2},{3,7},{7,3},{8,12},{12,8},{9,1... | collective-permute-start | bytes 491528 | tf_op jit(solution)/shard_map/ppermute | solution.py:51
  57.0 11.0 %collective-permute-start.14 = (bf16[144,1024]{1,0:T(8,128)(2,1)S(1)}, bf16[144,1024]{1,0:T(8,128)(2,1)S(1)}, u32[]{:S(2)}, u32[]{:S(2)}) collective-permute-start(bf16[144,1024]{1,0:T(8,128)(2,1)S(1)} %get-tuple-element.54.pay), channel_id=1, source_target_pairs={{0,32},{32,64},{64,96},{96,128},{128,160},{160,192},{192,224},{1,3... | collective-permute-start | bytes 884744 | tf_op jit(solution)/shard_map/ppermute | solution.py:59
  59.0 11.2 %collective-permute-start.18 = (bf16[144,1024]{1,0:T(8,128)(2,1)S(1)}, bf16[144,1024]{1,0:T(8,128)(2,1)S(1)}, u32[]{:S(2)}, u32[]{:S(2)}) collective-permute-start(bf16[144,1024]{1,0:T(8,128)(2,1)S(1)} %get-tuple-element.54.pay), channel_id=1, source_target_pairs={{0,224},{32,0},{64,32},{1,225},{33,1},{65,33},{2,226},{34,2},{66,3... | collective-permute-start | bytes 884744 | tf_op jit(solution)/shard_map/ppermute | solution.py:63
  59.7 65.5 %collective-permute-start.28 = (bf16[2,8,64,256]{3,2,1,0:T(8,128)(2,1)S(1)}, bf16[2,8,64,256]{3,2,1,0:T(8,128)(2,1)S(1)}, u32[]{:S(2)}, u32[]{:S(2)}) collective-permute-start(bf16[2,8,64,256]{3,2,1,0:T(8,128)(2,1)S(1)} %pad_maximum_fusion.w0), channel_id=1, source_target_pairs={{0,1},{1,2},{2,3},{3,0},{4,5},{5,6},{6,7},{7,4},{8,9},{9,10},{10,1... | collective-permute-start | bytes 1572872 | tf_op jit(solution)/shard_map/ppermute | solution.py:51
  61.3 65.3 %collective-permute-start.29 = (bf16[2,8,64,256]{3,2,1,0:T(8,128)(2,1)S(1)}, bf16[2,8,64,256]{3,2,1,0:T(8,128)(2,1)S(1)}, u32[]{:S(2)}, u32[]{:S(2)}) collective-permute-start(bf16[2,8,64,256]{3,2,1,0:T(8,128)(2,1)S(1)} %pad_maximum_fusion.w0), channel_id=1, source_target_pairs={{0,2},{1,3},{2,0},{3,1},{4,6},{5,7},{6,4},{7,5},{8,10},{9,11},{10,... | collective-permute-start | bytes 1572872 | tf_op jit(solution)/shard_map/ppermute | solution.py:51
  64.1 62.5 %collective-permute-start.30 = (bf16[2,8,64,256]{3,2,1,0:T(8,128)(2,1)S(1)}, bf16[2,8,64,256]{3,2,1,0:T(8,128)(2,1)S(1)}, u32[]{:S(2)}, u32[]{:S(2)}) collective-permute-start(bf16[2,8,64,256]{3,2,1,0:T(8,128)(2,1)S(1)} %pad_maximum_fusion.w0), channel_id=1, source_target_pairs={{0,3},{1,0},{2,1},{3,2},{4,7},{5,4},{6,5},{7,6},{8,11},{9,8},{10,9... | collective-permute-start | bytes 1572872 | tf_op jit(solution)/shard_map/ppermute | solution.py:51
  68.1 10.1 %collective-permute-start.15 = (bf16[144,1024]{1,0:T(8,128)(2,1)S(1)}, bf16[144,1024]{1,0:T(8,128)(2,1)S(1)}, u32[]{:S(2)}, u32[]{:S(2)}) collective-permute-start(bf16[144,1024]{1,0:T(8,128)(2,1)S(1)} %collective-permute-done.14.refs_0_), channel_id=1, source_target_pairs={{32,64},{64,96},{96,128},{128,160},{160,192},{192,224},{33,65},{65... | collective-permute-start | bytes 884744 | tf_op jit(solution)/shard_map/ppermute | solution.py:59
  70.2 13.3 %collective-permute-start.19 = (bf16[144,1024]{1,0:T(8,128)(2,1)S(1)}, bf16[144,1024]{1,0:T(8,128)(2,1)S(1)}, u32[]{:S(2)}, u32[]{:S(2)}) collective-permute-start(bf16[144,1024]{1,0:T(8,128)(2,1)S(1)} %collective-permute-done.18.refs_1_), channel_id=1, source_target_pairs={{224,192},{0,224},{32,0},{225,193},{1,225},{33,1},{226,194},{2,226... | collective-permute-start | bytes 884744 | tf_op jit(solution)/shard_map/ppermute | solution.py:63
  78.2 13.9 %collective-permute-start.16 = (bf16[144,1024]{1,0:T(8,128)(2,1)S(1)}, bf16[144,1024]{1,0:T(8,128)(2,1)S(1)}, u32[]{:S(2)}, u32[]{:S(2)}) collective-permute-start(bf16[144,1024]{1,0:T(8,128)(2,1)S(1)} %collective-permute-done.15.refs_0_), channel_id=1, source_target_pairs={{64,96},{96,128},{128,160},{160,192},{192,224},{65,97},{97,129},{1... | collective-permute-start | bytes 884744 | tf_op jit(solution)/shard_map/ppermute | solution.py:59
  83.5 12.6 %collective-permute-start.20 = (bf16[144,1024]{1,0:T(8,128)(2,1)S(1)}, bf16[144,1024]{1,0:T(8,128)(2,1)S(1)}, u32[]{:S(2)}, u32[]{:S(2)}) collective-permute-start(bf16[144,1024]{1,0:T(8,128)(2,1)S(1)} %collective-permute-done.19.refs_1_), channel_id=1, source_target_pairs={{192,160},{224,192},{0,224},{193,161},{225,193},{1,225},{194,162},... | collective-permute-start | bytes 884744 | tf_op jit(solution)/shard_map/ppermute | solution.py:63
  92.1 10.7 %collective-permute-start.17 = (bf16[144,1024]{1,0:T(8,128)(2,1)S(1)}, bf16[144,1024]{1,0:T(8,128)(2,1)S(1)}, u32[]{:S(2)}, u32[]{:S(2)}) collective-permute-start(bf16[144,1024]{1,0:T(8,128)(2,1)S(1)} %collective-permute-done.16.refs_0_), channel_id=1, source_target_pairs={{96,128},{128,160},{160,192},{192,224},{97,129},{129,161},{161,193... | collective-permute-start | bytes 884744 | tf_op jit(solution)/shard_map/ppermute | solution.py:59
  106.8 1.7 %collective-permute-start.21 = (f32[72,1024]{1,0:T(8,128)S(1)}, f32[72,1024]{1,0:T(8,128)S(1)}, u32[]{:S(2)}, u32[]{:S(2)}) collective-permute-start(f32[72,1024]{1,0:T(8,128)S(1)} %get-tuple-element.68), channel_id=1, source_target_pairs={{0,4},{4,0},{1,5},{5,1},{2,6},{6,2},{3,7},{7,3},{8,12},{12,8},{9,1... | collective-permute-start | bytes 884744 | tf_op jit(solution)/shard_map/ppermute | solution.py:51
  109.3 6.8 %collective-permute-start.22 = (bf16[256,64]{1,0:T(8,128)(2,1)S(1)}, bf16[256,64]{1,0:T(8,128)(2,1)S(1)}, u32[]{:S(2)}, u32[]{:S(2)}) collective-permute-start(bf16[256,64]{1,0:T(8,128)(2,1)S(1)} %get-tuple-element.70), channel_id=1, source_target_pairs={{0,8},{8,16},{16,24},{24,0},{1,9},{9,17},{17,25},{25,1},{2,10},{10... | collective-permute-start | bytes 98312 | tf_op jit(solution)/shard_map/ppermute | solution.py:51
  109.3 6.7 %collective-permute-start.23 = (bf16[256,64]{1,0:T(8,128)(2,1)S(1)}, bf16[256,64]{1,0:T(8,128)(2,1)S(1)}, u32[]{:S(2)}, u32[]{:S(2)}) collective-permute-start(bf16[256,64]{1,0:T(8,128)(2,1)S(1)} %get-tuple-element.71), channel_id=1, source_target_pairs={{0,16},{8,24},{16,0},{24,8},{1,17},{9,25},{17,1},{25,9},{2,18},{10... | collective-permute-start | bytes 98312 | tf_op jit(solution)/shard_map/ppermute | solution.py:51
  116.1 4.3 %collective-permute-start.24 = (bf16[256,64]{1,0:T(8,128)(2,1)S(1)}, bf16[256,64]{1,0:T(8,128)(2,1)S(1)}, u32[]{:S(2)}, u32[]{:S(2)}) collective-permute-start(bf16[256,64]{1,0:T(8,128)(2,1)S(1)} %get-tuple-element.72), channel_id=1, source_target_pairs={{0,24},{8,0},{16,8},{24,16},{1,25},{9,1},{17,9},{25,17},{2,26},{10... | collective-permute-start | bytes 98312 | tf_op jit(solution)/shard_map/ppermute | solution.py:51
  121.0 6.6 %collective-permute-start.25 = (bf16[64,256]{1,0:T(8,128)(2,1)S(1)}, bf16[64,256]{1,0:T(8,128)(2,1)S(1)}, u32[]{:S(2)}, u32[]{:S(2)}) collective-permute-start(bf16[64,256]{1,0:T(8,128)(2,1)S(1)} %get-tuple-element.74), channel_id=1, source_target_pairs={{0,1},{1,2},{2,3},{3,0},{4,5},{5,6},{6,7},{7,4},{8,9},{9,10},{10,1... | collective-permute-start | bytes 98312 | tf_op jit(solution)/shard_map/ppermute | solution.py:51
  122.5 5.4 %collective-permute-start.26 = (bf16[64,256]{1,0:T(8,128)(2,1)S(1)}, bf16[64,256]{1,0:T(8,128)(2,1)S(1)}, u32[]{:S(2)}, u32[]{:S(2)}) collective-permute-start(bf16[64,256]{1,0:T(8,128)(2,1)S(1)} %get-tuple-element.75), channel_id=1, source_target_pairs={{0,2},{1,3},{2,0},{3,1},{4,6},{5,7},{6,4},{7,5},{8,10},{9,11},{10,... | collective-permute-start | bytes 98312 | tf_op jit(solution)/shard_map/ppermute | solution.py:51
  125.2 3.9 %copy-start = (f32[1024]{0:T(1024)S(1)}, f32[1024]{0:T(1024)}, u32[]{:S(2)}) copy-start(f32[1024]{0:T(1024)} %param.17) | copy-start | bytes 12292
  125.2 3.9 %collective-permute-start.27 = (bf16[64,256]{1,0:T(8,128)(2,1)S(1)}, bf16[64,256]{1,0:T(8,128)(2,1)S(1)}, u32[]{:S(2)}, u32[]{:S(2)}) collective-permute-start(bf16[64,256]{1,0:T(8,128)(2,1)S(1)} %get-tuple-element.76), channel_id=1, source_target_pairs={{0,3},{1,0},{2,1},{3,2},{4,7},{5,4},{6,5},{7,6},{8,11},{9,8},{10,9... | collective-permute-start | bytes 98312 | tf_op jit(solution)/shard_map/ppermute | solution.py:51

commit v4 on v3

--- a/solution.py
+++ b/solution.py
@@ -71,27 +71,26 @@
     return hi, mid, low
 
 
-def pack_body(idx, tok, w, lo, hi, p0, o0, s1, s2, s3, heads):
+def pack_body(idx, rows, lo, hi, p0, o0, s1, s2, s3, heads):
     x = idx[1]
-    lo[...] = tok[0:32, :]
-    hi[...] = tok[32:64, :]
-    o0[...] = w[48:64, :]
+    lo[...] = rows[0:32, :]
+    hi[...] = rows[32:64, :]
+    o0[...] = rows[64:80, 768:1024]
     head = lax.broadcasted_iota(jnp.int32, (16, HD), 0)
-    gates = w[64:80, 0:128].astype(F32)
+    gates = rows[80:96, 0:128].astype(F32)
     for h in range(NX):
-        lanes = slice(h * HD, (h + 1) * HD)
         pick = jnp.where(head == h, 1.0, 0.0)
         gate = lax.dot_general(
             gates, pick, (((0,), (0,)), ((), ())), precision=lax.Precision.HIGHEST,
             preferred_element_type=F32,
         )[0:16]
-        mine = [w[0:16, lanes], w[16:32, lanes], w[32:48, lanes], gate.astype(BF16)]
-        heads[h] = jnp.concatenate(mine, axis=1)
+        mine = [rows[64:80, i * 256 + h * HD : i * 256 + h * HD + HD] for i in range(3)]
+        heads[h] = jnp.concatenate(mine + [gate.astype(BF16)], axis=1)
     p0[...] = heads[x]
     for k, s in enumerate((s1, s2, s3)):
-        s[0:32, :] = tok[32:64, :]
+        s[0:32, :] = rows[32:64, :]
         s[32:48, 0:256] = heads[lax.rem(x + k + 1, NX)]
-        s[32:48, 256:512] = w[48:64, :]
+        s[32:48, 256:512] = rows[64:80, 768:1024]
         s[32:48, 512:1024] = jnp.zeros((16, 512), BF16)
 
 
@@ -333,9 +332,7 @@
                 out[64:72, to] = jnp.where(row < 4, both[64:65], top)
 
 
-def merge_body(idx, own, sib, *outs):
-    x = idx[1]
-    outs, parts = outs[:NX], outs[NX]
+def merge_body(own, sib, out):
     a, b = own[...], sib[...]
     m_a, m_b = a[68:69], b[68:69]
     top = jnp.maximum(m_a, m_b)
@@ -344,20 +341,7 @@
     att = (a[0:64] * f_a + b[0:64] * f_b) / total
     att = jnp.concatenate([att, jnp.zeros_like(att)], axis=0)
     for r in range(8):
-        tile = att[:, r * 128 : (r + 1) * 128].T[:, 0:64].astype(BF16)
-        parts[r // 2, (r % 2) * 128 : (r % 2) * 128 + 128, :] = tile
-    for k, out in enumerate(outs):
-        out[...] = parts[lax.rem(x + k, NX)]
-
-
-def regroup_body(idx, h0, h1, h2, h3, *outs):
-    x, y = idx[1], idx[3]
-    outs, heads = outs[:NY], outs[NY]
-    for k, h in enumerate((h0, h1, h2, h3)):
-        heads[lax.rem(x - k + NX, NX)] = h[...]
-    for k, out in enumerate(outs):
-        rows = pl.ds(pl.multiple_of(lax.rem(y + k, NY) * OWN, OWN), OWN)
-        out[...] = jnp.concatenate([heads[i, rows, :] for i in range(NX)], axis=1)
+        out[r * 128 : (r + 1) * 128, :] = att[:, r * 128 : (r + 1) * 128].T[:, 0:64].astype(BF16)
 
 
 def assemble_body(idx, w0, w1, w2, w3, w):
@@ -373,14 +357,10 @@
                     w[pl.ds(at, 16), cols] = ref[other, z, kx * 16 : kx * 16 + 16, :]
 
 
-def final_body(idx, a0, a1, a2, a3, gain, w, out, joined):
-    y = idx[3]
-    for k, a in enumerate((a0, a1, a2, a3)):
-        cols = pl.ds(pl.multiple_of(lax.rem(y - k + NY, NY) * 256, 256), 256)
-        joined[:, cols] = a[...]
-    proj = lax.dot_general(
-        joined[...], w[...], (((1,), (1,)), ((), ())), preferred_element_type=F32
-    )
+def final_body(att, gain, w, out):
+    pieces = [att[xs * NY + ys] for ys in range(NY) for xs in range(NX)]
+    joined = jnp.concatenate(pieces, axis=1)
+    proj = lax.dot_general(joined, w[...], (((1,), (1,)), ((), ())), preferred_element_type=F32)
     scale = lax.rsqrt(jnp.mean(proj * proj, axis=-1, keepdims=True) + EPS)
     out[...] = (proj * scale * gain[...]).astype(BF16)
 
@@ -390,14 +370,16 @@
     idx = jnp.stack([lax.axis_index(a) for a in AXES]).astype(jnp.int32)
 
     half, piece, send = sds((32, D), BF16), sds((16, 256), BF16), sds((48, D), BF16)
-    gate_rows = jnp.pad(w_forget.T, ((0, 16 - NX), (0, 256 - 16)))
-    weights = jnp.concatenate([w_query, w_key, w_value, w_out_t, gate_rows], axis=0)
+    rows = jnp.pad(tokens, ((0, 32), (0, 0)))
+    for i, w in enumerate((w_query, w_key, w_value, w_out_t)):
+        rows = rows + jnp.pad(w, ((64, 16), (256 * i, 768 - 256 * i)))
+    rows = rows + jnp.pad(w_forget.T, ((80, 16 - NX), (0, D - 16)))
     lo, hi, p0, o0, *sends = call(
         pack_body,
         (half, half, piece, piece, send, send, send),
-        [SMEM, VMEM, VMEM],
+        [SMEM, VMEM],
         [pltpu.VMEM((NX, 16, 256), BF16)],
-    )(idx, tokens, weights)
+    )(idx, rows)
 
     got = [shift(sends[k - 1], "x", k) for k in range(1, NX)]
     tok_a = direct(lo, "y")
@@ -417,11 +399,8 @@
     )(idx, forget_offset, *toks, norm_gain[None], w_own, w_sib)
 
     q_sib = shift(q_own, "c", 1)
-    w_o = direct(jnp.stack([w_own[:, 64:], w_sib[:, 64:]]), "y")
     q, pay = call(
-        prepare_body,
-        (sds((128, QS), BF16), sds((PAY, KEYS), BF16)),
-        [SMEM] + [VMEM] * 4,
+        prepare_body, (sds((128, QS), BF16), sds((PAY, KEYS), BF16)), [SMEM] + [VMEM] * 4
     )(idx, q_own, q_sib, kv, cum_own)
 
     acc_t, m_t, sums_t = sds((2, 80, QS), F32), sds((2, 8, QS), F32), sds((8, BLK), F32)
@@ -443,6 +422,10 @@
     acc, m, sums = call(
         first_body, (acc_t, m_t, sums_t), [SMEM, VMEM, VMEM], work, 3e9
     )(idx, q, pay)
+
+    w_o = jnp.stack([w_own[:, 64:], w_sib[:, 64:]])
+    w_o, _ = lax.optimization_barrier((w_o, sums))
+    w_o = direct(w_o, "y")
 
     for k in range(1, 5):
         pays = (right, left) if k < 4 else (right,)
@@ -468,24 +451,9 @@
             acc, m, sums = res
     sib = shift(res[1], "c", 1)
     w_full = call(assemble_body, sds((D, D), BF16), [SMEM] + [VMEM] * 4)(idx, *w_o)
-    rows = sds((BLK, HD), BF16)
-    parts = call(
-        merge_body, (rows,) * NX, [SMEM, VMEM, VMEM], [pltpu.VMEM((NX, BLK, HD), BF16)]
-    )(idx, res[0], sib)
-    parts = [parts[0]] + [shift(parts[k], "x", k) for k in range(1, NX)]
-    parts = call(
-        regroup_body,
-        (sds((OWN, 256), BF16),) * NY,
-        [SMEM] + [VMEM] * NX,
-        [pltpu.VMEM((NX, BLK, HD), BF16)],
-    )(idx, *parts)
-    parts = [parts[0]] + [shift(parts[k], "y", k) for k in range(1, NY)]
-    return call(
-        final_body,
-        sds((OWN, D), BF16),
-        [SMEM] + [VMEM] * (NY + 2),
-        [pltpu.VMEM((OWN, D), BF16)],
-    )(idx, *parts, out_gain[None], w_full)
+    att = call(merge_body, sds((KEYS, HD), BF16), [VMEM, VMEM])(res[0], sib)
+    att = lax.all_to_all(att.reshape(16, 64, HD), ("x", "y"), 0, 0, tiled=True)
+    return call(final_body, sds((OWN, D), BF16), [VMEM] * 3)(att, out_gain[None], w_full)
 
 
 def solution(mesh):

time: 132 us -> 123 us (0.932)
  the two profiles are of different devices: /device:TPU:192 before, /device:TPU:160 now
where the time goes in v4:
time: 123 us; the launch traced here: 122 us
  starting transfers between devices  52.6 us (43%)
  waiting for transfers between devices  34.8 us (28%)
  Pallas kernels  28.6 us (23%)
  local copies, waits for them, and re-layouts  4.87 us (4%)
    ppermute x18, waiting for transfers between devices, shift(): return lax.ppermute(x, axis, [(i, (i + k) % n) for i in range(n)])  25.2 us
    ppermute x18, starting transfers between devices, shift(): return lax.ppermute(x, axis, [(i, (i + k) % n) for i in range(n)])  20.3 us
    pallas_call x4, Pallas kernels, shards(): call(functools.partial(step_body, k), outs, [SMEM] + [VMEM] * (len(ins) -...  18.5 us
    ppermute x4, starting transfers between devices, step_right(): return lax.ppermute(x, 'z', [(i, i + 1) for i in range(k - 1, NZ - 1)])  17 us
    all_to_all x1, starting transfers between devices, shards(): w_own = lax.all_to_all(chunk, 'z', 0, 0, tiled=True)  6.75 us
    ppermute x4, waiting for transfers between devices, step_right(): return lax.ppermute(x, 'z', [(i, i + 1) for i in range(k - 1, NZ - 1)])  6.51 us
    all_to_all x1, starting transfers between devices, shards(): att = lax.all_to_all(att.reshape(16, 64, HD), ('x', 'y'), 0, 0, tiled=True)  5.9 us
    unnamed x19, local copies, waits for them, and re-layouts  4.82 us
  transfers between devices with their start and end apart: 27, of which 15 were waited for; matrix products, arithmetic and copies ran while one was open for 1% of the time, Pallas kernels for 18%

profile of v4, /device:TPU:160, one launch (start us, length us, event | category | flops | bytes accessed | tf_op | source)
XLA Modules:
  0.0 122.3 jit_solution(8889749204204804775)
XLA Ops:
  0.1 1.0 pad_add_fusion.rows
  1.1 1.0 shard_map.91
  2.1 1.6 %collective-permute-start.6 = (bf16[48,1024]{1,0:T(8,128)(2,1)S(1)}, bf16[48,1024]{1,0:T(8,128)(2,1)S(1)}, u32[]{:S(2)}, u32[]{:S(2)}) collective-permute-start(bf16[48,1024]{1,0:T(8,128)(2,1)S(1)} %get-tuple-element.38), channel_id=1, source_target_pairs={{0,8},{8,16},{16,24},{24,0},{1,9},{9,17},{17,25},{25,1},{2,10},{10... | collective-permute-start | bytes 294920 | tf_op jit(solution)/shard_map/ppermute | solution.py:51
  3.7 2.7 %collective-permute-start.7 = (bf16[48,1024]{1,0:T(8,128)(2,1)S(1)}, bf16[48,1024]{1,0:T(8,128)(2,1)S(1)}, u32[]{:S(2)}, u32[]{:S(2)}) collective-permute-start(bf16[48,1024]{1,0:T(8,128)(2,1)S(1)} %get-tuple-element.39), channel_id=1, source_target_pairs={{0,16},{8,24},{16,0},{24,8},{1,17},{9,25},{17,1},{25,9},{2,18},{10... | collective-permute-start | bytes 294920 | tf_op jit(solution)/shard_map/ppermute | solution.py:51
  6.4 1.4 %collective-permute-start.8 = (bf16[48,1024]{1,0:T(8,128)(2,1)S(1)}, bf16[48,1024]{1,0:T(8,128)(2,1)S(1)}, u32[]{:S(2)}, u32[]{:S(2)}) collective-permute-start(bf16[48,1024]{1,0:T(8,128)(2,1)S(1)} %get-tuple-element.40), channel_id=1, source_target_pairs={{0,24},{8,0},{16,8},{24,16},{1,25},{9,1},{17,9},{25,17},{2,26},{10... | collective-permute-start | bytes 294920 | tf_op jit(solution)/shard_map/ppermute | solution.py:51
  8.2 2.8 %collective-permute-done.7.r2 = bf16[48,1024]{1,0:T(8,128)(2,1)S(1)} collective-permute-done((bf16[48,1024]{1,0:T(8,128)(2,1)S(1)}, bf16[48,1024]{1,0:T(8,128)(2,1)S(1)}, u32[]{:S(2)}, u32[]{:S(2)}) %collective-permute-start.7) | collective-permute-done | bytes 98336 | tf_op jit(solution)/shard_map/ppermute | solution.py:51
  11.0 0.9 shard_map.92
  11.9 6.8 %all-to-all-start = ((bf16[8,128,256]{2,1,0:T(8,128)(2,1)}), bf16[8,128,256]{2,1,0:T(8,128)(2,1)S(1)}, u32[]{:S(2)}, u32[]{:S(2)}) async-start(bf16[8,128,256]{2,1,0:T(8,128)(2,1)} %get-tuple-element.42), calls=%async_computation | async-start | bytes 1048576 | tf_op jit(solution)/shard_map/all_to_all | solution.py:389
  18.6 3.0 %collective-permute-start.2 = (bf16[32,1024]{1,0:T(8,128)(2,1)S(1)}, bf16[32,1024]{1,0:T(8,128)(2,1)S(1)}, u32[]{:S(2)}, u32[]{:S(2)}) collective-permute-start(bf16[32,1024]{1,0:T(8,128)(2,1)S(1)} %get-tuple-element.34), channel_id=1, source_target_pairs={{0,3},{1,0},{2,1},{3,2},{4,7},{5,4},{6,5},{7,6},{8,11},{9,8},{10,9... | collective-permute-start | bytes 196616 | tf_op jit(solution)/shard_map/ppermute | solution.py:51
  22.3 1.0 collective-permute-start
  23.3 4.9 %collective-permute-done = bf16[32,1024]{1,0:T(8,128)(2,1)S(1)} collective-permute-done((bf16[32,1024]{1,0:T(8,128)(2,1)S(1)}, bf16[32,1024]{1,0:T(8,128)(2,1)S(1)}, u32[]{:S(2)}, u32[]{:S(2)}) %collective-permute-start) | collective-permute-done | bytes 65568 | tf_op jit(solution)/shard_map/ppermute | solution.py:51
  28.2 2.7 %collective-permute-start.5 = (bf16[128,1024]{1,0:T(8,128)(2,1)S(1)}, bf16[128,1024]{1,0:T(8,128)(2,1)S(1)}, u32[]{:S(2)}, u32[]{:S(2)}) collective-permute-start(bf16[128,1024]{1,0:T(8,128)(2,1)S(1)} %constant_dynamic-update-slice_fusion.refs_0_), channel_id=1, source_target_pairs={{0,24},{8,0},{16,8},{24,16},{1,25},{9,1},{17,9},{25,17},{2,26},{10... | collective-permute-start | bytes 786440 | tf_op jit(solution)/shard_map/ppermute | solution.py:51
  30.9 0.8 collective-permute-start.4
  32.3 2.4 %collective-permute-start.11 = (bf16[128,1024]{1,0:T(8,128)(2,1)S(1)}, bf16[128,1024]{1,0:T(8,128)(2,1)S(1)}, u32[]{:S(2)}, u32[]{:S(2)}) collective-permute-start(bf16[128,1024]{1,0:T(8,128)(2,1)S(1)} %get-tuple-element.41.refs_4_), channel_id=1, source_target_pairs={{0,3},{1,0},{2,1},{3,2},{4,7},{5,4},{6,5},{7,6},{8,11},{9,8},{10,9... | collective-permute-start | bytes 786440 | tf_op jit(solution)/shard_map/ppermute | solution.py:51
  34.8 4.6 %collective-permute-done.5.refs_3_ = bf16[128,1024]{1,0:T(8,128)(2,1)S(1)} collective-permute-done((bf16[128,1024]{1,0:T(8,128)(2,1)S(1)}, bf16[128,1024]{1,0:T(8,128)(2,1)S(1)}, u32[]{:S(2)}, u32[]{:S(2)}) %collective-permute-start.5) | collective-permute-done | bytes 262176 | tf_op jit(solution)/shard_map/ppermute | solution.py:51
  39.3 1.0 collective-permute-start.10
  40.4 1.1 collective-permute-done.4.refs_2_
  41.5 2.9 %collective-permute-done.3.refs_1_ = bf16[128,1024]{1,0:T(8,128)(2,1)S(1)} collective-permute-done((bf16[128,1024]{1,0:T(8,128)(2,1)S(1)}, bf16[128,1024]{1,0:T(8,128)(2,1)S(1)}, u32[]{:S(2)}, u32[]{:S(2)}) %collective-permute-start.3) | collective-permute-done | bytes 262176 | tf_op jit(solution)/shard_map/ppermute | solution.py:51
  44.4 2.0 %collective-permute-done.11.refs_7_ = bf16[128,1024]{1,0:T(8,128)(2,1)S(1)} collective-permute-done((bf16[128,1024]{1,0:T(8,128)(2,1)S(1)}, bf16[128,1024]{1,0:T(8,128)(2,1)S(1)}, u32[]{:S(2)}, u32[]{:S(2)}) %collective-permute-start.11) | collective-permute-done | bytes 262176 | tf_op jit(solution)/shard_map/ppermute | solution.py:51
  46.4 1.0 collective-permute-done.10.refs_6_
  47.4 2.7 %collective-permute-done.9.refs_5_ = bf16[128,1024]{1,0:T(8,128)(2,1)S(1)} collective-permute-done((bf16[128,1024]{1,0:T(8,128)(2,1)S(1)}, bf16[128,1024]{1,0:T(8,128)(2,1)S(1)}, u32[]{:S(2)}, u32[]{:S(2)}) %collective-permute-start.9) | collective-permute-done | bytes 262176 | tf_op jit(solution)/shard_map/ppermute | solution.py:51
  50.1 2.1 %shard_map.93 = (bf16[80,1024]{1,0:T(8,128)(2,1)S(1)}, bf16[128,1024]{1,0:T(8,128)(2,1)S(1)}, f32[8,1024]{1,0:T(8,128)S(1)}) custom-call(s32[4]{0:T(128)S(1)} %pad_add_fusion.1.idx, f32[4]{0:T(128)S(1)} %copy-done.6, bf16[128,1024]{1,0:T(8,128)(2,1)S(1)} %constant_dynamic-update-slice_fusion.refs_0_, bf16[128,1024]{1,0:T(8,128)(2,1)S(1)} %collective-permute-done.3.refs_1_, ...), custom_call_target="tpu_custom_call" | custom-call | flops 2000000000 | bytes 1048576 | tf_op jit(solution)/shard_map/pallas_call | solution.py:393
  52.4 1.4 %collective-permute-done.13.q_sib = bf16[80,1024]{1,0:T(8,128)(2,1)S(1)} collective-permute-done((bf16[80,1024]{1,0:T(8,128)(2,1)S(1)}, bf16[80,1024]{1,0:T(8,128)(2,1)S(1)}, u32[]{:S(2)}, u32[]{:S(2)}) %collective-permute-start.13) | collective-permute-done | bytes 163872 | tf_op jit(solution)/shard_map/ppermute | solution.py:51
  55.1 3.3 %collective-permute-start.14 = (bf16[144,1024]{1,0:T(8,128)(2,1)S(1)}, bf16[144,1024]{1,0:T(8,128)(2,1)S(1)}, u32[]{:S(2)}, u32[]{:S(2)}) collective-permute-start(bf16[144,1024]{1,0:T(8,128)(2,1)S(1)} %get-tuple-element.47.pay), channel_id=1, source_target_pairs={{0,32},{32,64},{64,96},{96,128},{128,160},{160,192},{192,224},{1,3... | collective-permute-start | bytes 884744 | tf_op jit(solution)/shard_map/ppermute | solution.py:59
  58.5 2.6 %shard_map.95 = (f32[2,80,2048]{2,1,0:T(8,128)S(1)}, f32[2,8,2048]{2,1,0:T(8,128)S(1)}, f32[8,256]{1,0:T(8,128)S(1)}) custom-call(s32[4]{0:T(128)S(1)} %pad_add_fusion.1.idx, bf16[128,2048]{1,0:T(8,128)(2,1)S(1)} %get-tuple-element.46.q, bf16[144,1024]{1,0:T(8,128)(2,1)S(1)} %get-tuple-element.47.pay), custom_call_target="tpu_custom_call" | custom-call | flops 3000000000 | bytes 1048576 | tf_op jit(solution)/shard_map/pallas_call | solution.py:422
  61.1 0.7 collective-permute-start.24
  62.5 0.8 collective-permute-start.22
  63.9 2.1 %collective-permute-done.14.refs_0_ = bf16[144,1024]{1,0:T(8,128)(2,1)S(1)} collective-permute-done((bf16[144,1024]{1,0:T(8,128)(2,1)S(1)}, bf16[144,1024]{1,0:T(8,128)(2,1)S(1)}, u32[]{:S(2)}, u32[]{:S(2)}) %collective-permute-start.14) | collective-permute-done | bytes 294944 | tf_op jit(solution)/shard_map/ppermute | solution.py:59
  66.0 3.2 %collective-permute-start.15 = (bf16[144,1024]{1,0:T(8,128)(2,1)S(1)}, bf16[144,1024]{1,0:T(8,128)(2,1)S(1)}, u32[]{:S(2)}, u32[]{:S(2)}) collective-permute-start(bf16[144,1024]{1,0:T(8,128)(2,1)S(1)} %collective-permute-done.14.refs_0_), channel_id=1, source_target_pairs={{32,64},{64,96},{96,128},{128,160},{160,192},{192,224},{33,65},{65... | collective-permute-start | bytes 884744 | tf_op jit(solution)/shard_map/ppermute | solution.py:59
  69.2 3.9 %shard_map.96 = (f32[2,80,2048]{2,1,0:T(8,128)S(1)}, f32[2,8,2048]{2,1,0:T(8,128)S(1)}, f32[8,256]{1,0:T(8,128)S(1)}) custom-call(s32[4]{0:T(128)S(1)} %pad_add_fusion.1.idx, bf16[128,2048]{1,0:T(8,128)(2,1)S(1)} %get-tuple-element.46.q, bf16[144,1024]{1,0:T(8,128)(2,1)S(1)} %collective-permute-done.14.refs_0_, ...), custom_call_target="tpu_custom_call", output_to_operand_aliasing={{0}: (4, {}), {1}: (5, {})} | custom-call | flops 6000000000 | bytes 1048576 | tf_op jit(solution)/shard_map/pallas_call | solution.py:442
  73.1 1.3 %collective-permute-start.20 = (bf16[144,1024]{1,0:T(8,128)(2,1)S(1)}, bf16[144,1024]{1,0:T(8,128)(2,1)S(1)}, u32[]{:S(2)}, u32[]{:S(2)}) collective-permute-start(bf16[144,1024]{1,0:T(8,128)(2,1)S(1)} %collective-permute-done.19.refs_1_), channel_id=1, source_target_pairs={{192,160},{224,192},{0,224},{193,161},{225,193},{1,225},{194,162},... | collective-permute-start | bytes 884744 | tf_op jit(solution)/shard_map/ppermute | solution.py:63
  74.4 2.6 %collective-permute-done.15.refs_0_ = bf16[144,1024]{1,0:T(8,128)(2,1)S(1)} collective-permute-done((bf16[144,1024]{1,0:T(8,128)(2,1)S(1)}, bf16[144,1024]{1,0:T(8,128)(2,1)S(1)}, u32[]{:S(2)}, u32[]{:S(2)}) %collective-permute-start.15) | collective-permute-done | bytes 294944 | tf_op jit(solution)/shard_map/ppermute | solution.py:59
  77.0 4.7 %collective-permute-start.16 = (bf16[144,1024]{1,0:T(8,128)(2,1)S(1)}, bf16[144,1024]{1,0:T(8,128)(2,1)S(1)}, u32[]{:S(2)}, u32[]{:S(2)}) collective-permute-start(bf16[144,1024]{1,0:T(8,128)(2,1)S(1)} %collective-permute-done.15.refs_0_), channel_id=1, source_target_pairs={{64,96},{96,128},{128,160},{160,192},{192,224},{65,97},{97,129},{1... | collective-permute-start | bytes 884744 | tf_op jit(solution)/shard_map/ppermute | solution.py:59
  81.6 3.9 %shard_map.97 = (f32[2,80,2048]{2,1,0:T(8,128)S(1)}, f32[2,8,2048]{2,1,0:T(8,128)S(1)}, f32[8,256]{1,0:T(8,128)S(1)}) custom-call(s32[4]{0:T(128)S(1)} %pad_add_fusion.1.idx, bf16[128,2048]{1,0:T(8,128)(2,1)S(1)} %get-tuple-element.46.q, bf16[144,1024]{1,0:T(8,128)(2,1)S(1)} %collective-permute-done.15.refs_0_, ...), custom_call_target="tpu_custom_call", output_to_operand_aliasing={{0}: (4, {}), {1}: (5, {})} | custom-call | flops 6000000000 | bytes 1048576 | tf_op jit(solution)/shard_map/pallas_call | solution.py:442
  85.5 1.9 %collective-permute-done.16.refs_0_ = bf16[144,1024]{1,0:T(8,128)(2,1)S(1)} collective-permute-done((bf16[144,1024]{1,0:T(8,128)(2,1)S(1)}, bf16[144,1024]{1,0:T(8,128)(2,1)S(1)}, u32[]{:S(2)}, u32[]{:S(2)}) %collective-permute-start.16) | collective-permute-done | bytes 294944 | tf_op jit(solution)/shard_map/ppermute | solution.py:59
  87.4 5.8 %collective-permute-start.17 = (bf16[144,1024]{1,0:T(8,128)(2,1)S(1)}, bf16[144,1024]{1,0:T(8,128)(2,1)S(1)}, u32[]{:S(2)}, u32[]{:S(2)}) collective-permute-start(bf16[144,1024]{1,0:T(8,128)(2,1)S(1)} %collective-permute-done.16.refs_0_), channel_id=1, source_target_pairs={{96,128},{128,160},{160,192},{192,224},{97,129},{129,161},{161,193... | collective-permute-start | bytes 884744 | tf_op jit(solution)/shard_map/ppermute | solution.py:59
  93.3 6.7 %shard_map.98 = (f32[2,80,2048]{2,1,0:T(8,128)S(1)}, f32[2,8,2048]{2,1,0:T(8,128)S(1)}, f32[8,256]{1,0:T(8,128)S(1)}) custom-call(s32[4]{0:T(128)S(1)} %pad_add_fusion.1.idx, bf16[128,2048]{1,0:T(8,128)(2,1)S(1)} %get-tuple-element.46.q, bf16[144,1024]{1,0:T(8,128)(2,1)S(1)} %collective-permute-done.16.refs_0_, ...), custom_call_target="tpu_custom_call", output_to_operand_aliasing={{0}: (4, {}), {1}: (5, {})} | custom-call | flops 6000000000 | bytes 1048576 | tf_op jit(solution)/shard_map/pallas_call | solution.py:442
  100.0 4.0 %shard_map.99 = (f32[72,1024]{1,0:T(8,128)S(1)}, f32[72,1024]{1,0:T(8,128)S(1)}) custom-call(s32[4]{0:T(128)S(1)} %pad_add_fusion.1.idx, bf16[128,2048]{1,0:T(8,128)(2,1)S(1)} %get-tuple-element.46.q, bf16[144,1024]{1,0:T(8,128)(2,1)S(1)} %collective-permute-done.17.refs_0_, f32[2,80,2048]{2,1,0:T(8,128)S(1)} %get-tuple-element.57.refs_1_, ...), custom_call_target="tpu_custom_call" | custom-call | flops 6000000000 | bytes 1048576 | tf_op jit(solution)/shard_map/pallas_call | solution.py:442
  104.1 1.6 %collective-permute-done.21.sib = f32[72,1024]{1,0:T(8,128)S(1)} collective-permute-done((f32[72,1024]{1,0:T(8,128)S(1)}, f32[72,1024]{1,0:T(8,128)S(1)}, u32[]{:S(2)}, u32[]{:S(2)}) %collective-permute-start.21) | collective-permute-done | bytes 294944 | tf_op jit(solution)/shard_map/ppermute | solution.py:51
  105.9 0.9 reshape.4
  106.8 5.9 %all-to-all-start.1 = ((bf16[16,2,2048]{2,1,0:T(2,128)(2,1)}), bf16[16,2,2048]{2,1,0:T(2,128)(2,1)S(1)}, u32[]{:S(2)}, u32[]{:S(2)}) async-start(bf16[16,2,2048]{2,1,0:T(2,128)(2,1)} %reshape.4), calls=%async_computation.1 | async-start | bytes 262144 | tf_op jit(solution)/shard_map/all_to_all | solution.py:455
  112.7 0.8 copy-done
  113.5 0.8 copy-done.2
  114.3 1.0 copy-done.1
  115.4 1.0 copy-done.3
  116.4 1.0 shard_map.101.w
  117.5 3.1 %all-to-all-done.1 = bf16[16,2,2048]{2,1,0:T(2,128)(2,1)S(1)} async-done(((bf16[16,2,2048]{2,1,0:T(2,128)(2,1)}), bf16[16,2,2048]{2,1,0:T(2,128)(2,1)S(1)}, u32[]{:S(2)}, u32[]{:S(2)}) %all-to-all-start.1) | async-done | bytes 131104 | tf_op jit(solution)/shard_map/all_to_all | solution.py:455
  120.8 1.5 %shard_map.102 = bf16[64,1024]{1,0:T(8,128)(2,1)} custom-call(bf16[16,64,64]{2,1,0:T(8,128)(2,1)S(1)} %reshape.5.att, f32[1,1024]{1,0:T(1,128)S(1)} %bitcast.13, bf16[1024,1024]{1,0:T(8,128)(2,1)S(1)} %shard_map.101.w), custom_call_target="tpu_custom_call" | custom-call | flops 100000000 | bytes 1048576 | tf_op jit(solution)/shard_map/pallas_call | solution.py:456
  (43 shorter events, 5.1 us)
Async XLA Ops:
  2.1 48.0 %copy-start.5 = (f32[1024]{0:T(1024)S(1)}, f32[1024]{0:T(1024)}, u32[]{:S(2)}) copy-start(f32[1024]{0:T(1024)} %param.10) | copy-start | bytes 12292
  2.1 48.0 %copy-start.6 = (f32[4]{0:T(128)S(1)}, f32[4]{0:T(128)}, u32[]{:S(2)}) copy-start(f32[4]{0:T(128)} %offs.1) | copy-start | bytes 52
  2.1 6.1 %collective-permute-start.6 = (bf16[48,1024]{1,0:T(8,128)(2,1)S(1)}, bf16[48,1024]{1,0:T(8,128)(2,1)S(1)}, u32[]{:S(2)}, u32[]{:S(2)}) collective-permute-start(bf16[48,1024]{1,0:T(8,128)(2,1)S(1)} %get-tuple-element.38), channel_id=1, source_target_pairs={{0,8},{8,16},{16,24},{24,0},{1,9},{9,17},{17,25},{25,1},{2,10},{10... | collective-permute-start | bytes 294920 | tf_op jit(solution)/shard_map/ppermute | solution.py:51
  3.7 7.3 %collective-permute-start.7 = (bf16[48,1024]{1,0:T(8,128)(2,1)S(1)}, bf16[48,1024]{1,0:T(8,128)(2,1)S(1)}, u32[]{:S(2)}, u32[]{:S(2)}) collective-permute-start(bf16[48,1024]{1,0:T(8,128)(2,1)S(1)} %get-tuple-element.39), channel_id=1, source_target_pairs={{0,16},{8,24},{16,0},{24,8},{1,17},{9,25},{17,1},{25,9},{2,18},{10... | collective-permute-start | bytes 294920 | tf_op jit(solution)/shard_map/ppermute | solution.py:51
  6.4 4.6 %collective-permute-start.8 = (bf16[48,1024]{1,0:T(8,128)(2,1)S(1)}, bf16[48,1024]{1,0:T(8,128)(2,1)S(1)}, u32[]{:S(2)}, u32[]{:S(2)}) collective-permute-start(bf16[48,1024]{1,0:T(8,128)(2,1)S(1)} %get-tuple-element.40), channel_id=1, source_target_pairs={{0,24},{8,0},{16,8},{24,16},{1,25},{9,1},{17,9},{25,17},{2,26},{10... | collective-permute-start | bytes 294920 | tf_op jit(solution)/shard_map/ppermute | solution.py:51
  11.9 19.8 %all-to-all-start = ((bf16[8,128,256]{2,1,0:T(8,128)(2,1)}), bf16[8,128,256]{2,1,0:T(8,128)(2,1)S(1)}, u32[]{:S(2)}, u32[]{:S(2)}) async-start(bf16[8,128,256]{2,1,0:T(8,128)(2,1)} %get-tuple-element.42), calls=%async_computation | async-start | bytes 1048576 | tf_op jit(solution)/shard_map/all_to_all | solution.py:389
  18.6 9.5 %collective-permute-start.2 = (bf16[32,1024]{1,0:T(8,128)(2,1)S(1)}, bf16[32,1024]{1,0:T(8,128)(2,1)S(1)}, u32[]{:S(2)}, u32[]{:S(2)}) collective-permute-start(bf16[32,1024]{1,0:T(8,128)(2,1)S(1)} %get-tuple-element.34), channel_id=1, source_target_pairs={{0,3},{1,0},{2,1},{3,2},{4,7},{5,4},{6,5},{7,6},{8,11},{9,8},{10,9... | collective-permute-start | bytes 196616 | tf_op jit(solution)/shard_map/ppermute | solution.py:51
  21.7 6.5 %collective-permute-start.1 = (bf16[32,1024]{1,0:T(8,128)(2,1)S(1)}, bf16[32,1024]{1,0:T(8,128)(2,1)S(1)}, u32[]{:S(2)}, u32[]{:S(2)}) collective-permute-start(bf16[32,1024]{1,0:T(8,128)(2,1)S(1)} %get-tuple-element.34), channel_id=1, source_target_pairs={{0,2},{1,3},{2,0},{3,1},{4,6},{5,7},{6,4},{7,5},{8,10},{9,11},{10,... | collective-permute-start | bytes 196616 | tf_op jit(solution)/shard_map/ppermute | solution.py:51
  22.3 5.8 %collective-permute-start = (bf16[32,1024]{1,0:T(8,128)(2,1)S(1)}, bf16[32,1024]{1,0:T(8,128)(2,1)S(1)}, u32[]{:S(2)}, u32[]{:S(2)}) collective-permute-start(bf16[32,1024]{1,0:T(8,128)(2,1)S(1)} %get-tuple-element.34), channel_id=1, source_target_pairs={{0,1},{1,2},{2,3},{3,0},{4,5},{5,6},{6,7},{7,4},{8,9},{9,10},{10,1... | collective-permute-start | bytes 196616 | tf_op jit(solution)/shard_map/ppermute | solution.py:51
  28.2 11.2 %collective-permute-start.5 = (bf16[128,1024]{1,0:T(8,128)(2,1)S(1)}, bf16[128,1024]{1,0:T(8,128)(2,1)S(1)}, u32[]{:S(2)}, u32[]{:S(2)}) collective-permute-start(bf16[128,1024]{1,0:T(8,128)(2,1)S(1)} %constant_dynamic-update-slice_fusion.refs_0_), channel_id=1, source_target_pairs={{0,24},{8,0},{16,8},{24,16},{1,25},{9,1},{17,9},{25,17},{2,26},{10... | collective-permute-start | bytes 786440 | tf_op jit(solution)/shard_map/ppermute | solution.py:51
  30.9 10.6 %collective-permute-start.4 = (bf16[128,1024]{1,0:T(8,128)(2,1)S(1)}, bf16[128,1024]{1,0:T(8,128)(2,1)S(1)}, u32[]{:S(2)}, u32[]{:S(2)}) collective-permute-start(bf16[128,1024]{1,0:T(8,128)(2,1)S(1)} %constant_dynamic-update-slice_fusion.refs_0_), channel_id=1, source_target_pairs={{0,16},{8,24},{16,0},{24,8},{1,17},{9,25},{17,1},{25,9},{2,18},{10... | collective-permute-start | bytes 786440 | tf_op jit(solution)/shard_map/ppermute | solution.py:51
  31.7 18.4 %collective-permute-start.12 = (bf16[8,128,256]{2,1,0:T(8,128)(2,1)S(1)}, bf16[8,128,256]{2,1,0:T(8,128)(2,1)S(1)}, u32[]{:S(2)}, u32[]{:S(2)}) collective-permute-start(bf16[8,128,256]{2,1,0:T(8,128)(2,1)S(1)} %all-to-all-done.refs_9_), channel_id=1, source_target_pairs={{0,4},{4,0},{1,5},{5,1},{2,6},{6,2},{3,7},{7,3},{8,12},{12,8},{9,1... | collective-permute-start | bytes 1572872 | tf_op jit(solution)/shard_map/ppermute | solution.py:51
  31.7 12.7 %collective-permute-start.3 = (bf16[128,1024]{1,0:T(8,128)(2,1)S(1)}, bf16[128,1024]{1,0:T(8,128)(2,1)S(1)}, u32[]{:S(2)}, u32[]{:S(2)}) collective-permute-start(bf16[128,1024]{1,0:T(8,128)(2,1)S(1)} %constant_dynamic-update-slice_fusion.refs_0_), channel_id=1, source_target_pairs={{0,8},{8,16},{16,24},{24,0},{1,9},{9,17},{17,25},{25,1},{2,10},{10... | collective-permute-start | bytes 786440 | tf_op jit(solution)/shard_map/ppermute | solution.py:51
  32.3 14.0 %collective-permute-start.11 = (bf16[128,1024]{1,0:T(8,128)(2,1)S(1)}, bf16[128,1024]{1,0:T(8,128)(2,1)S(1)}, u32[]{:S(2)}, u32[]{:S(2)}) collective-permute-start(bf16[128,1024]{1,0:T(8,128)(2,1)S(1)} %get-tuple-element.41.refs_4_), channel_id=1, source_target_pairs={{0,3},{1,0},{2,1},{3,2},{4,7},{5,4},{6,5},{7,6},{8,11},{9,8},{10,9... | collective-permute-start | bytes 786440 | tf_op jit(solution)/shard_map/ppermute | solution.py:51
  39.3 8.1 %collective-permute-start.10 = (bf16[128,1024]{1,0:T(8,128)(2,1)S(1)}, bf16[128,1024]{1,0:T(8,128)(2,1)S(1)}, u32[]{:S(2)}, u32[]{:S(2)}) collective-permute-start(bf16[128,1024]{1,0:T(8,128)(2,1)S(1)} %get-tuple-element.41.refs_4_), channel_id=1, source_target_pairs={{0,2},{1,3},{2,0},{3,1},{4,6},{5,7},{6,4},{7,5},{8,10},{9,11},{10,... | collective-permute-start | bytes 786440 | tf_op jit(solution)/shard_map/ppermute | solution.py:51
  41.5 8.6 %collective-permute-start.9 = (bf16[128,1024]{1,0:T(8,128)(2,1)S(1)}, bf16[128,1024]{1,0:T(8,128)(2,1)S(1)}, u32[]{:S(2)}, u32[]{:S(2)}) collective-permute-start(bf16[128,1024]{1,0:T(8,128)(2,1)S(1)} %get-tuple-element.41.refs_4_), channel_id=1, source_target_pairs={{0,1},{1,2},{2,3},{3,0},{4,5},{5,6},{6,7},{7,4},{8,9},{9,10},{10,1... | collective-permute-start | bytes 786440 | tf_op jit(solution)/shard_map/ppermute | solution.py:51
  52.3 1.5 %collective-permute-start.13 = (bf16[80,1024]{1,0:T(8,128)(2,1)S(1)}, bf16[80,1024]{1,0:T(8,128)(2,1)S(1)}, u32[]{:S(2)}, u32[]{:S(2)}) collective-permute-start(bf16[80,1024]{1,0:T(8,128)(2,1)S(1)} %get-tuple-element.43.q_own), channel_id=1, source_target_pairs={{0,4},{4,0},{1,5},{5,1},{2,6},{6,2},{3,7},{7,3},{8,12},{12,8},{9,1... | collective-permute-start | bytes 491528 | tf_op jit(solution)/shard_map/ppermute | solution.py:51
  54.4 8.9 %collective-permute-start.18 = (bf16[144,1024]{1,0:T(8,128)(2,1)S(1)}, bf16[144,1024]{1,0:T(8,128)(2,1)S(1)}, u32[]{:S(2)}, u32[]{:S(2)}) collective-permute-start(bf16[144,1024]{1,0:T(8,128)(2,1)S(1)} %get-tuple-element.47.pay), channel_id=1, source_target_pairs={{0,224},{32,0},{64,32},{1,225},{33,1},{65,33},{2,226},{34,2},{66,3... | collective-permute-start | bytes 884744 | tf_op jit(solution)/shard_map/ppermute | solution.py:63
  55.1 10.9 %collective-permute-start.14 = (bf16[144,1024]{1,0:T(8,128)(2,1)S(1)}, bf16[144,1024]{1,0:T(8,128)(2,1)S(1)}, u32[]{:S(2)}, u32[]{:S(2)}) collective-permute-start(bf16[144,1024]{1,0:T(8,128)(2,1)S(1)} %get-tuple-element.47.pay), channel_id=1, source_target_pairs={{0,32},{32,64},{64,96},{96,128},{128,160},{160,192},{192,224},{1,3... | collective-permute-start | bytes 884744 | tf_op jit(solution)/shard_map/ppermute | solution.py:59
  61.1 51.6 %collective-permute-start.24 = (bf16[2,8,64,256]{3,2,1,0:T(8,128)(2,1)S(1)}, bf16[2,8,64,256]{3,2,1,0:T(8,128)(2,1)S(1)}, u32[]{:S(2)}, u32[]{:S(2)}) collective-permute-start(bf16[2,8,64,256]{3,2,1,0:T(8,128)(2,1)S(1)} %pad_maximum_fusion.w0), channel_id=1, source_target_pairs={{0,3},{1,0},{2,1},{3,2},{4,7},{5,4},{6,5},{7,6},{8,11},{9,8},{10,9... | collective-permute-start | bytes 1572872 | tf_op jit(solution)/shard_map/ppermute | solution.py:51
  61.8 50.9 %collective-permute-start.23 = (bf16[2,8,64,256]{3,2,1,0:T(8,128)(2,1)S(1)}, bf16[2,8,64,256]{3,2,1,0:T(8,128)(2,1)S(1)}, u32[]{:S(2)}, u32[]{:S(2)}) collective-permute-start(bf16[2,8,64,256]{3,2,1,0:T(8,128)(2,1)S(1)} %pad_maximum_fusion.w0), channel_id=1, source_target_pairs={{0,2},{1,3},{2,0},{3,1},{4,6},{5,7},{6,4},{7,5},{8,10},{9,11},{10,... | collective-permute-start | bytes 1572872 | tf_op jit(solution)/shard_map/ppermute | solution.py:51
  62.5 51.1 %collective-permute-start.22 = (bf16[2,8,64,256]{3,2,1,0:T(8,128)(2,1)S(1)}, bf16[2,8,64,256]{3,2,1,0:T(8,128)(2,1)S(1)}, u32[]{:S(2)}, u32[]{:S(2)}) collective-permute-start(bf16[2,8,64,256]{3,2,1,0:T(8,128)(2,1)S(1)} %pad_maximum_fusion.w0), channel_id=1, source_target_pairs={{0,1},{1,2},{2,3},{3,0},{4,5},{5,6},{6,7},{7,4},{8,9},{9,10},{10,1... | collective-permute-start | bytes 1572872 | tf_op jit(solution)/shard_map/ppermute | solution.py:51
  63.3 9.8 %collective-permute-start.19 = (bf16[144,1024]{1,0:T(8,128)(2,1)S(1)}, bf16[144,1024]{1,0:T(8,128)(2,1)S(1)}, u32[]{:S(2)}, u32[]{:S(2)}) collective-permute-start(bf16[144,1024]{1,0:T(8,128)(2,1)S(1)} %collective-permute-done.18.refs_1_), channel_id=1, source_target_pairs={{224,192},{0,224},{32,0},{225,193},{1,225},{33,1},{226,194},{2,226... | collective-permute-start | bytes 884744 | tf_op jit(solution)/shard_map/ppermute | solution.py:63
  66.0 10.9 %collective-permute-start.15 = (bf16[144,1024]{1,0:T(8,128)(2,1)S(1)}, bf16[144,1024]{1,0:T(8,128)(2,1)S(1)}, u32[]{:S(2)}, u32[]{:S(2)}) collective-permute-start(bf16[144,1024]{1,0:T(8,128)(2,1)S(1)} %collective-permute-done.14.refs_0_), channel_id=1, source_target_pairs={{32,64},{64,96},{96,128},{128,160},{160,192},{192,224},{33,65},{65... | collective-permute-start | bytes 884744 | tf_op jit(solution)/shard_map/ppermute | solution.py:59
  73.1 20.1 %collective-permute-start.20 = (bf16[144,1024]{1,0:T(8,128)(2,1)S(1)}, bf16[144,1024]{1,0:T(8,128)(2,1)S(1)}, u32[]{:S(2)}, u32[]{:S(2)}) collective-permute-start(bf16[144,1024]{1,0:T(8,128)(2,1)S(1)} %collective-permute-done.19.refs_1_), channel_id=1, source_target_pairs={{192,160},{224,192},{0,224},{193,161},{225,193},{1,225},{194,162},... | collective-permute-start | bytes 884744 | tf_op jit(solution)/shard_map/ppermute | solution.py:63
  77.0 10.4 %collective-permute-start.16 = (bf16[144,1024]{1,0:T(8,128)(2,1)S(1)}, bf16[144,1024]{1,0:T(8,128)(2,1)S(1)}, u32[]{:S(2)}, u32[]{:S(2)}) collective-permute-start(bf16[144,1024]{1,0:T(8,128)(2,1)S(1)} %collective-permute-done.15.refs_0_), channel_id=1, source_target_pairs={{64,96},{96,128},{128,160},{160,192},{192,224},{65,97},{97,129},{1... | collective-permute-start | bytes 884744 | tf_op jit(solution)/shard_map/ppermute | solution.py:59
  87.4 12.6 %collective-permute-start.17 = (bf16[144,1024]{1,0:T(8,128)(2,1)S(1)}, bf16[144,1024]{1,0:T(8,128)(2,1)S(1)}, u32[]{:S(2)}, u32[]{:S(2)}) collective-permute-start(bf16[144,1024]{1,0:T(8,128)(2,1)S(1)} %collective-permute-done.16.refs_0_), channel_id=1, source_target_pairs={{96,128},{128,160},{160,192},{192,224},{97,129},{129,161},{161,193... | collective-permute-start | bytes 884744 | tf_op jit(solution)/shard_map/ppermute | solution.py:59
  104.0 1.7 %collective-permute-start.21 = (f32[72,1024]{1,0:T(8,128)S(1)}, f32[72,1024]{1,0:T(8,128)S(1)}, u32[]{:S(2)}, u32[]{:S(2)}) collective-permute-start(f32[72,1024]{1,0:T(8,128)S(1)} %get-tuple-element.61), channel_id=1, source_target_pairs={{0,4},{4,0},{1,5},{5,1},{2,6},{6,2},{3,7},{7,3},{8,12},{12,8},{9,1... | collective-permute-start | bytes 884744 | tf_op jit(solution)/shard_map/ppermute | solution.py:51
  106.8 14.0 %copy-start.4 = (f32[1024]{0:T(1024)S(1)}, f32[1024]{0:T(1024)}, u32[]{:S(2)}) copy-start(f32[1024]{0:T(1024)} %param.17) | copy-start | bytes 12292
  106.8 13.8 %all-to-all-start.1 = ((bf16[16,2,2048]{2,1,0:T(2,128)(2,1)}), bf16[16,2,2048]{2,1,0:T(2,128)(2,1)S(1)}, u32[]{:S(2)}, u32[]{:S(2)}) async-start(bf16[16,2,2048]{2,1,0:T(2,128)(2,1)} %reshape.4), calls=%async_computation.1 | async-start | bytes 262144 | tf_op jit(solution)/shard_map/all_to_all | solution.py:455
  112.7 0.8 copy-start
  113.5 0.8 copy-start.2
  114.3 1.0 copy-start.1
  115.4 1.0 copy-start.3

commit v5 on v4

--- a/solution.py
+++ b/solution.py
@@ -51,8 +51,10 @@
     return lax.ppermute(x, axis, [(i, (i + k) % n) for i in range(n)])
 
 
-def direct(x, axis):
-    return [x] + [shift(x, axis, k) for k in range(1, SIZES[axis])]
+def gather(x, axis):
+    one, three = shift(x, axis, 1), shift(x, axis, -1)
+    two = shift(one, axis, 1)
+    return [x, one, two, three]
 
 
 def step_right(x, k):
@@ -71,7 +73,7 @@
     return hi, mid, low
 
 
-def pack_body(idx, rows, lo, hi, p0, o0, s1, s2, s3, heads):
+def pack_body(idx, rows, lo, hi, p0, o0, s1, s3, heads):
     x = idx[1]
     lo[...] = rows[0:32, :]
     hi[...] = rows[32:64, :]
@@ -87,11 +89,12 @@
         mine = [rows[64:80, i * 256 + h * HD : i * 256 + h * HD + HD] for i in range(3)]
         heads[h] = jnp.concatenate(mine + [gate.astype(BF16)], axis=1)
     p0[...] = heads[x]
-    for k, s in enumerate((s1, s2, s3)):
+    for k, s in ((1, s1), (3, s3)):
         s[0:32, :] = rows[32:64, :]
-        s[32:48, 0:256] = heads[lax.rem(x + k + 1, NX)]
+        s[32:48, 0:256] = heads[lax.rem(x + k, NX)]
         s[32:48, 256:512] = rows[64:80, 768:1024]
-        s[32:48, 512:1024] = jnp.zeros((16, 512), BF16)
+        s[32:48, 512:768] = heads[lax.rem(x + 2, NX)]
+        s[32:48, 768:1024] = jnp.zeros((16, 256), BF16)
 
 
 def spread_body(hi, p0, o0, r1, r2, r3, out, toks):
@@ -102,7 +105,8 @@
         out[z, 0:16, :] = p0[...]
         out[z, 64:80, :] = o0[...]
         for k, r in enumerate((r1, r2, r3)):
-            out[z, 16 * k + 16 : 16 * k + 32, :] = r[32:48, 0:256]
+            piece = 512 if k == 1 else 0
+            out[z, 16 * k + 16 : 16 * k + 32, :] = r[32:48, piece : piece + 256]
             out[z, 16 * k + 80 : 16 * k + 96, :] = r[32:48, 256:512]
 
 
@@ -374,20 +378,22 @@
     for i, w in enumerate((w_query, w_key, w_value, w_out_t)):
         rows = rows + jnp.pad(w, ((64, 16), (256 * i, 768 - 256 * i)))
     rows = rows + jnp.pad(w_forget.T, ((80, 16 - NX), (0, D - 16)))
-    lo, hi, p0, o0, *sends = call(
+    lo, hi, p0, o0, ahead, behind = call(
         pack_body,
-        (half, half, piece, piece, send, send, send),
+        (half, half, piece, piece, send, send),
         [SMEM, VMEM],
         [pltpu.VMEM((NX, 16, 256), BF16)],
     )(idx, rows)
 
-    got = [shift(sends[k - 1], "x", k) for k in range(1, NX)]
-    tok_a = direct(lo, "y")
+    got_1, got_3 = shift(ahead, "x", 1), shift(behind, "x", -1)
+    got = (got_1, shift(got_1, "x", 1), got_3)
+    tok_a = gather(lo, "y")
     chunk, tok_b = call(
         spread_body, (sds((NZ, 128, 256), BF16), sds((128, D), BF16)), [VMEM] * 6
     )(hi, p0, o0, *got)
     w_own = lax.all_to_all(chunk, "z", 0, 0, tiled=True)
-    toks = direct(jnp.concatenate(tok_a, axis=0), "x") + direct(tok_b, "y")
+    toks_b = gather(tok_b, "y")
+    toks = gather(jnp.concatenate(tok_a, axis=0), "x") + toks_b
     w_sib = shift(w_own, "c", 1)
 
     q_own, kv, cum_own = call(
@@ -425,7 +431,7 @@
 
     w_o = jnp.stack([w_own[:, 64:], w_sib[:, 64:]])
     w_o, _ = lax.optimization_barrier((w_o, sums))
-    w_o = direct(w_o, "y")
+    w_o = gather(w_o, "y")
 
     for k in range(1, 5):
         pays = (right, left) if k < 4 else (right,)

time: 123 us -> 125 us (1.016)
  waiting for transfers between devices: 34.8 us -> 44.2 us
  starting transfers between devices: 52.6 us -> 45.8 us
    ppermute x18, waiting for transfers between devices: 25.2 us -> 35.4 us  [shift(): return lax.ppermute(x, axis, [(i, (i + k) % n) for i in range(n)])]
    ppermute x18, starting transfers between devices: 20.3 us -> 16.1 us  [shift(): return lax.ppermute(x, axis, [(i, (i + k) % n) for i in range(n)])]
    ppermute x4, starting transfers between devices: 17 us -> 13.8 us  [step_right(): return lax.ppermute(x, 'z', [(i, i + 1) for i in range(k - 1, NZ - 1)])]
    ppermute x4, waiting for transfers between devices: 6.51 us -> 4.92 us  [step_right(): return lax.ppermute(x, 'z', [(i, i + 1) for i in range(k - 1, NZ - 1)])]
  transfers between devices with their start and end apart: 27 -> 27, of which waited for: 15 -> 16; matrix products, arithmetic and copies ran while one was open for 1% -> 1% of each run, Pallas kernels for 18% -> 18%
where the time goes in v5:
time: 125 us; the launch traced here: 124 us
  starting transfers between devices  45.8 us (37%)
  waiting for transfers between devices  44.2 us (35%)
  Pallas kernels  28.6 us (23%)
  local copies, waits for them, and re-layouts  4.07 us (3%)
    ppermute x18, waiting for transfers between devices, shift(): return lax.ppermute(x, axis, [(i, (i + k) % n) for i in range(n)])  35.4 us
    pallas_call x4, Pallas kernels, shards(): call(functools.partial(step_body, k), outs, [SMEM] + [VMEM] * (len(ins) -...  18.6 us
    ppermute x18, starting transfers between devices, shift(): return lax.ppermute(x, axis, [(i, (i + k) % n) for i in range(n)])  16.1 us
    ppermute x4, starting transfers between devices, step_right(): return lax.ppermute(x, 'z', [(i, i + 1) for i in range(k - 1, NZ - 1)])  13.8 us
    all_to_all x1, starting transfers between devices, shards(): w_own = lax.all_to_all(chunk, 'z', 0, 0, tiled=True)  6.75 us
    all_to_all x1, starting transfers between devices, shards(): att = lax.all_to_all(att.reshape(16, 64, HD), ('x', 'y'), 0, 0, tiled=True)  6.6 us
    ppermute x4, waiting for transfers between devices, step_right(): return lax.ppermute(x, 'z', [(i, i + 1) for i in range(k - 1, NZ - 1)])  4.92 us
    unnamed x19, local copies, waits for them, and re-layouts  4.03 us
  transfers between devices with their start and end apart: 27, of which 16 were waited for; matrix products, arithmetic and copies ran while one was open for 1% of the time, Pallas kernels for 18%

profile of v5, /device:TPU:160, one launch (start us, length us, event | category | flops | bytes accessed | tf_op | source)
XLA Modules:
  0.0 124.1 jit_solution(16231021749346515625)
XLA Ops:
  0.1 1.0 pad_add_fusion.rows
  1.1 1.0 shard_map.91
  2.1 1.6 %collective-permute-start.6 = (bf16[48,1024]{1,0:T(8,128)(2,1)S(1)}, bf16[48,1024]{1,0:T(8,128)(2,1)S(1)}, u32[]{:S(2)}, u32[]{:S(2)}) collective-permute-start(bf16[48,1024]{1,0:T(8,128)(2,1)S(1)} %get-tuple-element.37), channel_id=1, source_target_pairs={{0,8},{8,16},{16,24},{24,0},{1,9},{9,17},{17,25},{25,1},{2,10},{10... | collective-permute-start | bytes 294920 | tf_op jit(solution)/shard_map/ppermute | solution.py:51
  3.7 1.7 %collective-permute-start.8 = (bf16[48,1024]{1,0:T(8,128)(2,1)S(1)}, bf16[48,1024]{1,0:T(8,128)(2,1)S(1)}, u32[]{:S(2)}, u32[]{:S(2)}) collective-permute-start(bf16[48,1024]{1,0:T(8,128)(2,1)S(1)} %get-tuple-element.38), channel_id=1, source_target_pairs={{0,24},{8,0},{16,8},{24,16},{1,25},{9,1},{17,9},{25,17},{2,26},{10... | collective-permute-start | bytes 294920 | tf_op jit(solution)/shard_map/ppermute | solution.py:51
  5.4 2.6 %collective-permute-done.6.r1 = bf16[48,1024]{1,0:T(8,128)(2,1)S(1)} collective-permute-done((bf16[48,1024]{1,0:T(8,128)(2,1)S(1)}, bf16[48,1024]{1,0:T(8,128)(2,1)S(1)}, u32[]{:S(2)}, u32[]{:S(2)}) %collective-permute-start.6) | collective-permute-done | bytes 98336 | tf_op jit(solution)/shard_map/ppermute | solution.py:51
  8.0 0.3 collective-permute-start.7
  8.3 5.5 %collective-permute-done.7.r2 = bf16[48,1024]{1,0:T(8,128)(2,1)S(1)} collective-permute-done((bf16[48,1024]{1,0:T(8,128)(2,1)S(1)}, bf16[48,1024]{1,0:T(8,128)(2,1)S(1)}, u32[]{:S(2)}, u32[]{:S(2)}) %collective-permute-start.7) | collective-permute-done | bytes 98336 | tf_op jit(solution)/shard_map/ppermute | solution.py:51
  13.8 0.9 shard_map.92
  14.7 6.8 %all-to-all-start = ((bf16[8,128,256]{2,1,0:T(8,128)(2,1)}), bf16[8,128,256]{2,1,0:T(8,128)(2,1)S(1)}, u32[]{:S(2)}, u32[]{:S(2)}) async-start(bf16[8,128,256]{2,1,0:T(8,128)(2,1)} %get-tuple-element.40), calls=%async_computation | async-start | bytes 1048576 | tf_op jit(solution)/shard_map/all_to_all | solution.py:394
  21.5 3.0 %collective-permute-start.2 = (bf16[32,1024]{1,0:T(8,128)(2,1)S(1)}, bf16[32,1024]{1,0:T(8,128)(2,1)S(1)}, u32[]{:S(2)}, u32[]{:S(2)}) collective-permute-start(bf16[32,1024]{1,0:T(8,128)(2,1)S(1)} %get-tuple-element.33), channel_id=1, source_target_pairs={{0,3},{1,0},{2,1},{3,2},{4,7},{5,4},{6,5},{7,6},{8,11},{9,8},{10,9... | collective-permute-start | bytes 196616 | tf_op jit(solution)/shard_map/ppermute | solution.py:51
  24.5 5.8 %collective-permute-done = bf16[32,1024]{1,0:T(8,128)(2,1)S(1)} collective-permute-done((bf16[32,1024]{1,0:T(8,128)(2,1)S(1)}, bf16[32,1024]{1,0:T(8,128)(2,1)S(1)}, u32[]{:S(2)}, u32[]{:S(2)}) %collective-permute-start) | collective-permute-done | bytes 65568 | tf_op jit(solution)/shard_map/ppermute | solution.py:51
  30.3 6.2 %collective-permute-done.1 = bf16[32,1024]{1,0:T(8,128)(2,1)S(1)} collective-permute-done((bf16[32,1024]{1,0:T(8,128)(2,1)S(1)}, bf16[32,1024]{1,0:T(8,128)(2,1)S(1)}, u32[]{:S(2)}, u32[]{:S(2)}) %collective-permute-start.1) | collective-permute-done | bytes 65568 | tf_op jit(solution)/shard_map/ppermute | solution.py:51
  36.8 3.1 %collective-permute-start.5 = (bf16[128,1024]{1,0:T(8,128)(2,1)S(1)}, bf16[128,1024]{1,0:T(8,128)(2,1)S(1)}, u32[]{:S(2)}, u32[]{:S(2)}) collective-permute-start(bf16[128,1024]{1,0:T(8,128)(2,1)S(1)} %constant_dynamic-update-slice_fusion.refs_0_), channel_id=1, source_target_pairs={{0,24},{8,0},{16,8},{24,16},{1,25},{9,1},{17,9},{25,17},{2,26},{10... | collective-permute-start | bytes 786440 | tf_op jit(solution)/shard_map/ppermute | solution.py:51
  39.9 3.2 %collective-permute-start.11 = (bf16[128,1024]{1,0:T(8,128)(2,1)S(1)}, bf16[128,1024]{1,0:T(8,128)(2,1)S(1)}, u32[]{:S(2)}, u32[]{:S(2)}) collective-permute-start(bf16[128,1024]{1,0:T(8,128)(2,1)S(1)} %get-tuple-element.39.refs_4_), channel_id=1, source_target_pairs={{0,3},{1,0},{2,1},{3,2},{4,7},{5,4},{6,5},{7,6},{8,11},{9,8},{10,9... | collective-permute-start | bytes 786440 | tf_op jit(solution)/shard_map/ppermute | solution.py:51
  43.1 1.1 collective-permute-done.3.refs_1_
  44.3 1.8 %collective-permute-done.5.refs_3_ = bf16[128,1024]{1,0:T(8,128)(2,1)S(1)} collective-permute-done((bf16[128,1024]{1,0:T(8,128)(2,1)S(1)}, bf16[128,1024]{1,0:T(8,128)(2,1)S(1)}, u32[]{:S(2)}, u32[]{:S(2)}) %collective-permute-start.5) | collective-permute-done | bytes 262176 | tf_op jit(solution)/shard_map/ppermute | solution.py:51
  46.1 3.0 %collective-permute-done.11.refs_7_ = bf16[128,1024]{1,0:T(8,128)(2,1)S(1)} collective-permute-done((bf16[128,1024]{1,0:T(8,128)(2,1)S(1)}, bf16[128,1024]{1,0:T(8,128)(2,1)S(1)}, u32[]{:S(2)}, u32[]{:S(2)}) %collective-permute-start.11) | collective-permute-done | bytes 262176 | tf_op jit(solution)/shard_map/ppermute | solution.py:51
  49.0 3.4 %collective-permute-done.4.refs_2_ = bf16[128,1024]{1,0:T(8,128)(2,1)S(1)} collective-permute-done((bf16[128,1024]{1,0:T(8,128)(2,1)S(1)}, bf16[128,1024]{1,0:T(8,128)(2,1)S(1)}, u32[]{:S(2)}, u32[]{:S(2)}) %collective-permute-start.4) | collective-permute-done | bytes 262176 | tf_op jit(solution)/shard_map/ppermute | solution.py:51
  52.5 2.1 %shard_map.93 = (bf16[80,1024]{1,0:T(8,128)(2,1)S(1)}, bf16[128,1024]{1,0:T(8,128)(2,1)S(1)}, f32[8,1024]{1,0:T(8,128)S(1)}) custom-call(s32[4]{0:T(128)S(1)} %pad_add_fusion.1.idx, f32[4]{0:T(128)S(1)} %copy-done.6, bf16[128,1024]{1,0:T(8,128)(2,1)S(1)} %constant_dynamic-update-slice_fusion.refs_0_, bf16[128,1024]{1,0:T(8,128)(2,1)S(1)} %collective-permute-done.3.refs_1_, ...), custom_call_target="tpu_custom_call" | custom-call | flops 2000000000 | bytes 1048576 | tf_op jit(solution)/shard_map/pallas_call | solution.py:399
  55.0 1.4 %collective-permute-done.13.q_sib = bf16[80,1024]{1,0:T(8,128)(2,1)S(1)} collective-permute-done((bf16[80,1024]{1,0:T(8,128)(2,1)S(1)}, bf16[80,1024]{1,0:T(8,128)(2,1)S(1)}, u32[]{:S(2)}, u32[]{:S(2)}) %collective-permute-start.13) | collective-permute-done | bytes 163872 | tf_op jit(solution)/shard_map/ppermute | solution.py:51
  56.3 0.6 shard_map.94
  57.0 0.7 collective-permute-start.18
  57.7 2.5 %collective-permute-start.14 = (bf16[144,1024]{1,0:T(8,128)(2,1)S(1)}, bf16[144,1024]{1,0:T(8,128)(2,1)S(1)}, u32[]{:S(2)}, u32[]{:S(2)}) collective-permute-start(bf16[144,1024]{1,0:T(8,128)(2,1)S(1)} %get-tuple-element.45.pay), channel_id=1, source_target_pairs={{0,32},{32,64},{64,96},{96,128},{128,160},{160,192},{192,224},{1,3... | collective-permute-start | bytes 884744 | tf_op jit(solution)/shard_map/ppermute | solution.py:61
  60.2 2.6 %shard_map.95 = (f32[2,80,2048]{2,1,0:T(8,128)S(1)}, f32[2,8,2048]{2,1,0:T(8,128)S(1)}, f32[8,256]{1,0:T(8,128)S(1)}) custom-call(s32[4]{0:T(128)S(1)} %pad_add_fusion.1.idx, bf16[128,2048]{1,0:T(8,128)(2,1)S(1)} %get-tuple-element.44.q, bf16[144,1024]{1,0:T(8,128)(2,1)S(1)} %get-tuple-element.45.pay), custom_call_target="tpu_custom_call" | custom-call | flops 3000000000 | bytes 1048576 | tf_op jit(solution)/shard_map/pallas_call | solution.py:428
  62.9 0.3 collective-permute-start.24
  63.1 1.8 %collective-permute-start.22 = (bf16[2,8,64,256]{3,2,1,0:T(8,128)(2,1)S(1)}, bf16[2,8,64,256]{3,2,1,0:T(8,128)(2,1)S(1)}, u32[]{:S(2)}, u32[]{:S(2)}) collective-permute-start(bf16[2,8,64,256]{3,2,1,0:T(8,128)(2,1)S(1)} %pad_maximum_fusion.w0), channel_id=1, source_target_pairs={{0,1},{1,2},{2,3},{3,0},{4,5},{5,6},{6,7},{7,4},{8,9},{9,10},{10,1... | collective-permute-start | bytes 1572872 | tf_op jit(solution)/shard_map/ppermute | solution.py:51
  65.0 0.7 collective-permute-start.19
  65.6 3.0 %collective-permute-done.14.refs_0_ = bf16[144,1024]{1,0:T(8,128)(2,1)S(1)} collective-permute-done((bf16[144,1024]{1,0:T(8,128)(2,1)S(1)}, bf16[144,1024]{1,0:T(8,128)(2,1)S(1)}, u32[]{:S(2)}, u32[]{:S(2)}) %collective-permute-start.14) | collective-permute-done | bytes 294944 | tf_op jit(solution)/shard_map/ppermute | solution.py:61
  68.6 2.5 %collective-permute-start.15 = (bf16[144,1024]{1,0:T(8,128)(2,1)S(1)}, bf16[144,1024]{1,0:T(8,128)(2,1)S(1)}, u32[]{:S(2)}, u32[]{:S(2)}) collective-permute-start(bf16[144,1024]{1,0:T(8,128)(2,1)S(1)} %collective-permute-done.14.refs_0_), channel_id=1, source_target_pairs={{32,64},{64,96},{96,128},{128,160},{160,192},{192,224},{33,65},{65... | collective-permute-start | bytes 884744 | tf_op jit(solution)/shard_map/ppermute | solution.py:61
  71.1 3.9 %shard_map.96 = (f32[2,80,2048]{2,1,0:T(8,128)S(1)}, f32[2,8,2048]{2,1,0:T(8,128)S(1)}, f32[8,256]{1,0:T(8,128)S(1)}) custom-call(s32[4]{0:T(128)S(1)} %pad_add_fusion.1.idx, bf16[128,2048]{1,0:T(8,128)(2,1)S(1)} %get-tuple-element.44.q, bf16[144,1024]{1,0:T(8,128)(2,1)S(1)} %collective-permute-done.14.refs_0_, ...), custom_call_target="tpu_custom_call", output_to_operand_aliasing={{0}: (4, {}), {1}: (5, {})} | custom-call | flops 6000000000 | bytes 1048576 | tf_op jit(solution)/shard_map/pallas_call | solution.py:448
  75.0 2.9 %collective-permute-done.22.w1 = bf16[2,8,64,256]{3,2,1,0:T(8,128)(2,1)S(1)} collective-permute-done((bf16[2,8,64,256]{3,2,1,0:T(8,128)(2,1)S(1)}, bf16[2,8,64,256]{3,2,1,0:T(8,128)(2,1)S(1)}, u32[]{:S(2)}, u32[]{:S(2)}) %collective-permute-start.22) | collective-permute-done | bytes 524320 | tf_op jit(solution)/shard_map/ppermute | solution.py:51
  77.9 0.4 collective-permute-start.23
  78.4 1.3 %collective-permute-start.20 = (bf16[144,1024]{1,0:T(8,128)(2,1)S(1)}, bf16[144,1024]{1,0:T(8,128)(2,1)S(1)}, u32[]{:S(2)}, u32[]{:S(2)}) collective-permute-start(bf16[144,1024]{1,0:T(8,128)(2,1)S(1)} %collective-permute-done.19.refs_1_), channel_id=1, source_target_pairs={{192,160},{224,192},{0,224},{193,161},{225,193},{1,225},{194,162},... | collective-permute-start | bytes 884744 | tf_op jit(solution)/shard_map/ppermute | solution.py:65
  79.7 4.6 %collective-permute-start.16 = (bf16[144,1024]{1,0:T(8,128)(2,1)S(1)}, bf16[144,1024]{1,0:T(8,128)(2,1)S(1)}, u32[]{:S(2)}, u32[]{:S(2)}) collective-permute-start(bf16[144,1024]{1,0:T(8,128)(2,1)S(1)} %collective-permute-done.15.refs_0_), channel_id=1, source_target_pairs={{64,96},{96,128},{128,160},{160,192},{192,224},{65,97},{97,129},{1... | collective-permute-start | bytes 884744 | tf_op jit(solution)/shard_map/ppermute | solution.py:61
  84.2 3.9 %shard_map.97 = (f32[2,80,2048]{2,1,0:T(8,128)S(1)}, f32[2,8,2048]{2,1,0:T(8,128)S(1)}, f32[8,256]{1,0:T(8,128)S(1)}) custom-call(s32[4]{0:T(128)S(1)} %pad_add_fusion.1.idx, bf16[128,2048]{1,0:T(8,128)(2,1)S(1)} %get-tuple-element.44.q, bf16[144,1024]{1,0:T(8,128)(2,1)S(1)} %collective-permute-done.15.refs_0_, ...), custom_call_target="tpu_custom_call", output_to_operand_aliasing={{0}: (4, {}), {1}: (5, {})} | custom-call | flops 6000000000 | bytes 1048576 | tf_op jit(solution)/shard_map/pallas_call | solution.py:448
  88.2 1.9 %collective-permute-done.16.refs_0_ = bf16[144,1024]{1,0:T(8,128)(2,1)S(1)} collective-permute-done((bf16[144,1024]{1,0:T(8,128)(2,1)S(1)}, bf16[144,1024]{1,0:T(8,128)(2,1)S(1)}, u32[]{:S(2)}, u32[]{:S(2)}) %collective-permute-start.16) | collective-permute-done | bytes 294944 | tf_op jit(solution)/shard_map/ppermute | solution.py:61
  90.1 4.3 %collective-permute-start.17 = (bf16[144,1024]{1,0:T(8,128)(2,1)S(1)}, bf16[144,1024]{1,0:T(8,128)(2,1)S(1)}, u32[]{:S(2)}, u32[]{:S(2)}) collective-permute-start(bf16[144,1024]{1,0:T(8,128)(2,1)S(1)} %collective-permute-done.16.refs_0_), channel_id=1, source_target_pairs={{96,128},{128,160},{160,192},{192,224},{97,129},{129,161},{161,193... | collective-permute-start | bytes 884744 | tf_op jit(solution)/shard_map/ppermute | solution.py:61
  94.4 6.7 %shard_map.98 = (f32[2,80,2048]{2,1,0:T(8,128)S(1)}, f32[2,8,2048]{2,1,0:T(8,128)S(1)}, f32[8,256]{1,0:T(8,128)S(1)}) custom-call(s32[4]{0:T(128)S(1)} %pad_add_fusion.1.idx, bf16[128,2048]{1,0:T(8,128)(2,1)S(1)} %get-tuple-element.44.q, bf16[144,1024]{1,0:T(8,128)(2,1)S(1)} %collective-permute-done.16.refs_0_, ...), custom_call_target="tpu_custom_call", output_to_operand_aliasing={{0}: (4, {}), {1}: (5, {})} | custom-call | flops 6000000000 | bytes 1048576 | tf_op jit(solution)/shard_map/pallas_call | solution.py:448
  101.2 4.0 %shard_map.99 = (f32[72,1024]{1,0:T(8,128)S(1)}, f32[72,1024]{1,0:T(8,128)S(1)}) custom-call(s32[4]{0:T(128)S(1)} %pad_add_fusion.1.idx, bf16[128,2048]{1,0:T(8,128)(2,1)S(1)} %get-tuple-element.44.q, bf16[144,1024]{1,0:T(8,128)(2,1)S(1)} %collective-permute-done.17.refs_0_, f32[2,80,2048]{2,1,0:T(8,128)S(1)} %get-tuple-element.55.refs_1_, ...), custom_call_target="tpu_custom_call" | custom-call | flops 6000000000 | bytes 1048576 | tf_op jit(solution)/shard_map/pallas_call | solution.py:448
  105.3 1.6 %collective-permute-done.21.sib = f32[72,1024]{1,0:T(8,128)S(1)} collective-permute-done((f32[72,1024]{1,0:T(8,128)S(1)}, f32[72,1024]{1,0:T(8,128)S(1)}, u32[]{:S(2)}, u32[]{:S(2)}) %collective-permute-start.21) | collective-permute-done | bytes 294944 | tf_op jit(solution)/shard_map/ppermute | solution.py:51
  107.0 0.9 reshape.4
  107.9 6.6 %all-to-all-start.1 = ((bf16[16,2,2048]{2,1,0:T(2,128)(2,1)}), bf16[16,2,2048]{2,1,0:T(2,128)(2,1)S(1)}, u32[]{:S(2)}, u32[]{:S(2)}) async-start(bf16[16,2,2048]{2,1,0:T(2,128)(2,1)} %reshape.4), calls=%async_computation.1 | async-start | bytes 262144 | tf_op jit(solution)/shard_map/all_to_all | solution.py:461
  114.6 0.8 copy-done.2
  115.4 1.0 copy-done.1
  116.4 1.0 copy-done.3
  117.5 1.0 shard_map.101.w
  118.5 3.9 %all-to-all-done.1 = bf16[16,2,2048]{2,1,0:T(2,128)(2,1)S(1)} async-done(((bf16[16,2,2048]{2,1,0:T(2,128)(2,1)}), bf16[16,2,2048]{2,1,0:T(2,128)(2,1)S(1)}, u32[]{:S(2)}, u32[]{:S(2)}) %all-to-all-start.1) | async-done | bytes 131104 | tf_op jit(solution)/shard_map/all_to_all | solution.py:461
  122.6 1.5 %shard_map.102 = bf16[64,1024]{1,0:T(8,128)(2,1)} custom-call(bf16[16,64,64]{2,1,0:T(8,128)(2,1)S(1)} %reshape.5.att, f32[1,1024]{1,0:T(1,128)S(1)} %bitcast.13, bf16[1024,1024]{1,0:T(8,128)(2,1)S(1)} %shard_map.101.w), custom_call_target="tpu_custom_call" | custom-call | flops 100000000 | bytes 1048576 | tf_op jit(solution)/shard_map/pallas_call | solution.py:462
  (43 shorter events, 1.4 us)
Async XLA Ops:
  2.1 50.4 %copy-start.5 = (f32[1024]{0:T(1024)S(1)}, f32[1024]{0:T(1024)}, u32[]{:S(2)}) copy-start(f32[1024]{0:T(1024)} %param.10) | copy-start | bytes 12292
  2.1 50.4 %copy-start.6 = (f32[4]{0:T(128)S(1)}, f32[4]{0:T(128)}, u32[]{:S(2)}) copy-start(f32[4]{0:T(128)} %offs.1) | copy-start | bytes 52
  2.1 5.9 %collective-permute-start.6 = (bf16[48,1024]{1,0:T(8,128)(2,1)S(1)}, bf16[48,1024]{1,0:T(8,128)(2,1)S(1)}, u32[]{:S(2)}, u32[]{:S(2)}) collective-permute-start(bf16[48,1024]{1,0:T(8,128)(2,1)S(1)} %get-tuple-element.37), channel_id=1, source_target_pairs={{0,8},{8,16},{16,24},{24,0},{1,9},{9,17},{17,25},{25,1},{2,10},{10... | collective-permute-start | bytes 294920 | tf_op jit(solution)/shard_map/ppermute | solution.py:51
  3.7 4.6 %collective-permute-start.8 = (bf16[48,1024]{1,0:T(8,128)(2,1)S(1)}, bf16[48,1024]{1,0:T(8,128)(2,1)S(1)}, u32[]{:S(2)}, u32[]{:S(2)}) collective-permute-start(bf16[48,1024]{1,0:T(8,128)(2,1)S(1)} %get-tuple-element.38), channel_id=1, source_target_pairs={{0,24},{8,0},{16,8},{24,16},{1,25},{9,1},{17,9},{25,17},{2,26},{10... | collective-permute-start | bytes 294920 | tf_op jit(solution)/shard_map/ppermute | solution.py:51
  8.0 5.8 %collective-permute-start.7 = (bf16[48,1024]{1,0:T(8,128)(2,1)S(1)}, bf16[48,1024]{1,0:T(8,128)(2,1)S(1)}, u32[]{:S(2)}, u32[]{:S(2)}) collective-permute-start(bf16[48,1024]{1,0:T(8,128)(2,1)S(1)} %collective-permute-done.6.r1), channel_id=1, source_target_pairs={{0,8},{8,16},{16,24},{24,0},{1,9},{9,17},{17,25},{25,1},{2,10},{10... | collective-permute-start | bytes 294920 | tf_op jit(solution)/shard_map/ppermute | solution.py:51
  14.7 22.0 %all-to-all-start = ((bf16[8,128,256]{2,1,0:T(8,128)(2,1)}), bf16[8,128,256]{2,1,0:T(8,128)(2,1)S(1)}, u32[]{:S(2)}, u32[]{:S(2)}) async-start(bf16[8,128,256]{2,1,0:T(8,128)(2,1)} %get-tuple-element.40), calls=%async_computation | async-start | bytes 1048576 | tf_op jit(solution)/shard_map/all_to_all | solution.py:394
  21.5 15.0 %collective-permute-start.2 = (bf16[32,1024]{1,0:T(8,128)(2,1)S(1)}, bf16[32,1024]{1,0:T(8,128)(2,1)S(1)}, u32[]{:S(2)}, u32[]{:S(2)}) collective-permute-start(bf16[32,1024]{1,0:T(8,128)(2,1)S(1)} %get-tuple-element.33), channel_id=1, source_target_pairs={{0,3},{1,0},{2,1},{3,2},{4,7},{5,4},{6,5},{7,6},{8,11},{9,8},{10,9... | collective-permute-start | bytes 196616 | tf_op jit(solution)/shard_map/ppermute | solution.py:51
  24.5 5.8 %collective-permute-start = (bf16[32,1024]{1,0:T(8,128)(2,1)S(1)}, bf16[32,1024]{1,0:T(8,128)(2,1)S(1)}, u32[]{:S(2)}, u32[]{:S(2)}) collective-permute-start(bf16[32,1024]{1,0:T(8,128)(2,1)S(1)} %get-tuple-element.33), channel_id=1, source_target_pairs={{0,1},{1,2},{2,3},{3,0},{4,5},{5,6},{6,7},{7,4},{8,9},{9,10},{10,1... | collective-permute-start | bytes 196616 | tf_op jit(solution)/shard_map/ppermute | solution.py:51
  30.3 6.2 %collective-permute-start.1 = (bf16[32,1024]{1,0:T(8,128)(2,1)S(1)}, bf16[32,1024]{1,0:T(8,128)(2,1)S(1)}, u32[]{:S(2)}, u32[]{:S(2)}) collective-permute-start(bf16[32,1024]{1,0:T(8,128)(2,1)S(1)} %collective-permute-done), channel_id=1, source_target_pairs={{0,1},{1,2},{2,3},{3,0},{4,5},{5,6},{6,7},{7,4},{8,9},{9,10},{10,1... | collective-permute-start | bytes 196616 | tf_op jit(solution)/shard_map/ppermute | solution.py:51
  36.5 7.7 %collective-permute-start.3 = (bf16[128,1024]{1,0:T(8,128)(2,1)S(1)}, bf16[128,1024]{1,0:T(8,128)(2,1)S(1)}, u32[]{:S(2)}, u32[]{:S(2)}) collective-permute-start(bf16[128,1024]{1,0:T(8,128)(2,1)S(1)} %constant_dynamic-update-slice_fusion.refs_0_), channel_id=1, source_target_pairs={{0,8},{8,16},{16,24},{24,0},{1,9},{9,17},{17,25},{25,1},{2,10},{10... | collective-permute-start | bytes 786440 | tf_op jit(solution)/shard_map/ppermute | solution.py:51
  36.6 7.7 %collective-permute-start.9 = (bf16[128,1024]{1,0:T(8,128)(2,1)S(1)}, bf16[128,1024]{1,0:T(8,128)(2,1)S(1)}, u32[]{:S(2)}, u32[]{:S(2)}) collective-permute-start(bf16[128,1024]{1,0:T(8,128)(2,1)S(1)} %get-tuple-element.39.refs_4_), channel_id=1, source_target_pairs={{0,1},{1,2},{2,3},{3,0},{4,5},{5,6},{6,7},{7,4},{8,9},{9,10},{10,1... | collective-permute-start | bytes 786440 | tf_op jit(solution)/shard_map/ppermute | solution.py:51
  36.7 15.8 %collective-permute-start.12 = (bf16[8,128,256]{2,1,0:T(8,128)(2,1)S(1)}, bf16[8,128,256]{2,1,0:T(8,128)(2,1)S(1)}, u32[]{:S(2)}, u32[]{:S(2)}) collective-permute-start(bf16[8,128,256]{2,1,0:T(8,128)(2,1)S(1)} %all-to-all-done.refs_9_), channel_id=1, source_target_pairs={{0,4},{4,0},{1,5},{5,1},{2,6},{6,2},{3,7},{7,3},{8,12},{12,8},{9,1... | collective-permute-start | bytes 1572872 | tf_op jit(solution)/shard_map/ppermute | solution.py:51
  36.8 9.3 %collective-permute-start.5 = (bf16[128,1024]{1,0:T(8,128)(2,1)S(1)}, bf16[128,1024]{1,0:T(8,128)(2,1)S(1)}, u32[]{:S(2)}, u32[]{:S(2)}) collective-permute-start(bf16[128,1024]{1,0:T(8,128)(2,1)S(1)} %constant_dynamic-update-slice_fusion.refs_0_), channel_id=1, source_target_pairs={{0,24},{8,0},{16,8},{24,16},{1,25},{9,1},{17,9},{25,17},{2,26},{10... | collective-permute-start | bytes 786440 | tf_op jit(solution)/shard_map/ppermute | solution.py:51
  39.9 9.1 %collective-permute-start.11 = (bf16[128,1024]{1,0:T(8,128)(2,1)S(1)}, bf16[128,1024]{1,0:T(8,128)(2,1)S(1)}, u32[]{:S(2)}, u32[]{:S(2)}) collective-permute-start(bf16[128,1024]{1,0:T(8,128)(2,1)S(1)} %get-tuple-element.39.refs_4_), channel_id=1, source_target_pairs={{0,3},{1,0},{2,1},{3,2},{4,7},{5,4},{6,5},{7,6},{8,11},{9,8},{10,9... | collective-permute-start | bytes 786440 | tf_op jit(solution)/shard_map/ppermute | solution.py:51
  44.2 8.3 %collective-permute-start.4 = (bf16[128,1024]{1,0:T(8,128)(2,1)S(1)}, bf16[128,1024]{1,0:T(8,128)(2,1)S(1)}, u32[]{:S(2)}, u32[]{:S(2)}) collective-permute-start(bf16[128,1024]{1,0:T(8,128)(2,1)S(1)} %collective-permute-done.3.refs_1_), channel_id=1, source_target_pairs={{0,8},{8,16},{16,24},{24,0},{1,9},{9,17},{17,25},{25,1},{2,10},{10... | collective-permute-start | bytes 786440 | tf_op jit(solution)/shard_map/ppermute | solution.py:51
  44.3 8.3 %collective-permute-start.10 = (bf16[128,1024]{1,0:T(8,128)(2,1)S(1)}, bf16[128,1024]{1,0:T(8,128)(2,1)S(1)}, u32[]{:S(2)}, u32[]{:S(2)}) collective-permute-start(bf16[128,1024]{1,0:T(8,128)(2,1)S(1)} %collective-permute-done.9.refs_5_), channel_id=1, source_target_pairs={{0,1},{1,2},{2,3},{3,0},{4,5},{5,6},{6,7},{7,4},{8,9},{9,10},{10,1... | collective-permute-start | bytes 786440 | tf_op jit(solution)/shard_map/ppermute | solution.py:51
  54.7 1.7 %collective-permute-start.13 = (bf16[80,1024]{1,0:T(8,128)(2,1)S(1)}, bf16[80,1024]{1,0:T(8,128)(2,1)S(1)}, u32[]{:S(2)}, u32[]{:S(2)}) collective-permute-start(bf16[80,1024]{1,0:T(8,128)(2,1)S(1)} %get-tuple-element.41.q_own), channel_id=1, source_target_pairs={{0,4},{4,0},{1,5},{5,1},{2,6},{6,2},{3,7},{7,3},{8,12},{12,8},{9,1... | collective-permute-start | bytes 491528 | tf_op jit(solution)/shard_map/ppermute | solution.py:51
  57.0 8.0 %collective-permute-start.18 = (bf16[144,1024]{1,0:T(8,128)(2,1)S(1)}, bf16[144,1024]{1,0:T(8,128)(2,1)S(1)}, u32[]{:S(2)}, u32[]{:S(2)}) collective-permute-start(bf16[144,1024]{1,0:T(8,128)(2,1)S(1)} %get-tuple-element.45.pay), channel_id=1, source_target_pairs={{0,224},{32,0},{64,32},{1,225},{33,1},{65,33},{2,226},{34,2},{66,3... | collective-permute-start | bytes 884744 | tf_op jit(solution)/shard_map/ppermute | solution.py:65
  57.7 10.9 %collective-permute-start.14 = (bf16[144,1024]{1,0:T(8,128)(2,1)S(1)}, bf16[144,1024]{1,0:T(8,128)(2,1)S(1)}, u32[]{:S(2)}, u32[]{:S(2)}) collective-permute-start(bf16[144,1024]{1,0:T(8,128)(2,1)S(1)} %get-tuple-element.45.pay), channel_id=1, source_target_pairs={{0,32},{32,64},{64,96},{96,128},{128,160},{160,192},{192,224},{1,3... | collective-permute-start | bytes 884744 | tf_op jit(solution)/shard_map/ppermute | solution.py:61
  62.9 51.7 %collective-permute-start.24 = (bf16[2,8,64,256]{3,2,1,0:T(8,128)(2,1)S(1)}, bf16[2,8,64,256]{3,2,1,0:T(8,128)(2,1)S(1)}, u32[]{:S(2)}, u32[]{:S(2)}) collective-permute-start(bf16[2,8,64,256]{3,2,1,0:T(8,128)(2,1)S(1)} %pad_maximum_fusion.w0), channel_id=1, source_target_pairs={{0,3},{1,0},{2,1},{3,2},{4,7},{5,4},{6,5},{7,6},{8,11},{9,8},{10,9... | collective-permute-start | bytes 1572872 | tf_op jit(solution)/shard_map/ppermute | solution.py:51
  63.1 14.8 %collective-permute-start.22 = (bf16[2,8,64,256]{3,2,1,0:T(8,128)(2,1)S(1)}, bf16[2,8,64,256]{3,2,1,0:T(8,128)(2,1)S(1)}, u32[]{:S(2)}, u32[]{:S(2)}) collective-permute-start(bf16[2,8,64,256]{3,2,1,0:T(8,128)(2,1)S(1)} %pad_maximum_fusion.w0), channel_id=1, source_target_pairs={{0,1},{1,2},{2,3},{3,0},{4,5},{5,6},{6,7},{7,4},{8,9},{9,10},{10,1... | collective-permute-start | bytes 1572872 | tf_op jit(solution)/shard_map/ppermute | solution.py:51
  65.0 13.4 %collective-permute-start.19 = (bf16[144,1024]{1,0:T(8,128)(2,1)S(1)}, bf16[144,1024]{1,0:T(8,128)(2,1)S(1)}, u32[]{:S(2)}, u32[]{:S(2)}) collective-permute-start(bf16[144,1024]{1,0:T(8,128)(2,1)S(1)} %collective-permute-done.18.refs_1_), channel_id=1, source_target_pairs={{224,192},{0,224},{32,0},{225,193},{1,225},{33,1},{226,194},{2,226... | collective-permute-start | bytes 884744 | tf_op jit(solution)/shard_map/ppermute | solution.py:65
  68.6 11.0 %collective-permute-start.15 = (bf16[144,1024]{1,0:T(8,128)(2,1)S(1)}, bf16[144,1024]{1,0:T(8,128)(2,1)S(1)}, u32[]{:S(2)}, u32[]{:S(2)}) collective-permute-start(bf16[144,1024]{1,0:T(8,128)(2,1)S(1)} %collective-permute-done.14.refs_0_), channel_id=1, source_target_pairs={{32,64},{64,96},{96,128},{128,160},{160,192},{192,224},{33,65},{65... | collective-permute-start | bytes 884744 | tf_op jit(solution)/shard_map/ppermute | solution.py:61
  77.9 10.2 %copy-start = (bf16[2,8,64,256]{3,2,1,0:T(8,128)(2,1)}, bf16[2,8,64,256]{3,2,1,0:T(8,128)(2,1)S(1)}, u32[]{:S(2)}) copy-start(bf16[2,8,64,256]{3,2,1,0:T(8,128)(2,1)S(1)} %collective-permute-done.22.w1) | copy-start | bytes 1572868
  77.9 36.6 %collective-permute-start.23 = (bf16[2,8,64,256]{3,2,1,0:T(8,128)(2,1)S(1)}, bf16[2,8,64,256]{3,2,1,0:T(8,128)(2,1)S(1)}, u32[]{:S(2)}, u32[]{:S(2)}) collective-permute-start(bf16[2,8,64,256]{3,2,1,0:T(8,128)(2,1)S(1)} %collective-permute-done.22.w1), channel_id=1, source_target_pairs={{0,1},{1,2},{2,3},{3,0},{4,5},{5,6},{6,7},{7,4},{8,9},{9,10},{10,1... | collective-permute-start | bytes 1572872 | tf_op jit(solution)/shard_map/ppermute | solution.py:51
  78.4 16.0 %collective-permute-start.20 = (bf16[144,1024]{1,0:T(8,128)(2,1)S(1)}, bf16[144,1024]{1,0:T(8,128)(2,1)S(1)}, u32[]{:S(2)}, u32[]{:S(2)}) collective-permute-start(bf16[144,1024]{1,0:T(8,128)(2,1)S(1)} %collective-permute-done.19.refs_1_), channel_id=1, source_target_pairs={{192,160},{224,192},{0,224},{193,161},{225,193},{1,225},{194,162},... | collective-permute-start | bytes 884744 | tf_op jit(solution)/shard_map/ppermute | solution.py:65
  79.7 10.4 %collective-permute-start.16 = (bf16[144,1024]{1,0:T(8,128)(2,1)S(1)}, bf16[144,1024]{1,0:T(8,128)(2,1)S(1)}, u32[]{:S(2)}, u32[]{:S(2)}) collective-permute-start(bf16[144,1024]{1,0:T(8,128)(2,1)S(1)} %collective-permute-done.15.refs_0_), channel_id=1, source_target_pairs={{64,96},{96,128},{128,160},{160,192},{192,224},{65,97},{97,129},{1... | collective-permute-start | bytes 884744 | tf_op jit(solution)/shard_map/ppermute | solution.py:61
  90.1 11.1 %collective-permute-start.17 = (bf16[144,1024]{1,0:T(8,128)(2,1)S(1)}, bf16[144,1024]{1,0:T(8,128)(2,1)S(1)}, u32[]{:S(2)}, u32[]{:S(2)}) collective-permute-start(bf16[144,1024]{1,0:T(8,128)(2,1)S(1)} %collective-permute-done.16.refs_0_), channel_id=1, source_target_pairs={{96,128},{128,160},{160,192},{192,224},{97,129},{129,161},{161,193... | collective-permute-start | bytes 884744 | tf_op jit(solution)/shard_map/ppermute | solution.py:61
  105.2 1.7 %collective-permute-start.21 = (f32[72,1024]{1,0:T(8,128)S(1)}, f32[72,1024]{1,0:T(8,128)S(1)}, u32[]{:S(2)}, u32[]{:S(2)}) collective-permute-start(f32[72,1024]{1,0:T(8,128)S(1)} %get-tuple-element.59), channel_id=1, source_target_pairs={{0,4},{4,0},{1,5},{5,1},{2,6},{6,2},{3,7},{7,3},{8,12},{12,8},{9,1... | collective-permute-start | bytes 884744 | tf_op jit(solution)/shard_map/ppermute | solution.py:51
  107.9 14.7 %copy-start.4 = (f32[1024]{0:T(1024)S(1)}, f32[1024]{0:T(1024)}, u32[]{:S(2)}) copy-start(f32[1024]{0:T(1024)} %param.17) | copy-start | bytes 12292
  107.9 14.4 %all-to-all-start.1 = ((bf16[16,2,2048]{2,1,0:T(2,128)(2,1)}), bf16[16,2,2048]{2,1,0:T(2,128)(2,1)S(1)}, u32[]{:S(2)}, u32[]{:S(2)}) async-start(bf16[16,2,2048]{2,1,0:T(2,128)(2,1)} %reshape.4), calls=%async_computation.1 | async-start | bytes 262144 | tf_op jit(solution)/shard_map/all_to_all | solution.py:461
  114.6 0.8 copy-start.2
  115.4 1.0 copy-start.1
  116.4 1.0 copy-start.3

commit v6 on v4

--- a/solution.py
+++ b/solution.py
@@ -20,7 +20,7 @@
 BLK = 256
 KEYS = 1024
 QS = 2048
-PAY = 144
+PAY = 136
 EPS = 1e-06
 LOW = -1e30
 F32 = jnp.float32
@@ -53,6 +53,12 @@
 
 def direct(x, axis):
     return [x] + [shift(x, axis, k) for k in range(1, SIZES[axis])]
+
+
+def gather(x, axis):
+    one, three = shift(x, axis, 1), shift(x, axis, -1)
+    two = shift(one, axis, 1)
+    return [x, one, two, three]
 
 
 def step_right(x, k):
@@ -176,32 +182,32 @@
         bases.append(ahead + jnp.where(c == 1, sib[b], 0.0))
         ahead = ahead + (own[b] + sib[b])
     total = ahead
-    pay_out[0:64, :] = kv[0:64, :]
-    pay_out[80:144, :] = kv[64:128, :]
-    row = lax.broadcasted_iota(jnp.int32, (16, BLK), 0)
+    pay_out[0:64, :] = kv[64:128, :]
+    pay_out[64:128, :] = kv[0:64, :]
+    row = lax.broadcasted_iota(jnp.int32, (8, BLK), 0)
     for b in range(4):
         lanes = slice(b * BLK, (b + 1) * BLK)
         bias = (total - bases[b]) - cum_own[:, lanes]
         parts = [p[0:1].astype(F32) for p in three_parts(bias)]
         totals = [p[0:1].astype(F32) for p in three_parts(jnp.broadcast_to(total, bias.shape))]
-        block = jnp.zeros((16, BLK), F32)
+        block = jnp.zeros((8, BLK), F32)
         for i, part in enumerate(parts + totals):
             block = jnp.where(row == i, part, block)
-        pay_out[64:80, lanes] = block.astype(BF16)
+        pay_out[128:136, lanes] = block.astype(BF16)
 
 
 def chunk_total(pay):
-    rows = pay[64:80, 0:BLK].astype(F32)
+    rows = pay[128:136, 0:BLK].astype(F32)
     return rows[3:4] + rows[4:5] + rows[5:6]
 
 
 def place_chunk(pay, i, kx, vx):
-    fill = jnp.zeros((48, 128), F32)
+    fill = jnp.zeros((56, 128), F32)
     for r in range(8):
         lanes = slice(r * 128, (r + 1) * 128)
-        tile = jnp.concatenate([pay[0:80, lanes].astype(F32), fill], axis=0)
+        tile = jnp.concatenate([pay[64:136, lanes].astype(F32), fill], axis=0)
         kx[i, lanes, :] = tile.T.astype(BF16)
-    vx[i, 0:64, :] = pay[80:144, :]
+    vx[i, 0:64, :] = pay[0:64, :]
     vx[i, 64:80, :] = jnp.ones((16, KEYS), BF16)
 
 
@@ -387,7 +393,8 @@
         spread_body, (sds((NZ, 128, 256), BF16), sds((128, D), BF16)), [VMEM] * 6
     )(hi, p0, o0, *got)
     w_own = lax.all_to_all(chunk, "z", 0, 0, tiled=True)
-    toks = direct(jnp.concatenate(tok_a, axis=0), "x") + direct(tok_b, "y")
+    toks_b = gather(tok_b, "y")
+    toks = gather(jnp.concatenate(tok_a, axis=0), "x") + toks_b
     w_sib = shift(w_own, "c", 1)
 
     q_own, kv, cum_own = call(

time: 123 us -> 118 us (0.959)
  waiting for transfers between devices: 34.8 us -> 29.3 us
    ppermute x18, waiting for transfers between devices: 25.2 us -> 20.4 us  [shift(): return lax.ppermute(x, axis, [(i, (i + k) % n) for i in range(n)])]
    ppermute x4, waiting for transfers between devices: 6.51 us -> 4.93 us  [step_right(): return lax.ppermute(x, 'z', [(i, i + 1) for i in range(k - 1, NZ - 1)])]
  transfers between devices with their start and end apart: 27 -> 27, of which waited for: 15 -> 15; matrix products, arithmetic and copies ran while one was open for 1% -> 1% of each run, Pallas kernels for 18% -> 19%
where the time goes in v6:
time: 118 us; the launch traced here: 117 us
  starting transfers between devices  53.3 us (45%)
  waiting for transfers between devices  29.3 us (25%)
  Pallas kernels  28.6 us (24%)
  local copies, waits for them, and re-layouts  4.87 us (4%)
    ppermute x18, waiting for transfers between devices, shift(): return lax.ppermute(x, axis, [(i, (i + k) % n) for i in range(n)])  20.4 us
    ppermute x18, starting transfers between devices, shift(): return lax.ppermute(x, axis, [(i, (i + k) % n) for i in range(n)])  19.7 us
    pallas_call x4, Pallas kernels, shards(): call(functools.partial(step_body, k), outs, [SMEM] + [VMEM] * (len(ins) -...  18.5 us
    ppermute x4, starting transfers between devices, step_right(): return lax.ppermute(x, 'z', [(i, i + 1) for i in range(k - 1, NZ - 1)])  18 us
    all_to_all x1, starting transfers between devices, shards(): w_own = lax.all_to_all(chunk, 'z', 0, 0, tiled=True)  6.75 us
    all_to_all x1, starting transfers between devices, shards(): att = lax.all_to_all(att.reshape(16, 64, HD), ('x', 'y'), 0, 0, tiled=True)  6.15 us
    ppermute x4, waiting for transfers between devices, step_right(): return lax.ppermute(x, 'z', [(i, i + 1) for i in range(k - 1, NZ - 1)])  4.93 us
    unnamed x19, local copies, waits for them, and re-layouts  4.82 us
  transfers between devices with their start and end apart: 27, of which 15 were waited for; matrix products, arithmetic and copies ran while one was open for 1% of the time, Pallas kernels for 19%

profile of v6, /device:TPU:160, one launch (start us, length us, event | category | flops | bytes accessed | tf_op | source)
XLA Modules:
  0.0 117.5 jit_solution(13672195404755888519)
XLA Ops:
  0.1 1.0 pad_add_fusion.rows
  1.1 1.0 shard_map.91
  2.1 1.6 %collective-permute-start.6 = (bf16[48,1024]{1,0:T(8,128)(2,1)S(1)}, bf16[48,1024]{1,0:T(8,128)(2,1)S(1)}, u32[]{:S(2)}, u32[]{:S(2)}) collective-permute-start(bf16[48,1024]{1,0:T(8,128)(2,1)S(1)} %get-tuple-element.38), channel_id=1, source_target_pairs={{0,8},{8,16},{16,24},{24,0},{1,9},{9,17},{17,25},{25,1},{2,10},{10... | collective-permute-start | bytes 294920 | tf_op jit(solution)/shard_map/ppermute | solution.py:51
  3.7 2.7 %collective-permute-start.7 = (bf16[48,1024]{1,0:T(8,128)(2,1)S(1)}, bf16[48,1024]{1,0:T(8,128)(2,1)S(1)}, u32[]{:S(2)}, u32[]{:S(2)}) collective-permute-start(bf16[48,1024]{1,0:T(8,128)(2,1)S(1)} %get-tuple-element.39), channel_id=1, source_target_pairs={{0,16},{8,24},{16,0},{24,8},{1,17},{9,25},{17,1},{25,9},{2,18},{10... | collective-permute-start | bytes 294920 | tf_op jit(solution)/shard_map/ppermute | solution.py:51
  6.4 1.4 %collective-permute-start.8 = (bf16[48,1024]{1,0:T(8,128)(2,1)S(1)}, bf16[48,1024]{1,0:T(8,128)(2,1)S(1)}, u32[]{:S(2)}, u32[]{:S(2)}) collective-permute-start(bf16[48,1024]{1,0:T(8,128)(2,1)S(1)} %get-tuple-element.40), channel_id=1, source_target_pairs={{0,24},{8,0},{16,8},{24,16},{1,25},{9,1},{17,9},{25,17},{2,26},{10... | collective-permute-start | bytes 294920 | tf_op jit(solution)/shard_map/ppermute | solution.py:51
  8.2 2.8 %collective-permute-done.7.r2 = bf16[48,1024]{1,0:T(8,128)(2,1)S(1)} collective-permute-done((bf16[48,1024]{1,0:T(8,128)(2,1)S(1)}, bf16[48,1024]{1,0:T(8,128)(2,1)S(1)}, u32[]{:S(2)}, u32[]{:S(2)}) %collective-permute-start.7) | collective-permute-done | bytes 98336 | tf_op jit(solution)/shard_map/ppermute | solution.py:51
  11.0 0.9 shard_map.92
  11.9 6.8 %all-to-all-start = ((bf16[8,128,256]{2,1,0:T(8,128)(2,1)}), bf16[8,128,256]{2,1,0:T(8,128)(2,1)S(1)}, u32[]{:S(2)}, u32[]{:S(2)}) async-start(bf16[8,128,256]{2,1,0:T(8,128)(2,1)} %get-tuple-element.42), calls=%async_computation | async-start | bytes 1048576 | tf_op jit(solution)/shard_map/all_to_all | solution.py:395
  18.6 3.0 %collective-permute-start.2 = (bf16[32,1024]{1,0:T(8,128)(2,1)S(1)}, bf16[32,1024]{1,0:T(8,128)(2,1)S(1)}, u32[]{:S(2)}, u32[]{:S(2)}) collective-permute-start(bf16[32,1024]{1,0:T(8,128)(2,1)S(1)} %get-tuple-element.34), channel_id=1, source_target_pairs={{0,3},{1,0},{2,1},{3,2},{4,7},{5,4},{6,5},{7,6},{8,11},{9,8},{10,9... | collective-permute-start | bytes 196616 | tf_op jit(solution)/shard_map/ppermute | solution.py:51
  22.3 1.0 collective-permute-start
  23.3 4.9 %collective-permute-done = bf16[32,1024]{1,0:T(8,128)(2,1)S(1)} collective-permute-done((bf16[32,1024]{1,0:T(8,128)(2,1)S(1)}, bf16[32,1024]{1,0:T(8,128)(2,1)S(1)}, u32[]{:S(2)}, u32[]{:S(2)}) %collective-permute-start) | collective-permute-done | bytes 65568 | tf_op jit(solution)/shard_map/ppermute | solution.py:51
  28.2 1.4 %collective-permute-start.3 = (bf16[128,1024]{1,0:T(8,128)(2,1)S(1)}, bf16[128,1024]{1,0:T(8,128)(2,1)S(1)}, u32[]{:S(2)}, u32[]{:S(2)}) collective-permute-start(bf16[128,1024]{1,0:T(8,128)(2,1)S(1)} %constant_dynamic-update-slice_fusion.refs_0_), channel_id=1, source_target_pairs={{0,8},{8,16},{16,24},{24,0},{1,9},{9,17},{17,25},{25,1},{2,10},{10... | collective-permute-start | bytes 786440 | tf_op jit(solution)/shard_map/ppermute | solution.py:51
  29.6 1.0 all-to-all-done.refs_9_
  30.6 2.7 %collective-permute-start.5 = (bf16[128,1024]{1,0:T(8,128)(2,1)S(1)}, bf16[128,1024]{1,0:T(8,128)(2,1)S(1)}, u32[]{:S(2)}, u32[]{:S(2)}) collective-permute-start(bf16[128,1024]{1,0:T(8,128)(2,1)S(1)} %constant_dynamic-update-slice_fusion.refs_0_), channel_id=1, source_target_pairs={{0,24},{8,0},{16,8},{24,16},{1,25},{9,1},{17,9},{25,17},{2,26},{10... | collective-permute-start | bytes 786440 | tf_op jit(solution)/shard_map/ppermute | solution.py:51
  33.2 3.0 %collective-permute-start.11 = (bf16[128,1024]{1,0:T(8,128)(2,1)S(1)}, bf16[128,1024]{1,0:T(8,128)(2,1)S(1)}, u32[]{:S(2)}, u32[]{:S(2)}) collective-permute-start(bf16[128,1024]{1,0:T(8,128)(2,1)S(1)} %get-tuple-element.41.refs_4_), channel_id=1, source_target_pairs={{0,3},{1,0},{2,1},{3,2},{4,7},{5,4},{6,5},{7,6},{8,11},{9,8},{10,9... | collective-permute-start | bytes 786440 | tf_op jit(solution)/shard_map/ppermute | solution.py:51
  36.2 0.9 collective-permute-done.9.refs_5_
  37.2 2.3 %collective-permute-done.5.refs_3_ = bf16[128,1024]{1,0:T(8,128)(2,1)S(1)} collective-permute-done((bf16[128,1024]{1,0:T(8,128)(2,1)S(1)}, bf16[128,1024]{1,0:T(8,128)(2,1)S(1)}, u32[]{:S(2)}, u32[]{:S(2)}) %collective-permute-start.5) | collective-permute-done | bytes 262176 | tf_op jit(solution)/shard_map/ppermute | solution.py:51
  39.5 2.7 %collective-permute-done.11.refs_7_ = bf16[128,1024]{1,0:T(8,128)(2,1)S(1)} collective-permute-done((bf16[128,1024]{1,0:T(8,128)(2,1)S(1)}, bf16[128,1024]{1,0:T(8,128)(2,1)S(1)}, u32[]{:S(2)}, u32[]{:S(2)}) %collective-permute-start.11) | collective-permute-done | bytes 262176 | tf_op jit(solution)/shard_map/ppermute | solution.py:51
  42.2 3.4 %collective-permute-done.4.refs_2_ = bf16[128,1024]{1,0:T(8,128)(2,1)S(1)} collective-permute-done((bf16[128,1024]{1,0:T(8,128)(2,1)S(1)}, bf16[128,1024]{1,0:T(8,128)(2,1)S(1)}, u32[]{:S(2)}, u32[]{:S(2)}) %collective-permute-start.4) | collective-permute-done | bytes 262176 | tf_op jit(solution)/shard_map/ppermute | solution.py:51
  45.7 2.1 %shard_map.93 = (bf16[80,1024]{1,0:T(8,128)(2,1)S(1)}, bf16[128,1024]{1,0:T(8,128)(2,1)S(1)}, f32[8,1024]{1,0:T(8,128)S(1)}) custom-call(s32[4]{0:T(128)S(1)} %pad_add_fusion.1.idx, f32[4]{0:T(128)S(1)} %copy-done.6, bf16[128,1024]{1,0:T(8,128)(2,1)S(1)} %constant_dynamic-update-slice_fusion.refs_0_, bf16[128,1024]{1,0:T(8,128)(2,1)S(1)} %collective-permute-done.3.refs_1_, ...), custom_call_target="tpu_custom_call" | custom-call | flops 2000000000 | bytes 1048576 | tf_op jit(solution)/shard_map/pallas_call | solution.py:400
  48.1 1.3 %collective-permute-done.13.q_sib = bf16[80,1024]{1,0:T(8,128)(2,1)S(1)} collective-permute-done((bf16[80,1024]{1,0:T(8,128)(2,1)S(1)}, bf16[80,1024]{1,0:T(8,128)(2,1)S(1)}, u32[]{:S(2)}, u32[]{:S(2)}) %collective-permute-start.13) | collective-permute-done | bytes 163872 | tf_op jit(solution)/shard_map/ppermute | solution.py:51
  50.0 0.7 collective-permute-start.18
  50.7 3.3 %collective-permute-start.14 = (bf16[136,1024]{1,0:T(8,128)(2,1)S(1)}, bf16[136,1024]{1,0:T(8,128)(2,1)S(1)}, u32[]{:S(2)}, u32[]{:S(2)}) collective-permute-start(bf16[136,1024]{1,0:T(8,128)(2,1)S(1)} %get-tuple-element.47.pay), channel_id=1, source_target_pairs={{0,32},{32,64},{64,96},{96,128},{128,160},{160,192},{192,224},{1,3... | collective-permute-start | bytes 835592 | tf_op jit(solution)/shard_map/ppermute | solution.py:65
  54.0 2.6 %shard_map.95 = (f32[2,80,2048]{2,1,0:T(8,128)S(1)}, f32[2,8,2048]{2,1,0:T(8,128)S(1)}, f32[8,256]{1,0:T(8,128)S(1)}) custom-call(s32[4]{0:T(128)S(1)} %pad_add_fusion.1.idx, bf16[128,2048]{1,0:T(8,128)(2,1)S(1)} %get-tuple-element.46.q, bf16[136,1024]{1,0:T(8,128)(2,1)S(1)} %get-tuple-element.47.pay), custom_call_target="tpu_custom_call" | custom-call | flops 3000000000 | bytes 1048576 | tf_op jit(solution)/shard_map/pallas_call | solution.py:429
  56.6 0.8 collective-permute-start.24
  57.8 0.9 collective-permute-start.22
  58.7 0.7 collective-permute-start.19
  59.4 1.9 %collective-permute-done.14.refs_0_ = bf16[136,1024]{1,0:T(8,128)(2,1)S(1)} collective-permute-done((bf16[136,1024]{1,0:T(8,128)(2,1)S(1)}, bf16[136,1024]{1,0:T(8,128)(2,1)S(1)}, u32[]{:S(2)}, u32[]{:S(2)}) %collective-permute-start.14) | collective-permute-done | bytes 278560 | tf_op jit(solution)/shard_map/ppermute | solution.py:65
  61.3 3.1 %collective-permute-start.15 = (bf16[136,1024]{1,0:T(8,128)(2,1)S(1)}, bf16[136,1024]{1,0:T(8,128)(2,1)S(1)}, u32[]{:S(2)}, u32[]{:S(2)}) collective-permute-start(bf16[136,1024]{1,0:T(8,128)(2,1)S(1)} %collective-permute-done.14.refs_0_), channel_id=1, source_target_pairs={{32,64},{64,96},{96,128},{128,160},{160,192},{192,224},{33,65},{65... | collective-permute-start | bytes 835592 | tf_op jit(solution)/shard_map/ppermute | solution.py:65
  64.4 3.9 %shard_map.96 = (f32[2,80,2048]{2,1,0:T(8,128)S(1)}, f32[2,8,2048]{2,1,0:T(8,128)S(1)}, f32[8,256]{1,0:T(8,128)S(1)}) custom-call(s32[4]{0:T(128)S(1)} %pad_add_fusion.1.idx, bf16[128,2048]{1,0:T(8,128)(2,1)S(1)} %get-tuple-element.46.q, bf16[136,1024]{1,0:T(8,128)(2,1)S(1)} %collective-permute-done.14.refs_0_, ...), custom_call_target="tpu_custom_call", output_to_operand_aliasing={{0}: (4, {}), {1}: (5, {})} | custom-call | flops 6000000000 | bytes 1048576 | tf_op jit(solution)/shard_map/pallas_call | solution.py:449
  68.3 1.3 %collective-permute-start.20 = (bf16[136,1024]{1,0:T(8,128)(2,1)S(1)}, bf16[136,1024]{1,0:T(8,128)(2,1)S(1)}, u32[]{:S(2)}, u32[]{:S(2)}) collective-permute-start(bf16[136,1024]{1,0:T(8,128)(2,1)S(1)} %collective-permute-done.19.refs_1_), channel_id=1, source_target_pairs={{192,160},{224,192},{0,224},{193,161},{225,193},{1,225},{194,162},... | collective-permute-start | bytes 835592 | tf_op jit(solution)/shard_map/ppermute | solution.py:69
  69.6 1.5 %collective-permute-done.15.refs_0_ = bf16[136,1024]{1,0:T(8,128)(2,1)S(1)} collective-permute-done((bf16[136,1024]{1,0:T(8,128)(2,1)S(1)}, bf16[136,1024]{1,0:T(8,128)(2,1)S(1)}, u32[]{:S(2)}, u32[]{:S(2)}) %collective-permute-start.15) | collective-permute-done | bytes 278560 | tf_op jit(solution)/shard_map/ppermute | solution.py:65
  71.1 5.5 %collective-permute-start.16 = (bf16[136,1024]{1,0:T(8,128)(2,1)S(1)}, bf16[136,1024]{1,0:T(8,128)(2,1)S(1)}, u32[]{:S(2)}, u32[]{:S(2)}) collective-permute-start(bf16[136,1024]{1,0:T(8,128)(2,1)S(1)} %collective-permute-done.15.refs_0_), channel_id=1, source_target_pairs={{64,96},{96,128},{128,160},{160,192},{192,224},{65,97},{97,129},{1... | collective-permute-start | bytes 835592 | tf_op jit(solution)/shard_map/ppermute | solution.py:65
  76.6 3.9 %shard_map.97 = (f32[2,80,2048]{2,1,0:T(8,128)S(1)}, f32[2,8,2048]{2,1,0:T(8,128)S(1)}, f32[8,256]{1,0:T(8,128)S(1)}) custom-call(s32[4]{0:T(128)S(1)} %pad_add_fusion.1.idx, bf16[128,2048]{1,0:T(8,128)(2,1)S(1)} %get-tuple-element.46.q, bf16[136,1024]{1,0:T(8,128)(2,1)S(1)} %collective-permute-done.15.refs_0_, ...), custom_call_target="tpu_custom_call", output_to_operand_aliasing={{0}: (4, {}), {1}: (5, {})} | custom-call | flops 6000000000 | bytes 1048576 | tf_op jit(solution)/shard_map/pallas_call | solution.py:449
  80.5 1.6 %collective-permute-done.16.refs_0_ = bf16[136,1024]{1,0:T(8,128)(2,1)S(1)} collective-permute-done((bf16[136,1024]{1,0:T(8,128)(2,1)S(1)}, bf16[136,1024]{1,0:T(8,128)(2,1)S(1)}, u32[]{:S(2)}, u32[]{:S(2)}) %collective-permute-start.16) | collective-permute-done | bytes 278560 | tf_op jit(solution)/shard_map/ppermute | solution.py:65
  82.1 6.1 %collective-permute-start.17 = (bf16[136,1024]{1,0:T(8,128)(2,1)S(1)}, bf16[136,1024]{1,0:T(8,128)(2,1)S(1)}, u32[]{:S(2)}, u32[]{:S(2)}) collective-permute-start(bf16[136,1024]{1,0:T(8,128)(2,1)S(1)} %collective-permute-done.16.refs_0_), channel_id=1, source_target_pairs={{96,128},{128,160},{160,192},{192,224},{97,129},{129,161},{161,193... | collective-permute-start | bytes 835592 | tf_op jit(solution)/shard_map/ppermute | solution.py:65
  88.2 6.7 %shard_map.98 = (f32[2,80,2048]{2,1,0:T(8,128)S(1)}, f32[2,8,2048]{2,1,0:T(8,128)S(1)}, f32[8,256]{1,0:T(8,128)S(1)}) custom-call(s32[4]{0:T(128)S(1)} %pad_add_fusion.1.idx, bf16[128,2048]{1,0:T(8,128)(2,1)S(1)} %get-tuple-element.46.q, bf16[136,1024]{1,0:T(8,128)(2,1)S(1)} %collective-permute-done.16.refs_0_, ...), custom_call_target="tpu_custom_call", output_to_operand_aliasing={{0}: (4, {}), {1}: (5, {})} | custom-call | flops 6000000000 | bytes 1048576 | tf_op jit(solution)/shard_map/pallas_call | solution.py:449
  95.0 4.0 %shard_map.99 = (f32[72,1024]{1,0:T(8,128)S(1)}, f32[72,1024]{1,0:T(8,128)S(1)}) custom-call(s32[4]{0:T(128)S(1)} %pad_add_fusion.1.idx, bf16[128,2048]{1,0:T(8,128)(2,1)S(1)} %get-tuple-element.46.q, bf16[136,1024]{1,0:T(8,128)(2,1)S(1)} %collective-permute-done.17.refs_0_, f32[2,80,2048]{2,1,0:T(8,128)S(1)} %get-tuple-element.57.refs_1_, ...), custom_call_target="tpu_custom_call" | custom-call | flops 6000000000 | bytes 1048576 | tf_op jit(solution)/shard_map/pallas_call | solution.py:449
  99.1 1.6 %collective-permute-done.21.sib = f32[72,1024]{1,0:T(8,128)S(1)} collective-permute-done((f32[72,1024]{1,0:T(8,128)S(1)}, f32[72,1024]{1,0:T(8,128)S(1)}, u32[]{:S(2)}, u32[]{:S(2)}) %collective-permute-start.21) | collective-permute-done | bytes 294944 | tf_op jit(solution)/shard_map/ppermute | solution.py:51
  100.8 0.9 reshape.4
  101.7 6.1 %all-to-all-start.1 = ((bf16[16,2,2048]{2,1,0:T(2,128)(2,1)}), bf16[16,2,2048]{2,1,0:T(2,128)(2,1)S(1)}, u32[]{:S(2)}, u32[]{:S(2)}) async-start(bf16[16,2,2048]{2,1,0:T(2,128)(2,1)} %reshape.4), calls=%async_computation.1 | async-start | bytes 262144 | tf_op jit(solution)/shard_map/all_to_all | solution.py:462
  107.9 0.8 copy-done
  108.7 0.8 copy-done.2
  109.5 1.0 copy-done.1
  110.6 1.0 copy-done.3
  111.6 1.0 shard_map.101.w
  112.6 3.1 %all-to-all-done.1 = bf16[16,2,2048]{2,1,0:T(2,128)(2,1)S(1)} async-done(((bf16[16,2,2048]{2,1,0:T(2,128)(2,1)}), bf16[16,2,2048]{2,1,0:T(2,128)(2,1)S(1)}, u32[]{:S(2)}, u32[]{:S(2)}) %all-to-all-start.1) | async-done | bytes 131104 | tf_op jit(solution)/shard_map/all_to_all | solution.py:462
  115.9 1.5 %shard_map.102 = bf16[64,1024]{1,0:T(8,128)(2,1)} custom-call(bf16[16,64,64]{2,1,0:T(8,128)(2,1)S(1)} %reshape.5.att, f32[1,1024]{1,0:T(1,128)S(1)} %bitcast.13, bf16[1024,1024]{1,0:T(8,128)(2,1)S(1)} %shard_map.101.w), custom_call_target="tpu_custom_call" | custom-call | flops 100000000 | bytes 1048576 | tf_op jit(solution)/shard_map/pallas_call | solution.py:463
  (43 shorter events, 3.0 us)
Async XLA Ops:
  2.1 43.6 %copy-start.5 = (f32[1024]{0:T(1024)S(1)}, f32[1024]{0:T(1024)}, u32[]{:S(2)}) copy-start(f32[1024]{0:T(1024)} %param.10) | copy-start | bytes 12292
  2.1 43.6 %copy-start.6 = (f32[4]{0:T(128)S(1)}, f32[4]{0:T(128)}, u32[]{:S(2)}) copy-start(f32[4]{0:T(128)} %offs.1) | copy-start | bytes 52
  2.1 6.1 %collective-permute-start.6 = (bf16[48,1024]{1,0:T(8,128)(2,1)S(1)}, bf16[48,1024]{1,0:T(8,128)(2,1)S(1)}, u32[]{:S(2)}, u32[]{:S(2)}) collective-permute-start(bf16[48,1024]{1,0:T(8,128)(2,1)S(1)} %get-tuple-element.38), channel_id=1, source_target_pairs={{0,8},{8,16},{16,24},{24,0},{1,9},{9,17},{17,25},{25,1},{2,10},{10... | collective-permute-start | bytes 294920 | tf_op jit(solution)/shard_map/ppermute | solution.py:51
  3.7 7.3 %collective-permute-start.7 = (bf16[48,1024]{1,0:T(8,128)(2,1)S(1)}, bf16[48,1024]{1,0:T(8,128)(2,1)S(1)}, u32[]{:S(2)}, u32[]{:S(2)}) collective-permute-start(bf16[48,1024]{1,0:T(8,128)(2,1)S(1)} %get-tuple-element.39), channel_id=1, source_target_pairs={{0,16},{8,24},{16,0},{24,8},{1,17},{9,25},{17,1},{25,9},{2,18},{10... | collective-permute-start | bytes 294920 | tf_op jit(solution)/shard_map/ppermute | solution.py:51
  6.4 4.6 %collective-permute-start.8 = (bf16[48,1024]{1,0:T(8,128)(2,1)S(1)}, bf16[48,1024]{1,0:T(8,128)(2,1)S(1)}, u32[]{:S(2)}, u32[]{:S(2)}) collective-permute-start(bf16[48,1024]{1,0:T(8,128)(2,1)S(1)} %get-tuple-element.40), channel_id=1, source_target_pairs={{0,24},{8,0},{16,8},{24,16},{1,25},{9,1},{17,9},{25,17},{2,26},{10... | collective-permute-start | bytes 294920 | tf_op jit(solution)/shard_map/ppermute | solution.py:51
  11.9 18.7 %all-to-all-start = ((bf16[8,128,256]{2,1,0:T(8,128)(2,1)}), bf16[8,128,256]{2,1,0:T(8,128)(2,1)S(1)}, u32[]{:S(2)}, u32[]{:S(2)}) async-start(bf16[8,128,256]{2,1,0:T(8,128)(2,1)} %get-tuple-element.42), calls=%async_computation | async-start | bytes 1048576 | tf_op jit(solution)/shard_map/all_to_all | solution.py:395
  18.6 9.5 %collective-permute-start.2 = (bf16[32,1024]{1,0:T(8,128)(2,1)S(1)}, bf16[32,1024]{1,0:T(8,128)(2,1)S(1)}, u32[]{:S(2)}, u32[]{:S(2)}) collective-permute-start(bf16[32,1024]{1,0:T(8,128)(2,1)S(1)} %get-tuple-element.34), channel_id=1, source_target_pairs={{0,3},{1,0},{2,1},{3,2},{4,7},{5,4},{6,5},{7,6},{8,11},{9,8},{10,9... | collective-permute-start | bytes 196616 | tf_op jit(solution)/shard_map/ppermute | solution.py:51
  21.7 6.5 %collective-permute-start.1 = (bf16[32,1024]{1,0:T(8,128)(2,1)S(1)}, bf16[32,1024]{1,0:T(8,128)(2,1)S(1)}, u32[]{:S(2)}, u32[]{:S(2)}) collective-permute-start(bf16[32,1024]{1,0:T(8,128)(2,1)S(1)} %get-tuple-element.34), channel_id=1, source_target_pairs={{0,2},{1,3},{2,0},{3,1},{4,6},{5,7},{6,4},{7,5},{8,10},{9,11},{10,... | collective-permute-start | bytes 196616 | tf_op jit(solution)/shard_map/ppermute | solution.py:51
  22.3 5.8 %collective-permute-start = (bf16[32,1024]{1,0:T(8,128)(2,1)S(1)}, bf16[32,1024]{1,0:T(8,128)(2,1)S(1)}, u32[]{:S(2)}, u32[]{:S(2)}) collective-permute-start(bf16[32,1024]{1,0:T(8,128)(2,1)S(1)} %get-tuple-element.34), channel_id=1, source_target_pairs={{0,1},{1,2},{2,3},{3,0},{4,5},{5,6},{6,7},{7,4},{8,9},{9,10},{10,1... | collective-permute-start | bytes 196616 | tf_op jit(solution)/shard_map/ppermute | solution.py:51
  28.2 8.1 %collective-permute-start.3 = (bf16[128,1024]{1,0:T(8,128)(2,1)S(1)}, bf16[128,1024]{1,0:T(8,128)(2,1)S(1)}, u32[]{:S(2)}, u32[]{:S(2)}) collective-permute-start(bf16[128,1024]{1,0:T(8,128)(2,1)S(1)} %constant_dynamic-update-slice_fusion.refs_0_), channel_id=1, source_target_pairs={{0,8},{8,16},{16,24},{24,0},{1,9},{9,17},{17,25},{25,1},{2,10},{10... | collective-permute-start | bytes 786440 | tf_op jit(solution)/shard_map/ppermute | solution.py:51
  29.6 7.6 %collective-permute-start.9 = (bf16[128,1024]{1,0:T(8,128)(2,1)S(1)}, bf16[128,1024]{1,0:T(8,128)(2,1)S(1)}, u32[]{:S(2)}, u32[]{:S(2)}) collective-permute-start(bf16[128,1024]{1,0:T(8,128)(2,1)S(1)} %get-tuple-element.41.refs_4_), channel_id=1, source_target_pairs={{0,1},{1,2},{2,3},{3,0},{4,5},{5,6},{6,7},{7,4},{8,9},{9,10},{10,1... | collective-permute-start | bytes 786440 | tf_op jit(solution)/shard_map/ppermute | solution.py:51
  30.6 15.2 %collective-permute-start.12 = (bf16[8,128,256]{2,1,0:T(8,128)(2,1)S(1)}, bf16[8,128,256]{2,1,0:T(8,128)(2,1)S(1)}, u32[]{:S(2)}, u32[]{:S(2)}) collective-permute-start(bf16[8,128,256]{2,1,0:T(8,128)(2,1)S(1)} %all-to-all-done.refs_9_), channel_id=1, source_target_pairs={{0,4},{4,0},{1,5},{5,1},{2,6},{6,2},{3,7},{7,3},{8,12},{12,8},{9,1... | collective-permute-start | bytes 1572872 | tf_op jit(solution)/shard_map/ppermute | solution.py:51
  30.6 8.9 %collective-permute-start.5 = (bf16[128,1024]{1,0:T(8,128)(2,1)S(1)}, bf16[128,1024]{1,0:T(8,128)(2,1)S(1)}, u32[]{:S(2)}, u32[]{:S(2)}) collective-permute-start(bf16[128,1024]{1,0:T(8,128)(2,1)S(1)} %constant_dynamic-update-slice_fusion.refs_0_), channel_id=1, source_target_pairs={{0,24},{8,0},{16,8},{24,16},{1,25},{9,1},{17,9},{25,17},{2,26},{10... | collective-permute-start | bytes 786440 | tf_op jit(solution)/shard_map/ppermute | solution.py:51
  33.2 9.0 %collective-permute-start.11 = (bf16[128,1024]{1,0:T(8,128)(2,1)S(1)}, bf16[128,1024]{1,0:T(8,128)(2,1)S(1)}, u32[]{:S(2)}, u32[]{:S(2)}) collective-permute-start(bf16[128,1024]{1,0:T(8,128)(2,1)S(1)} %get-tuple-element.41.refs_4_), channel_id=1, source_target_pairs={{0,3},{1,0},{2,1},{3,2},{4,7},{5,4},{6,5},{7,6},{8,11},{9,8},{10,9... | collective-permute-start | bytes 786440 | tf_op jit(solution)/shard_map/ppermute | solution.py:51
  36.2 9.4 %collective-permute-start.4 = (bf16[128,1024]{1,0:T(8,128)(2,1)S(1)}, bf16[128,1024]{1,0:T(8,128)(2,1)S(1)}, u32[]{:S(2)}, u32[]{:S(2)}) collective-permute-start(bf16[128,1024]{1,0:T(8,128)(2,1)S(1)} %collective-permute-done.3.refs_1_), channel_id=1, source_target_pairs={{0,8},{8,16},{16,24},{24,0},{1,9},{9,17},{17,25},{25,1},{2,10},{10... | collective-permute-start | bytes 786440 | tf_op jit(solution)/shard_map/ppermute | solution.py:51
  37.2 8.5 %collective-permute-start.10 = (bf16[128,1024]{1,0:T(8,128)(2,1)S(1)}, bf16[128,1024]{1,0:T(8,128)(2,1)S(1)}, u32[]{:S(2)}, u32[]{:S(2)}) collective-permute-start(bf16[128,1024]{1,0:T(8,128)(2,1)S(1)} %collective-permute-done.9.refs_5_), channel_id=1, source_target_pairs={{0,1},{1,2},{2,3},{3,0},{4,5},{5,6},{6,7},{7,4},{8,9},{9,10},{10,1... | collective-permute-start | bytes 786440 | tf_op jit(solution)/shard_map/ppermute | solution.py:51
  47.9 1.5 %collective-permute-start.13 = (bf16[80,1024]{1,0:T(8,128)(2,1)S(1)}, bf16[80,1024]{1,0:T(8,128)(2,1)S(1)}, u32[]{:S(2)}, u32[]{:S(2)}) collective-permute-start(bf16[80,1024]{1,0:T(8,128)(2,1)S(1)} %get-tuple-element.43.q_own), channel_id=1, source_target_pairs={{0,4},{4,0},{1,5},{5,1},{2,6},{6,2},{3,7},{7,3},{8,12},{12,8},{9,1... | collective-permute-start | bytes 491528 | tf_op jit(solution)/shard_map/ppermute | solution.py:51
  50.0 8.7 %collective-permute-start.18 = (bf16[136,1024]{1,0:T(8,128)(2,1)S(1)}, bf16[136,1024]{1,0:T(8,128)(2,1)S(1)}, u32[]{:S(2)}, u32[]{:S(2)}) collective-permute-start(bf16[136,1024]{1,0:T(8,128)(2,1)S(1)} %get-tuple-element.47.pay), channel_id=1, source_target_pairs={{0,224},{32,0},{64,32},{1,225},{33,1},{65,33},{2,226},{34,2},{66,3... | collective-permute-start | bytes 835592 | tf_op jit(solution)/shard_map/ppermute | solution.py:69
  50.7 10.6 %collective-permute-start.14 = (bf16[136,1024]{1,0:T(8,128)(2,1)S(1)}, bf16[136,1024]{1,0:T(8,128)(2,1)S(1)}, u32[]{:S(2)}, u32[]{:S(2)}) collective-permute-start(bf16[136,1024]{1,0:T(8,128)(2,1)S(1)} %get-tuple-element.47.pay), channel_id=1, source_target_pairs={{0,32},{32,64},{64,96},{96,128},{128,160},{160,192},{192,224},{1,3... | collective-permute-start | bytes 835592 | tf_op jit(solution)/shard_map/ppermute | solution.py:65
  56.6 51.3 %collective-permute-start.24 = (bf16[2,8,64,256]{3,2,1,0:T(8,128)(2,1)S(1)}, bf16[2,8,64,256]{3,2,1,0:T(8,128)(2,1)S(1)}, u32[]{:S(2)}, u32[]{:S(2)}) collective-permute-start(bf16[2,8,64,256]{3,2,1,0:T(8,128)(2,1)S(1)} %pad_maximum_fusion.w0), channel_id=1, source_target_pairs={{0,3},{1,0},{2,1},{3,2},{4,7},{5,4},{6,5},{7,6},{8,11},{9,8},{10,9... | collective-permute-start | bytes 1572872 | tf_op jit(solution)/shard_map/ppermute | solution.py:51
  57.4 50.5 %collective-permute-start.23 = (bf16[2,8,64,256]{3,2,1,0:T(8,128)(2,1)S(1)}, bf16[2,8,64,256]{3,2,1,0:T(8,128)(2,1)S(1)}, u32[]{:S(2)}, u32[]{:S(2)}) collective-permute-start(bf16[2,8,64,256]{3,2,1,0:T(8,128)(2,1)S(1)} %pad_maximum_fusion.w0), channel_id=1, source_target_pairs={{0,2},{1,3},{2,0},{3,1},{4,6},{5,7},{6,4},{7,5},{8,10},{9,11},{10,... | collective-permute-start | bytes 1572872 | tf_op jit(solution)/shard_map/ppermute | solution.py:51
  57.8 50.9 %collective-permute-start.22 = (bf16[2,8,64,256]{3,2,1,0:T(8,128)(2,1)S(1)}, bf16[2,8,64,256]{3,2,1,0:T(8,128)(2,1)S(1)}, u32[]{:S(2)}, u32[]{:S(2)}) collective-permute-start(bf16[2,8,64,256]{3,2,1,0:T(8,128)(2,1)S(1)} %pad_maximum_fusion.w0), channel_id=1, source_target_pairs={{0,1},{1,2},{2,3},{3,0},{4,5},{5,6},{6,7},{7,4},{8,9},{9,10},{10,1... | collective-permute-start | bytes 1572872 | tf_op jit(solution)/shard_map/ppermute | solution.py:51
  58.7 9.6 %collective-permute-start.19 = (bf16[136,1024]{1,0:T(8,128)(2,1)S(1)}, bf16[136,1024]{1,0:T(8,128)(2,1)S(1)}, u32[]{:S(2)}, u32[]{:S(2)}) collective-permute-start(bf16[136,1024]{1,0:T(8,128)(2,1)S(1)} %collective-permute-done.18.refs_1_), channel_id=1, source_target_pairs={{224,192},{0,224},{32,0},{225,193},{1,225},{33,1},{226,194},{2,226... | collective-permute-start | bytes 835592 | tf_op jit(solution)/shard_map/ppermute | solution.py:69
  61.3 9.8 %collective-permute-start.15 = (bf16[136,1024]{1,0:T(8,128)(2,1)S(1)}, bf16[136,1024]{1,0:T(8,128)(2,1)S(1)}, u32[]{:S(2)}, u32[]{:S(2)}) collective-permute-start(bf16[136,1024]{1,0:T(8,128)(2,1)S(1)} %collective-permute-done.14.refs_0_), channel_id=1, source_target_pairs={{32,64},{64,96},{96,128},{128,160},{160,192},{192,224},{33,65},{65... | collective-permute-start | bytes 835592 | tf_op jit(solution)/shard_map/ppermute | solution.py:65
  68.3 19.9 %collective-permute-start.20 = (bf16[136,1024]{1,0:T(8,128)(2,1)S(1)}, bf16[136,1024]{1,0:T(8,128)(2,1)S(1)}, u32[]{:S(2)}, u32[]{:S(2)}) collective-permute-start(bf16[136,1024]{1,0:T(8,128)(2,1)S(1)} %collective-permute-done.19.refs_1_), channel_id=1, source_target_pairs={{192,160},{224,192},{0,224},{193,161},{225,193},{1,225},{194,162},... | collective-permute-start | bytes 835592 | tf_op jit(solution)/shard_map/ppermute | solution.py:69
  71.1 11.0 %collective-permute-start.16 = (bf16[136,1024]{1,0:T(8,128)(2,1)S(1)}, bf16[136,1024]{1,0:T(8,128)(2,1)S(1)}, u32[]{:S(2)}, u32[]{:S(2)}) collective-permute-start(bf16[136,1024]{1,0:T(8,128)(2,1)S(1)} %collective-permute-done.15.refs_0_), channel_id=1, source_target_pairs={{64,96},{96,128},{128,160},{160,192},{192,224},{65,97},{97,129},{1... | collective-permute-start | bytes 835592 | tf_op jit(solution)/shard_map/ppermute | solution.py:65
  82.1 12.9 %collective-permute-start.17 = (bf16[136,1024]{1,0:T(8,128)(2,1)S(1)}, bf16[136,1024]{1,0:T(8,128)(2,1)S(1)}, u32[]{:S(2)}, u32[]{:S(2)}) collective-permute-start(bf16[136,1024]{1,0:T(8,128)(2,1)S(1)} %collective-permute-done.16.refs_0_), channel_id=1, source_target_pairs={{96,128},{128,160},{160,192},{192,224},{97,129},{129,161},{161,193... | collective-permute-start | bytes 835592 | tf_op jit(solution)/shard_map/ppermute | solution.py:65
  99.0 1.7 %collective-permute-start.21 = (f32[72,1024]{1,0:T(8,128)S(1)}, f32[72,1024]{1,0:T(8,128)S(1)}, u32[]{:S(2)}, u32[]{:S(2)}) collective-permute-start(f32[72,1024]{1,0:T(8,128)S(1)} %get-tuple-element.61), channel_id=1, source_target_pairs={{0,4},{4,0},{1,5},{5,1},{2,6},{6,2},{3,7},{7,3},{8,12},{12,8},{9,1... | collective-permute-start | bytes 884744 | tf_op jit(solution)/shard_map/ppermute | solution.py:51
  101.7 14.2 %copy-start.4 = (f32[1024]{0:T(1024)S(1)}, f32[1024]{0:T(1024)}, u32[]{:S(2)}) copy-start(f32[1024]{0:T(1024)} %param.17) | copy-start | bytes 12292
  101.7 14.0 %all-to-all-start.1 = ((bf16[16,2,2048]{2,1,0:T(2,128)(2,1)}), bf16[16,2,2048]{2,1,0:T(2,128)(2,1)S(1)}, u32[]{:S(2)}, u32[]{:S(2)}) async-start(bf16[16,2,2048]{2,1,0:T(2,128)(2,1)} %reshape.4), calls=%async_computation.1 | async-start | bytes 262144 | tf_op jit(solution)/shard_map/all_to_all | solution.py:462
  107.9 0.8 copy-start
  108.7 0.8 copy-start.2
  109.5 1.0 copy-start.1
  110.6 1.0 copy-start.3

commit v7 on v6

--- a/solution.py
+++ b/solution.py
@@ -66,7 +66,7 @@
 
 
 def step_left(x, k):
-    return lax.ppermute(x, "z", [((i - k + 1) % NZ, (i - k) % NZ) for i in range(3)])
+    return lax.ppermute(x, "z", [((i - k + 1) % NZ, (i - k) % NZ) for i in range(4)])
 
 
 def three_parts(x):
@@ -201,13 +201,15 @@
     return rows[3:4] + rows[4:5] + rows[5:6]
 
 
-def place_chunk(pay, i, kx, vx):
+def place_chunk(pays, i, kx, vx):
     fill = jnp.zeros((56, 128), F32)
+    tiles = 8 // len(pays)
     for r in range(8):
-        lanes = slice(r * 128, (r + 1) * 128)
+        pay, at = pays[r // tiles], r % tiles
+        lanes = slice(at * 128, (at + 1) * 128)
         tile = jnp.concatenate([pay[64:136, lanes].astype(F32), fill], axis=0)
-        kx[i, lanes, :] = tile.T.astype(BF16)
-    vx[i, 0:64, :] = pay[0:64, :]
+        kx[i, r * 128 : (r + 1) * 128, :] = tile.T.astype(BF16)
+        vx[i, 0:64, r * 128 : (r + 1) * 128] = pay[0:64, lanes]
     vx[i, 64:80, :] = jnp.ones((16, KEYS), BF16)
 
 
@@ -275,7 +277,7 @@
     acc[...] = jnp.zeros_like(acc)
     m[...] = jnp.full(m.shape, LOW, F32)
     move[...] = jnp.zeros_like(move)
-    place_chunk(pay, 0, kx, vx)
+    place_chunk((pay,), 0, kx, vx)
     score, weigh, add = stages(q, acc, m, kx, vx, move, bufs)
     key = lax.broadcasted_iota(jnp.int32, (BLK, BLK), 0)
     query = lax.broadcasted_iota(jnp.int32, (BLK, BLK), 1)
@@ -294,8 +296,7 @@
 
 def step_body(k, idx, q, *refs):
     z = idx[0]
-    n_pay = 2 if k < 4 else 1
-    pays, refs = refs[:n_pay], refs[n_pay:]
+    pays, refs = refs[:2], refs[2:]
     acc0, m0, sums0, refs = refs[0], refs[1], refs[2], refs[3:]
     if k < 4:
         acc, m, sums, kx, vx, move, *bufs = refs
@@ -307,7 +308,7 @@
 
     @pl.when(z >= k)
     def _():
-        place_chunk(pays[0], 0, kx, vx)
+        place_chunk(pays[0:1] if k < 4 else pays, 0, kx, vx)
         move[0] = sums0[...]
         sums[...] = sums0[...] + jnp.broadcast_to(chunk_total(pays[0]), sums.shape)
 
@@ -316,7 +317,7 @@
 
         @pl.when(z + k >= 8)
         def _():
-            place_chunk(pays[1], 1, kx, vx)
+            place_chunk(pays[1:2], 1, kx, vx)
             move[1] = jnp.zeros(sums.shape, F32)
             m[1] = m[1] + chunk_total(pays[1])[:, 0:1]
 
@@ -435,11 +436,12 @@
     w_o = direct(w_o, "y")
 
     for k in range(1, 5):
-        pays = (right, left) if k < 4 else (right,)
-        if k < 4:
-            right = step_right(pays[0], k + 1)
+        pays = (right, left)
         if k < 3:
-            left = step_left(pays[1], k + 1)
+            right, left = step_right(right, k + 1), step_left(left, k + 1)
+        elif k == 3:
+            right = step_right(right[:, : KEYS // 2], 4)
+            left = step_left(left[:, KEYS // 2 :], 4)
         ins = (idx, q) + pays + (acc, m, sums)
         if k < 4:
             outs, scratch, aliases = (acc_t, m_t, sums_t), work, {4: 0, 5: 1}

time: 118 us -> 121 us (1.025)
  the two profiles are of different devices: /device:TPU:160 before, /device:TPU:192 now
where the time goes in v7:
time: 121 us; the launch traced here: 120 us
  starting transfers between devices  55 us (45%)
  Pallas kernels  31.4 us (26%)
  waiting for transfers between devices  27.7 us (23%)
  local copies, waits for them, and re-layouts  4.9 us (4%)
    pallas_call x4, Pallas kernels, shards(): call(functools.partial(step_body, k), outs, [SMEM] + [VMEM] * (len(ins) -...  21.3 us
    ppermute x18, waiting for transfers between devices, shift(): return lax.ppermute(x, axis, [(i, (i + k) % n) for i in range(n)])  20.4 us
    ppermute x18, starting transfers between devices, shift(): return lax.ppermute(x, axis, [(i, (i + k) % n) for i in range(n)])  19.7 us
    ppermute x4, starting transfers between devices, step_right(): return lax.ppermute(x, 'z', [(i, i + 1) for i in range(k - 1, NZ - 1)])  17 us
    all_to_all x1, starting transfers between devices, shards(): w_own = lax.all_to_all(chunk, 'z', 0, 0, tiled=True)  6.3 us
    all_to_all x1, starting transfers between devices, shards(): att = lax.all_to_all(att.reshape(16, 64, HD), ('x', 'y'), 0, 0, tiled=True)  6.16 us
    ppermute x4, starting transfers between devices, step_left(): lax.ppermute(x, 'z', [((i - k + 1) % NZ, (i - k) % NZ) for i in range(4)])  5.79 us
    unnamed x19, local copies, waits for them, and re-layouts  4.83 us
  transfers between devices with their start and end apart: 28, of which 14 were waited for; matrix products, arithmetic and copies ran while one was open for 1% of the time, Pallas kernels for 21%

profile of v7, /device:TPU:192, one launch (start us, length us, event | category | flops | bytes accessed | tf_op | source)
XLA Modules:
  0.0 120.4 jit_solution(13839267464876476335)
XLA Ops:
  0.1 1.0 pad_add_fusion.rows
  1.1 1.0 shard_map.91
  2.1 1.6 %collective-permute-start.6 = (bf16[48,1024]{1,0:T(8,128)(2,1)S(1)}, bf16[48,1024]{1,0:T(8,128)(2,1)S(1)}, u32[]{:S(2)}, u32[]{:S(2)}) collective-permute-start(bf16[48,1024]{1,0:T(8,128)(2,1)S(1)} %get-tuple-element.38), channel_id=1, source_target_pairs={{0,8},{8,16},{16,24},{24,0},{1,9},{9,17},{17,25},{25,1},{2,10},{10... | collective-permute-start | bytes 294920 | tf_op jit(solution)/shard_map/ppermute | solution.py:51
  3.7 2.7 %collective-permute-start.7 = (bf16[48,1024]{1,0:T(8,128)(2,1)S(1)}, bf16[48,1024]{1,0:T(8,128)(2,1)S(1)}, u32[]{:S(2)}, u32[]{:S(2)}) collective-permute-start(bf16[48,1024]{1,0:T(8,128)(2,1)S(1)} %get-tuple-element.39), channel_id=1, source_target_pairs={{0,16},{8,24},{16,0},{24,8},{1,17},{9,25},{17,1},{25,9},{2,18},{10... | collective-permute-start | bytes 294920 | tf_op jit(solution)/shard_map/ppermute | solution.py:51
  6.4 1.4 %collective-permute-start.8 = (bf16[48,1024]{1,0:T(8,128)(2,1)S(1)}, bf16[48,1024]{1,0:T(8,128)(2,1)S(1)}, u32[]{:S(2)}, u32[]{:S(2)}) collective-permute-start(bf16[48,1024]{1,0:T(8,128)(2,1)S(1)} %get-tuple-element.40), channel_id=1, source_target_pairs={{0,24},{8,0},{16,8},{24,16},{1,25},{9,1},{17,9},{25,17},{2,26},{10... | collective-permute-start | bytes 294920 | tf_op jit(solution)/shard_map/ppermute | solution.py:51
  8.2 2.8 %collective-permute-done.7.r2 = bf16[48,1024]{1,0:T(8,128)(2,1)S(1)} collective-permute-done((bf16[48,1024]{1,0:T(8,128)(2,1)S(1)}, bf16[48,1024]{1,0:T(8,128)(2,1)S(1)}, u32[]{:S(2)}, u32[]{:S(2)}) %collective-permute-start.7) | collective-permute-done | bytes 98336 | tf_op jit(solution)/shard_map/ppermute | solution.py:51
  11.0 0.8 shard_map.92
  11.9 6.3 %all-to-all-start = ((bf16[8,128,256]{2,1,0:T(8,128)(2,1)}), bf16[8,128,256]{2,1,0:T(8,128)(2,1)S(1)}, u32[]{:S(2)}, u32[]{:S(2)}) async-start(bf16[8,128,256]{2,1,0:T(8,128)(2,1)} %get-tuple-element.42), calls=%async_computation | async-start | bytes 1048576 | tf_op jit(solution)/shard_map/all_to_all | solution.py:396
  18.2 3.0 %collective-permute-start.2 = (bf16[32,1024]{1,0:T(8,128)(2,1)S(1)}, bf16[32,1024]{1,0:T(8,128)(2,1)S(1)}, u32[]{:S(2)}, u32[]{:S(2)}) collective-permute-start(bf16[32,1024]{1,0:T(8,128)(2,1)S(1)} %get-tuple-element.34), channel_id=1, source_target_pairs={{0,3},{1,0},{2,1},{3,2},{4,7},{5,4},{6,5},{7,6},{8,11},{9,8},{10,9... | collective-permute-start | bytes 196616 | tf_op jit(solution)/shard_map/ppermute | solution.py:51
  21.2 0.6 collective-permute-start.1
  21.8 1.0 collective-permute-start
  22.8 4.9 %collective-permute-done = bf16[32,1024]{1,0:T(8,128)(2,1)S(1)} collective-permute-done((bf16[32,1024]{1,0:T(8,128)(2,1)S(1)}, bf16[32,1024]{1,0:T(8,128)(2,1)S(1)}, u32[]{:S(2)}, u32[]{:S(2)}) %collective-permute-start) | collective-permute-done | bytes 65568 | tf_op jit(solution)/shard_map/ppermute | solution.py:51
  27.7 1.4 %collective-permute-start.3 = (bf16[128,1024]{1,0:T(8,128)(2,1)S(1)}, bf16[128,1024]{1,0:T(8,128)(2,1)S(1)}, u32[]{:S(2)}, u32[]{:S(2)}) collective-permute-start(bf16[128,1024]{1,0:T(8,128)(2,1)S(1)} %constant_dynamic-update-slice_fusion.refs_0_), channel_id=1, source_target_pairs={{0,8},{8,16},{16,24},{24,0},{1,9},{9,17},{17,25},{25,1},{2,10},{10... | collective-permute-start | bytes 786440 | tf_op jit(solution)/shard_map/ppermute | solution.py:51
  29.1 1.6 %all-to-all-done.refs_9_ = bf16[8,128,256]{2,1,0:T(8,128)(2,1)S(1)} async-done(((bf16[8,128,256]{2,1,0:T(8,128)(2,1)}), bf16[8,128,256]{2,1,0:T(8,128)(2,1)S(1)}, u32[]{:S(2)}, u32[]{:S(2)}) %all-to-all-start) | async-done | bytes 524320 | tf_op jit(solution)/shard_map/all_to_all | solution.py:396
  30.7 2.7 %collective-permute-start.5 = (bf16[128,1024]{1,0:T(8,128)(2,1)S(1)}, bf16[128,1024]{1,0:T(8,128)(2,1)S(1)}, u32[]{:S(2)}, u32[]{:S(2)}) collective-permute-start(bf16[128,1024]{1,0:T(8,128)(2,1)S(1)} %constant_dynamic-update-slice_fusion.refs_0_), channel_id=1, source_target_pairs={{0,24},{8,0},{16,8},{24,16},{1,25},{9,1},{17,9},{25,17},{2,26},{10... | collective-permute-start | bytes 786440 | tf_op jit(solution)/shard_map/ppermute | solution.py:51
  33.4 3.0 %collective-permute-start.11 = (bf16[128,1024]{1,0:T(8,128)(2,1)S(1)}, bf16[128,1024]{1,0:T(8,128)(2,1)S(1)}, u32[]{:S(2)}, u32[]{:S(2)}) collective-permute-start(bf16[128,1024]{1,0:T(8,128)(2,1)S(1)} %get-tuple-element.41.refs_4_), channel_id=1, source_target_pairs={{0,3},{1,0},{2,1},{3,2},{4,7},{5,4},{6,5},{7,6},{8,11},{9,8},{10,9... | collective-permute-start | bytes 786440 | tf_op jit(solution)/shard_map/ppermute | solution.py:51
  36.7 2.9 %collective-permute-done.5.refs_3_ = bf16[128,1024]{1,0:T(8,128)(2,1)S(1)} collective-permute-done((bf16[128,1024]{1,0:T(8,128)(2,1)S(1)}, bf16[128,1024]{1,0:T(8,128)(2,1)S(1)}, u32[]{:S(2)}, u32[]{:S(2)}) %collective-permute-start.5) | collective-permute-done | bytes 262176 | tf_op jit(solution)/shard_map/ppermute | solution.py:51
  39.6 2.7 %collective-permute-done.11.refs_7_ = bf16[128,1024]{1,0:T(8,128)(2,1)S(1)} collective-permute-done((bf16[128,1024]{1,0:T(8,128)(2,1)S(1)}, bf16[128,1024]{1,0:T(8,128)(2,1)S(1)}, u32[]{:S(2)}, u32[]{:S(2)}) %collective-permute-start.11) | collective-permute-done | bytes 262176 | tf_op jit(solution)/shard_map/ppermute | solution.py:51
  42.4 3.4 %collective-permute-done.4.refs_2_ = bf16[128,1024]{1,0:T(8,128)(2,1)S(1)} collective-permute-done((bf16[128,1024]{1,0:T(8,128)(2,1)S(1)}, bf16[128,1024]{1,0:T(8,128)(2,1)S(1)}, u32[]{:S(2)}, u32[]{:S(2)}) %collective-permute-start.4) | collective-permute-done | bytes 262176 | tf_op jit(solution)/shard_map/ppermute | solution.py:51
  45.9 2.1 %shard_map.93 = (bf16[80,1024]{1,0:T(8,128)(2,1)S(1)}, bf16[128,1024]{1,0:T(8,128)(2,1)S(1)}, f32[8,1024]{1,0:T(8,128)S(1)}) custom-call(s32[4]{0:T(128)S(1)} %pad_add_fusion.1.idx, f32[4]{0:T(128)S(1)} %copy-done.6, bf16[128,1024]{1,0:T(8,128)(2,1)S(1)} %constant_dynamic-update-slice_fusion.refs_0_, bf16[128,1024]{1,0:T(8,128)(2,1)S(1)} %collective-permute-done.3.refs_1_, ...), custom_call_target="tpu_custom_call" | custom-call | flops 2000000000 | bytes 1048576 | tf_op jit(solution)/shard_map/pallas_call | solution.py:401
  48.2 1.3 %collective-permute-done.13.q_sib = bf16[80,1024]{1,0:T(8,128)(2,1)S(1)} collective-permute-done((bf16[80,1024]{1,0:T(8,128)(2,1)S(1)}, bf16[80,1024]{1,0:T(8,128)(2,1)S(1)}, u32[]{:S(2)}, u32[]{:S(2)}) %collective-permute-start.13) | collective-permute-done | bytes 163872 | tf_op jit(solution)/shard_map/ppermute | solution.py:51
  49.5 0.6 shard_map.94
  50.2 0.7 collective-permute-start.18
  50.8 2.4 %collective-permute-start.14 = (bf16[136,1024]{1,0:T(8,128)(2,1)S(1)}, bf16[136,1024]{1,0:T(8,128)(2,1)S(1)}, u32[]{:S(2)}, u32[]{:S(2)}) collective-permute-start(bf16[136,1024]{1,0:T(8,128)(2,1)S(1)} %get-tuple-element.47.pay), channel_id=1, source_target_pairs={{0,32},{32,64},{64,96},{96,128},{128,160},{160,192},{192,224},{1,3... | collective-permute-start | bytes 835592 | tf_op jit(solution)/shard_map/ppermute | solution.py:65
  53.2 2.7 %shard_map.95 = (f32[2,80,2048]{2,1,0:T(8,128)S(1)}, f32[2,8,2048]{2,1,0:T(8,128)S(1)}, f32[8,256]{1,0:T(8,128)S(1)}) custom-call(s32[4]{0:T(128)S(1)} %pad_add_fusion.1.idx, bf16[128,2048]{1,0:T(8,128)(2,1)S(1)} %get-tuple-element.46.q, bf16[136,1024]{1,0:T(8,128)(2,1)S(1)} %get-tuple-element.47.pay), custom_call_target="tpu_custom_call" | custom-call | flops 3000000000 | bytes 1048576 | tf_op jit(solution)/shard_map/pallas_call | solution.py:430
  55.9 0.7 collective-permute-start.25
  57.1 0.9 collective-permute-start.23
  58.0 1.3 %collective-permute-start.19 = (bf16[136,1024]{1,0:T(8,128)(2,1)S(1)}, bf16[136,1024]{1,0:T(8,128)(2,1)S(1)}, u32[]{:S(2)}, u32[]{:S(2)}) collective-permute-start(bf16[136,1024]{1,0:T(8,128)(2,1)S(1)} %collective-permute-done.18.refs_1_), channel_id=1, source_target_pairs={{224,192},{0,224},{32,0},{64,32},{225,193},{1,225},{33,1},{65,33},... | collective-permute-start | bytes 835592 | tf_op jit(solution)/shard_map/ppermute | solution.py:69
  59.3 2.1 %collective-permute-done.14.refs_0_ = bf16[136,1024]{1,0:T(8,128)(2,1)S(1)} collective-permute-done((bf16[136,1024]{1,0:T(8,128)(2,1)S(1)}, bf16[136,1024]{1,0:T(8,128)(2,1)S(1)}, u32[]{:S(2)}, u32[]{:S(2)}) %collective-permute-start.14) | collective-permute-done | bytes 278560 | tf_op jit(solution)/shard_map/ppermute | solution.py:65
  61.4 5.8 %collective-permute-start.15 = (bf16[136,1024]{1,0:T(8,128)(2,1)S(1)}, bf16[136,1024]{1,0:T(8,128)(2,1)S(1)}, u32[]{:S(2)}, u32[]{:S(2)}) collective-permute-start(bf16[136,1024]{1,0:T(8,128)(2,1)S(1)} %collective-permute-done.14.refs_0_), channel_id=1, source_target_pairs={{32,64},{64,96},{96,128},{128,160},{160,192},{192,224},{33,65},{65... | collective-permute-start | bytes 835592 | tf_op jit(solution)/shard_map/ppermute | solution.py:65
  67.3 3.9 %shard_map.96 = (f32[2,80,2048]{2,1,0:T(8,128)S(1)}, f32[2,8,2048]{2,1,0:T(8,128)S(1)}, f32[8,256]{1,0:T(8,128)S(1)}) custom-call(s32[4]{0:T(128)S(1)} %pad_add_fusion.1.idx, bf16[128,2048]{1,0:T(8,128)(2,1)S(1)} %get-tuple-element.46.q, bf16[136,1024]{1,0:T(8,128)(2,1)S(1)} %collective-permute-done.14.refs_0_, ...), custom_call_target="tpu_custom_call", output_to_operand_aliasing={{0}: (4, {}), {1}: (5, {})} | custom-call | flops 6000000000 | bytes 1048576 | tf_op jit(solution)/shard_map/pallas_call | solution.py:451
  71.7 1.9 %collective-permute-start.20 = (bf16[136,1024]{1,0:T(8,128)(2,1)S(1)}, bf16[136,1024]{1,0:T(8,128)(2,1)S(1)}, u32[]{:S(2)}, u32[]{:S(2)}) collective-permute-start(bf16[136,1024]{1,0:T(8,128)(2,1)S(1)} %collective-permute-done.19.refs_1_), channel_id=1, source_target_pairs={{192,160},{224,192},{0,224},{32,0},{193,161},{225,193},{1,225},{33... | collective-permute-start | bytes 835592 | tf_op jit(solution)/shard_map/ppermute | solution.py:69
  73.6 4.9 %collective-permute-start.16 = (bf16[136,1024]{1,0:T(8,128)(2,1)S(1)}, bf16[136,1024]{1,0:T(8,128)(2,1)S(1)}, u32[]{:S(2)}, u32[]{:S(2)}) collective-permute-start(bf16[136,1024]{1,0:T(8,128)(2,1)S(1)} %collective-permute-done.15.refs_0_), channel_id=1, source_target_pairs={{64,96},{96,128},{128,160},{160,192},{192,224},{65,97},{97,129},{1... | collective-permute-start | bytes 835592 | tf_op jit(solution)/shard_map/ppermute | solution.py:65
  78.5 6.7 %shard_map.97 = (f32[2,80,2048]{2,1,0:T(8,128)S(1)}, f32[2,8,2048]{2,1,0:T(8,128)S(1)}, f32[8,256]{1,0:T(8,128)S(1)}) custom-call(s32[4]{0:T(128)S(1)} %pad_add_fusion.1.idx, bf16[128,2048]{1,0:T(8,128)(2,1)S(1)} %get-tuple-element.46.q, bf16[136,1024]{1,0:T(8,128)(2,1)S(1)} %collective-permute-done.15.refs_0_, ...), custom_call_target="tpu_custom_call", output_to_operand_aliasing={{0}: (4, {}), {1}: (5, {})} | custom-call | flops 6000000000 | bytes 1048576 | tf_op jit(solution)/shard_map/pallas_call | solution.py:451
  85.3 1.9 %collective-permute-start.21 = (bf16[136,512]{1,0:T(8,128)(2,1)S(1)}, bf16[136,512]{1,0:T(8,128)(2,1)S(1)}, u32[]{:S(2)}, u32[]{:S(2)}) collective-permute-start(bf16[136,512]{1,0:T(8,128)(2,1)S(1)} %slice.17), channel_id=1, source_target_pairs={{160,128},{192,160},{224,192},{0,224},{161,129},{193,161},{225,193... | collective-permute-start | bytes 417800 | tf_op jit(solution)/shard_map/ppermute | solution.py:69
  87.2 3.9 %collective-permute-start.17 = (bf16[136,512]{1,0:T(8,128)(2,1)S(1)}, bf16[136,512]{1,0:T(8,128)(2,1)S(1)}, u32[]{:S(2)}, u32[]{:S(2)}) collective-permute-start(bf16[136,512]{1,0:T(8,128)(2,1)S(1)} %slice.16), channel_id=1, source_target_pairs={{96,128},{128,160},{160,192},{192,224},{97,129},{129,161},{161,193... | collective-permute-start | bytes 417800 | tf_op jit(solution)/shard_map/ppermute | solution.py:65
  91.1 6.7 %shard_map.98 = (f32[2,80,2048]{2,1,0:T(8,128)S(1)}, f32[2,8,2048]{2,1,0:T(8,128)S(1)}, f32[8,256]{1,0:T(8,128)S(1)}) custom-call(s32[4]{0:T(128)S(1)} %pad_add_fusion.1.idx, bf16[128,2048]{1,0:T(8,128)(2,1)S(1)} %get-tuple-element.46.q, bf16[136,1024]{1,0:T(8,128)(2,1)S(1)} %collective-permute-done.16.refs_0_, ...), custom_call_target="tpu_custom_call", output_to_operand_aliasing={{0}: (4, {}), {1}: (5, {})} | custom-call | flops 6000000000 | bytes 1048576 | tf_op jit(solution)/shard_map/pallas_call | solution.py:451
  97.9 4.0 %shard_map.99 = (f32[72,1024]{1,0:T(8,128)S(1)}, f32[72,1024]{1,0:T(8,128)S(1)}) custom-call(s32[4]{0:T(128)S(1)} %pad_add_fusion.1.idx, bf16[128,2048]{1,0:T(8,128)(2,1)S(1)} %get-tuple-element.46.q, bf16[136,512]{1,0:T(8,128)(2,1)S(1)} %collective-permute-done.17.refs_0_, bf16[136,512]{1,0:T(8,128)(2,1)S(1)} %collective-permute-done.21.refs_1_, ...), custom_call_target="tpu_custom_call" | custom-call | flops 6000000000 | bytes 1048576 | tf_op jit(solution)/shard_map/pallas_call | solution.py:451
  102.0 1.6 %collective-permute-done.22.sib = f32[72,1024]{1,0:T(8,128)S(1)} collective-permute-done((f32[72,1024]{1,0:T(8,128)S(1)}, f32[72,1024]{1,0:T(8,128)S(1)}, u32[]{:S(2)}, u32[]{:S(2)}) %collective-permute-start.22) | collective-permute-done | bytes 294944 | tf_op jit(solution)/shard_map/ppermute | solution.py:51
  103.8 0.9 reshape.4
  104.7 6.2 %all-to-all-start.1 = ((bf16[16,2,2048]{2,1,0:T(2,128)(2,1)}), bf16[16,2,2048]{2,1,0:T(2,128)(2,1)S(1)}, u32[]{:S(2)}, u32[]{:S(2)}) async-start(bf16[16,2,2048]{2,1,0:T(2,128)(2,1)} %reshape.4), calls=%async_computation.1 | async-start | bytes 262144 | tf_op jit(solution)/shard_map/all_to_all | solution.py:464
  110.9 0.8 copy-done
  111.7 0.8 copy-done.2
  112.5 1.0 copy-done.1
  113.5 1.0 copy-done.3
  114.6 1.0 shard_map.101.w
  115.6 3.1 %all-to-all-done.1 = bf16[16,2,2048]{2,1,0:T(2,128)(2,1)S(1)} async-done(((bf16[16,2,2048]{2,1,0:T(2,128)(2,1)}), bf16[16,2,2048]{2,1,0:T(2,128)(2,1)S(1)}, u32[]{:S(2)}, u32[]{:S(2)}) %all-to-all-start.1) | async-done | bytes 131104 | tf_op jit(solution)/shard_map/all_to_all | solution.py:464
  118.9 1.5 %shard_map.102 = bf16[64,1024]{1,0:T(8,128)(2,1)} custom-call(bf16[16,64,64]{2,1,0:T(8,128)(2,1)S(1)} %reshape.5.att, f32[1,1024]{1,0:T(1,128)S(1)} %bitcast.13, bf16[1024,1024]{1,0:T(8,128)(2,1)S(1)} %shard_map.101.w), custom_call_target="tpu_custom_call" | custom-call | flops 100000000 | bytes 1048576 | tf_op jit(solution)/shard_map/pallas_call | solution.py:465
  (47 shorter events, 2.6 us)
Async XLA Ops:
  2.1 43.8 %copy-start.5 = (f32[1024]{0:T(1024)S(1)}, f32[1024]{0:T(1024)}, u32[]{:S(2)}) copy-start(f32[1024]{0:T(1024)} %param.10) | copy-start | bytes 12292
  2.1 43.8 %copy-start.6 = (f32[4]{0:T(128)S(1)}, f32[4]{0:T(128)}, u32[]{:S(2)}) copy-start(f32[4]{0:T(128)} %offs.1) | copy-start | bytes 52
  2.1 6.1 %collective-permute-start.6 = (bf16[48,1024]{1,0:T(8,128)(2,1)S(1)}, bf16[48,1024]{1,0:T(8,128)(2,1)S(1)}, u32[]{:S(2)}, u32[]{:S(2)}) collective-permute-start(bf16[48,1024]{1,0:T(8,128)(2,1)S(1)} %get-tuple-element.38), channel_id=1, source_target_pairs={{0,8},{8,16},{16,24},{24,0},{1,9},{9,17},{17,25},{25,1},{2,10},{10... | collective-permute-start | bytes 294920 | tf_op jit(solution)/shard_map/ppermute | solution.py:51
  3.7 7.3 %collective-permute-start.7 = (bf16[48,1024]{1,0:T(8,128)(2,1)S(1)}, bf16[48,1024]{1,0:T(8,128)(2,1)S(1)}, u32[]{:S(2)}, u32[]{:S(2)}) collective-permute-start(bf16[48,1024]{1,0:T(8,128)(2,1)S(1)} %get-tuple-element.39), channel_id=1, source_target_pairs={{0,16},{8,24},{16,0},{24,8},{1,17},{9,25},{17,1},{25,9},{2,18},{10... | collective-permute-start | bytes 294920 | tf_op jit(solution)/shard_map/ppermute | solution.py:51
  6.4 4.6 %collective-permute-start.8 = (bf16[48,1024]{1,0:T(8,128)(2,1)S(1)}, bf16[48,1024]{1,0:T(8,128)(2,1)S(1)}, u32[]{:S(2)}, u32[]{:S(2)}) collective-permute-start(bf16[48,1024]{1,0:T(8,128)(2,1)S(1)} %get-tuple-element.40), channel_id=1, source_target_pairs={{0,24},{8,0},{16,8},{24,16},{1,25},{9,1},{17,9},{25,17},{2,26},{10... | collective-permute-start | bytes 294920 | tf_op jit(solution)/shard_map/ppermute | solution.py:51
  11.9 18.8 %all-to-all-start = ((bf16[8,128,256]{2,1,0:T(8,128)(2,1)}), bf16[8,128,256]{2,1,0:T(8,128)(2,1)S(1)}, u32[]{:S(2)}, u32[]{:S(2)}) async-start(bf16[8,128,256]{2,1,0:T(8,128)(2,1)} %get-tuple-element.42), calls=%async_computation | async-start | bytes 1048576 | tf_op jit(solution)/shard_map/all_to_all | solution.py:396
  18.2 9.5 %collective-permute-start.2 = (bf16[32,1024]{1,0:T(8,128)(2,1)S(1)}, bf16[32,1024]{1,0:T(8,128)(2,1)S(1)}, u32[]{:S(2)}, u32[]{:S(2)}) collective-permute-start(bf16[32,1024]{1,0:T(8,128)(2,1)S(1)} %get-tuple-element.34), channel_id=1, source_target_pairs={{0,3},{1,0},{2,1},{3,2},{4,7},{5,4},{6,5},{7,6},{8,11},{9,8},{10,9... | collective-permute-start | bytes 196616 | tf_op jit(solution)/shard_map/ppermute | solution.py:51
  21.2 6.5 %collective-permute-start.1 = (bf16[32,1024]{1,0:T(8,128)(2,1)S(1)}, bf16[32,1024]{1,0:T(8,128)(2,1)S(1)}, u32[]{:S(2)}, u32[]{:S(2)}) collective-permute-start(bf16[32,1024]{1,0:T(8,128)(2,1)S(1)} %get-tuple-element.34), channel_id=1, source_target_pairs={{0,2},{1,3},{2,0},{3,1},{4,6},{5,7},{6,4},{7,5},{8,10},{9,11},{10,... | collective-permute-start | bytes 196616 | tf_op jit(solution)/shard_map/ppermute | solution.py:51
  21.8 5.8 %collective-permute-start = (bf16[32,1024]{1,0:T(8,128)(2,1)S(1)}, bf16[32,1024]{1,0:T(8,128)(2,1)S(1)}, u32[]{:S(2)}, u32[]{:S(2)}) collective-permute-start(bf16[32,1024]{1,0:T(8,128)(2,1)S(1)} %get-tuple-element.34), channel_id=1, source_target_pairs={{0,1},{1,2},{2,3},{3,0},{4,5},{5,6},{6,7},{7,4},{8,9},{9,10},{10,1... | collective-permute-start | bytes 196616 | tf_op jit(solution)/shard_map/ppermute | solution.py:51
  27.7 8.7 %collective-permute-start.3 = (bf16[128,1024]{1,0:T(8,128)(2,1)S(1)}, bf16[128,1024]{1,0:T(8,128)(2,1)S(1)}, u32[]{:S(2)}, u32[]{:S(2)}) collective-permute-start(bf16[128,1024]{1,0:T(8,128)(2,1)S(1)} %constant_dynamic-update-slice_fusion.refs_0_), channel_id=1, source_target_pairs={{0,8},{8,16},{16,24},{24,0},{1,9},{9,17},{17,25},{25,1},{2,10},{10... | collective-permute-start | bytes 786440 | tf_op jit(solution)/shard_map/ppermute | solution.py:51
  29.1 7.6 %collective-permute-start.9 = (bf16[128,1024]{1,0:T(8,128)(2,1)S(1)}, bf16[128,1024]{1,0:T(8,128)(2,1)S(1)}, u32[]{:S(2)}, u32[]{:S(2)}) collective-permute-start(bf16[128,1024]{1,0:T(8,128)(2,1)S(1)} %get-tuple-element.41.refs_4_), channel_id=1, source_target_pairs={{0,1},{1,2},{2,3},{3,0},{4,5},{5,6},{6,7},{7,4},{8,9},{9,10},{10,1... | collective-permute-start | bytes 786440 | tf_op jit(solution)/shard_map/ppermute | solution.py:51
  30.7 15.2 %collective-permute-start.12 = (bf16[8,128,256]{2,1,0:T(8,128)(2,1)S(1)}, bf16[8,128,256]{2,1,0:T(8,128)(2,1)S(1)}, u32[]{:S(2)}, u32[]{:S(2)}) collective-permute-start(bf16[8,128,256]{2,1,0:T(8,128)(2,1)S(1)} %all-to-all-done.refs_9_), channel_id=1, source_target_pairs={{0,4},{4,0},{1,5},{5,1},{2,6},{6,2},{3,7},{7,3},{8,12},{12,8},{9,1... | collective-permute-start | bytes 1572872 | tf_op jit(solution)/shard_map/ppermute | solution.py:51
  30.7 8.9 %collective-permute-start.5 = (bf16[128,1024]{1,0:T(8,128)(2,1)S(1)}, bf16[128,1024]{1,0:T(8,128)(2,1)S(1)}, u32[]{:S(2)}, u32[]{:S(2)}) collective-permute-start(bf16[128,1024]{1,0:T(8,128)(2,1)S(1)} %constant_dynamic-update-slice_fusion.refs_0_), channel_id=1, source_target_pairs={{0,24},{8,0},{16,8},{24,16},{1,25},{9,1},{17,9},{25,17},{2,26},{10... | collective-permute-start | bytes 786440 | tf_op jit(solution)/shard_map/ppermute | solution.py:51
  33.4 9.0 %collective-permute-start.11 = (bf16[128,1024]{1,0:T(8,128)(2,1)S(1)}, bf16[128,1024]{1,0:T(8,128)(2,1)S(1)}, u32[]{:S(2)}, u32[]{:S(2)}) collective-permute-start(bf16[128,1024]{1,0:T(8,128)(2,1)S(1)} %get-tuple-element.41.refs_4_), channel_id=1, source_target_pairs={{0,3},{1,0},{2,1},{3,2},{4,7},{5,4},{6,5},{7,6},{8,11},{9,8},{10,9... | collective-permute-start | bytes 786440 | tf_op jit(solution)/shard_map/ppermute | solution.py:51
  36.4 9.4 %collective-permute-start.4 = (bf16[128,1024]{1,0:T(8,128)(2,1)S(1)}, bf16[128,1024]{1,0:T(8,128)(2,1)S(1)}, u32[]{:S(2)}, u32[]{:S(2)}) collective-permute-start(bf16[128,1024]{1,0:T(8,128)(2,1)S(1)} %collective-permute-done.3.refs_1_), channel_id=1, source_target_pairs={{0,8},{8,16},{16,24},{24,0},{1,9},{9,17},{17,25},{25,1},{2,10},{10... | collective-permute-start | bytes 786440 | tf_op jit(solution)/shard_map/ppermute | solution.py:51
  36.7 9.1 %collective-permute-start.10 = (bf16[128,1024]{1,0:T(8,128)(2,1)S(1)}, bf16[128,1024]{1,0:T(8,128)(2,1)S(1)}, u32[]{:S(2)}, u32[]{:S(2)}) collective-permute-start(bf16[128,1024]{1,0:T(8,128)(2,1)S(1)} %collective-permute-done.9.refs_5_), channel_id=1, source_target_pairs={{0,1},{1,2},{2,3},{3,0},{4,5},{5,6},{6,7},{7,4},{8,9},{9,10},{10,1... | collective-permute-start | bytes 786440 | tf_op jit(solution)/shard_map/ppermute | solution.py:51
  48.0 1.5 %collective-permute-start.13 = (bf16[80,1024]{1,0:T(8,128)(2,1)S(1)}, bf16[80,1024]{1,0:T(8,128)(2,1)S(1)}, u32[]{:S(2)}, u32[]{:S(2)}) collective-permute-start(bf16[80,1024]{1,0:T(8,128)(2,1)S(1)} %get-tuple-element.43.q_own), channel_id=1, source_target_pairs={{0,4},{4,0},{1,5},{5,1},{2,6},{6,2},{3,7},{7,3},{8,12},{12,8},{9,1... | collective-permute-start | bytes 491528 | tf_op jit(solution)/shard_map/ppermute | solution.py:51
  50.2 7.9 %collective-permute-start.18 = (bf16[136,1024]{1,0:T(8,128)(2,1)S(1)}, bf16[136,1024]{1,0:T(8,128)(2,1)S(1)}, u32[]{:S(2)}, u32[]{:S(2)}) collective-permute-start(bf16[136,1024]{1,0:T(8,128)(2,1)S(1)} %get-tuple-element.47.pay), channel_id=1, source_target_pairs={{0,224},{32,0},{64,32},{96,64},{1,225},{33,1},{65,33},{97,65},{2,2... | collective-permute-start | bytes 835592 | tf_op jit(solution)/shard_map/ppermute | solution.py:69
  50.8 10.6 %collective-permute-start.14 = (bf16[136,1024]{1,0:T(8,128)(2,1)S(1)}, bf16[136,1024]{1,0:T(8,128)(2,1)S(1)}, u32[]{:S(2)}, u32[]{:S(2)}) collective-permute-start(bf16[136,1024]{1,0:T(8,128)(2,1)S(1)} %get-tuple-element.47.pay), channel_id=1, source_target_pairs={{0,32},{32,64},{64,96},{96,128},{128,160},{160,192},{192,224},{1,3... | collective-permute-start | bytes 835592 | tf_op jit(solution)/shard_map/ppermute | solution.py:65
  55.9 54.9 %collective-permute-start.25 = (bf16[2,8,64,256]{3,2,1,0:T(8,128)(2,1)S(1)}, bf16[2,8,64,256]{3,2,1,0:T(8,128)(2,1)S(1)}, u32[]{:S(2)}, u32[]{:S(2)}) collective-permute-start(bf16[2,8,64,256]{3,2,1,0:T(8,128)(2,1)S(1)} %pad_maximum_fusion.w0), channel_id=1, source_target_pairs={{0,3},{1,0},{2,1},{3,2},{4,7},{5,4},{6,5},{7,6},{8,11},{9,8},{10,9... | collective-permute-start | bytes 1572872 | tf_op jit(solution)/shard_map/ppermute | solution.py:51
  56.7 54.2 %collective-permute-start.24 = (bf16[2,8,64,256]{3,2,1,0:T(8,128)(2,1)S(1)}, bf16[2,8,64,256]{3,2,1,0:T(8,128)(2,1)S(1)}, u32[]{:S(2)}, u32[]{:S(2)}) collective-permute-start(bf16[2,8,64,256]{3,2,1,0:T(8,128)(2,1)S(1)} %pad_maximum_fusion.w0), channel_id=1, source_target_pairs={{0,2},{1,3},{2,0},{3,1},{4,6},{5,7},{6,4},{7,5},{8,10},{9,11},{10,... | collective-permute-start | bytes 1572872 | tf_op jit(solution)/shard_map/ppermute | solution.py:51
  57.1 54.5 %collective-permute-start.23 = (bf16[2,8,64,256]{3,2,1,0:T(8,128)(2,1)S(1)}, bf16[2,8,64,256]{3,2,1,0:T(8,128)(2,1)S(1)}, u32[]{:S(2)}, u32[]{:S(2)}) collective-permute-start(bf16[2,8,64,256]{3,2,1,0:T(8,128)(2,1)S(1)} %pad_maximum_fusion.w0), channel_id=1, source_target_pairs={{0,1},{1,2},{2,3},{3,0},{4,5},{5,6},{6,7},{7,4},{8,9},{9,10},{10,1... | collective-permute-start | bytes 1572872 | tf_op jit(solution)/shard_map/ppermute | solution.py:51
  58.0 13.7 %collective-permute-start.19 = (bf16[136,1024]{1,0:T(8,128)(2,1)S(1)}, bf16[136,1024]{1,0:T(8,128)(2,1)S(1)}, u32[]{:S(2)}, u32[]{:S(2)}) collective-permute-start(bf16[136,1024]{1,0:T(8,128)(2,1)S(1)} %collective-permute-done.18.refs_1_), channel_id=1, source_target_pairs={{224,192},{0,224},{32,0},{64,32},{225,193},{1,225},{33,1},{65,33},... | collective-permute-start | bytes 835592 | tf_op jit(solution)/shard_map/ppermute | solution.py:69
  61.4 12.2 %collective-permute-start.15 = (bf16[136,1024]{1,0:T(8,128)(2,1)S(1)}, bf16[136,1024]{1,0:T(8,128)(2,1)S(1)}, u32[]{:S(2)}, u32[]{:S(2)}) collective-permute-start(bf16[136,1024]{1,0:T(8,128)(2,1)S(1)} %collective-permute-done.14.refs_0_), channel_id=1, source_target_pairs={{32,64},{64,96},{96,128},{128,160},{160,192},{192,224},{33,65},{65... | collective-permute-start | bytes 835592 | tf_op jit(solution)/shard_map/ppermute | solution.py:65
  71.7 13.5 %collective-permute-start.20 = (bf16[136,1024]{1,0:T(8,128)(2,1)S(1)}, bf16[136,1024]{1,0:T(8,128)(2,1)S(1)}, u32[]{:S(2)}, u32[]{:S(2)}) collective-permute-start(bf16[136,1024]{1,0:T(8,128)(2,1)S(1)} %collective-permute-done.19.refs_1_), channel_id=1, source_target_pairs={{192,160},{224,192},{0,224},{32,0},{193,161},{225,193},{1,225},{33... | collective-permute-start | bytes 835592 | tf_op jit(solution)/shard_map/ppermute | solution.py:69
  73.6 13.5 %collective-permute-start.16 = (bf16[136,1024]{1,0:T(8,128)(2,1)S(1)}, bf16[136,1024]{1,0:T(8,128)(2,1)S(1)}, u32[]{:S(2)}, u32[]{:S(2)}) collective-permute-start(bf16[136,1024]{1,0:T(8,128)(2,1)S(1)} %collective-permute-done.15.refs_0_), channel_id=1, source_target_pairs={{64,96},{96,128},{128,160},{160,192},{192,224},{65,97},{97,129},{1... | collective-permute-start | bytes 835592 | tf_op jit(solution)/shard_map/ppermute | solution.py:65
  85.3 12.6 %collective-permute-start.21 = (bf16[136,512]{1,0:T(8,128)(2,1)S(1)}, bf16[136,512]{1,0:T(8,128)(2,1)S(1)}, u32[]{:S(2)}, u32[]{:S(2)}) collective-permute-start(bf16[136,512]{1,0:T(8,128)(2,1)S(1)} %slice.17), channel_id=1, source_target_pairs={{160,128},{192,160},{224,192},{0,224},{161,129},{193,161},{225,193... | collective-permute-start | bytes 417800 | tf_op jit(solution)/shard_map/ppermute | solution.py:69
  87.2 10.7 %collective-permute-start.17 = (bf16[136,512]{1,0:T(8,128)(2,1)S(1)}, bf16[136,512]{1,0:T(8,128)(2,1)S(1)}, u32[]{:S(2)}, u32[]{:S(2)}) collective-permute-start(bf16[136,512]{1,0:T(8,128)(2,1)S(1)} %slice.16), channel_id=1, source_target_pairs={{96,128},{128,160},{160,192},{192,224},{97,129},{129,161},{161,193... | collective-permute-start | bytes 417800 | tf_op jit(solution)/shard_map/ppermute | solution.py:65
  101.9 1.7 %collective-permute-start.22 = (f32[72,1024]{1,0:T(8,128)S(1)}, f32[72,1024]{1,0:T(8,128)S(1)}, u32[]{:S(2)}, u32[]{:S(2)}) collective-permute-start(f32[72,1024]{1,0:T(8,128)S(1)} %get-tuple-element.61), channel_id=1, source_target_pairs={{0,4},{4,0},{1,5},{5,1},{2,6},{6,2},{3,7},{7,3},{8,12},{12,8},{9,1... | collective-permute-start | bytes 884744 | tf_op jit(solution)/shard_map/ppermute | solution.py:51
  104.7 14.2 %copy-start.4 = (f32[1024]{0:T(1024)S(1)}, f32[1024]{0:T(1024)}, u32[]{:S(2)}) copy-start(f32[1024]{0:T(1024)} %param.17) | copy-start | bytes 12292
  104.7 14.0 %all-to-all-start.1 = ((bf16[16,2,2048]{2,1,0:T(2,128)(2,1)}), bf16[16,2,2048]{2,1,0:T(2,128)(2,1)S(1)}, u32[]{:S(2)}, u32[]{:S(2)}) async-start(bf16[16,2,2048]{2,1,0:T(2,128)(2,1)} %reshape.4), calls=%async_computation.1 | async-start | bytes 262144 | tf_op jit(solution)/shard_map/all_to_all | solution.py:464
  110.8 0.8 copy-start
  111.7 0.8 copy-start.2
  112.5 1.0 copy-start.1
  113.5 1.0 copy-start.3

commit v8 on v6

--- a/solution.py
+++ b/solution.py
@@ -82,16 +82,16 @@
     lo[...] = rows[0:32, :]
     hi[...] = rows[32:64, :]
     o0[...] = rows[64:80, 768:1024]
-    head = lax.broadcasted_iota(jnp.int32, (16, HD), 0)
-    gates = rows[80:96, 0:128].astype(F32)
+    head = lax.broadcasted_iota(jnp.int32, (16, 256), 0)
+    lane = lax.broadcasted_iota(jnp.int32, (16, 256), 1)
+    pick = jnp.where(lane // HD == head, 1.0, 0.0).astype(BF16)
+    gates = lax.dot_general(
+        rows[80:96, 0:128], pick, (((0,), (0,)), ((), ())), preferred_element_type=F32
+    )[0:16].astype(BF16)
     for h in range(NX):
-        pick = jnp.where(head == h, 1.0, 0.0)
-        gate = lax.dot_general(
-            gates, pick, (((0,), (0,)), ((), ())), precision=lax.Precision.HIGHEST,
-            preferred_element_type=F32,
-        )[0:16]
+        at = slice(h * HD, (h + 1) * HD)
         mine = [rows[64:80, i * 256 + h * HD : i * 256 + h * HD + HD] for i in range(3)]
-        heads[h] = jnp.concatenate(mine + [gate.astype(BF16)], axis=1)
+        heads[h] = jnp.concatenate(mine + [gates[:, at]], axis=1)
     p0[...] = heads[x]
     for k, s in enumerate((s1, s2, s3)):
         s[0:32, :] = rows[32:64, :]
@@ -202,13 +202,14 @@
 
 
 def place_chunk(pay, i, kx, vx):
+    n = pay.shape[1]
     fill = jnp.zeros((56, 128), F32)
-    for r in range(8):
+    for r in range(n // 128):
         lanes = slice(r * 128, (r + 1) * 128)
         tile = jnp.concatenate([pay[64:136, lanes].astype(F32), fill], axis=0)
         kx[i, lanes, :] = tile.T.astype(BF16)
-    vx[i, 0:64, :] = pay[0:64, :]
-    vx[i, 64:80, :] = jnp.ones((16, KEYS), BF16)
+    vx[i, 0:64, 0:n] = pay[0:64, :]
+    vx[i, 64:80, 0:n] = jnp.ones((16, n), BF16)
 
 
 def stages(q, acc, m, kx, vx, move, work):
@@ -245,30 +246,30 @@
     return score, weigh, add
 
 
-def absorb(count, q, acc, m, kx, vx, move, work):
+def absorb(count, q, acc, m, kx, vx, move, work, n=KEYS):
     tiles = QS // BLK
     score, weigh, add = stages(q, acc, m, kx, vx, move, work)
     probs, fades = work[4:6], work[6:8]
 
     @pl.when(count > 0)
     def _():
-        probs[1][...] = jnp.zeros((KEYS, BLK), BF16)
+        probs[1][0:n] = jnp.zeros((n, BLK), BF16)
         fades[1][...] = jnp.ones((8, BLK), F32)
-        score(0, 0)
+        score(0, 0, n)
         last = count * tiles - 1
 
         def two_tiles(j, carry):
             t = 2 * j
-            add(jnp.maximum(t - 1, 0), 1)
-            weigh(t, 0)
-            score(t + 1, 1)
-            add(t, 0)
-            weigh(t + 1, 1)
-            score(jnp.minimum(t + 2, last), 0)
+            add(jnp.maximum(t - 1, 0), 1, n)
+            weigh(t, 0, n)
+            score(t + 1, 1, n)
+            add(t, 0, n)
+            weigh(t + 1, 1, n)
+            score(jnp.minimum(t + 2, last), 0, n)
             return carry
 
         lax.fori_loop(0, count * (tiles // 2), two_tiles, 0)
-        add(last, 1)
+        add(last, 1, n)
 
 
 def first_body(idx, q, pay, acc, m, sums, kx, vx, move, *bufs):
@@ -292,12 +293,12 @@
     sums[...] = jnp.broadcast_to(chunk_total(pay), sums.shape)
 
 
-def step_body(k, idx, q, *refs):
+def step_body(k, part, idx, q, *refs):
     z = idx[0]
     n_pay = 2 if k < 4 else 1
     pays, refs = refs[:n_pay], refs[n_pay:]
     acc0, m0, sums0, refs = refs[0], refs[1], refs[2], refs[3:]
-    if k < 4:
+    if part < 2:
         acc, m, sums, kx, vx, move, *bufs = refs
     else:
         out_own, out_sib, kx, vx, move, *bufs, sums = refs
@@ -309,7 +310,8 @@
     def _():
         place_chunk(pays[0], 0, kx, vx)
         move[0] = sums0[...]
-        sums[...] = sums0[...] + jnp.broadcast_to(chunk_total(pays[0]), sums.shape)
+        if part != 1:
+            sums[...] = sums0[...] + jnp.broadcast_to(chunk_total(pays[0]), sums.shape)
 
     if k < 4:
         count = count + (z + k >= 8).astype(jnp.int32)
@@ -320,8 +322,8 @@
             move[1] = jnp.zeros(sums.shape, F32)
             m[1] = m[1] + chunk_total(pays[1])[:, 0:1]
 
-    absorb(count, q, acc, m, kx, vx, move, bufs)
-    if k == 4:
+    absorb(count, q, acc, m, kx, vx, move, bufs, pays[0].shape[1])
+    if part == 2:
         c = idx[2]
         row = lax.broadcasted_iota(jnp.int32, (8, BLK), 0)
         for b in range(4):
@@ -434,27 +436,28 @@
     w_o, _ = lax.optimization_barrier((w_o, sums))
     w_o = direct(w_o, "y")
 
-    for k in range(1, 5):
-        pays = (right, left) if k < 4 else (right,)
-        if k < 4:
-            right = step_right(pays[0], k + 1)
+    for k, part in ((1, 0), (2, 0), (3, 0), (4, 1), (4, 2)):
+        pays = (right, left) if k < 4 else (halves[part - 1],)
         if k < 3:
-            left = step_left(pays[1], k + 1)
+            right, left = step_right(right, k + 1), step_left(left, k + 1)
+        elif k == 3:
+            halves = [step_right(right[:, : KEYS // 2], 4), step_right(right[:, KEYS // 2 :], 4)]
         ins = (idx, q) + pays + (acc, m, sums)
-        if k < 4:
-            outs, scratch, aliases = (acc_t, m_t, sums_t), work, {4: 0, 5: 1}
+        at = len(pays) + 2
+        if part < 2:
+            outs, scratch, aliases = (acc_t, m_t, sums_t), work, {at: 0, at + 1: 1}
         else:
             outs, aliases = (sds((72, KEYS), F32), sds((72, KEYS), F32)), None
             scratch = work + [pltpu.VMEM(sums_t.shape, F32)]
         res = call(
-            functools.partial(step_body, k),
+            functools.partial(step_body, k, part),
             outs,
             [SMEM] + [VMEM] * (len(ins) - 1),
             scratch,
-            6e9,
+            6e9 if k < 4 else 2e9,
             aliases,
         )(*ins)
-        if k < 4:
+        if part < 2:
             acc, m, sums = res
     sib = shift(res[1], "c", 1)
     w_full = call(assemble_body, sds((D, D), BF16), [SMEM] + [VMEM] * 4)(idx, *w_o)

time: 118 us -> 121 us (1.025)
  starting transfers between devices: 53.3 us -> 55.2 us
    ppermute x4 -> x5, starting transfers between devices: 18 us -> 20.4 us  [step_right(): return lax.ppermute(x, 'z', [(i, i + 1) for i in range(k - 1, NZ - 1)])]
    pallas_call x4 -> x5, Pallas kernels: 18.5 us -> 19.9 us  [shards(): call(functools.partial(step_body, k, part), outs, [SMEM] + [VMEM] * (len(...]
    ppermute x4 -> x5, waiting for transfers between devices: 4.93 us -> 4.94 us  [step_right(): return lax.ppermute(x, 'z', [(i, i + 1) for i in range(k - 1, NZ - 1)])]
  transfers between devices with their start and end apart: 27 -> 28, of which waited for: 15 -> 15; matrix products, arithmetic and copies ran while one was open for 1% -> 1% of each run, Pallas kernels for 19% -> 20%
where the time goes in v8:
time: 121 us
  starting transfers between devices  55.2 us (46%)
  Pallas kernels  29.7 us (25%)
  waiting for transfers between devices  29.3 us (24%)
  local copies, waits for them, and re-layouts  4.91 us (4%)
    ppermute x5, starting transfers between devices, step_right(): return lax.ppermute(x, 'z', [(i, i + 1) for i in range(k - 1, NZ - 1)])  20.4 us
    ppermute x18, waiting for transfers between devices, shift(): return lax.ppermute(x, axis, [(i, (i + k) % n) for i in range(n)])  20.4 us
    pallas_call x5, Pallas kernels, shards(): call(functools.partial(step_body, k, part), outs, [SMEM] + [VMEM] * (len(...  19.9 us
    ppermute x18, starting transfers between devices, shift(): return lax.ppermute(x, axis, [(i, (i + k) % n) for i in range(n)])  19.7 us
    all_to_all x1, starting transfers between devices, shards(): w_own = lax.all_to_all(chunk, 'z', 0, 0, tiled=True)  6.75 us
    all_to_all x1, starting transfers between devices, shards(): att = lax.all_to_all(att.reshape(16, 64, HD), ('x', 'y'), 0, 0, tiled=True)  5.67 us
    ppermute x5, waiting for transfers between devices, step_right(): return lax.ppermute(x, 'z', [(i, i + 1) for i in range(k - 1, NZ - 1)])  4.94 us
    unnamed x19, local copies, waits for them, and re-layouts  4.85 us
  transfers between devices with their start and end apart: 28, of which 15 were waited for; matrix products, arithmetic and copies ran while one was open for 1% of the time, Pallas kernels for 20%

profile of v8, /device:TPU:160, one launch (start us, length us, event | category | flops | bytes accessed | tf_op | source)
XLA Modules:
  0.0 120.6 jit_solution(2475545752663347384)
XLA Ops:
  0.1 1.0 pad_add_fusion.rows
  1.1 0.8 shard_map.91
  1.9 1.6 %collective-permute-start.6 = (bf16[48,1024]{1,0:T(8,128)(2,1)S(1)}, bf16[48,1024]{1,0:T(8,128)(2,1)S(1)}, u32[]{:S(2)}, u32[]{:S(2)}) collective-permute-start(bf16[48,1024]{1,0:T(8,128)(2,1)S(1)} %get-tuple-element.41), channel_id=1, source_target_pairs={{0,8},{8,16},{16,24},{24,0},{1,9},{9,17},{17,25},{25,1},{2,10},{10... | collective-permute-start | bytes 294920 | tf_op jit(solution)/shard_map/ppermute | solution.py:51
  3.5 2.7 %collective-permute-start.7 = (bf16[48,1024]{1,0:T(8,128)(2,1)S(1)}, bf16[48,1024]{1,0:T(8,128)(2,1)S(1)}, u32[]{:S(2)}, u32[]{:S(2)}) collective-permute-start(bf16[48,1024]{1,0:T(8,128)(2,1)S(1)} %get-tuple-element.42), channel_id=1, source_target_pairs={{0,16},{8,24},{16,0},{24,8},{1,17},{9,25},{17,1},{25,9},{2,18},{10... | collective-permute-start | bytes 294920 | tf_op jit(solution)/shard_map/ppermute | solution.py:51
  6.2 1.4 %collective-permute-start.8 = (bf16[48,1024]{1,0:T(8,128)(2,1)S(1)}, bf16[48,1024]{1,0:T(8,128)(2,1)S(1)}, u32[]{:S(2)}, u32[]{:S(2)}) collective-permute-start(bf16[48,1024]{1,0:T(8,128)(2,1)S(1)} %get-tuple-element.43), channel_id=1, source_target_pairs={{0,24},{8,0},{16,8},{24,16},{1,25},{9,1},{17,9},{25,17},{2,26},{10... | collective-permute-start | bytes 294920 | tf_op jit(solution)/shard_map/ppermute | solution.py:51
  8.0 2.8 %collective-permute-done.7.r2 = bf16[48,1024]{1,0:T(8,128)(2,1)S(1)} collective-permute-done((bf16[48,1024]{1,0:T(8,128)(2,1)S(1)}, bf16[48,1024]{1,0:T(8,128)(2,1)S(1)}, u32[]{:S(2)}, u32[]{:S(2)}) %collective-permute-start.7) | collective-permute-done | bytes 98336 | tf_op jit(solution)/shard_map/ppermute | solution.py:51
  10.8 0.9 shard_map.92
  11.7 6.8 %all-to-all-start = ((bf16[8,128,256]{2,1,0:T(8,128)(2,1)}), bf16[8,128,256]{2,1,0:T(8,128)(2,1)S(1)}, u32[]{:S(2)}, u32[]{:S(2)}) async-start(bf16[8,128,256]{2,1,0:T(8,128)(2,1)} %get-tuple-element.45), calls=%async_computation | async-start | bytes 1048576 | tf_op jit(solution)/shard_map/all_to_all | solution.py:397
  18.4 3.0 %collective-permute-start.2 = (bf16[32,1024]{1,0:T(8,128)(2,1)S(1)}, bf16[32,1024]{1,0:T(8,128)(2,1)S(1)}, u32[]{:S(2)}, u32[]{:S(2)}) collective-permute-start(bf16[32,1024]{1,0:T(8,128)(2,1)S(1)} %get-tuple-element.37), channel_id=1, source_target_pairs={{0,3},{1,0},{2,1},{3,2},{4,7},{5,4},{6,5},{7,6},{8,11},{9,8},{10,9... | collective-permute-start | bytes 196616 | tf_op jit(solution)/shard_map/ppermute | solution.py:51
  22.1 1.0 collective-permute-start
  23.0 4.9 %collective-permute-done = bf16[32,1024]{1,0:T(8,128)(2,1)S(1)} collective-permute-done((bf16[32,1024]{1,0:T(8,128)(2,1)S(1)}, bf16[32,1024]{1,0:T(8,128)(2,1)S(1)}, u32[]{:S(2)}, u32[]{:S(2)}) %collective-permute-start) | collective-permute-done | bytes 65568 | tf_op jit(solution)/shard_map/ppermute | solution.py:51
  28.0 1.4 %collective-permute-start.3 = (bf16[128,1024]{1,0:T(8,128)(2,1)S(1)}, bf16[128,1024]{1,0:T(8,128)(2,1)S(1)}, u32[]{:S(2)}, u32[]{:S(2)}) collective-permute-start(bf16[128,1024]{1,0:T(8,128)(2,1)S(1)} %constant_dynamic-update-slice_fusion.refs_0_), channel_id=1, source_target_pairs={{0,8},{8,16},{16,24},{24,0},{1,9},{9,17},{17,25},{25,1},{2,10},{10... | collective-permute-start | bytes 786440 | tf_op jit(solution)/shard_map/ppermute | solution.py:51
  29.4 1.0 all-to-all-done.refs_9_
  30.3 2.7 %collective-permute-start.5 = (bf16[128,1024]{1,0:T(8,128)(2,1)S(1)}, bf16[128,1024]{1,0:T(8,128)(2,1)S(1)}, u32[]{:S(2)}, u32[]{:S(2)}) collective-permute-start(bf16[128,1024]{1,0:T(8,128)(2,1)S(1)} %constant_dynamic-update-slice_fusion.refs_0_), channel_id=1, source_target_pairs={{0,24},{8,0},{16,8},{24,16},{1,25},{9,1},{17,9},{25,17},{2,26},{10... | collective-permute-start | bytes 786440 | tf_op jit(solution)/shard_map/ppermute | solution.py:51
  33.0 3.0 %collective-permute-start.11 = (bf16[128,1024]{1,0:T(8,128)(2,1)S(1)}, bf16[128,1024]{1,0:T(8,128)(2,1)S(1)}, u32[]{:S(2)}, u32[]{:S(2)}) collective-permute-start(bf16[128,1024]{1,0:T(8,128)(2,1)S(1)} %get-tuple-element.44.refs_4_), channel_id=1, source_target_pairs={{0,3},{1,0},{2,1},{3,2},{4,7},{5,4},{6,5},{7,6},{8,11},{9,8},{10,9... | collective-permute-start | bytes 786440 | tf_op jit(solution)/shard_map/ppermute | solution.py:51
  36.0 0.9 collective-permute-done.9.refs_5_
  37.0 2.3 %collective-permute-done.5.refs_3_ = bf16[128,1024]{1,0:T(8,128)(2,1)S(1)} collective-permute-done((bf16[128,1024]{1,0:T(8,128)(2,1)S(1)}, bf16[128,1024]{1,0:T(8,128)(2,1)S(1)}, u32[]{:S(2)}, u32[]{:S(2)}) %collective-permute-start.5) | collective-permute-done | bytes 262176 | tf_op jit(solution)/shard_map/ppermute | solution.py:51
  39.2 2.7 %collective-permute-done.11.refs_7_ = bf16[128,1024]{1,0:T(8,128)(2,1)S(1)} collective-permute-done((bf16[128,1024]{1,0:T(8,128)(2,1)S(1)}, bf16[128,1024]{1,0:T(8,128)(2,1)S(1)}, u32[]{:S(2)}, u32[]{:S(2)}) %collective-permute-start.11) | collective-permute-done | bytes 262176 | tf_op jit(solution)/shard_map/ppermute | solution.py:51
  42.0 3.4 %collective-permute-done.4.refs_2_ = bf16[128,1024]{1,0:T(8,128)(2,1)S(1)} collective-permute-done((bf16[128,1024]{1,0:T(8,128)(2,1)S(1)}, bf16[128,1024]{1,0:T(8,128)(2,1)S(1)}, u32[]{:S(2)}, u32[]{:S(2)}) %collective-permute-start.4) | collective-permute-done | bytes 262176 | tf_op jit(solution)/shard_map/ppermute | solution.py:51
  45.5 2.1 %shard_map.93 = (bf16[80,1024]{1,0:T(8,128)(2,1)S(1)}, bf16[128,1024]{1,0:T(8,128)(2,1)S(1)}, f32[8,1024]{1,0:T(8,128)S(1)}) custom-call(s32[4]{0:T(128)S(1)} %pad_add_fusion.1.idx, f32[4]{0:T(128)S(1)} %copy-done.6, bf16[128,1024]{1,0:T(8,128)(2,1)S(1)} %constant_dynamic-update-slice_fusion.refs_0_, bf16[128,1024]{1,0:T(8,128)(2,1)S(1)} %collective-permute-done.3.refs_1_, ...), custom_call_target="tpu_custom_call" | custom-call | flops 2000000000 | bytes 1048576 | tf_op jit(solution)/shard_map/pallas_call | solution.py:402
  47.8 1.3 %collective-permute-done.13.q_sib = bf16[80,1024]{1,0:T(8,128)(2,1)S(1)} collective-permute-done((bf16[80,1024]{1,0:T(8,128)(2,1)S(1)}, bf16[80,1024]{1,0:T(8,128)(2,1)S(1)}, u32[]{:S(2)}, u32[]{:S(2)}) %collective-permute-start.13) | collective-permute-done | bytes 163872 | tf_op jit(solution)/shard_map/ppermute | solution.py:51
  50.5 3.3 %collective-permute-start.14 = (bf16[136,1024]{1,0:T(8,128)(2,1)S(1)}, bf16[136,1024]{1,0:T(8,128)(2,1)S(1)}, u32[]{:S(2)}, u32[]{:S(2)}) collective-permute-start(bf16[136,1024]{1,0:T(8,128)(2,1)S(1)} %get-tuple-element.50.pay), channel_id=1, source_target_pairs={{0,32},{32,64},{64,96},{96,128},{128,160},{160,192},{192,224},{1,3... | collective-permute-start | bytes 835592 | tf_op jit(solution)/shard_map/ppermute | solution.py:65
  53.7 2.7 %shard_map.95 = (f32[2,80,2048]{2,1,0:T(8,128)S(1)}, f32[2,8,2048]{2,1,0:T(8,128)S(1)}, f32[8,256]{1,0:T(8,128)S(1)}) custom-call(s32[4]{0:T(128)S(1)} %pad_add_fusion.1.idx, bf16[128,2048]{1,0:T(8,128)(2,1)S(1)} %get-tuple-element.49.q, bf16[136,1024]{1,0:T(8,128)(2,1)S(1)} %get-tuple-element.50.pay), custom_call_target="tpu_custom_call" | custom-call | flops 3000000000 | bytes 1048576 | tf_op jit(solution)/shard_map/pallas_call | solution.py:431
  56.4 0.7 collective-permute-start.25
  57.6 0.9 collective-permute-start.23
  59.2 1.9 %collective-permute-done.14.refs_0_ = bf16[136,1024]{1,0:T(8,128)(2,1)S(1)} collective-permute-done((bf16[136,1024]{1,0:T(8,128)(2,1)S(1)}, bf16[136,1024]{1,0:T(8,128)(2,1)S(1)}, u32[]{:S(2)}, u32[]{:S(2)}) %collective-permute-start.14) | collective-permute-done | bytes 278560 | tf_op jit(solution)/shard_map/ppermute | solution.py:65
  61.1 3.1 %collective-permute-start.15 = (bf16[136,1024]{1,0:T(8,128)(2,1)S(1)}, bf16[136,1024]{1,0:T(8,128)(2,1)S(1)}, u32[]{:S(2)}, u32[]{:S(2)}) collective-permute-start(bf16[136,1024]{1,0:T(8,128)(2,1)S(1)} %collective-permute-done.14.refs_0_), channel_id=1, source_target_pairs={{32,64},{64,96},{96,128},{128,160},{160,192},{192,224},{33,65},{65... | collective-permute-start | bytes 835592 | tf_op jit(solution)/shard_map/ppermute | solution.py:65
  64.2 3.9 %shard_map.96 = (f32[2,80,2048]{2,1,0:T(8,128)S(1)}, f32[2,8,2048]{2,1,0:T(8,128)S(1)}, f32[8,256]{1,0:T(8,128)S(1)}) custom-call(s32[4]{0:T(128)S(1)} %pad_add_fusion.1.idx, bf16[128,2048]{1,0:T(8,128)(2,1)S(1)} %get-tuple-element.49.q, bf16[136,1024]{1,0:T(8,128)(2,1)S(1)} %collective-permute-done.14.refs_0_, ...), custom_call_target="tpu_custom_call", output_to_operand_aliasing={{0}: (4, {}), {1}: (5, {})} | custom-call | flops 6000000000 | bytes 1048576 | tf_op jit(solution)/shard_map/pallas_call | solution.py:452
  68.1 1.3 %collective-permute-start.21 = (bf16[136,1024]{1,0:T(8,128)(2,1)S(1)}, bf16[136,1024]{1,0:T(8,128)(2,1)S(1)}, u32[]{:S(2)}, u32[]{:S(2)}) collective-permute-start(bf16[136,1024]{1,0:T(8,128)(2,1)S(1)} %collective-permute-done.20.refs_1_), channel_id=1, source_target_pairs={{192,160},{224,192},{0,224},{193,161},{225,193},{1,225},{194,162},... | collective-permute-start | bytes 835592 | tf_op jit(solution)/shard_map/ppermute | solution.py:69
  69.4 1.5 %collective-permute-done.15.refs_0_ = bf16[136,1024]{1,0:T(8,128)(2,1)S(1)} collective-permute-done((bf16[136,1024]{1,0:T(8,128)(2,1)S(1)}, bf16[136,1024]{1,0:T(8,128)(2,1)S(1)}, u32[]{:S(2)}, u32[]{:S(2)}) %collective-permute-start.15) | collective-permute-done | bytes 278560 | tf_op jit(solution)/shard_map/ppermute | solution.py:65
  70.8 5.5 %collective-permute-start.16 = (bf16[136,1024]{1,0:T(8,128)(2,1)S(1)}, bf16[136,1024]{1,0:T(8,128)(2,1)S(1)}, u32[]{:S(2)}, u32[]{:S(2)}) collective-permute-start(bf16[136,1024]{1,0:T(8,128)(2,1)S(1)} %collective-permute-done.15.refs_0_), channel_id=1, source_target_pairs={{64,96},{96,128},{128,160},{160,192},{192,224},{65,97},{97,129},{1... | collective-permute-start | bytes 835592 | tf_op jit(solution)/shard_map/ppermute | solution.py:65
  76.4 3.9 %shard_map.97 = (f32[2,80,2048]{2,1,0:T(8,128)S(1)}, f32[2,8,2048]{2,1,0:T(8,128)S(1)}, f32[8,256]{1,0:T(8,128)S(1)}) custom-call(s32[4]{0:T(128)S(1)} %pad_add_fusion.1.idx, bf16[128,2048]{1,0:T(8,128)(2,1)S(1)} %get-tuple-element.49.q, bf16[136,1024]{1,0:T(8,128)(2,1)S(1)} %collective-permute-done.15.refs_0_, ...), custom_call_target="tpu_custom_call", output_to_operand_aliasing={{0}: (4, {}), {1}: (5, {})} | custom-call | flops 6000000000 | bytes 1048576 | tf_op jit(solution)/shard_map/pallas_call | solution.py:452
  80.3 1.6 %collective-permute-done.16.refs_0_ = bf16[136,1024]{1,0:T(8,128)(2,1)S(1)} collective-permute-done((bf16[136,1024]{1,0:T(8,128)(2,1)S(1)}, bf16[136,1024]{1,0:T(8,128)(2,1)S(1)}, u32[]{:S(2)}, u32[]{:S(2)}) %collective-permute-start.16) | collective-permute-done | bytes 278560 | tf_op jit(solution)/shard_map/ppermute | solution.py:65
  81.9 6.1 %collective-permute-start.18 = (bf16[136,512]{1,0:T(8,128)(2,1)S(1)}, bf16[136,512]{1,0:T(8,128)(2,1)S(1)}, u32[]{:S(2)}, u32[]{:S(2)}) collective-permute-start(bf16[136,512]{1,0:T(8,128)(2,1)S(1)} %get-tuple-element.69), channel_id=1, source_target_pairs={{96,128},{128,160},{160,192},{192,224},{97,129},{129,161},{161,193... | collective-permute-start | bytes 417800 | tf_op jit(solution)/shard_map/ppermute | solution.py:65
  88.0 2.4 %collective-permute-start.17 = (bf16[136,512]{1,0:T(8,128)(2,1)S(1)}, bf16[136,512]{1,0:T(8,128)(2,1)S(1)}, u32[]{:S(2)}, u32[]{:S(2)}) collective-permute-start(bf16[136,512]{1,0:T(8,128)(2,1)S(1)} %get-tuple-element.70), channel_id=1, source_target_pairs={{96,128},{128,160},{160,192},{192,224},{97,129},{129,161},{161,193... | collective-permute-start | bytes 417800 | tf_op jit(solution)/shard_map/ppermute | solution.py:65
  90.4 6.7 %shard_map.98 = (f32[2,80,2048]{2,1,0:T(8,128)S(1)}, f32[2,8,2048]{2,1,0:T(8,128)S(1)}, f32[8,256]{1,0:T(8,128)S(1)}) custom-call(s32[4]{0:T(128)S(1)} %pad_add_fusion.1.idx, bf16[128,2048]{1,0:T(8,128)(2,1)S(1)} %get-tuple-element.49.q, bf16[136,1024]{1,0:T(8,128)(2,1)S(1)} %collective-permute-done.16.refs_0_, ...), custom_call_target="tpu_custom_call", output_to_operand_aliasing={{0}: (4, {}), {1}: (5, {})} | custom-call | flops 6000000000 | bytes 1048576 | tf_op jit(solution)/shard_map/pallas_call | solution.py:452
  97.2 2.6 %shard_map.99 = (f32[2,80,2048]{2,1,0:T(8,128)S(1)}, f32[2,8,2048]{2,1,0:T(8,128)S(1)}, f32[8,256]{1,0:T(8,128)S(1)}) custom-call(s32[4]{0:T(128)S(1)} %pad_add_fusion.1.idx, bf16[128,2048]{1,0:T(8,128)(2,1)S(1)} %get-tuple-element.49.q, bf16[136,512]{1,0:T(8,128)(2,1)S(1)} %collective-permute-done.18.refs_0_, ...), custom_call_target="tpu_custom_call", output_to_operand_aliasing={{0}: (3, {}), {1}: (4, {})} | custom-call | flops 2000000000 | bytes 1048576 | tf_op jit(solution)/shard_map/pallas_call | solution.py:452
  99.8 2.7 %shard_map.100 = (f32[72,1024]{1,0:T(8,128)S(1)}, f32[72,1024]{1,0:T(8,128)S(1)}) custom-call(s32[4]{0:T(128)S(1)} %pad_add_fusion.1.idx, bf16[128,2048]{1,0:T(8,128)(2,1)S(1)} %get-tuple-element.49.q, bf16[136,512]{1,0:T(8,128)(2,1)S(1)} %collective-permute-done.17.refs_0_, f32[2,80,2048]{2,1,0:T(8,128)S(1)} %get-tuple-element.63.refs_1_, ...), custom_call_target="tpu_custom_call" | custom-call | flops 2000000000 | bytes 1048576 | tf_op jit(solution)/shard_map/pallas_call | solution.py:452
  102.7 1.6 %collective-permute-done.22.sib = f32[72,1024]{1,0:T(8,128)S(1)} collective-permute-done((f32[72,1024]{1,0:T(8,128)S(1)}, f32[72,1024]{1,0:T(8,128)S(1)}, u32[]{:S(2)}, u32[]{:S(2)}) %collective-permute-start.22) | collective-permute-done | bytes 294944 | tf_op jit(solution)/shard_map/ppermute | solution.py:51
  104.4 0.9 reshape.4
  105.3 5.7 %all-to-all-start.1 = ((bf16[16,2,2048]{2,1,0:T(2,128)(2,1)}), bf16[16,2,2048]{2,1,0:T(2,128)(2,1)S(1)}, u32[]{:S(2)}, u32[]{:S(2)}) async-start(bf16[16,2,2048]{2,1,0:T(2,128)(2,1)} %reshape.4), calls=%async_computation.1 | async-start | bytes 262144 | tf_op jit(solution)/shard_map/all_to_all | solution.py:465
  111.0 0.8 copy-done
  111.8 0.8 copy-done.2
  112.6 1.0 copy-done.1
  113.7 1.0 copy-done.3
  114.7 1.0 shard_map.102.w
  115.8 3.1 %all-to-all-done.1 = bf16[16,2,2048]{2,1,0:T(2,128)(2,1)S(1)} async-done(((bf16[16,2,2048]{2,1,0:T(2,128)(2,1)}), bf16[16,2,2048]{2,1,0:T(2,128)(2,1)S(1)}, u32[]{:S(2)}, u32[]{:S(2)}) %all-to-all-start.1) | async-done | bytes 131104 | tf_op jit(solution)/shard_map/all_to_all | solution.py:465
  119.0 1.5 %shard_map.103 = bf16[64,1024]{1,0:T(8,128)(2,1)} custom-call(bf16[16,64,64]{2,1,0:T(8,128)(2,1)S(1)} %reshape.5.att, f32[1,1024]{1,0:T(1,128)S(1)} %bitcast.13, bf16[1024,1024]{1,0:T(8,128)(2,1)S(1)} %shard_map.102.w), custom_call_target="tpu_custom_call" | custom-call | flops 100000000 | bytes 1048576 | tf_op jit(solution)/shard_map/pallas_call | solution.py:466
  (47 shorter events, 4.4 us)
Async XLA Ops:
  1.9 43.6 %copy-start.5 = (f32[1024]{0:T(1024)S(1)}, f32[1024]{0:T(1024)}, u32[]{:S(2)}) copy-start(f32[1024]{0:T(1024)} %param.10) | copy-start | bytes 12292
  1.9 43.6 %copy-start.6 = (f32[4]{0:T(128)S(1)}, f32[4]{0:T(128)}, u32[]{:S(2)}) copy-start(f32[4]{0:T(128)} %offs.1) | copy-start | bytes 52
  1.9 6.1 %collective-permute-start.6 = (bf16[48,1024]{1,0:T(8,128)(2,1)S(1)}, bf16[48,1024]{1,0:T(8,128)(2,1)S(1)}, u32[]{:S(2)}, u32[]{:S(2)}) collective-permute-start(bf16[48,1024]{1,0:T(8,128)(2,1)S(1)} %get-tuple-element.41), channel_id=1, source_target_pairs={{0,8},{8,16},{16,24},{24,0},{1,9},{9,17},{17,25},{25,1},{2,10},{10... | collective-permute-start | bytes 294920 | tf_op jit(solution)/shard_map/ppermute | solution.py:51
  3.5 7.3 %collective-permute-start.7 = (bf16[48,1024]{1,0:T(8,128)(2,1)S(1)}, bf16[48,1024]{1,0:T(8,128)(2,1)S(1)}, u32[]{:S(2)}, u32[]{:S(2)}) collective-permute-start(bf16[48,1024]{1,0:T(8,128)(2,1)S(1)} %get-tuple-element.42), channel_id=1, source_target_pairs={{0,16},{8,24},{16,0},{24,8},{1,17},{9,25},{17,1},{25,9},{2,18},{10... | collective-permute-start | bytes 294920 | tf_op jit(solution)/shard_map/ppermute | solution.py:51
  6.2 4.6 %collective-permute-start.8 = (bf16[48,1024]{1,0:T(8,128)(2,1)S(1)}, bf16[48,1024]{1,0:T(8,128)(2,1)S(1)}, u32[]{:S(2)}, u32[]{:S(2)}) collective-permute-start(bf16[48,1024]{1,0:T(8,128)(2,1)S(1)} %get-tuple-element.43), channel_id=1, source_target_pairs={{0,24},{8,0},{16,8},{24,16},{1,25},{9,1},{17,9},{25,17},{2,26},{10... | collective-permute-start | bytes 294920 | tf_op jit(solution)/shard_map/ppermute | solution.py:51
  11.7 18.7 %all-to-all-start = ((bf16[8,128,256]{2,1,0:T(8,128)(2,1)}), bf16[8,128,256]{2,1,0:T(8,128)(2,1)S(1)}, u32[]{:S(2)}, u32[]{:S(2)}) async-start(bf16[8,128,256]{2,1,0:T(8,128)(2,1)} %get-tuple-element.45), calls=%async_computation | async-start | bytes 1048576 | tf_op jit(solution)/shard_map/all_to_all | solution.py:397
  18.4 9.5 %collective-permute-start.2 = (bf16[32,1024]{1,0:T(8,128)(2,1)S(1)}, bf16[32,1024]{1,0:T(8,128)(2,1)S(1)}, u32[]{:S(2)}, u32[]{:S(2)}) collective-permute-start(bf16[32,1024]{1,0:T(8,128)(2,1)S(1)} %get-tuple-element.37), channel_id=1, source_target_pairs={{0,3},{1,0},{2,1},{3,2},{4,7},{5,4},{6,5},{7,6},{8,11},{9,8},{10,9... | collective-permute-start | bytes 196616 | tf_op jit(solution)/shard_map/ppermute | solution.py:51
  21.4 6.5 %collective-permute-start.1 = (bf16[32,1024]{1,0:T(8,128)(2,1)S(1)}, bf16[32,1024]{1,0:T(8,128)(2,1)S(1)}, u32[]{:S(2)}, u32[]{:S(2)}) collective-permute-start(bf16[32,1024]{1,0:T(8,128)(2,1)S(1)} %get-tuple-element.37), channel_id=1, source_target_pairs={{0,2},{1,3},{2,0},{3,1},{4,6},{5,7},{6,4},{7,5},{8,10},{9,11},{10,... | collective-permute-start | bytes 196616 | tf_op jit(solution)/shard_map/ppermute | solution.py:51
  22.1 5.8 %collective-permute-start = (bf16[32,1024]{1,0:T(8,128)(2,1)S(1)}, bf16[32,1024]{1,0:T(8,128)(2,1)S(1)}, u32[]{:S(2)}, u32[]{:S(2)}) collective-permute-start(bf16[32,1024]{1,0:T(8,128)(2,1)S(1)} %get-tuple-element.37), channel_id=1, source_target_pairs={{0,1},{1,2},{2,3},{3,0},{4,5},{5,6},{6,7},{7,4},{8,9},{9,10},{10,1... | collective-permute-start | bytes 196616 | tf_op jit(solution)/shard_map/ppermute | solution.py:51
  28.0 8.1 %collective-permute-start.3 = (bf16[128,1024]{1,0:T(8,128)(2,1)S(1)}, bf16[128,1024]{1,0:T(8,128)(2,1)S(1)}, u32[]{:S(2)}, u32[]{:S(2)}) collective-permute-start(bf16[128,1024]{1,0:T(8,128)(2,1)S(1)} %constant_dynamic-update-slice_fusion.refs_0_), channel_id=1, source_target_pairs={{0,8},{8,16},{16,24},{24,0},{1,9},{9,17},{17,25},{25,1},{2,10},{10... | collective-permute-start | bytes 786440 | tf_op jit(solution)/shard_map/ppermute | solution.py:51
  29.4 7.6 %collective-permute-start.9 = (bf16[128,1024]{1,0:T(8,128)(2,1)S(1)}, bf16[128,1024]{1,0:T(8,128)(2,1)S(1)}, u32[]{:S(2)}, u32[]{:S(2)}) collective-permute-start(bf16[128,1024]{1,0:T(8,128)(2,1)S(1)} %get-tuple-element.44.refs_4_), channel_id=1, source_target_pairs={{0,1},{1,2},{2,3},{3,0},{4,5},{5,6},{6,7},{7,4},{8,9},{9,10},{10,1... | collective-permute-start | bytes 786440 | tf_op jit(solution)/shard_map/ppermute | solution.py:51
  30.3 15.2 %collective-permute-start.12 = (bf16[8,128,256]{2,1,0:T(8,128)(2,1)S(1)}, bf16[8,128,256]{2,1,0:T(8,128)(2,1)S(1)}, u32[]{:S(2)}, u32[]{:S(2)}) collective-permute-start(bf16[8,128,256]{2,1,0:T(8,128)(2,1)S(1)} %all-to-all-done.refs_9_), channel_id=1, source_target_pairs={{0,4},{4,0},{1,5},{5,1},{2,6},{6,2},{3,7},{7,3},{8,12},{12,8},{9,1... | collective-permute-start | bytes 1572872 | tf_op jit(solution)/shard_map/ppermute | solution.py:51
  30.3 8.9 %collective-permute-start.5 = (bf16[128,1024]{1,0:T(8,128)(2,1)S(1)}, bf16[128,1024]{1,0:T(8,128)(2,1)S(1)}, u32[]{:S(2)}, u32[]{:S(2)}) collective-permute-start(bf16[128,1024]{1,0:T(8,128)(2,1)S(1)} %constant_dynamic-update-slice_fusion.refs_0_), channel_id=1, source_target_pairs={{0,24},{8,0},{16,8},{24,16},{1,25},{9,1},{17,9},{25,17},{2,26},{10... | collective-permute-start | bytes 786440 | tf_op jit(solution)/shard_map/ppermute | solution.py:51
  33.0 9.0 %collective-permute-start.11 = (bf16[128,1024]{1,0:T(8,128)(2,1)S(1)}, bf16[128,1024]{1,0:T(8,128)(2,1)S(1)}, u32[]{:S(2)}, u32[]{:S(2)}) collective-permute-start(bf16[128,1024]{1,0:T(8,128)(2,1)S(1)} %get-tuple-element.44.refs_4_), channel_id=1, source_target_pairs={{0,3},{1,0},{2,1},{3,2},{4,7},{5,4},{6,5},{7,6},{8,11},{9,8},{10,9... | collective-permute-start | bytes 786440 | tf_op jit(solution)/shard_map/ppermute | solution.py:51
  36.0 9.4 %collective-permute-start.4 = (bf16[128,1024]{1,0:T(8,128)(2,1)S(1)}, bf16[128,1024]{1,0:T(8,128)(2,1)S(1)}, u32[]{:S(2)}, u32[]{:S(2)}) collective-permute-start(bf16[128,1024]{1,0:T(8,128)(2,1)S(1)} %collective-permute-done.3.refs_1_), channel_id=1, source_target_pairs={{0,8},{8,16},{16,24},{24,0},{1,9},{9,17},{17,25},{25,1},{2,10},{10... | collective-permute-start | bytes 786440 | tf_op jit(solution)/shard_map/ppermute | solution.py:51
  37.0 8.5 %collective-permute-start.10 = (bf16[128,1024]{1,0:T(8,128)(2,1)S(1)}, bf16[128,1024]{1,0:T(8,128)(2,1)S(1)}, u32[]{:S(2)}, u32[]{:S(2)}) collective-permute-start(bf16[128,1024]{1,0:T(8,128)(2,1)S(1)} %collective-permute-done.9.refs_5_), channel_id=1, source_target_pairs={{0,1},{1,2},{2,3},{3,0},{4,5},{5,6},{6,7},{7,4},{8,9},{9,10},{10,1... | collective-permute-start | bytes 786440 | tf_op jit(solution)/shard_map/ppermute | solution.py:51
  47.6 1.5 %collective-permute-start.13 = (bf16[80,1024]{1,0:T(8,128)(2,1)S(1)}, bf16[80,1024]{1,0:T(8,128)(2,1)S(1)}, u32[]{:S(2)}, u32[]{:S(2)}) collective-permute-start(bf16[80,1024]{1,0:T(8,128)(2,1)S(1)} %get-tuple-element.46.q_own), channel_id=1, source_target_pairs={{0,4},{4,0},{1,5},{5,1},{2,6},{6,2},{3,7},{7,3},{8,12},{12,8},{9,1... | collective-permute-start | bytes 491528 | tf_op jit(solution)/shard_map/ppermute | solution.py:51
  49.8 8.8 %collective-permute-start.19 = (bf16[136,1024]{1,0:T(8,128)(2,1)S(1)}, bf16[136,1024]{1,0:T(8,128)(2,1)S(1)}, u32[]{:S(2)}, u32[]{:S(2)}) collective-permute-start(bf16[136,1024]{1,0:T(8,128)(2,1)S(1)} %get-tuple-element.50.pay), channel_id=1, source_target_pairs={{0,224},{32,0},{64,32},{1,225},{33,1},{65,33},{2,226},{34,2},{66,3... | collective-permute-start | bytes 835592 | tf_op jit(solution)/shard_map/ppermute | solution.py:69
  50.5 10.6 %collective-permute-start.14 = (bf16[136,1024]{1,0:T(8,128)(2,1)S(1)}, bf16[136,1024]{1,0:T(8,128)(2,1)S(1)}, u32[]{:S(2)}, u32[]{:S(2)}) collective-permute-start(bf16[136,1024]{1,0:T(8,128)(2,1)S(1)} %get-tuple-element.50.pay), channel_id=1, source_target_pairs={{0,32},{32,64},{64,96},{96,128},{128,160},{160,192},{192,224},{1,3... | collective-permute-start | bytes 835592 | tf_op jit(solution)/shard_map/ppermute | solution.py:65
  56.4 54.6 %collective-permute-start.25 = (bf16[2,8,64,256]{3,2,1,0:T(8,128)(2,1)S(1)}, bf16[2,8,64,256]{3,2,1,0:T(8,128)(2,1)S(1)}, u32[]{:S(2)}, u32[]{:S(2)}) collective-permute-start(bf16[2,8,64,256]{3,2,1,0:T(8,128)(2,1)S(1)} %pad_maximum_fusion.w0), channel_id=1, source_target_pairs={{0,3},{1,0},{2,1},{3,2},{4,7},{5,4},{6,5},{7,6},{8,11},{9,8},{10,9... | collective-permute-start | bytes 1572872 | tf_op jit(solution)/shard_map/ppermute | solution.py:51
  57.2 53.8 %collective-permute-start.24 = (bf16[2,8,64,256]{3,2,1,0:T(8,128)(2,1)S(1)}, bf16[2,8,64,256]{3,2,1,0:T(8,128)(2,1)S(1)}, u32[]{:S(2)}, u32[]{:S(2)}) collective-permute-start(bf16[2,8,64,256]{3,2,1,0:T(8,128)(2,1)S(1)} %pad_maximum_fusion.w0), channel_id=1, source_target_pairs={{0,2},{1,3},{2,0},{3,1},{4,6},{5,7},{6,4},{7,5},{8,10},{9,11},{10,... | collective-permute-start | bytes 1572872 | tf_op jit(solution)/shard_map/ppermute | solution.py:51
  57.6 54.2 %collective-permute-start.23 = (bf16[2,8,64,256]{3,2,1,0:T(8,128)(2,1)S(1)}, bf16[2,8,64,256]{3,2,1,0:T(8,128)(2,1)S(1)}, u32[]{:S(2)}, u32[]{:S(2)}) collective-permute-start(bf16[2,8,64,256]{3,2,1,0:T(8,128)(2,1)S(1)} %pad_maximum_fusion.w0), channel_id=1, source_target_pairs={{0,1},{1,2},{2,3},{3,0},{4,5},{5,6},{6,7},{7,4},{8,9},{9,10},{10,1... | collective-permute-start | bytes 1572872 | tf_op jit(solution)/shard_map/ppermute | solution.py:51
  58.5 9.5 %collective-permute-start.20 = (bf16[136,1024]{1,0:T(8,128)(2,1)S(1)}, bf16[136,1024]{1,0:T(8,128)(2,1)S(1)}, u32[]{:S(2)}, u32[]{:S(2)}) collective-permute-start(bf16[136,1024]{1,0:T(8,128)(2,1)S(1)} %collective-permute-done.19.refs_1_), channel_id=1, source_target_pairs={{224,192},{0,224},{32,0},{225,193},{1,225},{33,1},{226,194},{2,226... | collective-permute-start | bytes 835592 | tf_op jit(solution)/shard_map/ppermute | solution.py:69
  61.1 9.8 %collective-permute-start.15 = (bf16[136,1024]{1,0:T(8,128)(2,1)S(1)}, bf16[136,1024]{1,0:T(8,128)(2,1)S(1)}, u32[]{:S(2)}, u32[]{:S(2)}) collective-permute-start(bf16[136,1024]{1,0:T(8,128)(2,1)S(1)} %collective-permute-done.14.refs_0_), channel_id=1, source_target_pairs={{32,64},{64,96},{96,128},{128,160},{160,192},{192,224},{33,65},{65... | collective-permute-start | bytes 835592 | tf_op jit(solution)/shard_map/ppermute | solution.py:65
  68.1 19.9 %collective-permute-start.21 = (bf16[136,1024]{1,0:T(8,128)(2,1)S(1)}, bf16[136,1024]{1,0:T(8,128)(2,1)S(1)}, u32[]{:S(2)}, u32[]{:S(2)}) collective-permute-start(bf16[136,1024]{1,0:T(8,128)(2,1)S(1)} %collective-permute-done.20.refs_1_), channel_id=1, source_target_pairs={{192,160},{224,192},{0,224},{193,161},{225,193},{1,225},{194,162},... | collective-permute-start | bytes 835592 | tf_op jit(solution)/shard_map/ppermute | solution.py:69
  70.8 11.0 %collective-permute-start.16 = (bf16[136,1024]{1,0:T(8,128)(2,1)S(1)}, bf16[136,1024]{1,0:T(8,128)(2,1)S(1)}, u32[]{:S(2)}, u32[]{:S(2)}) collective-permute-start(bf16[136,1024]{1,0:T(8,128)(2,1)S(1)} %collective-permute-done.15.refs_0_), channel_id=1, source_target_pairs={{64,96},{96,128},{128,160},{160,192},{192,224},{65,97},{97,129},{1... | collective-permute-start | bytes 835592 | tf_op jit(solution)/shard_map/ppermute | solution.py:65
  81.9 15.3 %collective-permute-start.18 = (bf16[136,512]{1,0:T(8,128)(2,1)S(1)}, bf16[136,512]{1,0:T(8,128)(2,1)S(1)}, u32[]{:S(2)}, u32[]{:S(2)}) collective-permute-start(bf16[136,512]{1,0:T(8,128)(2,1)S(1)} %get-tuple-element.69), channel_id=1, source_target_pairs={{96,128},{128,160},{160,192},{192,224},{97,129},{129,161},{161,193... | collective-permute-start | bytes 417800 | tf_op jit(solution)/shard_map/ppermute | solution.py:65
  88.0 11.8 %collective-permute-start.17 = (bf16[136,512]{1,0:T(8,128)(2,1)S(1)}, bf16[136,512]{1,0:T(8,128)(2,1)S(1)}, u32[]{:S(2)}, u32[]{:S(2)}) collective-permute-start(bf16[136,512]{1,0:T(8,128)(2,1)S(1)} %get-tuple-element.70), channel_id=1, source_target_pairs={{96,128},{128,160},{160,192},{192,224},{97,129},{129,161},{161,193... | collective-permute-start | bytes 417800 | tf_op jit(solution)/shard_map/ppermute | solution.py:65
  102.6 1.7 %collective-permute-start.22 = (f32[72,1024]{1,0:T(8,128)S(1)}, f32[72,1024]{1,0:T(8,128)S(1)}, u32[]{:S(2)}, u32[]{:S(2)}) collective-permute-start(f32[72,1024]{1,0:T(8,128)S(1)} %get-tuple-element.67), channel_id=1, source_target_pairs={{0,4},{4,0},{1,5},{5,1},{2,6},{6,2},{3,7},{7,3},{8,12},{12,8},{9,1... | collective-permute-start | bytes 884744 | tf_op jit(solution)/shard_map/ppermute | solution.py:51
  105.3 13.7 %copy-start.4 = (f32[1024]{0:T(1024)S(1)}, f32[1024]{0:T(1024)}, u32[]{:S(2)}) copy-start(f32[1024]{0:T(1024)} %param.17) | copy-start | bytes 12292
  105.3 13.5 %all-to-all-start.1 = ((bf16[16,2,2048]{2,1,0:T(2,128)(2,1)}), bf16[16,2,2048]{2,1,0:T(2,128)(2,1)S(1)}, u32[]{:S(2)}, u32[]{:S(2)}) async-start(bf16[16,2,2048]{2,1,0:T(2,128)(2,1)} %reshape.4), calls=%async_computation.1 | async-start | bytes 262144 | tf_op jit(solution)/shard_map/all_to_all | solution.py:465
  111.0 0.8 copy-start
  111.8 0.8 copy-start.2
  112.6 1.0 copy-start.1
  113.7 1.0 copy-start.3

commit v9 on v6

--- a/solution.py
+++ b/solution.py
@@ -82,16 +82,16 @@
     lo[...] = rows[0:32, :]
     hi[...] = rows[32:64, :]
     o0[...] = rows[64:80, 768:1024]
-    head = lax.broadcasted_iota(jnp.int32, (16, HD), 0)
-    gates = rows[80:96, 0:128].astype(F32)
+    head = lax.broadcasted_iota(jnp.int32, (16, 256), 0)
+    lane = lax.broadcasted_iota(jnp.int32, (16, 256), 1)
+    pick = jnp.where(lane // HD == head, 1.0, 0.0).astype(BF16)
+    gates = lax.dot_general(
+        rows[80:96, 0:128], pick, (((0,), (0,)), ((), ())), preferred_element_type=F32
+    )[0:16].astype(BF16)
     for h in range(NX):
-        pick = jnp.where(head == h, 1.0, 0.0)
-        gate = lax.dot_general(
-            gates, pick, (((0,), (0,)), ((), ())), precision=lax.Precision.HIGHEST,
-            preferred_element_type=F32,
-        )[0:16]
+        at = slice(h * HD, (h + 1) * HD)
         mine = [rows[64:80, i * 256 + h * HD : i * 256 + h * HD + HD] for i in range(3)]
-        heads[h] = jnp.concatenate(mine + [gate.astype(BF16)], axis=1)
+        heads[h] = jnp.concatenate(mine + [gates[:, at]], axis=1)
     p0[...] = heads[x]
     for k, s in enumerate((s1, s2, s3)):
         s[0:32, :] = rows[32:64, :]

time: 118 us -> 118 us (level)
  no operation moved by 1% of the time
where the time goes in v9:
time: 118 us; the launch traced here: 117 us
  starting transfers between devices  53.3 us (45%)
  waiting for transfers between devices  29.3 us (25%)
  Pallas kernels  28.3 us (24%)
  local copies, waits for them, and re-layouts  4.88 us (4%)
    ppermute x18, waiting for transfers between devices, shift(): return lax.ppermute(x, axis, [(i, (i + k) % n) for i in range(n)])  20.4 us
    ppermute x18, starting transfers between devices, shift(): return lax.ppermute(x, axis, [(i, (i + k) % n) for i in range(n)])  19.7 us
    pallas_call x4, Pallas kernels, shards(): call(functools.partial(step_body, k), outs, [SMEM] + [VMEM] * (len(ins) -...  18.5 us
    ppermute x4, starting transfers between devices, step_right(): return lax.ppermute(x, 'z', [(i, i + 1) for i in range(k - 1, NZ - 1)])  18 us
    all_to_all x1, starting transfers between devices, shards(): w_own = lax.all_to_all(chunk, 'z', 0, 0, tiled=True)  6.75 us
    all_to_all x1, starting transfers between devices, shards(): att = lax.all_to_all(att.reshape(16, 64, HD), ('x', 'y'), 0, 0, tiled=True)  6.15 us
    ppermute x4, waiting for transfers between devices, step_right(): return lax.ppermute(x, 'z', [(i, i + 1) for i in range(k - 1, NZ - 1)])  4.93 us
    unnamed x19, local copies, waits for them, and re-layouts  4.83 us
  transfers between devices with their start and end apart: 27, of which 15 were waited for; matrix products, arithmetic and copies ran while one was open for 1% of the time, Pallas kernels for 19%

profile of v9, /device:TPU:160, one launch (start us, length us, event | category | flops | bytes accessed | tf_op | source)
XLA Modules:
  0.0 117.2 jit_solution(2920761026358303750)
XLA Ops:
  0.1 1.0 pad_add_fusion.rows
  1.1 0.8 shard_map.91
  1.9 1.6 %collective-permute-start.6 = (bf16[48,1024]{1,0:T(8,128)(2,1)S(1)}, bf16[48,1024]{1,0:T(8,128)(2,1)S(1)}, u32[]{:S(2)}, u32[]{:S(2)}) collective-permute-start(bf16[48,1024]{1,0:T(8,128)(2,1)S(1)} %get-tuple-element.38), channel_id=1, source_target_pairs={{0,8},{8,16},{16,24},{24,0},{1,9},{9,17},{17,25},{25,1},{2,10},{10... | collective-permute-start | bytes 294920 | tf_op jit(solution)/shard_map/ppermute | solution.py:51
  3.5 2.7 %collective-permute-start.7 = (bf16[48,1024]{1,0:T(8,128)(2,1)S(1)}, bf16[48,1024]{1,0:T(8,128)(2,1)S(1)}, u32[]{:S(2)}, u32[]{:S(2)}) collective-permute-start(bf16[48,1024]{1,0:T(8,128)(2,1)S(1)} %get-tuple-element.39), channel_id=1, source_target_pairs={{0,16},{8,24},{16,0},{24,8},{1,17},{9,25},{17,1},{25,9},{2,18},{10... | collective-permute-start | bytes 294920 | tf_op jit(solution)/shard_map/ppermute | solution.py:51
  6.2 1.4 %collective-permute-start.8 = (bf16[48,1024]{1,0:T(8,128)(2,1)S(1)}, bf16[48,1024]{1,0:T(8,128)(2,1)S(1)}, u32[]{:S(2)}, u32[]{:S(2)}) collective-permute-start(bf16[48,1024]{1,0:T(8,128)(2,1)S(1)} %get-tuple-element.40), channel_id=1, source_target_pairs={{0,24},{8,0},{16,8},{24,16},{1,25},{9,1},{17,9},{25,17},{2,26},{10... | collective-permute-start | bytes 294920 | tf_op jit(solution)/shard_map/ppermute | solution.py:51
  8.0 2.8 %collective-permute-done.7.r2 = bf16[48,1024]{1,0:T(8,128)(2,1)S(1)} collective-permute-done((bf16[48,1024]{1,0:T(8,128)(2,1)S(1)}, bf16[48,1024]{1,0:T(8,128)(2,1)S(1)}, u32[]{:S(2)}, u32[]{:S(2)}) %collective-permute-start.7) | collective-permute-done | bytes 98336 | tf_op jit(solution)/shard_map/ppermute | solution.py:51
  10.8 0.9 shard_map.92
  11.7 6.8 %all-to-all-start = ((bf16[8,128,256]{2,1,0:T(8,128)(2,1)}), bf16[8,128,256]{2,1,0:T(8,128)(2,1)S(1)}, u32[]{:S(2)}, u32[]{:S(2)}) async-start(bf16[8,128,256]{2,1,0:T(8,128)(2,1)} %get-tuple-element.42), calls=%async_computation | async-start | bytes 1048576 | tf_op jit(solution)/shard_map/all_to_all | solution.py:395
  18.4 3.0 %collective-permute-start.2 = (bf16[32,1024]{1,0:T(8,128)(2,1)S(1)}, bf16[32,1024]{1,0:T(8,128)(2,1)S(1)}, u32[]{:S(2)}, u32[]{:S(2)}) collective-permute-start(bf16[32,1024]{1,0:T(8,128)(2,1)S(1)} %get-tuple-element.34), channel_id=1, source_target_pairs={{0,3},{1,0},{2,1},{3,2},{4,7},{5,4},{6,5},{7,6},{8,11},{9,8},{10,9... | collective-permute-start | bytes 196616 | tf_op jit(solution)/shard_map/ppermute | solution.py:51
  22.1 1.0 collective-permute-start
  23.0 4.9 %collective-permute-done = bf16[32,1024]{1,0:T(8,128)(2,1)S(1)} collective-permute-done((bf16[32,1024]{1,0:T(8,128)(2,1)S(1)}, bf16[32,1024]{1,0:T(8,128)(2,1)S(1)}, u32[]{:S(2)}, u32[]{:S(2)}) %collective-permute-start) | collective-permute-done | bytes 65568 | tf_op jit(solution)/shard_map/ppermute | solution.py:51
  28.0 1.4 %collective-permute-start.3 = (bf16[128,1024]{1,0:T(8,128)(2,1)S(1)}, bf16[128,1024]{1,0:T(8,128)(2,1)S(1)}, u32[]{:S(2)}, u32[]{:S(2)}) collective-permute-start(bf16[128,1024]{1,0:T(8,128)(2,1)S(1)} %constant_dynamic-update-slice_fusion.refs_0_), channel_id=1, source_target_pairs={{0,8},{8,16},{16,24},{24,0},{1,9},{9,17},{17,25},{25,1},{2,10},{10... | collective-permute-start | bytes 786440 | tf_op jit(solution)/shard_map/ppermute | solution.py:51
  29.4 1.0 all-to-all-done.refs_9_
  30.3 2.7 %collective-permute-start.5 = (bf16[128,1024]{1,0:T(8,128)(2,1)S(1)}, bf16[128,1024]{1,0:T(8,128)(2,1)S(1)}, u32[]{:S(2)}, u32[]{:S(2)}) collective-permute-start(bf16[128,1024]{1,0:T(8,128)(2,1)S(1)} %constant_dynamic-update-slice_fusion.refs_0_), channel_id=1, source_target_pairs={{0,24},{8,0},{16,8},{24,16},{1,25},{9,1},{17,9},{25,17},{2,26},{10... | collective-permute-start | bytes 786440 | tf_op jit(solution)/shard_map/ppermute | solution.py:51
  33.0 3.0 %collective-permute-start.11 = (bf16[128,1024]{1,0:T(8,128)(2,1)S(1)}, bf16[128,1024]{1,0:T(8,128)(2,1)S(1)}, u32[]{:S(2)}, u32[]{:S(2)}) collective-permute-start(bf16[128,1024]{1,0:T(8,128)(2,1)S(1)} %get-tuple-element.41.refs_4_), channel_id=1, source_target_pairs={{0,3},{1,0},{2,1},{3,2},{4,7},{5,4},{6,5},{7,6},{8,11},{9,8},{10,9... | collective-permute-start | bytes 786440 | tf_op jit(solution)/shard_map/ppermute | solution.py:51
  36.0 0.9 collective-permute-done.9.refs_5_
  37.0 2.3 %collective-permute-done.5.refs_3_ = bf16[128,1024]{1,0:T(8,128)(2,1)S(1)} collective-permute-done((bf16[128,1024]{1,0:T(8,128)(2,1)S(1)}, bf16[128,1024]{1,0:T(8,128)(2,1)S(1)}, u32[]{:S(2)}, u32[]{:S(2)}) %collective-permute-start.5) | collective-permute-done | bytes 262176 | tf_op jit(solution)/shard_map/ppermute | solution.py:51
  39.2 2.7 %collective-permute-done.11.refs_7_ = bf16[128,1024]{1,0:T(8,128)(2,1)S(1)} collective-permute-done((bf16[128,1024]{1,0:T(8,128)(2,1)S(1)}, bf16[128,1024]{1,0:T(8,128)(2,1)S(1)}, u32[]{:S(2)}, u32[]{:S(2)}) %collective-permute-start.11) | collective-permute-done | bytes 262176 | tf_op jit(solution)/shard_map/ppermute | solution.py:51
  42.0 3.4 %collective-permute-done.4.refs_2_ = bf16[128,1024]{1,0:T(8,128)(2,1)S(1)} collective-permute-done((bf16[128,1024]{1,0:T(8,128)(2,1)S(1)}, bf16[128,1024]{1,0:T(8,128)(2,1)S(1)}, u32[]{:S(2)}, u32[]{:S(2)}) %collective-permute-start.4) | collective-permute-done | bytes 262176 | tf_op jit(solution)/shard_map/ppermute | solution.py:51
  45.5 2.1 %shard_map.93 = (bf16[80,1024]{1,0:T(8,128)(2,1)S(1)}, bf16[128,1024]{1,0:T(8,128)(2,1)S(1)}, f32[8,1024]{1,0:T(8,128)S(1)}) custom-call(s32[4]{0:T(128)S(1)} %pad_add_fusion.1.idx, f32[4]{0:T(128)S(1)} %copy-done.6, bf16[128,1024]{1,0:T(8,128)(2,1)S(1)} %constant_dynamic-update-slice_fusion.refs_0_, bf16[128,1024]{1,0:T(8,128)(2,1)S(1)} %collective-permute-done.3.refs_1_, ...), custom_call_target="tpu_custom_call" | custom-call | flops 2000000000 | bytes 1048576 | tf_op jit(solution)/shard_map/pallas_call | solution.py:400
  47.8 1.3 %collective-permute-done.13.q_sib = bf16[80,1024]{1,0:T(8,128)(2,1)S(1)} collective-permute-done((bf16[80,1024]{1,0:T(8,128)(2,1)S(1)}, bf16[80,1024]{1,0:T(8,128)(2,1)S(1)}, u32[]{:S(2)}, u32[]{:S(2)}) %collective-permute-start.13) | collective-permute-done | bytes 163872 | tf_op jit(solution)/shard_map/ppermute | solution.py:51
  49.8 0.7 collective-permute-start.18
  50.5 3.3 %collective-permute-start.14 = (bf16[136,1024]{1,0:T(8,128)(2,1)S(1)}, bf16[136,1024]{1,0:T(8,128)(2,1)S(1)}, u32[]{:S(2)}, u32[]{:S(2)}) collective-permute-start(bf16[136,1024]{1,0:T(8,128)(2,1)S(1)} %get-tuple-element.47.pay), channel_id=1, source_target_pairs={{0,32},{32,64},{64,96},{96,128},{128,160},{160,192},{192,224},{1,3... | collective-permute-start | bytes 835592 | tf_op jit(solution)/shard_map/ppermute | solution.py:65
  53.7 2.6 %shard_map.95 = (f32[2,80,2048]{2,1,0:T(8,128)S(1)}, f32[2,8,2048]{2,1,0:T(8,128)S(1)}, f32[8,256]{1,0:T(8,128)S(1)}) custom-call(s32[4]{0:T(128)S(1)} %pad_add_fusion.1.idx, bf16[128,2048]{1,0:T(8,128)(2,1)S(1)} %get-tuple-element.46.q, bf16[136,1024]{1,0:T(8,128)(2,1)S(1)} %get-tuple-element.47.pay), custom_call_target="tpu_custom_call" | custom-call | flops 3000000000 | bytes 1048576 | tf_op jit(solution)/shard_map/pallas_call | solution.py:429
  56.4 0.7 collective-permute-start.24
  57.6 0.9 collective-permute-start.22
  58.5 0.7 collective-permute-start.19
  59.2 1.9 %collective-permute-done.14.refs_0_ = bf16[136,1024]{1,0:T(8,128)(2,1)S(1)} collective-permute-done((bf16[136,1024]{1,0:T(8,128)(2,1)S(1)}, bf16[136,1024]{1,0:T(8,128)(2,1)S(1)}, u32[]{:S(2)}, u32[]{:S(2)}) %collective-permute-start.14) | collective-permute-done | bytes 278560 | tf_op jit(solution)/shard_map/ppermute | solution.py:65
  61.1 3.1 %collective-permute-start.15 = (bf16[136,1024]{1,0:T(8,128)(2,1)S(1)}, bf16[136,1024]{1,0:T(8,128)(2,1)S(1)}, u32[]{:S(2)}, u32[]{:S(2)}) collective-permute-start(bf16[136,1024]{1,0:T(8,128)(2,1)S(1)} %collective-permute-done.14.refs_0_), channel_id=1, source_target_pairs={{32,64},{64,96},{96,128},{128,160},{160,192},{192,224},{33,65},{65... | collective-permute-start | bytes 835592 | tf_op jit(solution)/shard_map/ppermute | solution.py:65
  64.2 3.9 %shard_map.96 = (f32[2,80,2048]{2,1,0:T(8,128)S(1)}, f32[2,8,2048]{2,1,0:T(8,128)S(1)}, f32[8,256]{1,0:T(8,128)S(1)}) custom-call(s32[4]{0:T(128)S(1)} %pad_add_fusion.1.idx, bf16[128,2048]{1,0:T(8,128)(2,1)S(1)} %get-tuple-element.46.q, bf16[136,1024]{1,0:T(8,128)(2,1)S(1)} %collective-permute-done.14.refs_0_, ...), custom_call_target="tpu_custom_call", output_to_operand_aliasing={{0}: (4, {}), {1}: (5, {})} | custom-call | flops 6000000000 | bytes 1048576 | tf_op jit(solution)/shard_map/pallas_call | solution.py:449
  68.1 1.3 %collective-permute-start.20 = (bf16[136,1024]{1,0:T(8,128)(2,1)S(1)}, bf16[136,1024]{1,0:T(8,128)(2,1)S(1)}, u32[]{:S(2)}, u32[]{:S(2)}) collective-permute-start(bf16[136,1024]{1,0:T(8,128)(2,1)S(1)} %collective-permute-done.19.refs_1_), channel_id=1, source_target_pairs={{192,160},{224,192},{0,224},{193,161},{225,193},{1,225},{194,162},... | collective-permute-start | bytes 835592 | tf_op jit(solution)/shard_map/ppermute | solution.py:69
  69.4 1.5 %collective-permute-done.15.refs_0_ = bf16[136,1024]{1,0:T(8,128)(2,1)S(1)} collective-permute-done((bf16[136,1024]{1,0:T(8,128)(2,1)S(1)}, bf16[136,1024]{1,0:T(8,128)(2,1)S(1)}, u32[]{:S(2)}, u32[]{:S(2)}) %collective-permute-start.15) | collective-permute-done | bytes 278560 | tf_op jit(solution)/shard_map/ppermute | solution.py:65
  70.8 5.5 %collective-permute-start.16 = (bf16[136,1024]{1,0:T(8,128)(2,1)S(1)}, bf16[136,1024]{1,0:T(8,128)(2,1)S(1)}, u32[]{:S(2)}, u32[]{:S(2)}) collective-permute-start(bf16[136,1024]{1,0:T(8,128)(2,1)S(1)} %collective-permute-done.15.refs_0_), channel_id=1, source_target_pairs={{64,96},{96,128},{128,160},{160,192},{192,224},{65,97},{97,129},{1... | collective-permute-start | bytes 835592 | tf_op jit(solution)/shard_map/ppermute | solution.py:65
  76.4 3.9 %shard_map.97 = (f32[2,80,2048]{2,1,0:T(8,128)S(1)}, f32[2,8,2048]{2,1,0:T(8,128)S(1)}, f32[8,256]{1,0:T(8,128)S(1)}) custom-call(s32[4]{0:T(128)S(1)} %pad_add_fusion.1.idx, bf16[128,2048]{1,0:T(8,128)(2,1)S(1)} %get-tuple-element.46.q, bf16[136,1024]{1,0:T(8,128)(2,1)S(1)} %collective-permute-done.15.refs_0_, ...), custom_call_target="tpu_custom_call", output_to_operand_aliasing={{0}: (4, {}), {1}: (5, {})} | custom-call | flops 6000000000 | bytes 1048576 | tf_op jit(solution)/shard_map/pallas_call | solution.py:449
  80.3 1.6 %collective-permute-done.16.refs_0_ = bf16[136,1024]{1,0:T(8,128)(2,1)S(1)} collective-permute-done((bf16[136,1024]{1,0:T(8,128)(2,1)S(1)}, bf16[136,1024]{1,0:T(8,128)(2,1)S(1)}, u32[]{:S(2)}, u32[]{:S(2)}) %collective-permute-start.16) | collective-permute-done | bytes 278560 | tf_op jit(solution)/shard_map/ppermute | solution.py:65
  81.9 6.1 %collective-permute-start.17 = (bf16[136,1024]{1,0:T(8,128)(2,1)S(1)}, bf16[136,1024]{1,0:T(8,128)(2,1)S(1)}, u32[]{:S(2)}, u32[]{:S(2)}) collective-permute-start(bf16[136,1024]{1,0:T(8,128)(2,1)S(1)} %collective-permute-done.16.refs_0_), channel_id=1, source_target_pairs={{96,128},{128,160},{160,192},{192,224},{97,129},{129,161},{161,193... | collective-permute-start | bytes 835592 | tf_op jit(solution)/shard_map/ppermute | solution.py:65
  88.0 6.7 %shard_map.98 = (f32[2,80,2048]{2,1,0:T(8,128)S(1)}, f32[2,8,2048]{2,1,0:T(8,128)S(1)}, f32[8,256]{1,0:T(8,128)S(1)}) custom-call(s32[4]{0:T(128)S(1)} %pad_add_fusion.1.idx, bf16[128,2048]{1,0:T(8,128)(2,1)S(1)} %get-tuple-element.46.q, bf16[136,1024]{1,0:T(8,128)(2,1)S(1)} %collective-permute-done.16.refs_0_, ...), custom_call_target="tpu_custom_call", output_to_operand_aliasing={{0}: (4, {}), {1}: (5, {})} | custom-call | flops 6000000000 | bytes 1048576 | tf_op jit(solution)/shard_map/pallas_call | solution.py:449
  94.7 4.0 %shard_map.99 = (f32[72,1024]{1,0:T(8,128)S(1)}, f32[72,1024]{1,0:T(8,128)S(1)}) custom-call(s32[4]{0:T(128)S(1)} %pad_add_fusion.1.idx, bf16[128,2048]{1,0:T(8,128)(2,1)S(1)} %get-tuple-element.46.q, bf16[136,1024]{1,0:T(8,128)(2,1)S(1)} %collective-permute-done.17.refs_0_, f32[2,80,2048]{2,1,0:T(8,128)S(1)} %get-tuple-element.57.refs_1_, ...), custom_call_target="tpu_custom_call" | custom-call | flops 6000000000 | bytes 1048576 | tf_op jit(solution)/shard_map/pallas_call | solution.py:449
  98.9 1.6 %collective-permute-done.21.sib = f32[72,1024]{1,0:T(8,128)S(1)} collective-permute-done((f32[72,1024]{1,0:T(8,128)S(1)}, f32[72,1024]{1,0:T(8,128)S(1)}, u32[]{:S(2)}, u32[]{:S(2)}) %collective-permute-start.21) | collective-permute-done | bytes 294944 | tf_op jit(solution)/shard_map/ppermute | solution.py:51
  100.6 0.9 reshape.4
  101.5 6.1 %all-to-all-start.1 = ((bf16[16,2,2048]{2,1,0:T(2,128)(2,1)}), bf16[16,2,2048]{2,1,0:T(2,128)(2,1)S(1)}, u32[]{:S(2)}, u32[]{:S(2)}) async-start(bf16[16,2,2048]{2,1,0:T(2,128)(2,1)} %reshape.4), calls=%async_computation.1 | async-start | bytes 262144 | tf_op jit(solution)/shard_map/all_to_all | solution.py:462
  107.7 0.8 copy-done
  108.5 0.8 copy-done.2
  109.3 1.0 copy-done.1
  110.3 1.0 copy-done.3
  111.4 1.0 shard_map.101.w
  112.4 3.1 %all-to-all-done.1 = bf16[16,2,2048]{2,1,0:T(2,128)(2,1)S(1)} async-done(((bf16[16,2,2048]{2,1,0:T(2,128)(2,1)}), bf16[16,2,2048]{2,1,0:T(2,128)(2,1)S(1)}, u32[]{:S(2)}, u32[]{:S(2)}) %all-to-all-start.1) | async-done | bytes 131104 | tf_op jit(solution)/shard_map/all_to_all | solution.py:462
  115.7 1.5 %shard_map.102 = bf16[64,1024]{1,0:T(8,128)(2,1)} custom-call(bf16[16,64,64]{2,1,0:T(8,128)(2,1)S(1)} %reshape.5.att, f32[1,1024]{1,0:T(1,128)S(1)} %bitcast.13, bf16[1024,1024]{1,0:T(8,128)(2,1)S(1)} %shard_map.101.w), custom_call_target="tpu_custom_call" | custom-call | flops 100000000 | bytes 1048576 | tf_op jit(solution)/shard_map/pallas_call | solution.py:463
  (43 shorter events, 3.1 us)
Async XLA Ops:
  1.9 43.6 %copy-start.5 = (f32[1024]{0:T(1024)S(1)}, f32[1024]{0:T(1024)}, u32[]{:S(2)}) copy-start(f32[1024]{0:T(1024)} %param.10) | copy-start | bytes 12292
  1.9 43.6 %copy-start.6 = (f32[4]{0:T(128)S(1)}, f32[4]{0:T(128)}, u32[]{:S(2)}) copy-start(f32[4]{0:T(128)} %offs.1) | copy-start | bytes 52
  1.9 6.1 %collective-permute-start.6 = (bf16[48,1024]{1,0:T(8,128)(2,1)S(1)}, bf16[48,1024]{1,0:T(8,128)(2,1)S(1)}, u32[]{:S(2)}, u32[]{:S(2)}) collective-permute-start(bf16[48,1024]{1,0:T(8,128)(2,1)S(1)} %get-tuple-element.38), channel_id=1, source_target_pairs={{0,8},{8,16},{16,24},{24,0},{1,9},{9,17},{17,25},{25,1},{2,10},{10... | collective-permute-start | bytes 294920 | tf_op jit(solution)/shard_map/ppermute | solution.py:51
  3.5 7.3 %collective-permute-start.7 = (bf16[48,1024]{1,0:T(8,128)(2,1)S(1)}, bf16[48,1024]{1,0:T(8,128)(2,1)S(1)}, u32[]{:S(2)}, u32[]{:S(2)}) collective-permute-start(bf16[48,1024]{1,0:T(8,128)(2,1)S(1)} %get-tuple-element.39), channel_id=1, source_target_pairs={{0,16},{8,24},{16,0},{24,8},{1,17},{9,25},{17,1},{25,9},{2,18},{10... | collective-permute-start | bytes 294920 | tf_op jit(solution)/shard_map/ppermute | solution.py:51
  6.2 4.6 %collective-permute-start.8 = (bf16[48,1024]{1,0:T(8,128)(2,1)S(1)}, bf16[48,1024]{1,0:T(8,128)(2,1)S(1)}, u32[]{:S(2)}, u32[]{:S(2)}) collective-permute-start(bf16[48,1024]{1,0:T(8,128)(2,1)S(1)} %get-tuple-element.40), channel_id=1, source_target_pairs={{0,24},{8,0},{16,8},{24,16},{1,25},{9,1},{17,9},{25,17},{2,26},{10... | collective-permute-start | bytes 294920 | tf_op jit(solution)/shard_map/ppermute | solution.py:51
  11.7 18.7 %all-to-all-start = ((bf16[8,128,256]{2,1,0:T(8,128)(2,1)}), bf16[8,128,256]{2,1,0:T(8,128)(2,1)S(1)}, u32[]{:S(2)}, u32[]{:S(2)}) async-start(bf16[8,128,256]{2,1,0:T(8,128)(2,1)} %get-tuple-element.42), calls=%async_computation | async-start | bytes 1048576 | tf_op jit(solution)/shard_map/all_to_all | solution.py:395
  18.4 9.5 %collective-permute-start.2 = (bf16[32,1024]{1,0:T(8,128)(2,1)S(1)}, bf16[32,1024]{1,0:T(8,128)(2,1)S(1)}, u32[]{:S(2)}, u32[]{:S(2)}) collective-permute-start(bf16[32,1024]{1,0:T(8,128)(2,1)S(1)} %get-tuple-element.34), channel_id=1, source_target_pairs={{0,3},{1,0},{2,1},{3,2},{4,7},{5,4},{6,5},{7,6},{8,11},{9,8},{10,9... | collective-permute-start | bytes 196616 | tf_op jit(solution)/shard_map/ppermute | solution.py:51
  21.4 6.5 %collective-permute-start.1 = (bf16[32,1024]{1,0:T(8,128)(2,1)S(1)}, bf16[32,1024]{1,0:T(8,128)(2,1)S(1)}, u32[]{:S(2)}, u32[]{:S(2)}) collective-permute-start(bf16[32,1024]{1,0:T(8,128)(2,1)S(1)} %get-tuple-element.34), channel_id=1, source_target_pairs={{0,2},{1,3},{2,0},{3,1},{4,6},{5,7},{6,4},{7,5},{8,10},{9,11},{10,... | collective-permute-start | bytes 196616 | tf_op jit(solution)/shard_map/ppermute | solution.py:51
  22.1 5.8 %collective-permute-start = (bf16[32,1024]{1,0:T(8,128)(2,1)S(1)}, bf16[32,1024]{1,0:T(8,128)(2,1)S(1)}, u32[]{:S(2)}, u32[]{:S(2)}) collective-permute-start(bf16[32,1024]{1,0:T(8,128)(2,1)S(1)} %get-tuple-element.34), channel_id=1, source_target_pairs={{0,1},{1,2},{2,3},{3,0},{4,5},{5,6},{6,7},{7,4},{8,9},{9,10},{10,1... | collective-permute-start | bytes 196616 | tf_op jit(solution)/shard_map/ppermute | solution.py:51
  28.0 8.1 %collective-permute-start.3 = (bf16[128,1024]{1,0:T(8,128)(2,1)S(1)}, bf16[128,1024]{1,0:T(8,128)(2,1)S(1)}, u32[]{:S(2)}, u32[]{:S(2)}) collective-permute-start(bf16[128,1024]{1,0:T(8,128)(2,1)S(1)} %constant_dynamic-update-slice_fusion.refs_0_), channel_id=1, source_target_pairs={{0,8},{8,16},{16,24},{24,0},{1,9},{9,17},{17,25},{25,1},{2,10},{10... | collective-permute-start | bytes 786440 | tf_op jit(solution)/shard_map/ppermute | solution.py:51
  29.4 7.6 %collective-permute-start.9 = (bf16[128,1024]{1,0:T(8,128)(2,1)S(1)}, bf16[128,1024]{1,0:T(8,128)(2,1)S(1)}, u32[]{:S(2)}, u32[]{:S(2)}) collective-permute-start(bf16[128,1024]{1,0:T(8,128)(2,1)S(1)} %get-tuple-element.41.refs_4_), channel_id=1, source_target_pairs={{0,1},{1,2},{2,3},{3,0},{4,5},{5,6},{6,7},{7,4},{8,9},{9,10},{10,1... | collective-permute-start | bytes 786440 | tf_op jit(solution)/shard_map/ppermute | solution.py:51
  30.3 15.2 %collective-permute-start.12 = (bf16[8,128,256]{2,1,0:T(8,128)(2,1)S(1)}, bf16[8,128,256]{2,1,0:T(8,128)(2,1)S(1)}, u32[]{:S(2)}, u32[]{:S(2)}) collective-permute-start(bf16[8,128,256]{2,1,0:T(8,128)(2,1)S(1)} %all-to-all-done.refs_9_), channel_id=1, source_target_pairs={{0,4},{4,0},{1,5},{5,1},{2,6},{6,2},{3,7},{7,3},{8,12},{12,8},{9,1... | collective-permute-start | bytes 1572872 | tf_op jit(solution)/shard_map/ppermute | solution.py:51
  30.3 8.9 %collective-permute-start.5 = (bf16[128,1024]{1,0:T(8,128)(2,1)S(1)}, bf16[128,1024]{1,0:T(8,128)(2,1)S(1)}, u32[]{:S(2)}, u32[]{:S(2)}) collective-permute-start(bf16[128,1024]{1,0:T(8,128)(2,1)S(1)} %constant_dynamic-update-slice_fusion.refs_0_), channel_id=1, source_target_pairs={{0,24},{8,0},{16,8},{24,16},{1,25},{9,1},{17,9},{25,17},{2,26},{10... | collective-permute-start | bytes 786440 | tf_op jit(solution)/shard_map/ppermute | solution.py:51
  33.0 9.0 %collective-permute-start.11 = (bf16[128,1024]{1,0:T(8,128)(2,1)S(1)}, bf16[128,1024]{1,0:T(8,128)(2,1)S(1)}, u32[]{:S(2)}, u32[]{:S(2)}) collective-permute-start(bf16[128,1024]{1,0:T(8,128)(2,1)S(1)} %get-tuple-element.41.refs_4_), channel_id=1, source_target_pairs={{0,3},{1,0},{2,1},{3,2},{4,7},{5,4},{6,5},{7,6},{8,11},{9,8},{10,9... | collective-permute-start | bytes 786440 | tf_op jit(solution)/shard_map/ppermute | solution.py:51
  36.0 9.4 %collective-permute-start.4 = (bf16[128,1024]{1,0:T(8,128)(2,1)S(1)}, bf16[128,1024]{1,0:T(8,128)(2,1)S(1)}, u32[]{:S(2)}, u32[]{:S(2)}) collective-permute-start(bf16[128,1024]{1,0:T(8,128)(2,1)S(1)} %collective-permute-done.3.refs_1_), channel_id=1, source_target_pairs={{0,8},{8,16},{16,24},{24,0},{1,9},{9,17},{17,25},{25,1},{2,10},{10... | collective-permute-start | bytes 786440 | tf_op jit(solution)/shard_map/ppermute | solution.py:51
  37.0 8.5 %collective-permute-start.10 = (bf16[128,1024]{1,0:T(8,128)(2,1)S(1)}, bf16[128,1024]{1,0:T(8,128)(2,1)S(1)}, u32[]{:S(2)}, u32[]{:S(2)}) collective-permute-start(bf16[128,1024]{1,0:T(8,128)(2,1)S(1)} %collective-permute-done.9.refs_5_), channel_id=1, source_target_pairs={{0,1},{1,2},{2,3},{3,0},{4,5},{5,6},{6,7},{7,4},{8,9},{9,10},{10,1... | collective-permute-start | bytes 786440 | tf_op jit(solution)/shard_map/ppermute | solution.py:51
  47.6 1.5 %collective-permute-start.13 = (bf16[80,1024]{1,0:T(8,128)(2,1)S(1)}, bf16[80,1024]{1,0:T(8,128)(2,1)S(1)}, u32[]{:S(2)}, u32[]{:S(2)}) collective-permute-start(bf16[80,1024]{1,0:T(8,128)(2,1)S(1)} %get-tuple-element.43.q_own), channel_id=1, source_target_pairs={{0,4},{4,0},{1,5},{5,1},{2,6},{6,2},{3,7},{7,3},{8,12},{12,8},{9,1... | collective-permute-start | bytes 491528 | tf_op jit(solution)/shard_map/ppermute | solution.py:51
  49.8 8.7 %collective-permute-start.18 = (bf16[136,1024]{1,0:T(8,128)(2,1)S(1)}, bf16[136,1024]{1,0:T(8,128)(2,1)S(1)}, u32[]{:S(2)}, u32[]{:S(2)}) collective-permute-start(bf16[136,1024]{1,0:T(8,128)(2,1)S(1)} %get-tuple-element.47.pay), channel_id=1, source_target_pairs={{0,224},{32,0},{64,32},{1,225},{33,1},{65,33},{2,226},{34,2},{66,3... | collective-permute-start | bytes 835592 | tf_op jit(solution)/shard_map/ppermute | solution.py:69
  50.5 10.6 %collective-permute-start.14 = (bf16[136,1024]{1,0:T(8,128)(2,1)S(1)}, bf16[136,1024]{1,0:T(8,128)(2,1)S(1)}, u32[]{:S(2)}, u32[]{:S(2)}) collective-permute-start(bf16[136,1024]{1,0:T(8,128)(2,1)S(1)} %get-tuple-element.47.pay), channel_id=1, source_target_pairs={{0,32},{32,64},{64,96},{96,128},{128,160},{160,192},{192,224},{1,3... | collective-permute-start | bytes 835592 | tf_op jit(solution)/shard_map/ppermute | solution.py:65
  56.4 51.3 %collective-permute-start.24 = (bf16[2,8,64,256]{3,2,1,0:T(8,128)(2,1)S(1)}, bf16[2,8,64,256]{3,2,1,0:T(8,128)(2,1)S(1)}, u32[]{:S(2)}, u32[]{:S(2)}) collective-permute-start(bf16[2,8,64,256]{3,2,1,0:T(8,128)(2,1)S(1)} %pad_maximum_fusion.w0), channel_id=1, source_target_pairs={{0,3},{1,0},{2,1},{3,2},{4,7},{5,4},{6,5},{7,6},{8,11},{9,8},{10,9... | collective-permute-start | bytes 1572872 | tf_op jit(solution)/shard_map/ppermute | solution.py:51
  57.1 50.5 %collective-permute-start.23 = (bf16[2,8,64,256]{3,2,1,0:T(8,128)(2,1)S(1)}, bf16[2,8,64,256]{3,2,1,0:T(8,128)(2,1)S(1)}, u32[]{:S(2)}, u32[]{:S(2)}) collective-permute-start(bf16[2,8,64,256]{3,2,1,0:T(8,128)(2,1)S(1)} %pad_maximum_fusion.w0), channel_id=1, source_target_pairs={{0,2},{1,3},{2,0},{3,1},{4,6},{5,7},{6,4},{7,5},{8,10},{9,11},{10,... | collective-permute-start | bytes 1572872 | tf_op jit(solution)/shard_map/ppermute | solution.py:51
  57.6 50.9 %collective-permute-start.22 = (bf16[2,8,64,256]{3,2,1,0:T(8,128)(2,1)S(1)}, bf16[2,8,64,256]{3,2,1,0:T(8,128)(2,1)S(1)}, u32[]{:S(2)}, u32[]{:S(2)}) collective-permute-start(bf16[2,8,64,256]{3,2,1,0:T(8,128)(2,1)S(1)} %pad_maximum_fusion.w0), channel_id=1, source_target_pairs={{0,1},{1,2},{2,3},{3,0},{4,5},{5,6},{6,7},{7,4},{8,9},{9,10},{10,1... | collective-permute-start | bytes 1572872 | tf_op jit(solution)/shard_map/ppermute | solution.py:51
  58.5 9.6 %collective-permute-start.19 = (bf16[136,1024]{1,0:T(8,128)(2,1)S(1)}, bf16[136,1024]{1,0:T(8,128)(2,1)S(1)}, u32[]{:S(2)}, u32[]{:S(2)}) collective-permute-start(bf16[136,1024]{1,0:T(8,128)(2,1)S(1)} %collective-permute-done.18.refs_1_), channel_id=1, source_target_pairs={{224,192},{0,224},{32,0},{225,193},{1,225},{33,1},{226,194},{2,226... | collective-permute-start | bytes 835592 | tf_op jit(solution)/shard_map/ppermute | solution.py:69
  61.1 9.8 %collective-permute-start.15 = (bf16[136,1024]{1,0:T(8,128)(2,1)S(1)}, bf16[136,1024]{1,0:T(8,128)(2,1)S(1)}, u32[]{:S(2)}, u32[]{:S(2)}) collective-permute-start(bf16[136,1024]{1,0:T(8,128)(2,1)S(1)} %collective-permute-done.14.refs_0_), channel_id=1, source_target_pairs={{32,64},{64,96},{96,128},{128,160},{160,192},{192,224},{33,65},{65... | collective-permute-start | bytes 835592 | tf_op jit(solution)/shard_map/ppermute | solution.py:65
  68.1 19.9 %collective-permute-start.20 = (bf16[136,1024]{1,0:T(8,128)(2,1)S(1)}, bf16[136,1024]{1,0:T(8,128)(2,1)S(1)}, u32[]{:S(2)}, u32[]{:S(2)}) collective-permute-start(bf16[136,1024]{1,0:T(8,128)(2,1)S(1)} %collective-permute-done.19.refs_1_), channel_id=1, source_target_pairs={{192,160},{224,192},{0,224},{193,161},{225,193},{1,225},{194,162},... | collective-permute-start | bytes 835592 | tf_op jit(solution)/shard_map/ppermute | solution.py:69
  70.8 11.0 %collective-permute-start.16 = (bf16[136,1024]{1,0:T(8,128)(2,1)S(1)}, bf16[136,1024]{1,0:T(8,128)(2,1)S(1)}, u32[]{:S(2)}, u32[]{:S(2)}) collective-permute-start(bf16[136,1024]{1,0:T(8,128)(2,1)S(1)} %collective-permute-done.15.refs_0_), channel_id=1, source_target_pairs={{64,96},{96,128},{128,160},{160,192},{192,224},{65,97},{97,129},{1... | collective-permute-start | bytes 835592 | tf_op jit(solution)/shard_map/ppermute | solution.py:65
  81.9 12.9 %collective-permute-start.17 = (bf16[136,1024]{1,0:T(8,128)(2,1)S(1)}, bf16[136,1024]{1,0:T(8,128)(2,1)S(1)}, u32[]{:S(2)}, u32[]{:S(2)}) collective-permute-start(bf16[136,1024]{1,0:T(8,128)(2,1)S(1)} %collective-permute-done.16.refs_0_), channel_id=1, source_target_pairs={{96,128},{128,160},{160,192},{192,224},{97,129},{129,161},{161,193... | collective-permute-start | bytes 835592 | tf_op jit(solution)/shard_map/ppermute | solution.py:65
  98.8 1.7 %collective-permute-start.21 = (f32[72,1024]{1,0:T(8,128)S(1)}, f32[72,1024]{1,0:T(8,128)S(1)}, u32[]{:S(2)}, u32[]{:S(2)}) collective-permute-start(f32[72,1024]{1,0:T(8,128)S(1)} %get-tuple-element.61), channel_id=1, source_target_pairs={{0,4},{4,0},{1,5},{5,1},{2,6},{6,2},{3,7},{7,3},{8,12},{12,8},{9,1... | collective-permute-start | bytes 884744 | tf_op jit(solution)/shard_map/ppermute | solution.py:51
  101.5 14.2 %copy-start.4 = (f32[1024]{0:T(1024)S(1)}, f32[1024]{0:T(1024)}, u32[]{:S(2)}) copy-start(f32[1024]{0:T(1024)} %param.17) | copy-start | bytes 12292
  101.5 14.0 %all-to-all-start.1 = ((bf16[16,2,2048]{2,1,0:T(2,128)(2,1)}), bf16[16,2,2048]{2,1,0:T(2,128)(2,1)S(1)}, u32[]{:S(2)}, u32[]{:S(2)}) async-start(bf16[16,2,2048]{2,1,0:T(2,128)(2,1)} %reshape.4), calls=%async_computation.1 | async-start | bytes 262144 | tf_op jit(solution)/shard_map/all_to_all | solution.py:462
  107.7 0.8 copy-start
  108.5 0.8 copy-start.2
  109.3 1.0 copy-start.1
  110.3 1.0 copy-start.3

commit v10 on v9

--- a/solution.py
+++ b/solution.py
@@ -56,7 +56,8 @@
 
 
 def gather(x, axis):
-    one, three = shift(x, axis, 1), shift(x, axis, -1)
+    one = shift(x, axis, 1)
+    three = shift(x, axis, -1)
     two = shift(one, axis, 1)
     return [x, one, two, three]
 
@@ -116,7 +117,7 @@
     toks = refs[:8]
     gain, w_own, w_sib = refs[8:11]
     qc_out, kv_out, cum_out = refs[11:14]
-    w, rows = refs[14:]
+    w, normed = refs[14:]
     x, c, y = idx[1], idx[2], idx[3]
     for z in range(NZ):
         for xx in range(NX):
@@ -129,19 +130,21 @@
         for outer in range(4):
             tok = toks[half * 4 + outer][...].astype(F32)
             scale = lax.rsqrt(jnp.mean(tok * tok, axis=-1, keepdims=True) + EPS)
-            normed = (tok * scale * gain[...]).astype(BF16)
-            out = jnp.dot(normed, w[...], preferred_element_type=F32)
+            out = (tok * scale * gain[...]).astype(BF16)
             for inner in range(4):
                 kx, ky = (outer, inner) if half == 0 else (inner, outer)
                 xx = lax.rem(x - kx + NX, NX)
                 yy = lax.rem(y - ky + NY, NY)
                 at = pl.multiple_of(xx * BLK + yy * OWN + half * 32, 32)
-                rows[pl.ds(at, 32), :] = out[inner * 32 : inner * 32 + 32, :]
+                normed[pl.ds(at, 32), :] = out[inner * 32 : inner * 32 + 32, :]
     before = lax.broadcasted_iota(jnp.int32, (BLK, BLK), 0)
     after = lax.broadcasted_iota(jnp.int32, (BLK, BLK), 1)
     ones = jnp.where(before <= after, 1.0, 0.0).astype(BF16)
     for b in range(4):
-        t = rows[b * BLK : (b + 1) * BLK, :].T
+        if b % 2 == 0:
+            pair = normed[b * BLK : (b + 2) * BLK, :]
+            columns = jnp.dot(pair, w[...], preferred_element_type=F32)
+        t = columns[b % 2 * BLK : (b % 2 + 1) * BLK].T
         lanes = slice(b * BLK, (b + 1) * BLK)
         qc_out[0:64, lanes] = t[:64].astype(BF16)
         kv_out[:, lanes] = t[64:192].astype(BF16)
@@ -401,7 +404,7 @@
         project_body,
         (sds((80, KEYS), BF16), sds((128, KEYS), BF16), sds((8, KEYS), F32)),
         [SMEM, SMEM] + [VMEM] * 11,
-        [pltpu.VMEM((D, 256), BF16), pltpu.VMEM((KEYS, 256), F32)],
+        [pltpu.VMEM((D, 256), BF16), pltpu.VMEM((KEYS, D), BF16)],
         2e9,
     )(idx, forget_offset, *toks, norm_gain[None], w_own, w_sib)
 

time: 118 us -> 119 us (level)
  Pallas kernels: 28.3 us -> 29.6 us
    pallas_call x1, Pallas kernels: 2.15 us -> 3.37 us  [shards(): call(project_body, (sds((80, KEYS), BF16), sds((128, KEYS), BF16), sds((8...]
where the time goes in v10:
time: 119 us; the launch traced here: 118 us
  starting transfers between devices  53.1 us (45%)
  Pallas kernels  29.6 us (25%)
  waiting for transfers between devices  29.5 us (25%)
  local copies, waits for them, and re-layouts  4.88 us (4%)
    ppermute x18, waiting for transfers between devices, shift(): return lax.ppermute(x, axis, [(i, (i + k) % n) for i in range(n)])  20.4 us
    ppermute x18, starting transfers between devices, shift(): return lax.ppermute(x, axis, [(i, (i + k) % n) for i in range(n)])  19.9 us
    pallas_call x4, Pallas kernels, shards(): call(functools.partial(step_body, k), outs, [SMEM] + [VMEM] * (len(ins) -...  18.5 us
    ppermute x4, starting transfers between devices, step_right(): return lax.ppermute(x, 'z', [(i, i + 1) for i in range(k - 1, NZ - 1)])  17.8 us
    all_to_all x1, starting transfers between devices, shards(): w_own = lax.all_to_all(chunk, 'z', 0, 0, tiled=True)  6.75 us
    all_to_all x1, starting transfers between devices, shards(): att = lax.all_to_all(att.reshape(16, 64, HD), ('x', 'y'), 0, 0, tiled=True)  5.96 us
    ppermute x4, waiting for transfers between devices, step_right(): return lax.ppermute(x, 'z', [(i, i + 1) for i in range(k - 1, NZ - 1)])  5.1 us
    unnamed x19, local copies, waits for them, and re-layouts  4.83 us
  transfers between devices with their start and end apart: 27, of which 15 were waited for; matrix products, arithmetic and copies ran while one was open for 1% of the time, Pallas kernels for 19%

profile of v10, /device:TPU:160, one launch (start us, length us, event | category | flops | bytes accessed | tf_op | source)
XLA Modules:
  0.0 118.5 jit_solution(3017565124314072639)
XLA Ops:
  0.1 1.0 pad_add_fusion.rows
  1.1 0.8 shard_map.91
  1.9 1.6 %collective-permute-start.6 = (bf16[48,1024]{1,0:T(8,128)(2,1)S(1)}, bf16[48,1024]{1,0:T(8,128)(2,1)S(1)}, u32[]{:S(2)}, u32[]{:S(2)}) collective-permute-start(bf16[48,1024]{1,0:T(8,128)(2,1)S(1)} %get-tuple-element.38), channel_id=1, source_target_pairs={{0,8},{8,16},{16,24},{24,0},{1,9},{9,17},{17,25},{25,1},{2,10},{10... | collective-permute-start | bytes 294920 | tf_op jit(solution)/shard_map/ppermute | solution.py:51
  3.5 2.7 %collective-permute-start.7 = (bf16[48,1024]{1,0:T(8,128)(2,1)S(1)}, bf16[48,1024]{1,0:T(8,128)(2,1)S(1)}, u32[]{:S(2)}, u32[]{:S(2)}) collective-permute-start(bf16[48,1024]{1,0:T(8,128)(2,1)S(1)} %get-tuple-element.39), channel_id=1, source_target_pairs={{0,16},{8,24},{16,0},{24,8},{1,17},{9,25},{17,1},{25,9},{2,18},{10... | collective-permute-start | bytes 294920 | tf_op jit(solution)/shard_map/ppermute | solution.py:51
  6.2 1.4 %collective-permute-start.8 = (bf16[48,1024]{1,0:T(8,128)(2,1)S(1)}, bf16[48,1024]{1,0:T(8,128)(2,1)S(1)}, u32[]{:S(2)}, u32[]{:S(2)}) collective-permute-start(bf16[48,1024]{1,0:T(8,128)(2,1)S(1)} %get-tuple-element.40), channel_id=1, source_target_pairs={{0,24},{8,0},{16,8},{24,16},{1,25},{9,1},{17,9},{25,17},{2,26},{10... | collective-permute-start | bytes 294920 | tf_op jit(solution)/shard_map/ppermute | solution.py:51
  8.0 2.8 %collective-permute-done.7.r2 = bf16[48,1024]{1,0:T(8,128)(2,1)S(1)} collective-permute-done((bf16[48,1024]{1,0:T(8,128)(2,1)S(1)}, bf16[48,1024]{1,0:T(8,128)(2,1)S(1)}, u32[]{:S(2)}, u32[]{:S(2)}) %collective-permute-start.7) | collective-permute-done | bytes 98336 | tf_op jit(solution)/shard_map/ppermute | solution.py:51
  10.8 0.9 shard_map.92
  11.7 6.8 %all-to-all-start = ((bf16[8,128,256]{2,1,0:T(8,128)(2,1)}), bf16[8,128,256]{2,1,0:T(8,128)(2,1)S(1)}, u32[]{:S(2)}, u32[]{:S(2)}) async-start(bf16[8,128,256]{2,1,0:T(8,128)(2,1)} %get-tuple-element.42), calls=%async_computation | async-start | bytes 1048576 | tf_op jit(solution)/shard_map/all_to_all | solution.py:398
  18.4 3.0 %collective-permute-start.2 = (bf16[32,1024]{1,0:T(8,128)(2,1)S(1)}, bf16[32,1024]{1,0:T(8,128)(2,1)S(1)}, u32[]{:S(2)}, u32[]{:S(2)}) collective-permute-start(bf16[32,1024]{1,0:T(8,128)(2,1)S(1)} %get-tuple-element.34), channel_id=1, source_target_pairs={{0,3},{1,0},{2,1},{3,2},{4,7},{5,4},{6,5},{7,6},{8,11},{9,8},{10,9... | collective-permute-start | bytes 196616 | tf_op jit(solution)/shard_map/ppermute | solution.py:51
  22.1 1.0 collective-permute-start
  23.0 4.9 %collective-permute-done = bf16[32,1024]{1,0:T(8,128)(2,1)S(1)} collective-permute-done((bf16[32,1024]{1,0:T(8,128)(2,1)S(1)}, bf16[32,1024]{1,0:T(8,128)(2,1)S(1)}, u32[]{:S(2)}, u32[]{:S(2)}) %collective-permute-start) | collective-permute-done | bytes 65568 | tf_op jit(solution)/shard_map/ppermute | solution.py:51
  28.0 1.4 %collective-permute-start.3 = (bf16[128,1024]{1,0:T(8,128)(2,1)S(1)}, bf16[128,1024]{1,0:T(8,128)(2,1)S(1)}, u32[]{:S(2)}, u32[]{:S(2)}) collective-permute-start(bf16[128,1024]{1,0:T(8,128)(2,1)S(1)} %constant_dynamic-update-slice_fusion.refs_0_), channel_id=1, source_target_pairs={{0,8},{8,16},{16,24},{24,0},{1,9},{9,17},{17,25},{25,1},{2,10},{10... | collective-permute-start | bytes 786440 | tf_op jit(solution)/shard_map/ppermute | solution.py:51
  29.4 1.0 all-to-all-done.refs_9_
  30.3 2.7 %collective-permute-start.5 = (bf16[128,1024]{1,0:T(8,128)(2,1)S(1)}, bf16[128,1024]{1,0:T(8,128)(2,1)S(1)}, u32[]{:S(2)}, u32[]{:S(2)}) collective-permute-start(bf16[128,1024]{1,0:T(8,128)(2,1)S(1)} %constant_dynamic-update-slice_fusion.refs_0_), channel_id=1, source_target_pairs={{0,24},{8,0},{16,8},{24,16},{1,25},{9,1},{17,9},{25,17},{2,26},{10... | collective-permute-start | bytes 786440 | tf_op jit(solution)/shard_map/ppermute | solution.py:51
  33.0 3.0 %collective-permute-start.11 = (bf16[128,1024]{1,0:T(8,128)(2,1)S(1)}, bf16[128,1024]{1,0:T(8,128)(2,1)S(1)}, u32[]{:S(2)}, u32[]{:S(2)}) collective-permute-start(bf16[128,1024]{1,0:T(8,128)(2,1)S(1)} %get-tuple-element.41.refs_4_), channel_id=1, source_target_pairs={{0,3},{1,0},{2,1},{3,2},{4,7},{5,4},{6,5},{7,6},{8,11},{9,8},{10,9... | collective-permute-start | bytes 786440 | tf_op jit(solution)/shard_map/ppermute | solution.py:51
  36.0 0.9 collective-permute-done.9.refs_5_
  37.0 2.3 %collective-permute-done.5.refs_3_ = bf16[128,1024]{1,0:T(8,128)(2,1)S(1)} collective-permute-done((bf16[128,1024]{1,0:T(8,128)(2,1)S(1)}, bf16[128,1024]{1,0:T(8,128)(2,1)S(1)}, u32[]{:S(2)}, u32[]{:S(2)}) %collective-permute-start.5) | collective-permute-done | bytes 262176 | tf_op jit(solution)/shard_map/ppermute | solution.py:51
  39.2 2.7 %collective-permute-done.11.refs_7_ = bf16[128,1024]{1,0:T(8,128)(2,1)S(1)} collective-permute-done((bf16[128,1024]{1,0:T(8,128)(2,1)S(1)}, bf16[128,1024]{1,0:T(8,128)(2,1)S(1)}, u32[]{:S(2)}, u32[]{:S(2)}) %collective-permute-start.11) | collective-permute-done | bytes 262176 | tf_op jit(solution)/shard_map/ppermute | solution.py:51
  42.0 3.4 %collective-permute-done.4.refs_2_ = bf16[128,1024]{1,0:T(8,128)(2,1)S(1)} collective-permute-done((bf16[128,1024]{1,0:T(8,128)(2,1)S(1)}, bf16[128,1024]{1,0:T(8,128)(2,1)S(1)}, u32[]{:S(2)}, u32[]{:S(2)}) %collective-permute-start.4) | collective-permute-done | bytes 262176 | tf_op jit(solution)/shard_map/ppermute | solution.py:51
  45.5 3.4 %shard_map.93 = (bf16[80,1024]{1,0:T(8,128)(2,1)S(1)}, bf16[128,1024]{1,0:T(8,128)(2,1)S(1)}, f32[8,1024]{1,0:T(8,128)S(1)}) custom-call(s32[4]{0:T(128)S(1)} %pad_add_fusion.1.idx, f32[4]{0:T(128)S(1)} %copy-done.6, bf16[128,1024]{1,0:T(8,128)(2,1)S(1)} %constant_dynamic-update-slice_fusion.refs_0_, bf16[128,1024]{1,0:T(8,128)(2,1)S(1)} %collective-permute-done.3.refs_1_, ...), custom_call_target="tpu_custom_call" | custom-call | flops 2000000000 | bytes 1048576 | tf_op jit(solution)/shard_map/pallas_call | solution.py:403
  49.2 1.3 %collective-permute-done.13.q_sib = bf16[80,1024]{1,0:T(8,128)(2,1)S(1)} collective-permute-done((bf16[80,1024]{1,0:T(8,128)(2,1)S(1)}, bf16[80,1024]{1,0:T(8,128)(2,1)S(1)}, u32[]{:S(2)}, u32[]{:S(2)}) %collective-permute-start.13) | collective-permute-done | bytes 163872 | tf_op jit(solution)/shard_map/ppermute | solution.py:51
  51.2 0.7 collective-permute-start.18
  51.9 3.1 %collective-permute-start.14 = (bf16[136,1024]{1,0:T(8,128)(2,1)S(1)}, bf16[136,1024]{1,0:T(8,128)(2,1)S(1)}, u32[]{:S(2)}, u32[]{:S(2)}) collective-permute-start(bf16[136,1024]{1,0:T(8,128)(2,1)S(1)} %get-tuple-element.47.pay), channel_id=1, source_target_pairs={{0,32},{32,64},{64,96},{96,128},{128,160},{160,192},{192,224},{1,3... | collective-permute-start | bytes 835592 | tf_op jit(solution)/shard_map/ppermute | solution.py:66
  55.0 2.7 %shard_map.95 = (f32[2,80,2048]{2,1,0:T(8,128)S(1)}, f32[2,8,2048]{2,1,0:T(8,128)S(1)}, f32[8,256]{1,0:T(8,128)S(1)}) custom-call(s32[4]{0:T(128)S(1)} %pad_add_fusion.1.idx, bf16[128,2048]{1,0:T(8,128)(2,1)S(1)} %get-tuple-element.46.q, bf16[136,1024]{1,0:T(8,128)(2,1)S(1)} %get-tuple-element.47.pay), custom_call_target="tpu_custom_call" | custom-call | flops 3000000000 | bytes 1048576 | tf_op jit(solution)/shard_map/pallas_call | solution.py:432
  57.6 0.7 collective-permute-start.24
  58.9 0.9 collective-permute-start.22
  59.7 0.7 collective-permute-start.19
  60.4 2.0 %collective-permute-done.14.refs_0_ = bf16[136,1024]{1,0:T(8,128)(2,1)S(1)} collective-permute-done((bf16[136,1024]{1,0:T(8,128)(2,1)S(1)}, bf16[136,1024]{1,0:T(8,128)(2,1)S(1)}, u32[]{:S(2)}, u32[]{:S(2)}) %collective-permute-start.14) | collective-permute-done | bytes 278560 | tf_op jit(solution)/shard_map/ppermute | solution.py:66
  62.5 3.1 %collective-permute-start.15 = (bf16[136,1024]{1,0:T(8,128)(2,1)S(1)}, bf16[136,1024]{1,0:T(8,128)(2,1)S(1)}, u32[]{:S(2)}, u32[]{:S(2)}) collective-permute-start(bf16[136,1024]{1,0:T(8,128)(2,1)S(1)} %collective-permute-done.14.refs_0_), channel_id=1, source_target_pairs={{32,64},{64,96},{96,128},{128,160},{160,192},{192,224},{33,65},{65... | collective-permute-start | bytes 835592 | tf_op jit(solution)/shard_map/ppermute | solution.py:66
  65.6 3.9 %shard_map.96 = (f32[2,80,2048]{2,1,0:T(8,128)S(1)}, f32[2,8,2048]{2,1,0:T(8,128)S(1)}, f32[8,256]{1,0:T(8,128)S(1)}) custom-call(s32[4]{0:T(128)S(1)} %pad_add_fusion.1.idx, bf16[128,2048]{1,0:T(8,128)(2,1)S(1)} %get-tuple-element.46.q, bf16[136,1024]{1,0:T(8,128)(2,1)S(1)} %collective-permute-done.14.refs_0_, ...), custom_call_target="tpu_custom_call", output_to_operand_aliasing={{0}: (4, {}), {1}: (5, {})} | custom-call | flops 6000000000 | bytes 1048576 | tf_op jit(solution)/shard_map/pallas_call | solution.py:452
  69.5 1.3 %collective-permute-start.20 = (bf16[136,1024]{1,0:T(8,128)(2,1)S(1)}, bf16[136,1024]{1,0:T(8,128)(2,1)S(1)}, u32[]{:S(2)}, u32[]{:S(2)}) collective-permute-start(bf16[136,1024]{1,0:T(8,128)(2,1)S(1)} %collective-permute-done.19.refs_1_), channel_id=1, source_target_pairs={{192,160},{224,192},{0,224},{193,161},{225,193},{1,225},{194,162},... | collective-permute-start | bytes 835592 | tf_op jit(solution)/shard_map/ppermute | solution.py:70
  70.8 1.5 %collective-permute-done.15.refs_0_ = bf16[136,1024]{1,0:T(8,128)(2,1)S(1)} collective-permute-done((bf16[136,1024]{1,0:T(8,128)(2,1)S(1)}, bf16[136,1024]{1,0:T(8,128)(2,1)S(1)}, u32[]{:S(2)}, u32[]{:S(2)}) %collective-permute-start.15) | collective-permute-done | bytes 278560 | tf_op jit(solution)/shard_map/ppermute | solution.py:66
  72.2 5.5 %collective-permute-start.16 = (bf16[136,1024]{1,0:T(8,128)(2,1)S(1)}, bf16[136,1024]{1,0:T(8,128)(2,1)S(1)}, u32[]{:S(2)}, u32[]{:S(2)}) collective-permute-start(bf16[136,1024]{1,0:T(8,128)(2,1)S(1)} %collective-permute-done.15.refs_0_), channel_id=1, source_target_pairs={{64,96},{96,128},{128,160},{160,192},{192,224},{65,97},{97,129},{1... | collective-permute-start | bytes 835592 | tf_op jit(solution)/shard_map/ppermute | solution.py:66
  77.8 3.9 %shard_map.97 = (f32[2,80,2048]{2,1,0:T(8,128)S(1)}, f32[2,8,2048]{2,1,0:T(8,128)S(1)}, f32[8,256]{1,0:T(8,128)S(1)}) custom-call(s32[4]{0:T(128)S(1)} %pad_add_fusion.1.idx, bf16[128,2048]{1,0:T(8,128)(2,1)S(1)} %get-tuple-element.46.q, bf16[136,1024]{1,0:T(8,128)(2,1)S(1)} %collective-permute-done.15.refs_0_, ...), custom_call_target="tpu_custom_call", output_to_operand_aliasing={{0}: (4, {}), {1}: (5, {})} | custom-call | flops 6000000000 | bytes 1048576 | tf_op jit(solution)/shard_map/pallas_call | solution.py:452
  81.7 1.6 %collective-permute-done.16.refs_0_ = bf16[136,1024]{1,0:T(8,128)(2,1)S(1)} collective-permute-done((bf16[136,1024]{1,0:T(8,128)(2,1)S(1)}, bf16[136,1024]{1,0:T(8,128)(2,1)S(1)}, u32[]{:S(2)}, u32[]{:S(2)}) %collective-permute-start.16) | collective-permute-done | bytes 278560 | tf_op jit(solution)/shard_map/ppermute | solution.py:66
  83.3 6.1 %collective-permute-start.17 = (bf16[136,1024]{1,0:T(8,128)(2,1)S(1)}, bf16[136,1024]{1,0:T(8,128)(2,1)S(1)}, u32[]{:S(2)}, u32[]{:S(2)}) collective-permute-start(bf16[136,1024]{1,0:T(8,128)(2,1)S(1)} %collective-permute-done.16.refs_0_), channel_id=1, source_target_pairs={{96,128},{128,160},{160,192},{192,224},{97,129},{129,161},{161,193... | collective-permute-start | bytes 835592 | tf_op jit(solution)/shard_map/ppermute | solution.py:66
  89.4 6.7 %shard_map.98 = (f32[2,80,2048]{2,1,0:T(8,128)S(1)}, f32[2,8,2048]{2,1,0:T(8,128)S(1)}, f32[8,256]{1,0:T(8,128)S(1)}) custom-call(s32[4]{0:T(128)S(1)} %pad_add_fusion.1.idx, bf16[128,2048]{1,0:T(8,128)(2,1)S(1)} %get-tuple-element.46.q, bf16[136,1024]{1,0:T(8,128)(2,1)S(1)} %collective-permute-done.16.refs_0_, ...), custom_call_target="tpu_custom_call", output_to_operand_aliasing={{0}: (4, {}), {1}: (5, {})} | custom-call | flops 6000000000 | bytes 1048576 | tf_op jit(solution)/shard_map/pallas_call | solution.py:452
  96.1 4.0 %shard_map.99 = (f32[72,1024]{1,0:T(8,128)S(1)}, f32[72,1024]{1,0:T(8,128)S(1)}) custom-call(s32[4]{0:T(128)S(1)} %pad_add_fusion.1.idx, bf16[128,2048]{1,0:T(8,128)(2,1)S(1)} %get-tuple-element.46.q, bf16[136,1024]{1,0:T(8,128)(2,1)S(1)} %collective-permute-done.17.refs_0_, f32[2,80,2048]{2,1,0:T(8,128)S(1)} %get-tuple-element.57.refs_1_, ...), custom_call_target="tpu_custom_call" | custom-call | flops 6000000000 | bytes 1048576 | tf_op jit(solution)/shard_map/pallas_call | solution.py:452
  100.3 1.6 %collective-permute-done.21.sib = f32[72,1024]{1,0:T(8,128)S(1)} collective-permute-done((f32[72,1024]{1,0:T(8,128)S(1)}, f32[72,1024]{1,0:T(8,128)S(1)}, u32[]{:S(2)}, u32[]{:S(2)}) %collective-permute-start.21) | collective-permute-done | bytes 294944 | tf_op jit(solution)/shard_map/ppermute | solution.py:51
  102.0 0.9 reshape.4
  102.9 6.0 %all-to-all-start.1 = ((bf16[16,2,2048]{2,1,0:T(2,128)(2,1)}), bf16[16,2,2048]{2,1,0:T(2,128)(2,1)S(1)}, u32[]{:S(2)}, u32[]{:S(2)}) async-start(bf16[16,2,2048]{2,1,0:T(2,128)(2,1)} %reshape.4), calls=%async_computation.1 | async-start | bytes 262144 | tf_op jit(solution)/shard_map/all_to_all | solution.py:465
  108.9 0.8 copy-done
  109.7 0.8 copy-done.2
  110.5 1.0 copy-done.1
  111.6 1.0 copy-done.3
  112.6 1.0 shard_map.101.w
  113.6 3.1 %all-to-all-done.1 = bf16[16,2,2048]{2,1,0:T(2,128)(2,1)S(1)} async-done(((bf16[16,2,2048]{2,1,0:T(2,128)(2,1)}), bf16[16,2,2048]{2,1,0:T(2,128)(2,1)S(1)}, u32[]{:S(2)}, u32[]{:S(2)}) %all-to-all-start.1) | async-done | bytes 131104 | tf_op jit(solution)/shard_map/all_to_all | solution.py:465
  116.9 1.5 %shard_map.102 = bf16[64,1024]{1,0:T(8,128)(2,1)} custom-call(bf16[16,64,64]{2,1,0:T(8,128)(2,1)S(1)} %reshape.5.att, f32[1,1024]{1,0:T(1,128)S(1)} %bitcast.13, bf16[1024,1024]{1,0:T(8,128)(2,1)S(1)} %shard_map.101.w), custom_call_target="tpu_custom_call" | custom-call | flops 100000000 | bytes 1048576 | tf_op jit(solution)/shard_map/pallas_call | solution.py:466
  (43 shorter events, 3.2 us)
Async XLA Ops:
  1.9 43.6 %copy-start.5 = (f32[1024]{0:T(1024)S(1)}, f32[1024]{0:T(1024)}, u32[]{:S(2)}) copy-start(f32[1024]{0:T(1024)} %param.10) | copy-start | bytes 12292
  1.9 43.6 %copy-start.6 = (f32[4]{0:T(128)S(1)}, f32[4]{0:T(128)}, u32[]{:S(2)}) copy-start(f32[4]{0:T(128)} %offs.1) | copy-start | bytes 52
  1.9 6.1 %collective-permute-start.6 = (bf16[48,1024]{1,0:T(8,128)(2,1)S(1)}, bf16[48,1024]{1,0:T(8,128)(2,1)S(1)}, u32[]{:S(2)}, u32[]{:S(2)}) collective-permute-start(bf16[48,1024]{1,0:T(8,128)(2,1)S(1)} %get-tuple-element.38), channel_id=1, source_target_pairs={{0,8},{8,16},{16,24},{24,0},{1,9},{9,17},{17,25},{25,1},{2,10},{10... | collective-permute-start | bytes 294920 | tf_op jit(solution)/shard_map/ppermute | solution.py:51
  3.5 7.3 %collective-permute-start.7 = (bf16[48,1024]{1,0:T(8,128)(2,1)S(1)}, bf16[48,1024]{1,0:T(8,128)(2,1)S(1)}, u32[]{:S(2)}, u32[]{:S(2)}) collective-permute-start(bf16[48,1024]{1,0:T(8,128)(2,1)S(1)} %get-tuple-element.39), channel_id=1, source_target_pairs={{0,16},{8,24},{16,0},{24,8},{1,17},{9,25},{17,1},{25,9},{2,18},{10... | collective-permute-start | bytes 294920 | tf_op jit(solution)/shard_map/ppermute | solution.py:51
  6.2 4.6 %collective-permute-start.8 = (bf16[48,1024]{1,0:T(8,128)(2,1)S(1)}, bf16[48,1024]{1,0:T(8,128)(2,1)S(1)}, u32[]{:S(2)}, u32[]{:S(2)}) collective-permute-start(bf16[48,1024]{1,0:T(8,128)(2,1)S(1)} %get-tuple-element.40), channel_id=1, source_target_pairs={{0,24},{8,0},{16,8},{24,16},{1,25},{9,1},{17,9},{25,17},{2,26},{10... | collective-permute-start | bytes 294920 | tf_op jit(solution)/shard_map/ppermute | solution.py:51
  11.7 18.7 %all-to-all-start = ((bf16[8,128,256]{2,1,0:T(8,128)(2,1)}), bf16[8,128,256]{2,1,0:T(8,128)(2,1)S(1)}, u32[]{:S(2)}, u32[]{:S(2)}) async-start(bf16[8,128,256]{2,1,0:T(8,128)(2,1)} %get-tuple-element.42), calls=%async_computation | async-start | bytes 1048576 | tf_op jit(solution)/shard_map/all_to_all | solution.py:398
  18.4 9.5 %collective-permute-start.2 = (bf16[32,1024]{1,0:T(8,128)(2,1)S(1)}, bf16[32,1024]{1,0:T(8,128)(2,1)S(1)}, u32[]{:S(2)}, u32[]{:S(2)}) collective-permute-start(bf16[32,1024]{1,0:T(8,128)(2,1)S(1)} %get-tuple-element.34), channel_id=1, source_target_pairs={{0,3},{1,0},{2,1},{3,2},{4,7},{5,4},{6,5},{7,6},{8,11},{9,8},{10,9... | collective-permute-start | bytes 196616 | tf_op jit(solution)/shard_map/ppermute | solution.py:51
  21.4 6.5 %collective-permute-start.1 = (bf16[32,1024]{1,0:T(8,128)(2,1)S(1)}, bf16[32,1024]{1,0:T(8,128)(2,1)S(1)}, u32[]{:S(2)}, u32[]{:S(2)}) collective-permute-start(bf16[32,1024]{1,0:T(8,128)(2,1)S(1)} %get-tuple-element.34), channel_id=1, source_target_pairs={{0,2},{1,3},{2,0},{3,1},{4,6},{5,7},{6,4},{7,5},{8,10},{9,11},{10,... | collective-permute-start | bytes 196616 | tf_op jit(solution)/shard_map/ppermute | solution.py:51
  22.1 5.8 %collective-permute-start = (bf16[32,1024]{1,0:T(8,128)(2,1)S(1)}, bf16[32,1024]{1,0:T(8,128)(2,1)S(1)}, u32[]{:S(2)}, u32[]{:S(2)}) collective-permute-start(bf16[32,1024]{1,0:T(8,128)(2,1)S(1)} %get-tuple-element.34), channel_id=1, source_target_pairs={{0,1},{1,2},{2,3},{3,0},{4,5},{5,6},{6,7},{7,4},{8,9},{9,10},{10,1... | collective-permute-start | bytes 196616 | tf_op jit(solution)/shard_map/ppermute | solution.py:51
  28.0 8.1 %collective-permute-start.3 = (bf16[128,1024]{1,0:T(8,128)(2,1)S(1)}, bf16[128,1024]{1,0:T(8,128)(2,1)S(1)}, u32[]{:S(2)}, u32[]{:S(2)}) collective-permute-start(bf16[128,1024]{1,0:T(8,128)(2,1)S(1)} %constant_dynamic-update-slice_fusion.refs_0_), channel_id=1, source_target_pairs={{0,8},{8,16},{16,24},{24,0},{1,9},{9,17},{17,25},{25,1},{2,10},{10... | collective-permute-start | bytes 786440 | tf_op jit(solution)/shard_map/ppermute | solution.py:51
  29.4 7.6 %collective-permute-start.9 = (bf16[128,1024]{1,0:T(8,128)(2,1)S(1)}, bf16[128,1024]{1,0:T(8,128)(2,1)S(1)}, u32[]{:S(2)}, u32[]{:S(2)}) collective-permute-start(bf16[128,1024]{1,0:T(8,128)(2,1)S(1)} %get-tuple-element.41.refs_4_), channel_id=1, source_target_pairs={{0,1},{1,2},{2,3},{3,0},{4,5},{5,6},{6,7},{7,4},{8,9},{9,10},{10,1... | collective-permute-start | bytes 786440 | tf_op jit(solution)/shard_map/ppermute | solution.py:51
  30.3 15.2 %collective-permute-start.12 = (bf16[8,128,256]{2,1,0:T(8,128)(2,1)S(1)}, bf16[8,128,256]{2,1,0:T(8,128)(2,1)S(1)}, u32[]{:S(2)}, u32[]{:S(2)}) collective-permute-start(bf16[8,128,256]{2,1,0:T(8,128)(2,1)S(1)} %all-to-all-done.refs_9_), channel_id=1, source_target_pairs={{0,4},{4,0},{1,5},{5,1},{2,6},{6,2},{3,7},{7,3},{8,12},{12,8},{9,1... | collective-permute-start | bytes 1572872 | tf_op jit(solution)/shard_map/ppermute | solution.py:51
  30.3 8.9 %collective-permute-start.5 = (bf16[128,1024]{1,0:T(8,128)(2,1)S(1)}, bf16[128,1024]{1,0:T(8,128)(2,1)S(1)}, u32[]{:S(2)}, u32[]{:S(2)}) collective-permute-start(bf16[128,1024]{1,0:T(8,128)(2,1)S(1)} %constant_dynamic-update-slice_fusion.refs_0_), channel_id=1, source_target_pairs={{0,24},{8,0},{16,8},{24,16},{1,25},{9,1},{17,9},{25,17},{2,26},{10... | collective-permute-start | bytes 786440 | tf_op jit(solution)/shard_map/ppermute | solution.py:51
  33.0 9.0 %collective-permute-start.11 = (bf16[128,1024]{1,0:T(8,128)(2,1)S(1)}, bf16[128,1024]{1,0:T(8,128)(2,1)S(1)}, u32[]{:S(2)}, u32[]{:S(2)}) collective-permute-start(bf16[128,1024]{1,0:T(8,128)(2,1)S(1)} %get-tuple-element.41.refs_4_), channel_id=1, source_target_pairs={{0,3},{1,0},{2,1},{3,2},{4,7},{5,4},{6,5},{7,6},{8,11},{9,8},{10,9... | collective-permute-start | bytes 786440 | tf_op jit(solution)/shard_map/ppermute | solution.py:51
  36.0 9.4 %collective-permute-start.4 = (bf16[128,1024]{1,0:T(8,128)(2,1)S(1)}, bf16[128,1024]{1,0:T(8,128)(2,1)S(1)}, u32[]{:S(2)}, u32[]{:S(2)}) collective-permute-start(bf16[128,1024]{1,0:T(8,128)(2,1)S(1)} %collective-permute-done.3.refs_1_), channel_id=1, source_target_pairs={{0,8},{8,16},{16,24},{24,0},{1,9},{9,17},{17,25},{25,1},{2,10},{10... | collective-permute-start | bytes 786440 | tf_op jit(solution)/shard_map/ppermute | solution.py:51
  37.0 8.5 %collective-permute-start.10 = (bf16[128,1024]{1,0:T(8,128)(2,1)S(1)}, bf16[128,1024]{1,0:T(8,128)(2,1)S(1)}, u32[]{:S(2)}, u32[]{:S(2)}) collective-permute-start(bf16[128,1024]{1,0:T(8,128)(2,1)S(1)} %collective-permute-done.9.refs_5_), channel_id=1, source_target_pairs={{0,1},{1,2},{2,3},{3,0},{4,5},{5,6},{6,7},{7,4},{8,9},{9,10},{10,1... | collective-permute-start | bytes 786440 | tf_op jit(solution)/shard_map/ppermute | solution.py:51
  48.9 1.7 %collective-permute-start.13 = (bf16[80,1024]{1,0:T(8,128)(2,1)S(1)}, bf16[80,1024]{1,0:T(8,128)(2,1)S(1)}, u32[]{:S(2)}, u32[]{:S(2)}) collective-permute-start(bf16[80,1024]{1,0:T(8,128)(2,1)S(1)} %get-tuple-element.43.q_own), channel_id=1, source_target_pairs={{0,4},{4,0},{1,5},{5,1},{2,6},{6,2},{3,7},{7,3},{8,12},{12,8},{9,1... | collective-permute-start | bytes 491528 | tf_op jit(solution)/shard_map/ppermute | solution.py:51
  51.2 8.6 %collective-permute-start.18 = (bf16[136,1024]{1,0:T(8,128)(2,1)S(1)}, bf16[136,1024]{1,0:T(8,128)(2,1)S(1)}, u32[]{:S(2)}, u32[]{:S(2)}) collective-permute-start(bf16[136,1024]{1,0:T(8,128)(2,1)S(1)} %get-tuple-element.47.pay), channel_id=1, source_target_pairs={{0,224},{32,0},{64,32},{1,225},{33,1},{65,33},{2,226},{34,2},{66,3... | collective-permute-start | bytes 835592 | tf_op jit(solution)/shard_map/ppermute | solution.py:70
  51.9 10.6 %collective-permute-start.14 = (bf16[136,1024]{1,0:T(8,128)(2,1)S(1)}, bf16[136,1024]{1,0:T(8,128)(2,1)S(1)}, u32[]{:S(2)}, u32[]{:S(2)}) collective-permute-start(bf16[136,1024]{1,0:T(8,128)(2,1)S(1)} %get-tuple-element.47.pay), channel_id=1, source_target_pairs={{0,32},{32,64},{64,96},{96,128},{128,160},{160,192},{192,224},{1,3... | collective-permute-start | bytes 835592 | tf_op jit(solution)/shard_map/ppermute | solution.py:66
  57.6 51.2 %collective-permute-start.24 = (bf16[2,8,64,256]{3,2,1,0:T(8,128)(2,1)S(1)}, bf16[2,8,64,256]{3,2,1,0:T(8,128)(2,1)S(1)}, u32[]{:S(2)}, u32[]{:S(2)}) collective-permute-start(bf16[2,8,64,256]{3,2,1,0:T(8,128)(2,1)S(1)} %pad_maximum_fusion.w0), channel_id=1, source_target_pairs={{0,3},{1,0},{2,1},{3,2},{4,7},{5,4},{6,5},{7,6},{8,11},{9,8},{10,9... | collective-permute-start | bytes 1572872 | tf_op jit(solution)/shard_map/ppermute | solution.py:51
  58.4 50.5 %collective-permute-start.23 = (bf16[2,8,64,256]{3,2,1,0:T(8,128)(2,1)S(1)}, bf16[2,8,64,256]{3,2,1,0:T(8,128)(2,1)S(1)}, u32[]{:S(2)}, u32[]{:S(2)}) collective-permute-start(bf16[2,8,64,256]{3,2,1,0:T(8,128)(2,1)S(1)} %pad_maximum_fusion.w0), channel_id=1, source_target_pairs={{0,2},{1,3},{2,0},{3,1},{4,6},{5,7},{6,4},{7,5},{8,10},{9,11},{10,... | collective-permute-start | bytes 1572872 | tf_op jit(solution)/shard_map/ppermute | solution.py:51
  58.9 50.9 %collective-permute-start.22 = (bf16[2,8,64,256]{3,2,1,0:T(8,128)(2,1)S(1)}, bf16[2,8,64,256]{3,2,1,0:T(8,128)(2,1)S(1)}, u32[]{:S(2)}, u32[]{:S(2)}) collective-permute-start(bf16[2,8,64,256]{3,2,1,0:T(8,128)(2,1)S(1)} %pad_maximum_fusion.w0), channel_id=1, source_target_pairs={{0,1},{1,2},{2,3},{3,0},{4,5},{5,6},{6,7},{7,4},{8,9},{9,10},{10,1... | collective-permute-start | bytes 1572872 | tf_op jit(solution)/shard_map/ppermute | solution.py:51
  59.7 9.7 %collective-permute-start.19 = (bf16[136,1024]{1,0:T(8,128)(2,1)S(1)}, bf16[136,1024]{1,0:T(8,128)(2,1)S(1)}, u32[]{:S(2)}, u32[]{:S(2)}) collective-permute-start(bf16[136,1024]{1,0:T(8,128)(2,1)S(1)} %collective-permute-done.18.refs_1_), channel_id=1, source_target_pairs={{224,192},{0,224},{32,0},{225,193},{1,225},{33,1},{226,194},{2,226... | collective-permute-start | bytes 835592 | tf_op jit(solution)/shard_map/ppermute | solution.py:70
  62.5 9.8 %collective-permute-start.15 = (bf16[136,1024]{1,0:T(8,128)(2,1)S(1)}, bf16[136,1024]{1,0:T(8,128)(2,1)S(1)}, u32[]{:S(2)}, u32[]{:S(2)}) collective-permute-start(bf16[136,1024]{1,0:T(8,128)(2,1)S(1)} %collective-permute-done.14.refs_0_), channel_id=1, source_target_pairs={{32,64},{64,96},{96,128},{128,160},{160,192},{192,224},{33,65},{65... | collective-permute-start | bytes 835592 | tf_op jit(solution)/shard_map/ppermute | solution.py:66
  69.5 19.9 %collective-permute-start.20 = (bf16[136,1024]{1,0:T(8,128)(2,1)S(1)}, bf16[136,1024]{1,0:T(8,128)(2,1)S(1)}, u32[]{:S(2)}, u32[]{:S(2)}) collective-permute-start(bf16[136,1024]{1,0:T(8,128)(2,1)S(1)} %collective-permute-done.19.refs_1_), channel_id=1, source_target_pairs={{192,160},{224,192},{0,224},{193,161},{225,193},{1,225},{194,162},... | collective-permute-start | bytes 835592 | tf_op jit(solution)/shard_map/ppermute | solution.py:70
  72.2 11.0 %collective-permute-start.16 = (bf16[136,1024]{1,0:T(8,128)(2,1)S(1)}, bf16[136,1024]{1,0:T(8,128)(2,1)S(1)}, u32[]{:S(2)}, u32[]{:S(2)}) collective-permute-start(bf16[136,1024]{1,0:T(8,128)(2,1)S(1)} %collective-permute-done.15.refs_0_), channel_id=1, source_target_pairs={{64,96},{96,128},{128,160},{160,192},{192,224},{65,97},{97,129},{1... | collective-permute-start | bytes 835592 | tf_op jit(solution)/shard_map/ppermute | solution.py:66
  83.3 12.9 %collective-permute-start.17 = (bf16[136,1024]{1,0:T(8,128)(2,1)S(1)}, bf16[136,1024]{1,0:T(8,128)(2,1)S(1)}, u32[]{:S(2)}, u32[]{:S(2)}) collective-permute-start(bf16[136,1024]{1,0:T(8,128)(2,1)S(1)} %collective-permute-done.16.refs_0_), channel_id=1, source_target_pairs={{96,128},{128,160},{160,192},{192,224},{97,129},{129,161},{161,193... | collective-permute-start | bytes 835592 | tf_op jit(solution)/shard_map/ppermute | solution.py:66
  100.2 1.7 %collective-permute-start.21 = (f32[72,1024]{1,0:T(8,128)S(1)}, f32[72,1024]{1,0:T(8,128)S(1)}, u32[]{:S(2)}, u32[]{:S(2)}) collective-permute-start(f32[72,1024]{1,0:T(8,128)S(1)} %get-tuple-element.61), channel_id=1, source_target_pairs={{0,4},{4,0},{1,5},{5,1},{2,6},{6,2},{3,7},{7,3},{8,12},{12,8},{9,1... | collective-permute-start | bytes 884744 | tf_op jit(solution)/shard_map/ppermute | solution.py:51
  102.9 14.0 %copy-start.4 = (f32[1024]{0:T(1024)S(1)}, f32[1024]{0:T(1024)}, u32[]{:S(2)}) copy-start(f32[1024]{0:T(1024)} %param.17) | copy-start | bytes 12292
  102.9 13.8 %all-to-all-start.1 = ((bf16[16,2,2048]{2,1,0:T(2,128)(2,1)}), bf16[16,2,2048]{2,1,0:T(2,128)(2,1)S(1)}, u32[]{:S(2)}, u32[]{:S(2)}) async-start(bf16[16,2,2048]{2,1,0:T(2,128)(2,1)} %reshape.4), calls=%async_computation.1 | async-start | bytes 262144 | tf_op jit(solution)/shard_map/all_to_all | solution.py:465
  108.9 0.8 copy-start
  109.7 0.8 copy-start.2
  110.5 1.0 copy-start.1
  111.6 1.0 copy-start.3

commit v11 on v9

--- a/solution.py
+++ b/solution.py
@@ -126,17 +126,20 @@
             w[pl.ds(own_at, 16), :] = w_own[z, xx * 16 : xx * 16 + 16, :]
             w[pl.ds(sib_at, 16), :] = w_sib[z, xx * 16 : xx * 16 + 16, :]
     for half in range(2):
-        for outer in range(4):
-            tok = toks[half * 4 + outer][...].astype(F32)
-            scale = lax.rsqrt(jnp.mean(tok * tok, axis=-1, keepdims=True) + EPS)
-            normed = (tok * scale * gain[...]).astype(BF16)
-            out = jnp.dot(normed, w[...], preferred_element_type=F32)
-            for inner in range(4):
+        for two in range(2):
+            parts = []
+            for outer in (2 * two, 2 * two + 1):
+                tok = toks[half * 4 + outer][...].astype(F32)
+                scale = lax.rsqrt(jnp.mean(tok * tok, axis=-1, keepdims=True) + EPS)
+                parts.append((tok * scale * gain[...]).astype(BF16))
+            out = jnp.dot(jnp.concatenate(parts, axis=0), w[...], preferred_element_type=F32)
+            for piece in range(8):
+                outer, inner = 2 * two + piece // 4, piece % 4
                 kx, ky = (outer, inner) if half == 0 else (inner, outer)
                 xx = lax.rem(x - kx + NX, NX)
                 yy = lax.rem(y - ky + NY, NY)
                 at = pl.multiple_of(xx * BLK + yy * OWN + half * 32, 32)
-                rows[pl.ds(at, 32), :] = out[inner * 32 : inner * 32 + 32, :]
+                rows[pl.ds(at, 32), :] = out[piece * 32 : piece * 32 + 32, :]
     before = lax.broadcasted_iota(jnp.int32, (BLK, BLK), 0)
     after = lax.broadcasted_iota(jnp.int32, (BLK, BLK), 1)
     ones = jnp.where(before <= after, 1.0, 0.0).astype(BF16)

time: 118 us -> 118 us (level)
  no operation moved by 1% of the time
where the time goes in v11:
time: 118 us; the launch traced here: 117 us
  starting transfers between devices  53.3 us (45%)
  waiting for transfers between devices  29.3 us (25%)
  Pallas kernels  28.3 us (24%)
  local copies, waits for them, and re-layouts  4.88 us (4%)
    ppermute x18, waiting for transfers between devices, shift(): return lax.ppermute(x, axis, [(i, (i + k) % n) for i in range(n)])  20.4 us
    ppermute x18, starting transfers between devices, shift(): return lax.ppermute(x, axis, [(i, (i + k) % n) for i in range(n)])  19.7 us
    pallas_call x4, Pallas kernels, shards(): call(functools.partial(step_body, k), outs, [SMEM] + [VMEM] * (len(ins) -...  18.5 us
    ppermute x4, starting transfers between devices, step_right(): return lax.ppermute(x, 'z', [(i, i + 1) for i in range(k - 1, NZ - 1)])  18 us
    all_to_all x1, starting transfers between devices, shards(): w_own = lax.all_to_all(chunk, 'z', 0, 0, tiled=True)  6.75 us
    all_to_all x1, starting transfers between devices, shards(): att = lax.all_to_all(att.reshape(16, 64, HD), ('x', 'y'), 0, 0, tiled=True)  6.15 us
    ppermute x4, waiting for transfers between devices, step_right(): return lax.ppermute(x, 'z', [(i, i + 1) for i in range(k - 1, NZ - 1)])  4.93 us
    unnamed x19, local copies, waits for them, and re-layouts  4.83 us
  transfers between devices with their start and end apart: 27, of which 15 were waited for; matrix products, arithmetic and copies ran while one was open for 1% of the time, Pallas kernels for 19%

profile of v11, /device:TPU:160, one launch (start us, length us, event | category | flops | bytes accessed | tf_op | source)
XLA Modules:
  0.0 117.2 jit_solution(7840051162427291645)
XLA Ops:
  0.1 1.0 pad_add_fusion.rows
  1.1 0.8 shard_map.91
  1.9 1.6 %collective-permute-start.6 = (bf16[48,1024]{1,0:T(8,128)(2,1)S(1)}, bf16[48,1024]{1,0:T(8,128)(2,1)S(1)}, u32[]{:S(2)}, u32[]{:S(2)}) collective-permute-start(bf16[48,1024]{1,0:T(8,128)(2,1)S(1)} %get-tuple-element.38), channel_id=1, source_target_pairs={{0,8},{8,16},{16,24},{24,0},{1,9},{9,17},{17,25},{25,1},{2,10},{10... | collective-permute-start | bytes 294920 | tf_op jit(solution)/shard_map/ppermute | solution.py:51
  3.5 2.7 %collective-permute-start.7 = (bf16[48,1024]{1,0:T(8,128)(2,1)S(1)}, bf16[48,1024]{1,0:T(8,128)(2,1)S(1)}, u32[]{:S(2)}, u32[]{:S(2)}) collective-permute-start(bf16[48,1024]{1,0:T(8,128)(2,1)S(1)} %get-tuple-element.39), channel_id=1, source_target_pairs={{0,16},{8,24},{16,0},{24,8},{1,17},{9,25},{17,1},{25,9},{2,18},{10... | collective-permute-start | bytes 294920 | tf_op jit(solution)/shard_map/ppermute | solution.py:51
  6.2 1.4 %collective-permute-start.8 = (bf16[48,1024]{1,0:T(8,128)(2,1)S(1)}, bf16[48,1024]{1,0:T(8,128)(2,1)S(1)}, u32[]{:S(2)}, u32[]{:S(2)}) collective-permute-start(bf16[48,1024]{1,0:T(8,128)(2,1)S(1)} %get-tuple-element.40), channel_id=1, source_target_pairs={{0,24},{8,0},{16,8},{24,16},{1,25},{9,1},{17,9},{25,17},{2,26},{10... | collective-permute-start | bytes 294920 | tf_op jit(solution)/shard_map/ppermute | solution.py:51
  8.0 2.8 %collective-permute-done.7.r2 = bf16[48,1024]{1,0:T(8,128)(2,1)S(1)} collective-permute-done((bf16[48,1024]{1,0:T(8,128)(2,1)S(1)}, bf16[48,1024]{1,0:T(8,128)(2,1)S(1)}, u32[]{:S(2)}, u32[]{:S(2)}) %collective-permute-start.7) | collective-permute-done | bytes 98336 | tf_op jit(solution)/shard_map/ppermute | solution.py:51
  10.8 0.9 shard_map.92
  11.7 6.8 %all-to-all-start = ((bf16[8,128,256]{2,1,0:T(8,128)(2,1)}), bf16[8,128,256]{2,1,0:T(8,128)(2,1)S(1)}, u32[]{:S(2)}, u32[]{:S(2)}) async-start(bf16[8,128,256]{2,1,0:T(8,128)(2,1)} %get-tuple-element.42), calls=%async_computation | async-start | bytes 1048576 | tf_op jit(solution)/shard_map/all_to_all | solution.py:398
  18.4 3.0 %collective-permute-start.2 = (bf16[32,1024]{1,0:T(8,128)(2,1)S(1)}, bf16[32,1024]{1,0:T(8,128)(2,1)S(1)}, u32[]{:S(2)}, u32[]{:S(2)}) collective-permute-start(bf16[32,1024]{1,0:T(8,128)(2,1)S(1)} %get-tuple-element.34), channel_id=1, source_target_pairs={{0,3},{1,0},{2,1},{3,2},{4,7},{5,4},{6,5},{7,6},{8,11},{9,8},{10,9... | collective-permute-start | bytes 196616 | tf_op jit(solution)/shard_map/ppermute | solution.py:51
  22.1 1.0 collective-permute-start
  23.0 4.9 %collective-permute-done = bf16[32,1024]{1,0:T(8,128)(2,1)S(1)} collective-permute-done((bf16[32,1024]{1,0:T(8,128)(2,1)S(1)}, bf16[32,1024]{1,0:T(8,128)(2,1)S(1)}, u32[]{:S(2)}, u32[]{:S(2)}) %collective-permute-start) | collective-permute-done | bytes 65568 | tf_op jit(solution)/shard_map/ppermute | solution.py:51
  28.0 1.4 %collective-permute-start.3 = (bf16[128,1024]{1,0:T(8,128)(2,1)S(1)}, bf16[128,1024]{1,0:T(8,128)(2,1)S(1)}, u32[]{:S(2)}, u32[]{:S(2)}) collective-permute-start(bf16[128,1024]{1,0:T(8,128)(2,1)S(1)} %constant_dynamic-update-slice_fusion.refs_0_), channel_id=1, source_target_pairs={{0,8},{8,16},{16,24},{24,0},{1,9},{9,17},{17,25},{25,1},{2,10},{10... | collective-permute-start | bytes 786440 | tf_op jit(solution)/shard_map/ppermute | solution.py:51
  29.4 1.0 all-to-all-done.refs_9_
  30.3 2.7 %collective-permute-start.5 = (bf16[128,1024]{1,0:T(8,128)(2,1)S(1)}, bf16[128,1024]{1,0:T(8,128)(2,1)S(1)}, u32[]{:S(2)}, u32[]{:S(2)}) collective-permute-start(bf16[128,1024]{1,0:T(8,128)(2,1)S(1)} %constant_dynamic-update-slice_fusion.refs_0_), channel_id=1, source_target_pairs={{0,24},{8,0},{16,8},{24,16},{1,25},{9,1},{17,9},{25,17},{2,26},{10... | collective-permute-start | bytes 786440 | tf_op jit(solution)/shard_map/ppermute | solution.py:51
  33.0 3.0 %collective-permute-start.11 = (bf16[128,1024]{1,0:T(8,128)(2,1)S(1)}, bf16[128,1024]{1,0:T(8,128)(2,1)S(1)}, u32[]{:S(2)}, u32[]{:S(2)}) collective-permute-start(bf16[128,1024]{1,0:T(8,128)(2,1)S(1)} %get-tuple-element.41.refs_4_), channel_id=1, source_target_pairs={{0,3},{1,0},{2,1},{3,2},{4,7},{5,4},{6,5},{7,6},{8,11},{9,8},{10,9... | collective-permute-start | bytes 786440 | tf_op jit(solution)/shard_map/ppermute | solution.py:51
  36.0 0.9 collective-permute-done.9.refs_5_
  37.0 2.3 %collective-permute-done.5.refs_3_ = bf16[128,1024]{1,0:T(8,128)(2,1)S(1)} collective-permute-done((bf16[128,1024]{1,0:T(8,128)(2,1)S(1)}, bf16[128,1024]{1,0:T(8,128)(2,1)S(1)}, u32[]{:S(2)}, u32[]{:S(2)}) %collective-permute-start.5) | collective-permute-done | bytes 262176 | tf_op jit(solution)/shard_map/ppermute | solution.py:51
  39.2 2.7 %collective-permute-done.11.refs_7_ = bf16[128,1024]{1,0:T(8,128)(2,1)S(1)} collective-permute-done((bf16[128,1024]{1,0:T(8,128)(2,1)S(1)}, bf16[128,1024]{1,0:T(8,128)(2,1)S(1)}, u32[]{:S(2)}, u32[]{:S(2)}) %collective-permute-start.11) | collective-permute-done | bytes 262176 | tf_op jit(solution)/shard_map/ppermute | solution.py:51
  42.0 3.4 %collective-permute-done.4.refs_2_ = bf16[128,1024]{1,0:T(8,128)(2,1)S(1)} collective-permute-done((bf16[128,1024]{1,0:T(8,128)(2,1)S(1)}, bf16[128,1024]{1,0:T(8,128)(2,1)S(1)}, u32[]{:S(2)}, u32[]{:S(2)}) %collective-permute-start.4) | collective-permute-done | bytes 262176 | tf_op jit(solution)/shard_map/ppermute | solution.py:51
  45.5 2.1 %shard_map.93 = (bf16[80,1024]{1,0:T(8,128)(2,1)S(1)}, bf16[128,1024]{1,0:T(8,128)(2,1)S(1)}, f32[8,1024]{1,0:T(8,128)S(1)}) custom-call(s32[4]{0:T(128)S(1)} %pad_add_fusion.1.idx, f32[4]{0:T(128)S(1)} %copy-done.6, bf16[128,1024]{1,0:T(8,128)(2,1)S(1)} %constant_dynamic-update-slice_fusion.refs_0_, bf16[128,1024]{1,0:T(8,128)(2,1)S(1)} %collective-permute-done.3.refs_1_, ...), custom_call_target="tpu_custom_call" | custom-call | flops 2000000000 | bytes 1048576 | tf_op jit(solution)/shard_map/pallas_call | solution.py:403
  47.8 1.3 %collective-permute-done.13.q_sib = bf16[80,1024]{1,0:T(8,128)(2,1)S(1)} collective-permute-done((bf16[80,1024]{1,0:T(8,128)(2,1)S(1)}, bf16[80,1024]{1,0:T(8,128)(2,1)S(1)}, u32[]{:S(2)}, u32[]{:S(2)}) %collective-permute-start.13) | collective-permute-done | bytes 163872 | tf_op jit(solution)/shard_map/ppermute | solution.py:51
  49.7 0.7 collective-permute-start.18
  50.4 3.3 %collective-permute-start.14 = (bf16[136,1024]{1,0:T(8,128)(2,1)S(1)}, bf16[136,1024]{1,0:T(8,128)(2,1)S(1)}, u32[]{:S(2)}, u32[]{:S(2)}) collective-permute-start(bf16[136,1024]{1,0:T(8,128)(2,1)S(1)} %get-tuple-element.47.pay), channel_id=1, source_target_pairs={{0,32},{32,64},{64,96},{96,128},{128,160},{160,192},{192,224},{1,3... | collective-permute-start | bytes 835592 | tf_op jit(solution)/shard_map/ppermute | solution.py:65
  53.7 2.6 %shard_map.95 = (f32[2,80,2048]{2,1,0:T(8,128)S(1)}, f32[2,8,2048]{2,1,0:T(8,128)S(1)}, f32[8,256]{1,0:T(8,128)S(1)}) custom-call(s32[4]{0:T(128)S(1)} %pad_add_fusion.1.idx, bf16[128,2048]{1,0:T(8,128)(2,1)S(1)} %get-tuple-element.46.q, bf16[136,1024]{1,0:T(8,128)(2,1)S(1)} %get-tuple-element.47.pay), custom_call_target="tpu_custom_call" | custom-call | flops 3000000000 | bytes 1048576 | tf_op jit(solution)/shard_map/pallas_call | solution.py:432
  56.3 0.8 collective-permute-start.24
  57.6 0.9 collective-permute-start.22
  58.5 0.7 collective-permute-start.19
  59.1 1.9 %collective-permute-done.14.refs_0_ = bf16[136,1024]{1,0:T(8,128)(2,1)S(1)} collective-permute-done((bf16[136,1024]{1,0:T(8,128)(2,1)S(1)}, bf16[136,1024]{1,0:T(8,128)(2,1)S(1)}, u32[]{:S(2)}, u32[]{:S(2)}) %collective-permute-start.14) | collective-permute-done | bytes 278560 | tf_op jit(solution)/shard_map/ppermute | solution.py:65
  61.0 3.1 %collective-permute-start.15 = (bf16[136,1024]{1,0:T(8,128)(2,1)S(1)}, bf16[136,1024]{1,0:T(8,128)(2,1)S(1)}, u32[]{:S(2)}, u32[]{:S(2)}) collective-permute-start(bf16[136,1024]{1,0:T(8,128)(2,1)S(1)} %collective-permute-done.14.refs_0_), channel_id=1, source_target_pairs={{32,64},{64,96},{96,128},{128,160},{160,192},{192,224},{33,65},{65... | collective-permute-start | bytes 835592 | tf_op jit(solution)/shard_map/ppermute | solution.py:65
  64.1 3.9 %shard_map.96 = (f32[2,80,2048]{2,1,0:T(8,128)S(1)}, f32[2,8,2048]{2,1,0:T(8,128)S(1)}, f32[8,256]{1,0:T(8,128)S(1)}) custom-call(s32[4]{0:T(128)S(1)} %pad_add_fusion.1.idx, bf16[128,2048]{1,0:T(8,128)(2,1)S(1)} %get-tuple-element.46.q, bf16[136,1024]{1,0:T(8,128)(2,1)S(1)} %collective-permute-done.14.refs_0_, ...), custom_call_target="tpu_custom_call", output_to_operand_aliasing={{0}: (4, {}), {1}: (5, {})} | custom-call | flops 6000000000 | bytes 1048576 | tf_op jit(solution)/shard_map/pallas_call | solution.py:452
  68.0 1.3 %collective-permute-start.20 = (bf16[136,1024]{1,0:T(8,128)(2,1)S(1)}, bf16[136,1024]{1,0:T(8,128)(2,1)S(1)}, u32[]{:S(2)}, u32[]{:S(2)}) collective-permute-start(bf16[136,1024]{1,0:T(8,128)(2,1)S(1)} %collective-permute-done.19.refs_1_), channel_id=1, source_target_pairs={{192,160},{224,192},{0,224},{193,161},{225,193},{1,225},{194,162},... | collective-permute-start | bytes 835592 | tf_op jit(solution)/shard_map/ppermute | solution.py:69
  69.3 1.5 %collective-permute-done.15.refs_0_ = bf16[136,1024]{1,0:T(8,128)(2,1)S(1)} collective-permute-done((bf16[136,1024]{1,0:T(8,128)(2,1)S(1)}, bf16[136,1024]{1,0:T(8,128)(2,1)S(1)}, u32[]{:S(2)}, u32[]{:S(2)}) %collective-permute-start.15) | collective-permute-done | bytes 278560 | tf_op jit(solution)/shard_map/ppermute | solution.py:65
  70.8 5.5 %collective-permute-start.16 = (bf16[136,1024]{1,0:T(8,128)(2,1)S(1)}, bf16[136,1024]{1,0:T(8,128)(2,1)S(1)}, u32[]{:S(2)}, u32[]{:S(2)}) collective-permute-start(bf16[136,1024]{1,0:T(8,128)(2,1)S(1)} %collective-permute-done.15.refs_0_), channel_id=1, source_target_pairs={{64,96},{96,128},{128,160},{160,192},{192,224},{65,97},{97,129},{1... | collective-permute-start | bytes 835592 | tf_op jit(solution)/shard_map/ppermute | solution.py:65
  76.3 3.9 %shard_map.97 = (f32[2,80,2048]{2,1,0:T(8,128)S(1)}, f32[2,8,2048]{2,1,0:T(8,128)S(1)}, f32[8,256]{1,0:T(8,128)S(1)}) custom-call(s32[4]{0:T(128)S(1)} %pad_add_fusion.1.idx, bf16[128,2048]{1,0:T(8,128)(2,1)S(1)} %get-tuple-element.46.q, bf16[136,1024]{1,0:T(8,128)(2,1)S(1)} %collective-permute-done.15.refs_0_, ...), custom_call_target="tpu_custom_call", output_to_operand_aliasing={{0}: (4, {}), {1}: (5, {})} | custom-call | flops 6000000000 | bytes 1048576 | tf_op jit(solution)/shard_map/pallas_call | solution.py:452
  80.2 1.6 %collective-permute-done.16.refs_0_ = bf16[136,1024]{1,0:T(8,128)(2,1)S(1)} collective-permute-done((bf16[136,1024]{1,0:T(8,128)(2,1)S(1)}, bf16[136,1024]{1,0:T(8,128)(2,1)S(1)}, u32[]{:S(2)}, u32[]{:S(2)}) %collective-permute-start.16) | collective-permute-done | bytes 278560 | tf_op jit(solution)/shard_map/ppermute | solution.py:65
  81.8 6.1 %collective-permute-start.17 = (bf16[136,1024]{1,0:T(8,128)(2,1)S(1)}, bf16[136,1024]{1,0:T(8,128)(2,1)S(1)}, u32[]{:S(2)}, u32[]{:S(2)}) collective-permute-start(bf16[136,1024]{1,0:T(8,128)(2,1)S(1)} %collective-permute-done.16.refs_0_), channel_id=1, source_target_pairs={{96,128},{128,160},{160,192},{192,224},{97,129},{129,161},{161,193... | collective-permute-start | bytes 835592 | tf_op jit(solution)/shard_map/ppermute | solution.py:65
  87.9 6.7 %shard_map.98 = (f32[2,80,2048]{2,1,0:T(8,128)S(1)}, f32[2,8,2048]{2,1,0:T(8,128)S(1)}, f32[8,256]{1,0:T(8,128)S(1)}) custom-call(s32[4]{0:T(128)S(1)} %pad_add_fusion.1.idx, bf16[128,2048]{1,0:T(8,128)(2,1)S(1)} %get-tuple-element.46.q, bf16[136,1024]{1,0:T(8,128)(2,1)S(1)} %collective-permute-done.16.refs_0_, ...), custom_call_target="tpu_custom_call", output_to_operand_aliasing={{0}: (4, {}), {1}: (5, {})} | custom-call | flops 6000000000 | bytes 1048576 | tf_op jit(solution)/shard_map/pallas_call | solution.py:452
  94.7 4.0 %shard_map.99 = (f32[72,1024]{1,0:T(8,128)S(1)}, f32[72,1024]{1,0:T(8,128)S(1)}) custom-call(s32[4]{0:T(128)S(1)} %pad_add_fusion.1.idx, bf16[128,2048]{1,0:T(8,128)(2,1)S(1)} %get-tuple-element.46.q, bf16[136,1024]{1,0:T(8,128)(2,1)S(1)} %collective-permute-done.17.refs_0_, f32[2,80,2048]{2,1,0:T(8,128)S(1)} %get-tuple-element.57.refs_1_, ...), custom_call_target="tpu_custom_call" | custom-call | flops 6000000000 | bytes 1048576 | tf_op jit(solution)/shard_map/pallas_call | solution.py:452
  98.8 1.6 %collective-permute-done.21.sib = f32[72,1024]{1,0:T(8,128)S(1)} collective-permute-done((f32[72,1024]{1,0:T(8,128)S(1)}, f32[72,1024]{1,0:T(8,128)S(1)}, u32[]{:S(2)}, u32[]{:S(2)}) %collective-permute-start.21) | collective-permute-done | bytes 294944 | tf_op jit(solution)/shard_map/ppermute | solution.py:51
  100.5 0.9 reshape.4
  101.4 6.1 %all-to-all-start.1 = ((bf16[16,2,2048]{2,1,0:T(2,128)(2,1)}), bf16[16,2,2048]{2,1,0:T(2,128)(2,1)S(1)}, u32[]{:S(2)}, u32[]{:S(2)}) async-start(bf16[16,2,2048]{2,1,0:T(2,128)(2,1)} %reshape.4), calls=%async_computation.1 | async-start | bytes 262144 | tf_op jit(solution)/shard_map/all_to_all | solution.py:465
  107.6 0.8 copy-done
  108.4 0.8 copy-done.2
  109.2 1.0 copy-done.1
  110.3 1.0 copy-done.3
  111.3 1.0 shard_map.101.w
  112.4 3.1 %all-to-all-done.1 = bf16[16,2,2048]{2,1,0:T(2,128)(2,1)S(1)} async-done(((bf16[16,2,2048]{2,1,0:T(2,128)(2,1)}), bf16[16,2,2048]{2,1,0:T(2,128)(2,1)S(1)}, u32[]{:S(2)}, u32[]{:S(2)}) %all-to-all-start.1) | async-done | bytes 131104 | tf_op jit(solution)/shard_map/all_to_all | solution.py:465
  115.7 1.5 %shard_map.102 = bf16[64,1024]{1,0:T(8,128)(2,1)} custom-call(bf16[16,64,64]{2,1,0:T(8,128)(2,1)S(1)} %reshape.5.att, f32[1,1024]{1,0:T(1,128)S(1)} %bitcast.13, bf16[1024,1024]{1,0:T(8,128)(2,1)S(1)} %shard_map.101.w), custom_call_target="tpu_custom_call" | custom-call | flops 100000000 | bytes 1048576 | tf_op jit(solution)/shard_map/pallas_call | solution.py:466
  (43 shorter events, 3.1 us)
Async XLA Ops:
  1.9 43.6 %copy-start.5 = (f32[1024]{0:T(1024)S(1)}, f32[1024]{0:T(1024)}, u32[]{:S(2)}) copy-start(f32[1024]{0:T(1024)} %param.10) | copy-start | bytes 12292
  1.9 43.6 %copy-start.6 = (f32[4]{0:T(128)S(1)}, f32[4]{0:T(128)}, u32[]{:S(2)}) copy-start(f32[4]{0:T(128)} %offs.1) | copy-start | bytes 52
  1.9 6.1 %collective-permute-start.6 = (bf16[48,1024]{1,0:T(8,128)(2,1)S(1)}, bf16[48,1024]{1,0:T(8,128)(2,1)S(1)}, u32[]{:S(2)}, u32[]{:S(2)}) collective-permute-start(bf16[48,1024]{1,0:T(8,128)(2,1)S(1)} %get-tuple-element.38), channel_id=1, source_target_pairs={{0,8},{8,16},{16,24},{24,0},{1,9},{9,17},{17,25},{25,1},{2,10},{10... | collective-permute-start | bytes 294920 | tf_op jit(solution)/shard_map/ppermute | solution.py:51
  3.5 7.3 %collective-permute-start.7 = (bf16[48,1024]{1,0:T(8,128)(2,1)S(1)}, bf16[48,1024]{1,0:T(8,128)(2,1)S(1)}, u32[]{:S(2)}, u32[]{:S(2)}) collective-permute-start(bf16[48,1024]{1,0:T(8,128)(2,1)S(1)} %get-tuple-element.39), channel_id=1, source_target_pairs={{0,16},{8,24},{16,0},{24,8},{1,17},{9,25},{17,1},{25,9},{2,18},{10... | collective-permute-start | bytes 294920 | tf_op jit(solution)/shard_map/ppermute | solution.py:51
  6.2 4.6 %collective-permute-start.8 = (bf16[48,1024]{1,0:T(8,128)(2,1)S(1)}, bf16[48,1024]{1,0:T(8,128)(2,1)S(1)}, u32[]{:S(2)}, u32[]{:S(2)}) collective-permute-start(bf16[48,1024]{1,0:T(8,128)(2,1)S(1)} %get-tuple-element.40), channel_id=1, source_target_pairs={{0,24},{8,0},{16,8},{24,16},{1,25},{9,1},{17,9},{25,17},{2,26},{10... | collective-permute-start | bytes 294920 | tf_op jit(solution)/shard_map/ppermute | solution.py:51
  11.7 18.7 %all-to-all-start = ((bf16[8,128,256]{2,1,0:T(8,128)(2,1)}), bf16[8,128,256]{2,1,0:T(8,128)(2,1)S(1)}, u32[]{:S(2)}, u32[]{:S(2)}) async-start(bf16[8,128,256]{2,1,0:T(8,128)(2,1)} %get-tuple-element.42), calls=%async_computation | async-start | bytes 1048576 | tf_op jit(solution)/shard_map/all_to_all | solution.py:398
  18.4 9.5 %collective-permute-start.2 = (bf16[32,1024]{1,0:T(8,128)(2,1)S(1)}, bf16[32,1024]{1,0:T(8,128)(2,1)S(1)}, u32[]{:S(2)}, u32[]{:S(2)}) collective-permute-start(bf16[32,1024]{1,0:T(8,128)(2,1)S(1)} %get-tuple-element.34), channel_id=1, source_target_pairs={{0,3},{1,0},{2,1},{3,2},{4,7},{5,4},{6,5},{7,6},{8,11},{9,8},{10,9... | collective-permute-start | bytes 196616 | tf_op jit(solution)/shard_map/ppermute | solution.py:51
  21.4 6.5 %collective-permute-start.1 = (bf16[32,1024]{1,0:T(8,128)(2,1)S(1)}, bf16[32,1024]{1,0:T(8,128)(2,1)S(1)}, u32[]{:S(2)}, u32[]{:S(2)}) collective-permute-start(bf16[32,1024]{1,0:T(8,128)(2,1)S(1)} %get-tuple-element.34), channel_id=1, source_target_pairs={{0,2},{1,3},{2,0},{3,1},{4,6},{5,7},{6,4},{7,5},{8,10},{9,11},{10,... | collective-permute-start | bytes 196616 | tf_op jit(solution)/shard_map/ppermute | solution.py:51
  22.1 5.8 %collective-permute-start = (bf16[32,1024]{1,0:T(8,128)(2,1)S(1)}, bf16[32,1024]{1,0:T(8,128)(2,1)S(1)}, u32[]{:S(2)}, u32[]{:S(2)}) collective-permute-start(bf16[32,1024]{1,0:T(8,128)(2,1)S(1)} %get-tuple-element.34), channel_id=1, source_target_pairs={{0,1},{1,2},{2,3},{3,0},{4,5},{5,6},{6,7},{7,4},{8,9},{9,10},{10,1... | collective-permute-start | bytes 196616 | tf_op jit(solution)/shard_map/ppermute | solution.py:51
  28.0 8.1 %collective-permute-start.3 = (bf16[128,1024]{1,0:T(8,128)(2,1)S(1)}, bf16[128,1024]{1,0:T(8,128)(2,1)S(1)}, u32[]{:S(2)}, u32[]{:S(2)}) collective-permute-start(bf16[128,1024]{1,0:T(8,128)(2,1)S(1)} %constant_dynamic-update-slice_fusion.refs_0_), channel_id=1, source_target_pairs={{0,8},{8,16},{16,24},{24,0},{1,9},{9,17},{17,25},{25,1},{2,10},{10... | collective-permute-start | bytes 786440 | tf_op jit(solution)/shard_map/ppermute | solution.py:51
  29.4 7.6 %collective-permute-start.9 = (bf16[128,1024]{1,0:T(8,128)(2,1)S(1)}, bf16[128,1024]{1,0:T(8,128)(2,1)S(1)}, u32[]{:S(2)}, u32[]{:S(2)}) collective-permute-start(bf16[128,1024]{1,0:T(8,128)(2,1)S(1)} %get-tuple-element.41.refs_4_), channel_id=1, source_target_pairs={{0,1},{1,2},{2,3},{3,0},{4,5},{5,6},{6,7},{7,4},{8,9},{9,10},{10,1... | collective-permute-start | bytes 786440 | tf_op jit(solution)/shard_map/ppermute | solution.py:51
  30.3 15.2 %collective-permute-start.12 = (bf16[8,128,256]{2,1,0:T(8,128)(2,1)S(1)}, bf16[8,128,256]{2,1,0:T(8,128)(2,1)S(1)}, u32[]{:S(2)}, u32[]{:S(2)}) collective-permute-start(bf16[8,128,256]{2,1,0:T(8,128)(2,1)S(1)} %all-to-all-done.refs_9_), channel_id=1, source_target_pairs={{0,4},{4,0},{1,5},{5,1},{2,6},{6,2},{3,7},{7,3},{8,12},{12,8},{9,1... | collective-permute-start | bytes 1572872 | tf_op jit(solution)/shard_map/ppermute | solution.py:51
  30.3 8.9 %collective-permute-start.5 = (bf16[128,1024]{1,0:T(8,128)(2,1)S(1)}, bf16[128,1024]{1,0:T(8,128)(2,1)S(1)}, u32[]{:S(2)}, u32[]{:S(2)}) collective-permute-start(bf16[128,1024]{1,0:T(8,128)(2,1)S(1)} %constant_dynamic-update-slice_fusion.refs_0_), channel_id=1, source_target_pairs={{0,24},{8,0},{16,8},{24,16},{1,25},{9,1},{17,9},{25,17},{2,26},{10... | collective-permute-start | bytes 786440 | tf_op jit(solution)/shard_map/ppermute | solution.py:51
  33.0 9.0 %collective-permute-start.11 = (bf16[128,1024]{1,0:T(8,128)(2,1)S(1)}, bf16[128,1024]{1,0:T(8,128)(2,1)S(1)}, u32[]{:S(2)}, u32[]{:S(2)}) collective-permute-start(bf16[128,1024]{1,0:T(8,128)(2,1)S(1)} %get-tuple-element.41.refs_4_), channel_id=1, source_target_pairs={{0,3},{1,0},{2,1},{3,2},{4,7},{5,4},{6,5},{7,6},{8,11},{9,8},{10,9... | collective-permute-start | bytes 786440 | tf_op jit(solution)/shard_map/ppermute | solution.py:51
  36.0 9.4 %collective-permute-start.4 = (bf16[128,1024]{1,0:T(8,128)(2,1)S(1)}, bf16[128,1024]{1,0:T(8,128)(2,1)S(1)}, u32[]{:S(2)}, u32[]{:S(2)}) collective-permute-start(bf16[128,1024]{1,0:T(8,128)(2,1)S(1)} %collective-permute-done.3.refs_1_), channel_id=1, source_target_pairs={{0,8},{8,16},{16,24},{24,0},{1,9},{9,17},{17,25},{25,1},{2,10},{10... | collective-permute-start | bytes 786440 | tf_op jit(solution)/shard_map/ppermute | solution.py:51
  37.0 8.5 %collective-permute-start.10 = (bf16[128,1024]{1,0:T(8,128)(2,1)S(1)}, bf16[128,1024]{1,0:T(8,128)(2,1)S(1)}, u32[]{:S(2)}, u32[]{:S(2)}) collective-permute-start(bf16[128,1024]{1,0:T(8,128)(2,1)S(1)} %collective-permute-done.9.refs_5_), channel_id=1, source_target_pairs={{0,1},{1,2},{2,3},{3,0},{4,5},{5,6},{6,7},{7,4},{8,9},{9,10},{10,1... | collective-permute-start | bytes 786440 | tf_op jit(solution)/shard_map/ppermute | solution.py:51
  47.6 1.5 %collective-permute-start.13 = (bf16[80,1024]{1,0:T(8,128)(2,1)S(1)}, bf16[80,1024]{1,0:T(8,128)(2,1)S(1)}, u32[]{:S(2)}, u32[]{:S(2)}) collective-permute-start(bf16[80,1024]{1,0:T(8,128)(2,1)S(1)} %get-tuple-element.43.q_own), channel_id=1, source_target_pairs={{0,4},{4,0},{1,5},{5,1},{2,6},{6,2},{3,7},{7,3},{8,12},{12,8},{9,1... | collective-permute-start | bytes 491528 | tf_op jit(solution)/shard_map/ppermute | solution.py:51
  49.7 8.7 %collective-permute-start.18 = (bf16[136,1024]{1,0:T(8,128)(2,1)S(1)}, bf16[136,1024]{1,0:T(8,128)(2,1)S(1)}, u32[]{:S(2)}, u32[]{:S(2)}) collective-permute-start(bf16[136,1024]{1,0:T(8,128)(2,1)S(1)} %get-tuple-element.47.pay), channel_id=1, source_target_pairs={{0,224},{32,0},{64,32},{1,225},{33,1},{65,33},{2,226},{34,2},{66,3... | collective-permute-start | bytes 835592 | tf_op jit(solution)/shard_map/ppermute | solution.py:69
  50.4 10.6 %collective-permute-start.14 = (bf16[136,1024]{1,0:T(8,128)(2,1)S(1)}, bf16[136,1024]{1,0:T(8,128)(2,1)S(1)}, u32[]{:S(2)}, u32[]{:S(2)}) collective-permute-start(bf16[136,1024]{1,0:T(8,128)(2,1)S(1)} %get-tuple-element.47.pay), channel_id=1, source_target_pairs={{0,32},{32,64},{64,96},{96,128},{128,160},{160,192},{192,224},{1,3... | collective-permute-start | bytes 835592 | tf_op jit(solution)/shard_map/ppermute | solution.py:65
  56.3 51.3 %collective-permute-start.24 = (bf16[2,8,64,256]{3,2,1,0:T(8,128)(2,1)S(1)}, bf16[2,8,64,256]{3,2,1,0:T(8,128)(2,1)S(1)}, u32[]{:S(2)}, u32[]{:S(2)}) collective-permute-start(bf16[2,8,64,256]{3,2,1,0:T(8,128)(2,1)S(1)} %pad_maximum_fusion.w0), channel_id=1, source_target_pairs={{0,3},{1,0},{2,1},{3,2},{4,7},{5,4},{6,5},{7,6},{8,11},{9,8},{10,9... | collective-permute-start | bytes 1572872 | tf_op jit(solution)/shard_map/ppermute | solution.py:51
  57.1 50.5 %collective-permute-start.23 = (bf16[2,8,64,256]{3,2,1,0:T(8,128)(2,1)S(1)}, bf16[2,8,64,256]{3,2,1,0:T(8,128)(2,1)S(1)}, u32[]{:S(2)}, u32[]{:S(2)}) collective-permute-start(bf16[2,8,64,256]{3,2,1,0:T(8,128)(2,1)S(1)} %pad_maximum_fusion.w0), channel_id=1, source_target_pairs={{0,2},{1,3},{2,0},{3,1},{4,6},{5,7},{6,4},{7,5},{8,10},{9,11},{10,... | collective-permute-start | bytes 1572872 | tf_op jit(solution)/shard_map/ppermute | solution.py:51
  57.6 50.9 %collective-permute-start.22 = (bf16[2,8,64,256]{3,2,1,0:T(8,128)(2,1)S(1)}, bf16[2,8,64,256]{3,2,1,0:T(8,128)(2,1)S(1)}, u32[]{:S(2)}, u32[]{:S(2)}) collective-permute-start(bf16[2,8,64,256]{3,2,1,0:T(8,128)(2,1)S(1)} %pad_maximum_fusion.w0), channel_id=1, source_target_pairs={{0,1},{1,2},{2,3},{3,0},{4,5},{5,6},{6,7},{7,4},{8,9},{9,10},{10,1... | collective-permute-start | bytes 1572872 | tf_op jit(solution)/shard_map/ppermute | solution.py:51
  58.5 9.6 %collective-permute-start.19 = (bf16[136,1024]{1,0:T(8,128)(2,1)S(1)}, bf16[136,1024]{1,0:T(8,128)(2,1)S(1)}, u32[]{:S(2)}, u32[]{:S(2)}) collective-permute-start(bf16[136,1024]{1,0:T(8,128)(2,1)S(1)} %collective-permute-done.18.refs_1_), channel_id=1, source_target_pairs={{224,192},{0,224},{32,0},{225,193},{1,225},{33,1},{226,194},{2,226... | collective-permute-start | bytes 835592 | tf_op jit(solution)/shard_map/ppermute | solution.py:69
  61.0 9.8 %collective-permute-start.15 = (bf16[136,1024]{1,0:T(8,128)(2,1)S(1)}, bf16[136,1024]{1,0:T(8,128)(2,1)S(1)}, u32[]{:S(2)}, u32[]{:S(2)}) collective-permute-start(bf16[136,1024]{1,0:T(8,128)(2,1)S(1)} %collective-permute-done.14.refs_0_), channel_id=1, source_target_pairs={{32,64},{64,96},{96,128},{128,160},{160,192},{192,224},{33,65},{65... | collective-permute-start | bytes 835592 | tf_op jit(solution)/shard_map/ppermute | solution.py:65
  68.0 19.9 %collective-permute-start.20 = (bf16[136,1024]{1,0:T(8,128)(2,1)S(1)}, bf16[136,1024]{1,0:T(8,128)(2,1)S(1)}, u32[]{:S(2)}, u32[]{:S(2)}) collective-permute-start(bf16[136,1024]{1,0:T(8,128)(2,1)S(1)} %collective-permute-done.19.refs_1_), channel_id=1, source_target_pairs={{192,160},{224,192},{0,224},{193,161},{225,193},{1,225},{194,162},... | collective-permute-start | bytes 835592 | tf_op jit(solution)/shard_map/ppermute | solution.py:69
  70.8 11.0 %collective-permute-start.16 = (bf16[136,1024]{1,0:T(8,128)(2,1)S(1)}, bf16[136,1024]{1,0:T(8,128)(2,1)S(1)}, u32[]{:S(2)}, u32[]{:S(2)}) collective-permute-start(bf16[136,1024]{1,0:T(8,128)(2,1)S(1)} %collective-permute-done.15.refs_0_), channel_id=1, source_target_pairs={{64,96},{96,128},{128,160},{160,192},{192,224},{65,97},{97,129},{1... | collective-permute-start | bytes 835592 | tf_op jit(solution)/shard_map/ppermute | solution.py:65
  81.8 12.9 %collective-permute-start.17 = (bf16[136,1024]{1,0:T(8,128)(2,1)S(1)}, bf16[136,1024]{1,0:T(8,128)(2,1)S(1)}, u32[]{:S(2)}, u32[]{:S(2)}) collective-permute-start(bf16[136,1024]{1,0:T(8,128)(2,1)S(1)} %collective-permute-done.16.refs_0_), channel_id=1, source_target_pairs={{96,128},{128,160},{160,192},{192,224},{97,129},{129,161},{161,193... | collective-permute-start | bytes 835592 | tf_op jit(solution)/shard_map/ppermute | solution.py:65
  98.7 1.7 %collective-permute-start.21 = (f32[72,1024]{1,0:T(8,128)S(1)}, f32[72,1024]{1,0:T(8,128)S(1)}, u32[]{:S(2)}, u32[]{:S(2)}) collective-permute-start(f32[72,1024]{1,0:T(8,128)S(1)} %get-tuple-element.61), channel_id=1, source_target_pairs={{0,4},{4,0},{1,5},{5,1},{2,6},{6,2},{3,7},{7,3},{8,12},{12,8},{9,1... | collective-permute-start | bytes 884744 | tf_op jit(solution)/shard_map/ppermute | solution.py:51
  101.4 14.2 %copy-start.4 = (f32[1024]{0:T(1024)S(1)}, f32[1024]{0:T(1024)}, u32[]{:S(2)}) copy-start(f32[1024]{0:T(1024)} %param.17) | copy-start | bytes 12292
  101.4 14.0 %all-to-all-start.1 = ((bf16[16,2,2048]{2,1,0:T(2,128)(2,1)}), bf16[16,2,2048]{2,1,0:T(2,128)(2,1)S(1)}, u32[]{:S(2)}, u32[]{:S(2)}) async-start(bf16[16,2,2048]{2,1,0:T(2,128)(2,1)} %reshape.4), calls=%async_computation.1 | async-start | bytes 262144 | tf_op jit(solution)/shard_map/all_to_all | solution.py:465
  107.6 0.8 copy-start
  108.4 0.8 copy-start.2
  109.2 1.0 copy-start.1
  110.3 1.0 copy-start.3
